TPU v7x, 512 devices: a whole 4x4x16 slice. The times are simulated.
512 devices in a mesh: sp: 32 (over z, core), tp: 16 (over y, x).
Axes of the slice: x: 4, y: 4, z: 16, core: 2. Of those that a mesh axis runs over, the one named last changes fastest.
Arguments:
- residual: bfloat16 [8192, 2048], P('sp'), may hold values from -6 to 6
- queries: bfloat16 [8192, 16, 128], P('sp', 'tp'), may hold values from -256 to 256
- key_vectors: bfloat16 [8192, 16, 128], P('sp', 'tp'), may hold values from -5.3 to 5.3
- value_rows: bfloat16 [8192, 16, 128], P('sp', 'tp'), may hold values from -6 to 6
- head_lambda: float32 [16], P('tp'), may hold values from 0.3 to 0.8
- head_gain: float32 [128], replicated, may hold values from 0.1 to 1.9
- out_weight: bfloat16 [2048, 2048], P('tp'), may hold values from -0.125 to 0.125
- ffn_gain: float32 [2048], replicated, may hold values from 0.1 to 1.9
- expert_gate: bfloat16 [32, 2048, 4096], P('sp', None, 'tp'), may hold values from -0.125 to 0.125
- expert_up: bfloat16 [32, 2048, 4096], P('sp', None, 'tp'), may hold values from -0.125 to 0.125
- expert_down: bfloat16 [32, 4096, 2048], P('sp', None, 'tp'), may hold values from -0.09375 to 0.09375
- routing: int32 [8192, 2], P('sp'), may hold values from 0 to 31, as said below
- route_weight: float32 [8192, 2], P('sp'), may hold values from 0.1 to 0.9
Outputs:
- layer_out: bfloat16 [8192, 2048], P('sp')
Inputs may be any that keep to these rules, and one draw needn't show every extreme that they name: `routing`: each row names two different experts of one group of 8 consecutive experts. In each aligned block of 256 rows no expert is named by more than 32 rows, and in every block some expert is named by exactly 32 rows.
All inputs are finite; a program needn't handle non-finite values.
Results may differ from a plain program's by a relative error of at most 0.015.
Values may be sent and summed in bfloat16 or wider, within the bound.
No kernel may reach another device: no remote copies, remote signals or barrier semaphores. Data moves between devices by JAX's collectives and lax.ppermute only.
A program may use at most 64 MiB of HBM per device.

v0:
```python
import math

import jax
import jax.numpy as jnp
from jax import lax
from jax.sharding import PartitionSpec as P

GROUPS = 4


norm_eps = 1e-06


def sent_together(arrays, axis, dim, along):
    ends, at = ([], 0)
    for a in arrays[:-1]:
        at += a.shape[along]
        ends.append(at)
    both = jnp.concatenate(arrays, axis=along)
    return tuple(jnp.split(lax.all_gather(both, axis, axis=dim, tiled=True), ends, axis=along))


def in_blocks(array, dim, peers):
    before, after = (array.shape[:dim], array.shape[dim + 1 :])
    return jnp.moveaxis(array.reshape(*before, peers, -1, *after), dim, 0)


def sum_at_owner(array, axis, dim):
    parts = in_blocks(array, dim, lax.axis_size(axis))
    arrived = lax.all_to_all(parts, axis, split_axis=0, concat_axis=0, tiled=True)
    return arrived.astype(jnp.float32).sum(axis=0)


def padded_to(lines, peers):
    spare = -len(lines) % peers
    return jnp.pad(lines, [(0, spare)] + [(0, 0)] * (lines.ndim - 1))


def from_everyone(array, axis):
    peers = lax.axis_size(axis)
    return lax.all_to_all(
        jnp.broadcast_to(array[None], (peers, *array.shape)), axis, 0, 0, tiled=True
    )


def laid_out(parts, dim):
    parts = jnp.moveaxis(parts, 0, dim)
    dims = parts.shape
    return parts.reshape(*dims[:dim], dims[dim] * dims[dim + 1], *dims[dim + 2 :])


def collect(array, axis, dim):
    parts = from_everyone(array, axis)
    return laid_out(parts, dim)


def sum_by_parts(array, axes):
    lines = array.reshape(-1, array.shape[-1])
    own = sum_at_owner(padded_to(lines, lax.axis_size(axes)), axes, 0)
    whole = collect(own.astype(jnp.bfloat16), axes, 0)
    return whole[: len(lines)].reshape(array.shape).astype(jnp.float32)


def online_update(running, query_part, key_part, value_part, query_pos, key_pos, score_scale):
    highest, totals, accum = running
    scores = (
        jnp.einsum("qhd,khd->hqk", query_part, key_part, preferred_element_type=jnp.float32)
        * score_scale
    )
    scores = jnp.where(key_pos[None, None, :] <= query_pos[None, :, None], scores, -jnp.inf)
    new_high = jnp.maximum(highest, jnp.max(scores, axis=-1))
    shrink = jnp.exp(highest - new_high)
    weights = jnp.exp(scores - new_high[:, :, None])
    totals = shrink * totals + jnp.sum(weights, axis=-1)
    blended = jnp.einsum(
        "hqk,khe->qhe", weights.astype(jnp.bfloat16), value_part, preferred_element_type=jnp.float32
    )
    accum = jnp.transpose(shrink)[:, :, None] * accum + blended
    return (new_high, totals, accum)


def shards(
    residual,
    queries,
    key_vectors,
    value_rows,
    head_lambda,
    head_gain,
    out_weight,
    ffn_gain,
    expert_gate,
    expert_up,
    expert_down,
    routing,
    route_weight,
):
    tok_count = queries.shape[0]
    local_heads = queries.shape[1]
    half_width = queries.shape[2] // 2
    value_width = value_rows.shape[2]
    score_scale = half_width ** (-0.5)
    query_pos = lax.axis_index("sp") * tok_count + jnp.arange(tok_count, dtype=jnp.int32)
    last_query = query_pos[-1]
    first_half = queries[:, :, :half_width]
    second_half = queries[:, :, half_width:]
    start_high = jnp.full((local_heads, tok_count), -1e30, jnp.float32)
    start_total = jnp.zeros((local_heads, tok_count), jnp.float32)
    start_accum = jnp.zeros((tok_count, local_heads, value_width), jnp.float32)
    empty_state = (start_high, start_total, start_accum)
    running = (empty_state, empty_state)
    key_piece, value_piece = sent_together((key_vectors, value_rows), "sp", 0, 1)
    piece_len = key_piece.shape[0]
    block_len = math.gcd(piece_len, 512)
    block_count = piece_len // block_len
    key_blocks = key_piece.reshape(block_count, block_len, local_heads, 2 * half_width)
    value_blocks = value_piece.reshape(block_count, block_len, local_heads, value_width)

    def visit(current, stacked):
        block_index, key_block, value_block = stacked
        block_first = block_index * block_len
        key_pos = block_first + jnp.arange(block_len, dtype=jnp.int32)

        def compute(inside):
            first_state = online_update(
                inside[0],
                first_half,
                key_block[:, :, :half_width],
                value_block,
                query_pos,
                key_pos,
                score_scale,
            )
            second_state = online_update(
                inside[1],
                second_half,
                key_block[:, :, half_width:],
                value_block,
                query_pos,
                key_pos,
                score_scale,
            )
            return (first_state, second_state)

        return (lax.cond(block_first <= last_query, compute, lambda inside: inside, current), None)

    running, _ = lax.scan(
        visit, running, (jnp.arange(block_count, dtype=jnp.int32), key_blocks, value_blocks)
    )
    first_state, second_state = running
    first_out = first_state[2] / jnp.transpose(first_state[1])[:, :, None]
    second_out = second_state[2] / jnp.transpose(second_state[1])[:, :, None]
    combined = first_out - head_lambda[None, :, None] * second_out
    normed_heads = (
        combined
        * lax.rsqrt(jnp.mean(combined * combined, axis=-1, keepdims=True) + norm_eps)
        * head_gain
    )
    attended = normed_heads.astype(jnp.bfloat16).reshape(tok_count, local_heads * value_width)
    partial_proj = jnp.dot(attended, out_weight, preferred_element_type=jnp.float32)
    projected = sum_by_parts(partial_proj.astype(jnp.bfloat16), "tp")
    stream = residual.astype(jnp.float32) + projected
    block_normed = (
        stream * lax.rsqrt(jnp.mean(stream * stream, axis=-1, keepdims=True) + norm_eps) * ffn_gain
    ).astype(jnp.bfloat16)
    expert_count = lax.axis_size("sp")
    tp_count = lax.axis_size("tp")
    per_group = expert_count // GROUPS
    capacity = tok_count // per_group
    top_count = routing.shape[1]
    model_width = block_normed.shape[1]
    flat_routes = routing.reshape(-1)
    route_count = flat_routes.shape[0]
    onehot = (flat_routes[:, None] == jnp.arange(expert_count, dtype=jnp.int32)[None, :]).astype(
        jnp.int32
    )
    earlier = jnp.cumsum(onehot, axis=0) - onehot
    position = jnp.sum(earlier * onehot, axis=1)
    slot_index = flat_routes * capacity + position
    slot_token = (
        jnp.full((expert_count * capacity,), tok_count, jnp.int32)
        .at[slot_index]
        .set(jnp.arange(route_count, dtype=jnp.int32) // top_count)
    )
    slot_table = slot_token.reshape(expert_count, capacity)
    slice_width = model_width // tp_count
    own_columns = lax.dynamic_slice_in_dim(
        block_normed, lax.axis_index("tp") * slice_width, slice_width, 1
    )
    outgoing = jnp.take(own_columns, slot_table, axis=0, mode="fill", fill_value=0)
    landed = lax.all_to_all(outgoing, "sp", split_axis=0, concat_axis=0, tiled=True)
    arrived = collect(landed, "tp", 2)
    expert_rows = arrived.reshape(-1, model_width)
    gate_part = jnp.dot(expert_rows, expert_gate[0], preferred_element_type=jnp.float32)
    up_part = jnp.dot(expert_rows, expert_up[0], preferred_element_type=jnp.float32)
    inner_act = (jax.nn.silu(gate_part) * up_part).astype(jnp.bfloat16)
    down_width = expert_down.shape[2]
    weight_rows = expert_down[0]
    expert_sum = jnp.dot(
        lax.all_gather(inner_act, "tp", axis=1, tiled=True),
        weight_rows,
        preferred_element_type=jnp.float32,
    )
    expert_out = expert_sum.astype(jnp.bfloat16).reshape(expert_count, capacity, down_width)
    returned = lax.all_to_all(expert_out, "sp", split_axis=0, concat_axis=0, tiled=True)
    per_route = returned.reshape(expert_count * capacity, down_width)[slot_index]
    weighted = per_route.astype(jnp.float32) * route_weight.reshape(-1)[:, None]
    token_sum = jnp.sum(weighted.reshape(tok_count, top_count, down_width), axis=1)
    moe_rows = collect(token_sum.astype(jnp.bfloat16), "tp", 1).astype(token_sum.dtype)
    return (stream + moe_rows).astype(jnp.bfloat16)


def solution(mesh):
    in_specs = (
        P("sp", None),
        P("sp", "tp", None),
        P("sp", "tp", None),
        P("sp", "tp", None),
        P("tp"),
        P(),
        P("tp", None),
        P(),
        P("sp", None, "tp"),
        P("sp", None, "tp"),
        P("sp", None, "tp"),
        P("sp", None),
        P("sp", None),
    )
    out_specs = P("sp", None)
    return jax.shard_map(shards, mesh=mesh, in_specs=in_specs, out_specs=out_specs, check_vma=False)
```

profile of v0, /device:TPU:1, one launch (start us, length us, event | category | flops | bytes accessed | tf_op | source)
XLA Modules:
  0.0 460.8 jit_solution(17257785034887943455)
XLA Ops:
  6.5 1.6 pad_maximum_fusion
  10.7 78.0 %all-gather.3.cloned.1.call-done = bf16[8192,2,128]{2,0,1:T(8,128)(2,1)} async-done(((bf16[256,2,128]{2,0,1:T(8,128)(2,1)}), bf16[8192,2,128]{2,0,1:T(8,128)(2,1)}) %all-gather.3.cloned.1.call-update) | async-done | bytes 4194320 | tf_op jit(solution)/shard_map/all_gather | solution.py:20
  88.7 3.8 fusion.58
  92.6 33.3 %while.21 = (s32[]{:T(128)}, f32[1,256]{1,0:T(1,128)S(1)}, f32[1,256]{1,0:T(1,128)S(1)}, f32[256,1,128]{0,2,1:T(8,128)S(1)}, f32[1,256]{1,0:T(1,128)S(1)}, /*ind...) while((s32[]{:T(128)}, f32[1,256]{1,0:T(1,128)S(1)}, ...), condition=%wide.region_7.8_spmd.clone, body=%wide.region_0.7_spmd.clone.sunk | while | flops 102893312 | bytes 4570543 | solution.py:146
  94.5 2.4 conditional.3
  126.0 2.5 convolution_convert_fusion
  128.6 6.5 %all-to-all-start = ((bf16[16,16,2048]{2,1,0:T(8,128)(2,1)}), bf16[16,16,2048]{2,1,0:T(8,128)(2,1)S(1)}, u32[]{:S(2)}, u32[]{:S(2)}) async-start(bf16[16,16,2048]{2,1,0:T(8,128)(2,1)} %bitcast.29), calls=%async_computation | async-start | bytes 2097152 | tf_op jit(solution)/shard_map/all_to_all | solution.py:30
  137.4 14.1 %all-to-all-done = bf16[16,16,2048]{2,1,0:T(8,128)(2,1)S(1)} async-done(((bf16[16,16,2048]{2,1,0:T(8,128)(2,1)}), bf16[16,16,2048]{2,1,0:T(8,128)(2,1)S(1)}, u32[]{:S(2)}, u32[]{:S(2)}) %all-to-all-start) | async-done | bytes 1048608 | tf_op jit(solution)/shard_map/all_to_all | solution.py:30
  152.8 4.5 all-to-all-start.1
  157.4 2.4 scatter_custom_fusion
  160.8 12.4 %all-to-all-done.1 = bf16[16,16,2048]{2,1,0:T(8,128)(2,1)S(1)} async-done(((bf16[16,16,2048]{2,1,0:T(8,128)(2,1)}), bf16[16,16,2048]{2,1,0:T(8,128)(2,1)S(1)}, u32[]{:S(2)}, u32[]{:S(2)}) %all-to-all-start.1) | async-done | bytes 1048608 | tf_op jit(solution)/shard_map/all_to_all | solution.py:41
  173.7 3.2 gather_fusion
  177.2 65.0 %all_to_all.30 = bf16[32,32,128]{2,1,0:T(8,128)(2,1)S(1)} all-to-all(bf16[32,32,128]{2,1,0:T(8,128)(2,1)S(1)} %broadcast_select_fusion), channel_id=1, replica_groups=mesh['sp'=32,'tp'=16] {'sp'}, dimensions={0} | all-to-all | bytes 524288 | tf_op jit(solution)/shard_map/all_to_all | solution.py:190
  242.9 52.7 %all_to_all.31 = bf16[16,32,32,128]{3,2,1,0:T(8,128)(2,1)S(1)} all-to-all(bf16[16,32,32,128]{3,2,1,0:T(8,128)(2,1)S(1)} %broadcast_in_dim.42), channel_id=1, replica_groups=mesh['sp'=32,'tp'=16] {'tp'}, dimensions={0} | all-to-all | bytes 8388608 | tf_op jit(solution)/shard_map/all_to_all | solution.py:41
  295.6 4.9 %copy.34 = bf16[32,32,16,128]{3,2,1,0:T(8,128)(2,1)S(1)} copy(bf16[32,32,16,128]{3,1,0,2:T(8,128)(2,1)S(1)} %bitcast.139) | data formatting | bytes 8388608 | tf_op jit(solution)/shard_map/transpose | solution.py:47
  301.8 2.1 fusion.34
  303.9 81.9 %all-gather.5.cloned.1.call-done = bf16[1024,4096]{1,0:T(8,128)(2,1)} async-done(((bf16[1024,256]{1,0:T(8,128)(2,1)}), bf16[1024,4096]{1,0:T(8,128)(2,1)}) %all-gather.5.cloned.1.call-update) | async-done | bytes 8388624 | tf_op jit(solution)/shard_map/all_gather | solution.py:199
  385.8 6.6 %convolution_convert_fusion.1 = bf16[1024,128]{1,0:T(8,128)(2,1)} fusion(bf16[1024,4096]{1,0:T(8,128)(2,1)} %all-gather.5.cloned.1.call-done, bf16[1,4096,128]{2,1,0:T(8,128)(2,1)} %param.27), kind=kOutput, calls=%fused_computation.53 | convolution fusion | flops 1073872896 | bytes 9699328 | tf_op jit(solution)/shard_map/dot_general | solution.py:198
  392.4 14.4 %all-to-all-start.4 = ((bf16[32,32,128]{2,1,0:T(8,128)(2,1)}), bf16[32,32,128]{2,1,0:T(8,128)(2,1)S(1)}, u32[]{:S(2)}, u32[]{:S(2)}) async-start(bf16[32,32,128]{2,1,0:T(8,128)(2,1)} %bitcast.151), calls=%async_computation.4 | async-start | bytes 524288 | tf_op jit(solution)/shard_map/all_to_all | solution.py:204
  407.6 21.5 %all-to-all-done.4 = bf16[32,32,128]{2,1,0:T(8,128)(2,1)S(1)} async-done(((bf16[32,32,128]{2,1,0:T(8,128)(2,1)}), bf16[32,32,128]{2,1,0:T(8,128)(2,1)S(1)}, u32[]{:S(2)}, u32[]{:S(2)}) %all-to-all-start.4) | async-done | bytes 262176 | tf_op jit(solution)/shard_map/all_to_all | solution.py:204
  429.1 1.3 gather_fusion.1
  430.4 1.3 fusion.40
  432.0 20.5 %all_to_all.32 = bf16[16,256,128]{2,1,0:T(8,128)(2,1)S(1)} all-to-all(bf16[16,256,128]{2,1,0:T(8,128)(2,1)S(1)} %broadcast_in_dim.43), channel_id=1, replica_groups=mesh['sp'=32,'tp'=16] {'tp'}, dimensions={0} | all-to-all | bytes 2097152 | tf_op jit(solution)/shard_map/all_to_all | solution.py:41
  452.5 1.5 fusion.30
  (139 shorter events, 22.3 us)
Async XLA Ops:
  6.5 294.0 %copy-start = (bf16[1,2048,256]{2,1,0:T(8,128)(2,1)S(1)}, bf16[1,2048,256]{2,1,0:T(8,128)(2,1)}, u32[]{:S(2)}) copy-start(bf16[1,2048,256]{2,1,0:T(8,128)(2,1)} %param.25) | copy-start | bytes 3145732
  6.5 82.2 %all-gather.3.cloned.1.call-start = ((), (), s32[]{:S(2)}) async-start(), calls=%async_computation.6 | async-start | bytes 4325376 | tf_op jit(solution)/shard_map/all_gather | solution.py:20
  92.6 33.4 %copy-start.4 = (f32[128]{0:T(128)S(1)}, f32[128]{0:T(128)}, u32[]{:S(2)}) copy-start(f32[128]{0:T(128)} %param.22) | copy-start | bytes 1540
  126.0 9.2 %copy-start.2 = (s32[256,2]{0,1:T(2,128)S(1)}, s32[256,2]{0,1:T(2,128)}, u32[]{:S(2)}) copy-start(s32[256,2]{0,1:T(2,128)} %param.28) | copy-start | bytes 6148
  128.6 23.0 %all-to-all-start = ((bf16[16,16,2048]{2,1,0:T(8,128)(2,1)}), bf16[16,16,2048]{2,1,0:T(8,128)(2,1)S(1)}, u32[]{:S(2)}, u32[]{:S(2)}) async-start(bf16[16,16,2048]{2,1,0:T(8,128)(2,1)} %bitcast.29), calls=%async_computation | async-start | bytes 2097152 | tf_op jit(solution)/shard_map/all_to_all | solution.py:30
  137.4 35.8 %copy-start.1 = (bf16[256,2048]{1,0:T(8,128)(2,1)S(1)}, bf16[256,2048]{1,0:T(8,128)(2,1)}, u32[]{:S(2)}) copy-start(bf16[256,2048]{1,0:T(8,128)(2,1)} %param.17) | copy-start | bytes 3145732
  152.8 20.4 %all-to-all-start.1 = ((bf16[16,16,2048]{2,1,0:T(8,128)(2,1)}), bf16[16,16,2048]{2,1,0:T(8,128)(2,1)S(1)}, u32[]{:S(2)}, u32[]{:S(2)}) async-start(bf16[16,16,2048]{2,1,0:T(8,128)(2,1)} %broadcast_in_dim.38), calls=%async_computation.1 | async-start | bytes 2097152 | tf_op jit(solution)/shard_map/all_to_all | solution.py:41
  157.3 228.5 %all-gather.5.cloned.1.call-start = ((), (), s32[]{:S(2)}) async-start(), calls=%async_computation.7 | async-start | bytes 8912896 | tf_op jit(solution)/shard_map/all_gather | solution.py:199
  300.5 1.3 copy-start.5
  303.9 102.9 %copy-start.3 = (f32[256,2]{0,1:T(2,128)S(1)}, f32[256,2]{0,1:T(2,128)}, u32[]{:S(2)}) copy-start(f32[256,2]{0,1:T(2,128)} %param.29) | copy-start | bytes 6148
  392.4 36.6 %all-to-all-start.4 = ((bf16[32,32,128]{2,1,0:T(8,128)(2,1)}), bf16[32,32,128]{2,1,0:T(8,128)(2,1)S(1)}, u32[]{:S(2)}, u32[]{:S(2)}) async-start(bf16[32,32,128]{2,1,0:T(8,128)(2,1)} %bitcast.151), calls=%async_computation.4 | async-start | bytes 524288 | tf_op jit(solution)/shard_map/all_to_all | solution.py:204
Sparse Core Ops, SparseCore 0:
  9.5 79.1 all-gather.2
  304.0 81.7 all-gather.4
where the time goes:
time: 462 us; the launch traced here: 461 us
  waiting for transfers between devices  208 us (45%)
  blocking collectives  138 us (30%)
  local copies, waits for them, and re-layouts  32.7 us (7%)
  starting transfers between devices  25.4 us (5%)
  loops' own time  21.5 us (5%)
  between operations  14.4 us (3%)
  matrix products  13.6 us (3%)
  other arithmetic  7.04 us (2%)
    all_gather x1, waiting for transfers between devices, shards(): lax.all_gather(inner_act, 'tp', axis=1, tiled=True)  81.9 us
    all_gather x1, waiting for transfers between devices, sent_together(): lax.all_gather(both, axis, axis=dim, tiled=True)  78 us
    all_to_all x2, blocking collectives, from_everyone(): lax.all_to_all(jnp.broadcast_to(array[None], (peers, *array.shape)), axis...  73.2 us
    all_to_all x1, blocking collectives, shards(): lax.all_to_all(outgoing, 'sp', split_axis=0, concat_axis=0, tiled=True)  65 us
    all_to_all x1, waiting for transfers between devices, shards(): lax.all_to_all(expert_out, 'sp', split_axis=0, concat_axis=0, tiled=True)  21.5 us
    another operation x1, loops' own time, shards(): lax.scan(visit, running, (jnp.arange(block_count, dtype=jnp.int32), key_b...  21.2 us
    all_to_all x1, starting transfers between devices, shards(): lax.all_to_all(expert_out, 'sp', split_axis=0, concat_axis=0, tiled=True)  14.4 us
    all_to_all x1, waiting for transfers between devices, sum_at_owner(): lax.all_to_all(parts, axis, split_axis=0, concat_axis=0, tiled=True)  14.1 us
  transfers between devices with their start and end apart: 5, of which 5 were waited for; matrix products, arithmetic and copies ran while one was open for 2% of the time, Pallas kernels for 0%

commit v1 on v0

v1 whole, which is shorter than its diff:
```python
import jax
import jax.numpy as jnp
from jax import lax
from jax.experimental import pallas as pl
from jax.experimental.pallas import tpu as pltpu
from jax.sharding import PartitionSpec as P

norm_eps = 1e-06
KEY_BLOCK = 1024
GROUPS = 4


def attention_body(where_ref, lam_ref, q_ref, kv_ref, gain_ref, out_ref, stacked, highest, accum):
    step = pl.program_id(0)
    tok = q_ref.shape[0]
    width = q_ref.shape[1]
    first_query = where_ref[0] * tok
    last_step = (first_query + tok - 1) // KEY_BLOCK

    @pl.when(step == 0)
    def _():
        scaled = q_ref[...] * jnp.asarray((width // 2) ** -0.5, jnp.bfloat16)
        low = lax.broadcasted_iota(jnp.int32, scaled.shape, 1) < width // 2
        zero = jnp.zeros_like(scaled)
        stacked[:tok] = jnp.where(low, scaled, zero)
        stacked[tok:] = jnp.where(low, zero, scaled)
        highest[...] = jnp.full(highest.shape, -1e30, jnp.float32)
        accum[...] = jnp.zeros(accum.shape, jnp.float32)

    def update(masked):
        values = kv_ref[1]
        scores = lax.dot_general(
            stacked[...], kv_ref[0], (((1,), (1,)), ((), ())), preferred_element_type=jnp.float32
        )
        if masked:
            row = lax.broadcasted_iota(jnp.int32, scores.shape, 0)
            col = lax.broadcasted_iota(jnp.int32, scores.shape, 1)
            limit = jnp.where(row >= tok, row - tok, row) + (first_query - step * KEY_BLOCK)
            scores = jnp.where(col <= limit, scores, -1e30)
        before = highest[...]
        now = jnp.maximum(before, jnp.max(scores, axis=1, keepdims=True))
        weights = jnp.exp(scores - now[:, :1])
        shrink = jnp.exp(before - now)[:, :1]
        wide = jnp.concatenate([values, jnp.ones_like(values)], axis=1)
        blended = jnp.dot(weights.astype(jnp.bfloat16), wide, preferred_element_type=jnp.float32)
        accum[...] = accum[...] * shrink + blended
        highest[...] = now

    @pl.when(step < last_step)
    def _():
        update(False)

    @pl.when(step == last_step)
    def _():
        update(True)
        both = accum[:, :width] / accum[:, width:]
        combined = both[:tok] - lam_ref[0] * both[tok:]
        square = jnp.mean(combined * combined, axis=1, keepdims=True)
        out_ref[...] = (combined * lax.rsqrt(square + norm_eps) * gain_ref[...]).astype(jnp.bfloat16)


def attention(where, lam, q, kv, gain):
    tok, width = q.shape
    steps = kv.shape[1] // KEY_BLOCK

    def kv_at(j, where_ref, lam_ref):
        return (0, jnp.minimum(j, (where_ref[0] * tok + tok - 1) // KEY_BLOCK), 0)

    def fixed(j, where_ref, lam_ref):
        return (0, 0)

    grid = pltpu.PrefetchScalarGridSpec(
        num_scalar_prefetch=2,
        grid=(steps,),
        in_specs=[
            pl.BlockSpec((tok, width), fixed),
            pl.BlockSpec((2, KEY_BLOCK, width), kv_at),
            pl.BlockSpec((1, width), fixed),
        ],
        out_specs=pl.BlockSpec((tok, width), fixed),
        scratch_shapes=[
            pltpu.VMEM((2 * tok, width), jnp.bfloat16),
            pltpu.VMEM((2 * tok, 128), jnp.float32),
            pltpu.VMEM((2 * tok, 2 * width), jnp.float32),
        ],
    )
    return pl.pallas_call(
        attention_body,
        grid_spec=grid,
        out_shape=jax.ShapeDtypeStruct((tok, width), jnp.bfloat16),
        compiler_params=pltpu.CompilerParams(
            dimension_semantics=("arbitrary",), vmem_limit_bytes=48 * 2**20
        ),
        name="attention",
    )(where, lam, q, kv, gain)


def expert_body(rows_ref, gain_ref, gate_ref, up_ref, down_ref, out_ref):
    rows = rows_ref[...].astype(jnp.float32)
    square = jnp.mean(rows * rows, axis=1, keepdims=True)
    normed = (rows * lax.rsqrt(square + norm_eps) * gain_ref[...]).astype(jnp.bfloat16)
    gate = jnp.dot(normed, gate_ref[...], preferred_element_type=jnp.float32)
    up = jnp.dot(normed, up_ref[...], preferred_element_type=jnp.float32)
    hidden = (gate / (1.0 + jnp.exp(-gate)) * up).astype(jnp.bfloat16)
    peers = out_ref.shape[0]
    share = out_ref.shape[2]
    part = jnp.dot(hidden, down_ref[...], preferred_element_type=jnp.float32).astype(jnp.bfloat16)
    for p in range(peers):
        out_ref[p] = part[:, p * share : (p + 1) * share]


def expert(rows, gain, gate, up, down, peers):
    count, model = rows.shape
    hidden = gate.shape[1]
    share = model // peers
    tile = 256
    return pl.pallas_call(
        expert_body,
        grid=(count // tile,),
        in_specs=[
            pl.BlockSpec((tile, model), lambda i: (i, 0)),
            pl.BlockSpec((1, model), lambda i: (0, 0)),
            pl.BlockSpec((model, hidden), lambda i: (0, 0)),
            pl.BlockSpec((model, hidden), lambda i: (0, 0)),
            pl.BlockSpec((hidden, model), lambda i: (0, 0)),
        ],
        out_specs=pl.BlockSpec((peers, tile, share), lambda i: (0, i, 0)),
        out_shape=jax.ShapeDtypeStruct((peers, count, share), jnp.bfloat16),
        compiler_params=pltpu.CompilerParams(
            dimension_semantics=("arbitrary",), vmem_limit_bytes=48 * 2**20
        ),
        name="expert",
    )(rows, gain, gate, up, down)


def shards(
    residual,
    queries,
    key_vectors,
    value_rows,
    head_lambda,
    head_gain,
    out_weight,
    ffn_gain,
    expert_gate,
    expert_up,
    expert_down,
    routing,
    route_weight,
):
    tok, _, width = queries.shape
    experts = lax.axis_size("sp")
    peers = lax.axis_size("tp")
    model = residual.shape[1]
    share = model // peers
    where = lax.axis_index("sp").astype(jnp.int32)[None]
    column = lax.axis_index("tp") * share
    kv = jnp.stack([key_vectors[:, 0], value_rows[:, 0]])
    kv_all = lax.all_gather(kv, "sp", axis=1, tiled=True)

    out_cols = lax.all_to_all(
        out_weight.reshape(width, peers, share).swapaxes(0, 1), "tp", 0, 0, tiled=True
    ).reshape(peers * width, share)
    hidden = expert_gate.shape[2]
    down_rows = lax.all_to_all(
        expert_down[0].reshape(peers, hidden, share), "tp", 0, 0, tiled=True
    )
    down_rows = down_rows.swapaxes(0, 1).reshape(hidden, model)

    capacity = tok // (experts // GROUPS)
    named = routing[:, :, None] == jnp.arange(experts, dtype=jnp.int32)
    member = jnp.any(named, axis=1)
    order = jnp.arange(tok, dtype=jnp.int32)
    strict = (order[None, :] < order[:, None]).astype(jnp.bfloat16)
    earlier = jnp.dot(
        strict, member.astype(jnp.bfloat16), preferred_element_type=jnp.float32
    ).astype(jnp.int32)
    slot = jnp.arange(capacity, dtype=jnp.int32)
    at_slot = earlier[:, :, None] == slot
    send = (member[:, :, None] & at_slot).reshape(tok, experts * capacity).astype(jnp.bfloat16)
    take = [
        (named[:, k, :, None] & at_slot).reshape(tok, experts * capacity).astype(jnp.bfloat16)
        for k in range(routing.shape[1])
    ]

    attended = attention(where, head_lambda, queries[:, 0], kv_all, head_gain[None])
    heads = lax.all_gather(attended, "tp", axis=1, tiled=True)
    own_stream = lax.dynamic_slice_in_dim(residual, column, share, 1).astype(jnp.float32) + jnp.dot(
        heads, out_cols, preferred_element_type=jnp.float32
    )

    outgoing = lax.dot_general(
        send, own_stream.astype(jnp.bfloat16), (((0,), (0,)), ((), ())),
        preferred_element_type=jnp.float32,
    ).astype(jnp.bfloat16)
    landed = lax.all_to_all(
        outgoing.reshape(experts, capacity, share), "sp", 0, 0, tiled=True
    ).reshape(experts * capacity, share)
    rows = lax.all_gather(landed, "tp", axis=1, tiled=True)
    parts = expert(rows, ffn_gain[None], expert_gate[0], expert_up[0], down_rows, peers)
    expert_out = lax.psum_scatter(parts, "tp", scatter_dimension=0, tiled=True)
    back = lax.all_to_all(
        expert_out.reshape(experts, capacity, share), "sp", 0, 0, tiled=True
    ).reshape(experts * capacity, share)
    moe = sum(
        route_weight[:, k : k + 1] * jnp.dot(take[k], back, preferred_element_type=jnp.float32)
        for k in range(routing.shape[1])
    )
    own_out = (own_stream + moe).astype(jnp.bfloat16)
    return lax.all_gather(own_out, "tp", axis=1, tiled=True)


def solution(mesh):
    in_specs = (
        P("sp", None),
        P("sp", "tp", None),
        P("sp", "tp", None),
        P("sp", "tp", None),
        P("tp"),
        P(),
        P("tp", None),
        P(),
        P("sp", None, "tp"),
        P("sp", None, "tp"),
        P("sp", None, "tp"),
        P("sp", None),
        P("sp", None),
    )
    return jax.shard_map(
        shards, mesh=mesh, in_specs=in_specs, out_specs=P("sp", None), check_vma=False
    )
```

time: 462 us -> 452 us (0.978)
  waiting for transfers between devices: 208 us -> 331 us
  blocking collectives: 138 us -> 60.3 us
  local copies, waits for them, and re-layouts: 32.7 us -> 7.55 us
  loops' own time: 21.5 us -> 0 us
  Pallas kernels: 0 us -> 10.9 us
  matrix products: 13.6 us -> 3.72 us
    unnamed x2 -> x6, waiting for transfers between devices: 0.03 us -> 93.1 us
    all_to_all x3 -> x2, blocking collectives: 138 us -> 60.3 us  [the longest x1 36.8 us: shards(): lax.all_to_all(outgoing.reshape(experts, capacity, share), 'sp', 0, 0, ti...]
    all_gather x2 -> x4, waiting for transfers between devices: 160 us -> 206 us  [the longest x1 79.9 us: shards(): kv_all = lax.all_gather(kv, 'sp', axis=1, tiled=True)]
    another operation x17 -> x0, loops' own time: 21.5 us -> none  [the longest x1 21.2 us: shards(): lax.scan(visit, running, (jnp.arange(block_count, dtype=jnp.int32), key_b...]
    all_to_all x3 -> x2, waiting for transfers between devices: 47.9 us -> 31.7 us  [the longest x1 22.2 us: shards(): lax.all_to_all(expert_out.reshape(experts, capacity, share), 'sp', 0, 0,...]
    pallas_call x0 -> x2, Pallas kernels: none -> 10.9 us  [the longest x1 7.88 us: expert(): pl.pallas_call(expert_body, grid=(count // tile,), in_specs=[pl.BlockSpec...]
    dynamic_slice x17 -> x0, local copies, waits for them, and re-layouts: 10.2 us -> none  [the longest x16 9.39 us: shards(): lax.scan(visit, running, (jnp.arange(block_count, dtype=jnp.int32), key_b...]
    dot_general x8 -> x5, matrix products: 13.6 us -> 3.72 us  [the longest x1 1.66 us: shards(): jnp.dot(heads, out_cols, preferred_element_type=jnp.float32)]
  transfers between devices with their start and end apart: 5 -> 7, of which waited for: 5 -> 7; matrix products, arithmetic and copies ran while one was open for 2% -> 1% of each run, Pallas kernels for 0% -> 0%
where the time goes in v1:
time: 452 us; the launch traced here: 451 us
  waiting for transfers between devices  331 us (73%)
  blocking collectives  60.3 us (13%)
  starting transfers between devices  21.5 us (5%)
  between operations  13.9 us (3%)
  Pallas kernels  10.9 us (2%)
  local copies, waits for them, and re-layouts  7.55 us (2%)
    unnamed x6, waiting for transfers between devices  93.1 us
    all_gather x1, waiting for transfers between devices, shards(): kv_all = lax.all_gather(kv, 'sp', axis=1, tiled=True)  79.9 us
    all_gather x1, waiting for transfers between devices, shards(): return lax.all_gather(own_out, 'tp', axis=1, tiled=True)  46 us
    all_gather x1, waiting for transfers between devices, shards(): heads = lax.all_gather(attended, 'tp', axis=1, tiled=True)  43.5 us
    all_to_all x1, blocking collectives, shards(): lax.all_to_all(outgoing.reshape(experts, capacity, share), 'sp', 0, 0, ti...  36.8 us
    all_gather x1, waiting for transfers between devices, shards(): rows = lax.all_gather(landed, 'tp', axis=1, tiled=True)  36.4 us
    all_to_all x1, blocking collectives, shards(): lax.all_to_all(expert_down[0].reshape(peers, hidden, share), 'tp', 0, 0,...  23.5 us
    all_to_all x1, waiting for transfers between devices, shards(): lax.all_to_all(expert_out.reshape(experts, capacity, share), 'sp', 0, 0,...  22.2 us
  transfers between devices with their start and end apart: 7, of which 7 were waited for; matrix products, arithmetic and copies ran while one was open for 1% of the time, Pallas kernels for 0%

profile of v1, /device:TPU:1, one launch (start us, length us, event | category | flops | bytes accessed | tf_op | source)
XLA Modules:
  0.0 451.0 jit_solution(1714208439037813824)
XLA Ops:
  6.5 1.5 pad_maximum_fusion
  8.8 79.9 %all-gather.5.cloned.1.call-done.kv_ref = bf16[2,8192,128]{2,1,0:T(8,128)(2,1)} async-done(((bf16[2,256,128]{2,1,0:T(8,128)(2,1)}), bf16[2,8192,128]{2,1,0:T(8,128)(2,1)}) %all-gather.5.cloned.1.call-update) | async-done | bytes 4194320 | tf_op jit(solution)/shard_map/all_gather | solution.py:159
  88.7 2.2 copy-done
  90.9 0.8 copy-done.3
  91.7 0.7 copy-done.5
  92.4 3.0 attention.1
  95.4 1.0 copy.19
  96.4 6.5 %all-to-all-start = ((bf16[16,128,128]{1,2,0:T(8,128)(2,1)}), bf16[16,128,128]{1,2,0:T(8,128)(2,1)S(1)}, u32[]{:S(2)}, u32[]{:S(2)}) async-start(bf16[16,128,128]{1,2,0:T(8,128)(2,1)} %bitcast.6), calls=%async_computation | async-start | bytes 1048576 | tf_op jit(solution)/shard_map/all_to_all | solution.py:161
  103.1 0.6 iota_compare_fusion.3
  104.2 9.6 %all-to-all-done = bf16[16,128,128]{1,2,0:T(8,128)(2,1)S(1)} async-done(((bf16[16,128,128]{1,2,0:T(8,128)(2,1)}), bf16[16,128,128]{1,2,0:T(8,128)(2,1)S(1)}, u32[]{:S(2)}, u32[]{:S(2)}) %all-to-all-start) | async-done | bytes 524320 | tf_op jit(solution)/shard_map/all_to_all | solution.py:161
  114.1 43.5 %all-gather.7.cloned.1.call-done = bf16[256,2048]{1,0:T(8,128)(2,1)} async-done(((bf16[256,128]{1,0:T(8,128)(2,1)}), bf16[256,2048]{1,0:T(8,128)(2,1)}) %all-gather.7.cloned.1.call-update) | async-done | bytes 1048592 | tf_op jit(solution)/shard_map/all_gather | solution.py:187
  157.6 1.7 convolution_add_fusion
  159.3 0.3 convolution_convert_fusion
  159.6 36.8 %all_to_all.20 = bf16[32,32,128]{2,1,0:T(8,128)(2,1)} all-to-all(bf16[32,32,128]{2,1,0:T(8,128)(2,1)S(1)} %bitcast.63), channel_id=1, replica_groups=mesh['sp'=32,'tp'=16] {'sp'}, dimensions={0} | all-to-all | bytes 524288 | tf_op jit(solution)/shard_map/all_to_all | solution.py:196
  196.5 23.5 %all_to_all.21 = bf16[16,256,128]{2,1,0:T(8,128)(2,1)S(1)} all-to-all(bf16[16,256,128]{2,1,0:T(8,128)(2,1)} %bitcast.61), channel_id=1, replica_groups=mesh['sp'=32,'tp'=16] {'tp'}, dimensions={0} | all-to-all | bytes 2097152 | tf_op jit(solution)/shard_map/all_to_all | solution.py:165
  220.2 36.4 %all-gather.9.cloned.1.call-done.rows_ref = bf16[1024,2048]{1,0:T(8,128)(2,1)} async-done(((bf16[1024,128]{1,0:T(8,128)(2,1)}), bf16[1024,2048]{1,0:T(8,128)(2,1)}) %all-gather.9.cloned.1.call-update) | async-done | bytes 4194320 | tf_op jit(solution)/shard_map/all_gather | solution.py:199
  256.6 7.9 %expert.1 = bf16[16,1024,128]{2,1,0:T(8,128)(2,1)} custom-call(bf16[1024,2048]{1,0:T(8,128)(2,1)} %all-gather.9.cloned.1.call-done.rows_ref, f32[1,2048]{1,0:T(1,128)S(1)} %bitcast.58, bf16[2048,256]{1,0:T(8,128)(2,1)S(1)} %bitcast.55, bf16[2048,256]{1,0:T(8,128)(2,1)S(1)} %bitcast.56, bf16[256,2048]{1,0:T(8,128)(2,1)S(1)} %copy_bitcast_fusion.down_ref), custom_call_target="tpu_custom_call" | custom-call | tf_op jit(solution)/shard_map/expert/pallas_call | solution.py:117
  264.5 93.0 %reduce-scatter.4.cloned.1.call-done = bf16[1,1024,128]{2,1,0:T(8,128)(2,1)} async-done(((bf16[16,1024,128]{2,1,0:T(8,128)(2,1)}), bf16[1,1024,128]{2,1,0:T(8,128)(2,1)}) %reduce-scatter.4.cloned.1.call-update) | async-done | bytes 262160
  357.5 14.8 %all-to-all-start.3 = ((bf16[32,32,128]{2,1,0:T(8,128)(2,1)}), bf16[32,32,128]{2,1,0:T(8,128)(2,1)S(1)}, u32[]{:S(2)}, u32[]{:S(2)}) async-start(bf16[32,32,128]{2,1,0:T(8,128)(2,1)} %bitcast.64), calls=%async_computation.3 | async-start | bytes 524288 | tf_op jit(solution)/shard_map/all_to_all | solution.py:202
  372.4 22.2 %all-to-all-done.3 = bf16[32,32,128]{2,1,0:T(8,128)(2,1)S(1)} async-done(((bf16[32,32,128]{2,1,0:T(8,128)(2,1)}), bf16[32,32,128]{2,1,0:T(8,128)(2,1)S(1)}, u32[]{:S(2)}, u32[]{:S(2)}) %all-to-all-start.3) | async-done | bytes 262176 | tf_op jit(solution)/shard_map/all_to_all | solution.py:202
  394.5 0.5 fusion.3
  395.0 1.1 fusion.4
  396.1 46.0 %all-gather.11.cloned.1.call-done = bf16[256,2048]{1,0:T(8,128)(2,1)} async-done(((bf16[256,128]{1,0:T(8,128)(2,1)}), bf16[256,2048]{1,0:T(8,128)(2,1)}) %all-gather.11.cloned.1.call-update) | async-done | bytes 1048592 | tf_op jit(solution)/shard_map/all_gather | solution.py:210
  442.2 2.3 copy.28
  (39 shorter events, 1.3 us)
Async XLA Ops:
  6.5 96.6 %copy-start.11 = (s32[256,2]{0,1:T(2,128)S(1)}, s32[256,2]{0,1:T(2,128)}, u32[]{:S(2)}) copy-start(s32[256,2]{0,1:T(2,128)} %param.24) | copy-start | bytes 6148
  6.5 82.2 %all-gather.5.cloned.1.call-start = ((), (), s32[]{:S(2)}) async-start(), calls=%async_computation.5 | async-start | bytes 4325376 | tf_op jit(solution)/shard_map/all_gather | solution.py:159
  8.1 149.5 %all-gather.7.cloned.1.call-start = ((), (), s32[]{:S(2)}) async-start(), calls=%async_computation.6 | async-start | bytes 1114112 | tf_op jit(solution)/shard_map/all_gather | solution.py:187
  88.7 2.2 copy-start
  90.9 0.8 copy-start.3
  91.7 0.7 copy-start.5
  92.4 3.0 copy-start.6
  96.4 17.3 %all-to-all-start = ((bf16[16,128,128]{1,2,0:T(8,128)(2,1)}), bf16[16,128,128]{1,2,0:T(8,128)(2,1)S(1)}, u32[]{:S(2)}, u32[]{:S(2)}) async-start(bf16[16,128,128]{1,2,0:T(8,128)(2,1)} %bitcast.6), calls=%async_computation | async-start | bytes 1048576 | tf_op jit(solution)/shard_map/all_to_all | solution.py:161
  103.0 153.6 %all-gather.9.cloned.1.call-start = ((), (), s32[]{:S(2)}) async-start(), calls=%async_computation.7 | async-start | bytes 4456448 | tf_op jit(solution)/shard_map/all_gather | solution.py:199
  103.9 53.7 %copy-start.8 = (s32[256,32]{0,1:T(8,128)}, s32[256,32]{0,1:T(8,128)S(1)}, u32[]{:S(2)}) copy-start(s32[256,32]{0,1:T(8,128)S(1)} %convolution_convert_fusion.1) | copy-start | bytes 98308
  104.2 152.4 %copy-start.1 = (bf16[1,2048,256]{2,1,0:T(8,128)(2,1)S(1)}, bf16[1,2048,256]{2,1,0:T(8,128)(2,1)}, u32[]{:S(2)}) copy-start(bf16[1,2048,256]{2,1,0:T(8,128)(2,1)} %param.21) | copy-start | bytes 3145732
  104.2 152.4 %copy-start.2 = (bf16[1,2048,256]{2,1,0:T(8,128)(2,1)S(1)}, bf16[1,2048,256]{2,1,0:T(8,128)(2,1)}, u32[]{:S(2)}) copy-start(bf16[1,2048,256]{2,1,0:T(8,128)(2,1)} %param.22) | copy-start | bytes 3145732
  104.2 152.3 %copy-start.4 = (f32[2048]{0:T(1024)S(1)}, f32[2048]{0:T(1024)}, u32[]{:S(2)}) copy-start(f32[2048]{0:T(1024)} %param.20) | copy-start | bytes 24580
  196.4 161.1 %reduce-scatter.4.cloned.1.call-start = ((), (), s32[]{:S(2)}) async-start(), calls=%async_computation.9 | async-start | bytes 4456448
  264.4 107.9 %copy-start.10 = (f32[256,2]{0,1:T(2,128)S(1)}, f32[256,2]{0,1:T(2,128)}, u32[]{:S(2)}) copy-start(f32[256,2]{0,1:T(2,128)} %param.25) | copy-start | bytes 6148
  264.4 107.9 %copy-start.7 = (pred[256,2,32]{0,2,1:T(8,128)(4,1)S(1)}, pred[256,2,32]{0,2,1:T(8,128)(4,1)}, u32[]{:S(2)}) copy-start(pred[256,2,32]{0,2,1:T(8,128)(4,1)} %get-tuple-element.9) | copy-start | bytes 49156
  264.4 130.1 %copy-start.9 = (s32[256,32]{0,1:T(8,128)S(1)}, s32[256,32]{0,1:T(8,128)}, u32[]{:S(2)}) copy-start(s32[256,32]{0,1:T(8,128)} %copy-done.8) | copy-start | bytes 98308
  357.5 37.1 %all-to-all-start.3 = ((bf16[32,32,128]{2,1,0:T(8,128)(2,1)}), bf16[32,32,128]{2,1,0:T(8,128)(2,1)S(1)}, u32[]{:S(2)}, u32[]{:S(2)}) async-start(bf16[32,32,128]{2,1,0:T(8,128)(2,1)} %bitcast.64), calls=%async_computation.3 | async-start | bytes 524288 | tf_op jit(solution)/shard_map/all_to_all | solution.py:202
  372.3 69.9 %all-gather.11.cloned.1.call-start = ((), (), s32[]{:S(2)}) async-start(), calls=%async_computation.8 | async-start | bytes 1114112 | tf_op jit(solution)/shard_map/all_gather | solution.py:210
Sparse Core Ops, SparseCore 0:
  9.5 79.1 all-gather.4
  95.5 62.0 all-gather.6
  196.5 59.9 all-gather.8
  264.6 92.8 reduce-scatter.3
  396.3 45.8 all-gather.10

commit v2 on v1

v2 whole, which is shorter than its diff:
```python
import jax
import jax.numpy as jnp
from jax import lax
from jax.experimental import pallas as pl
from jax.experimental.pallas import tpu as pltpu
from jax.sharding import PartitionSpec as P

norm_eps = 1e-06
KEY_BLOCK = 1024
GROUPS = 4


def attention_body(where_ref, lam_ref, q_ref, kv_ref, gain_ref, out_ref, stacked, highest, accum):
    step = pl.program_id(0)
    tok = q_ref.shape[0]
    width = q_ref.shape[1]
    first_query = where_ref[0] * tok
    last_step = (first_query + tok - 1) // KEY_BLOCK

    @pl.when(step == 0)
    def _():
        scaled = q_ref[...] * jnp.asarray((width // 2) ** -0.5, jnp.bfloat16)
        low = lax.broadcasted_iota(jnp.int32, scaled.shape, 1) < width // 2
        zero = jnp.zeros_like(scaled)
        stacked[:tok] = jnp.where(low, scaled, zero)
        stacked[tok:] = jnp.where(low, zero, scaled)
        highest[...] = jnp.full(highest.shape, -1e30, jnp.float32)
        accum[...] = jnp.zeros(accum.shape, jnp.float32)

    def update(masked):
        values = kv_ref[1]
        scores = lax.dot_general(
            stacked[...], kv_ref[0], (((1,), (1,)), ((), ())), preferred_element_type=jnp.float32
        )
        if masked:
            row = lax.broadcasted_iota(jnp.int32, scores.shape, 0)
            col = lax.broadcasted_iota(jnp.int32, scores.shape, 1)
            limit = jnp.where(row >= tok, row - tok, row) + (first_query - step * KEY_BLOCK)
            scores = jnp.where(col <= limit, scores, -1e30)
        before = highest[...]
        now = jnp.maximum(before, jnp.max(scores, axis=1, keepdims=True))
        weights = jnp.exp(scores - now[:, :1])
        shrink = jnp.exp(before - now)[:, :1]
        wide = jnp.concatenate([values, jnp.ones_like(values)], axis=1)
        blended = jnp.dot(weights.astype(jnp.bfloat16), wide, preferred_element_type=jnp.float32)
        accum[...] = accum[...] * shrink + blended
        highest[...] = now

    @pl.when(step < last_step)
    def _():
        update(False)

    @pl.when(step == last_step)
    def _():
        update(True)
        both = accum[:, :width] / accum[:, width:]
        combined = both[:tok] - lam_ref[0] * both[tok:]
        square = jnp.mean(combined * combined, axis=1, keepdims=True)
        out_ref[...] = (combined * lax.rsqrt(square + norm_eps) * gain_ref[...]).astype(jnp.bfloat16)


def attention(where, lam, q, kv, gain):
    tok, width = q.shape
    steps = kv.shape[1] // KEY_BLOCK

    def kv_at(j, where_ref, lam_ref):
        return (0, jnp.minimum(j, (where_ref[0] * tok + tok - 1) // KEY_BLOCK), 0)

    def fixed(j, where_ref, lam_ref):
        return (0, 0)

    grid = pltpu.PrefetchScalarGridSpec(
        num_scalar_prefetch=2,
        grid=(steps,),
        in_specs=[
            pl.BlockSpec((tok, width), fixed),
            pl.BlockSpec((2, KEY_BLOCK, width), kv_at),
            pl.BlockSpec((1, width), fixed),
        ],
        out_specs=pl.BlockSpec((tok, width), fixed),
        scratch_shapes=[
            pltpu.VMEM((2 * tok, width), jnp.bfloat16),
            pltpu.VMEM((2 * tok, 128), jnp.float32),
            pltpu.VMEM((2 * tok, 2 * width), jnp.float32),
        ],
    )
    return pl.pallas_call(
        attention_body,
        grid_spec=grid,
        out_shape=jax.ShapeDtypeStruct((tok, width), jnp.bfloat16),
        compiler_params=pltpu.CompilerParams(
            dimension_semantics=("arbitrary",), vmem_limit_bytes=24 * 2**20
        ),
        name="attention",
    )(where, lam, q, kv, gain)


def project_body(column_ref, heads_ref, weight_ref, residual_ref, send_ref, stream_ref, out_ref):
    total = residual_ref[...].astype(jnp.float32)
    for p in range(0, heads_ref.shape[0], 2):
        both = jnp.concatenate([heads_ref[p], heads_ref[p + 1]], axis=1)
        rows = jnp.concatenate([weight_ref[p], weight_ref[p + 1]], axis=0)
        total += jnp.dot(both, rows, preferred_element_type=jnp.float32)
    stream_ref[...] = total
    picked = jnp.dot(send_ref[...], total.astype(jnp.bfloat16), preferred_element_type=jnp.float32)
    out_ref[...] = picked.astype(jnp.bfloat16)


def project(column, heads, weight, residual, send):
    peers, tok, width = heads.shape
    share = weight.shape[2]
    slots = send.shape[0]

    def whole(rank):
        return lambda i, column_ref: (0,) * rank

    grid = pltpu.PrefetchScalarGridSpec(
        num_scalar_prefetch=1,
        grid=(1,),
        in_specs=[
            pl.BlockSpec((peers, tok, width), whole(3)),
            pl.BlockSpec((peers, width, share), whole(3)),
            pl.BlockSpec((tok, share), lambda i, column_ref: (0, column_ref[0])),
            pl.BlockSpec((slots, tok), whole(2)),
        ],
        out_specs=[pl.BlockSpec((tok, share), whole(2)), pl.BlockSpec((slots, share), whole(2))],
    )
    return pl.pallas_call(
        project_body,
        grid_spec=grid,
        out_shape=[
            jax.ShapeDtypeStruct((tok, share), jnp.float32),
            jax.ShapeDtypeStruct((slots, share), jnp.bfloat16),
        ],
        compiler_params=pltpu.CompilerParams(vmem_limit_bytes=16 * 2**20),
        name="project",
    )(column, heads, weight, residual, send)


def expert_body(x_ref, rows_ref, gain_ref, *refs):
    pieces = (len(refs) - 4) // 2
    gates, ups, down_ref, out_ref = refs[:pieces], refs[pieces:-4], refs[-4], refs[-3]
    normed_ref, accum = refs[-2:]
    peers, count, share = rows_ref.shape
    hidden = gates[0].shape[1]
    total = jnp.zeros((count, 1), jnp.float32)
    for p in range(peers):
        part = rows_ref[p].astype(jnp.float32)
        total += jnp.sum(part * part, axis=1, keepdims=True)
    scale = lax.rsqrt(total / (peers * share) + norm_eps)
    for p in range(peers):
        cols = slice(p * share, (p + 1) * share)
        normed_ref[:, cols] = (rows_ref[p].astype(jnp.float32) * scale * gain_ref[:, cols]).astype(
            jnp.bfloat16
        )
    for k in range(pieces):
        normed = normed_ref[...]
        gate = jnp.dot(normed, gates[k][...], preferred_element_type=jnp.float32)
        up = jnp.dot(normed, ups[k][...], preferred_element_type=jnp.float32)
        act = (gate / (1.0 + jnp.exp(-gate)) * up).astype(jnp.bfloat16)
        source = lax.rem(x_ref[0] + (pieces - k), pieces)
        down = down_ref[pl.ds(pl.multiple_of(source * hidden, hidden), hidden), :]
        part = jnp.dot(act, down, preferred_element_type=jnp.float32)
        if k == 0:
            accum[...] = part
        elif k < pieces - 1:
            accum[...] += part
        else:
            done = (accum[...] + part).astype(jnp.bfloat16)
            for p in range(peers):
                out_ref[p] = done[:, p * share : (p + 1) * share]


def expert(x, rows, gain, gates, ups, down):
    peers, count, share = rows.shape
    vmem = pl.BlockSpec(memory_space=pltpu.VMEM)
    return pl.pallas_call(
        expert_body,
        in_specs=[pl.BlockSpec(memory_space=pltpu.SMEM)] + [vmem] * (3 + len(gates) + len(ups)),
        out_specs=vmem,
        out_shape=jax.ShapeDtypeStruct((peers, count, share), jnp.bfloat16),
        scratch_shapes=[
            pltpu.VMEM((count, peers * share), jnp.bfloat16),
            pltpu.VMEM((count, peers * share), jnp.float32),
        ],
        compiler_params=pltpu.CompilerParams(vmem_limit_bytes=40 * 2**20),
        name="expert",
    )(x, rows, gain, *gates, *ups, down)


def from_everyone(array, axes):
    peers = lax.axis_size(axes)
    return lax.all_to_all(
        jnp.broadcast_to(array[None], (peers, *array.shape)), axes, 0, 0, tiled=True
    )


def shards(
    residual,
    queries,
    key_vectors,
    value_rows,
    head_lambda,
    head_gain,
    out_weight,
    ffn_gain,
    expert_gate,
    expert_up,
    expert_down,
    routing,
    route_weight,
):
    tok, _, width = queries.shape
    experts = lax.axis_size("sp")
    across = lax.axis_size("x")
    along = lax.axis_size("y")
    peers = across * along
    model = residual.shape[1]
    share = model // peers
    hidden = expert_gate.shape[2]
    where = lax.axis_index("sp").astype(jnp.int32)[None]
    column = (lax.axis_index("y") * across + lax.axis_index("x")).astype(jnp.int32)[None]
    x_at = lax.axis_index("x").astype(jnp.int32)[None]
    kv = jnp.stack([key_vectors[:, 0], value_rows[:, 0]])
    kv_all = lax.all_gather(kv, "sp", axis=1, tiled=True)

    ahead = [(i, (i + 1) % across) for i in range(across)]
    behind = [(i, (i - 1) % across) for i in range(across)]
    gate, up = expert_gate[0], expert_up[0]
    gate_1, up_1 = lax.ppermute(gate, "x", ahead), lax.ppermute(up, "x", ahead)
    gate_3, up_3 = lax.ppermute(gate, "x", behind), lax.ppermute(up, "x", behind)
    gate_2, up_2 = lax.ppermute(gate_1, "x", ahead), lax.ppermute(up_3, "x", behind)
    gates, ups = [gate, gate_1, gate_2, gate_3], [up, up_1, up_2, up_3]

    down = expert_down[0].reshape(along, across * hidden, share)
    down = jnp.broadcast_to(down[:, None], (along, across, across * hidden, share))
    down = lax.all_to_all(
        down.reshape(peers, across * hidden, share), ("y", "x"), 0, 0, tiled=True
    )
    down = down.swapaxes(0, 1).reshape(across * hidden, model)
    out_cols = lax.all_to_all(
        out_weight.reshape(width, peers, share).swapaxes(0, 1), ("y", "x"), 0, 0, tiled=True
    )

    capacity = tok // (experts // GROUPS)
    order = jnp.arange(tok, dtype=jnp.int32)
    ids = jnp.arange(experts, dtype=jnp.int32)
    named = routing[:, :, None] == ids
    member = jnp.any(named, axis=1)
    strict = (order[None, :] < order[:, None]).astype(jnp.bfloat16)
    earlier = jnp.dot(
        strict, member.astype(jnp.bfloat16), preferred_element_type=jnp.float32
    ).astype(jnp.int32)
    slot = jnp.arange(capacity, dtype=jnp.int32)
    send = (member.T[:, None, :] & (earlier.T[:, None, :] == slot[None, :, None])).reshape(
        experts * capacity, tok
    )
    send = send.astype(jnp.bfloat16)
    take = [
        (named[:, k, :, None] & (earlier[:, :, None] == slot))
        .reshape(tok, experts * capacity)
        .astype(jnp.bfloat16)
        for k in range(routing.shape[1])
    ]

    attended = attention(where, head_lambda, queries[:, 0], kv_all, head_gain[None])
    heads = from_everyone(attended, ("y", "x"))
    own_stream, outgoing = project(column, heads, out_cols, residual, send)
    landed = lax.all_to_all(
        outgoing.reshape(experts, capacity, share), "sp", 0, 0, tiled=True
    )
    count = experts * capacity // across
    quarters = jnp.broadcast_to(
        landed.reshape(1, across, count, share), (along, across, count, share)
    )
    rows = lax.all_to_all(quarters.reshape(peers, count, share), ("y", "x"), 0, 0, tiled=True)
    parts = expert(x_at, rows, ffn_gain[None], gates, ups, down)
    arrived = lax.all_to_all(parts, ("y", "x"), 0, 0, tiled=True)
    expert_out = (
        arrived.reshape(along, across * count, share).astype(jnp.float32).sum(axis=0)
    ).astype(jnp.bfloat16)
    back = lax.all_to_all(
        expert_out.reshape(experts, capacity, share), "sp", 0, 0, tiled=True
    ).reshape(experts * capacity, share)
    moe = sum(
        route_weight[:, k : k + 1] * jnp.dot(take[k], back, preferred_element_type=jnp.float32)
        for k in range(routing.shape[1])
    )
    own_out = (own_stream + moe).astype(jnp.bfloat16)
    whole = from_everyone(own_out, ("y", "x"))
    return whole.swapaxes(0, 1).reshape(tok, model)


def solution(mesh):
    sizes = mesh.devices.shape
    y = int(sizes[1] ** 0.5)
    split = jax.sharding.Mesh(
        mesh.devices.reshape(sizes[0], y, sizes[1] // y), ("sp", "y", "x")
    )
    tp = ("y", "x")
    in_specs = (
        P("sp", None),
        P("sp", tp, None),
        P("sp", tp, None),
        P("sp", tp, None),
        P(tp),
        P(),
        P(tp, None),
        P(),
        P("sp", None, tp),
        P("sp", None, tp),
        P("sp", None, tp),
        P("sp", None),
        P("sp", None),
    )
    return jax.shard_map(
        shards, mesh=split, in_specs=in_specs, out_specs=P("sp", None), check_vma=False
    )
```

time: 452 us -> 366 us (0.81)
  waiting for transfers between devices: 331 us -> 186 us
  starting transfers between devices: 21.5 us -> 69.7 us
  local copies, waits for them, and re-layouts: 7.55 us -> 17.5 us
    all_gather x3 -> x0, waiting for transfers between devices: 126 us -> none  [the longest x1 46 us: shards(): return lax.all_gather(own_out, 'tp', axis=1, tiled=True)]
    unnamed x6 -> x1, waiting for transfers between devices: 93.1 us -> 0.02 us
    all_to_all x1 -> x4, waiting for transfers between devices: 9.56 us -> 69.9 us  [the longest x1 51.9 us: shards(): lax.all_to_all(down.reshape(peers, across * hidden, share), ('y', 'x'), 0...]
    all_to_all x1 -> x4, starting transfers between devices: 6.53 us -> 38 us  [the longest x1 21.2 us: shards(): lax.all_to_all(outgoing.reshape(experts, capacity, share), 'sp', 0, 0, ti...]
    ppermute x0 -> x6, waiting for transfers between devices: none -> 23.8 us  [the longest x1 23.8 us: shards(): lax.ppermute(gate_1, 'x', ahead)]
    ppermute x0 -> x6, starting transfers between devices: none -> 18.3 us  [the longest x1 4.57 us: shards(): lax.ppermute(up_3, 'x', behind)]
    all_gather x1, waiting for transfers between devices: 79.9 us -> 69.9 us  [shards(): kv_all = lax.all_gather(kv, 'sp', axis=1, tiled=True)]
    reshape x1 -> x3, local copies, waits for them, and re-layouts: 0.15 us -> 7.41 us  [the longest x1 4.97 us: shards(): down = down.swapaxes(0, 1).reshape(across * hidden, model)]
  transfers between devices with their start and end apart: 7 -> 12, of which waited for: 7 -> 6; matrix products, arithmetic and copies ran while one was open for 1% -> 2% of each run, Pallas kernels for 0% -> 1%
where the time goes in v2:
time: 366 us; the launch traced here: 365 us
  waiting for transfers between devices  186 us (51%)
  starting transfers between devices  69.7 us (19%)
  blocking collectives  61.8 us (17%)
  local copies, waits for them, and re-layouts  17.5 us (5%)
  between operations  14.3 us (4%)
  Pallas kernels  12.2 us (3%)
    all_gather x1, waiting for transfers between devices, shards(): kv_all = lax.all_gather(kv, 'sp', axis=1, tiled=True)  69.9 us
    all_to_all x1, waiting for transfers between devices, shards(): lax.all_to_all(down.reshape(peers, across * hidden, share), ('y', 'x'), 0...  51.9 us
    all_to_all x2, blocking collectives, from_everyone(): lax.all_to_all(jnp.broadcast_to(array[None], (peers, *array.shape)), axes...  41.5 us
    ppermute x1, waiting for transfers between devices, shards(): lax.ppermute(gate_1, 'x', ahead)  23.8 us
    all_to_all x1, waiting for transfers between devices, shards(): lax.all_to_all(expert_out.reshape(experts, capacity, share), 'sp', 0, 0,...  22.2 us
    all_to_all x1, starting transfers between devices, shards(): lax.all_to_all(outgoing.reshape(experts, capacity, share), 'sp', 0, 0, ti...  21.2 us
    all_to_all x1, blocking collectives, shards(): arrived = lax.all_to_all(parts, ('y', 'x'), 0, 0, tiled=True)  20.3 us
    all_to_all x1, starting transfers between devices, shards(): lax.all_to_all(expert_out.reshape(experts, capacity, share), 'sp', 0, 0,...  13.4 us
  transfers between devices with their start and end apart: 12, of which 6 were waited for; matrix products, arithmetic and copies ran while one was open for 2% of the time, Pallas kernels for 1%

profile of v2, /device:TPU:1, one launch (start us, length us, event | category | flops | bytes accessed | tf_op | source)
XLA Modules:
  0.0 365.2 jit_solution(9982081517493146938)
XLA Ops:
  10.4 7.7 %all-to-all-start.1 = ((bf16[16,128,128]{2,1,0:T(8,128)(2,1)}), bf16[16,128,128]{2,1,0:T(8,128)(2,1)S(1)}, u32[]{:S(2)}, u32[]{:S(2)}) async-start(bf16[16,128,128]{2,1,0:T(8,128)(2,1)} %bitcast.7), calls=%async_computation.1 | async-start | bytes 1048576 | tf_op jit(solution)/shard_map/all_to_all | solution.py:241
  18.8 69.9 %all-gather.2.cloned.1.call-done.kv_ref = bf16[2,8192,128]{2,1,0:T(8,128)(2,1)} async-done(((bf16[2,256,128]{2,1,0:T(8,128)(2,1)}), bf16[2,8192,128]{2,1,0:T(8,128)(2,1)}) %all-gather.2.cloned.1.call-update) | async-done | bytes 4194320 | tf_op jit(solution)/shard_map/all_gather | solution.py:225
  88.7 2.2 copy-done
  92.3 2.4 attention.1
  95.0 22.8 %all_to_all.40.heads_ref = bf16[16,256,128]{2,1,0:T(8,128)(2,1)S(1)} all-to-all(bf16[16,256,128]{2,1,0:T(8,128)(2,1)S(1)} %broadcast_in_dim.25), channel_id=1, replica_groups=mesh['sp'=32,'y'=4,'x'=4] {'y','x'}, dimensions={0} | all-to-all | bytes 2097152 | tf_op jit(solution)/shard_map/all_to_all | solution.py:193
  117.8 2.8 broadcast_in_dim.61
  120.6 4.7 %all-to-all-start.4 = ((bf16[16,1024,128]{2,1,0:T(8,128)(2,1)}), bf16[16,1024,128]{2,1,0:T(8,128)(2,1)}, u32[]{:S(2)}, u32[]{:S(2)}) async-start(bf16[16,1024,128]{2,1,0:T(8,128)(2,1)} %bitcast.72), calls=%async_computation.4 | async-start | bytes 8388608 | tf_op jit(solution)/shard_map/all_to_all | solution.py:237
  125.3 3.1 collective-permute-start
  128.4 3.4 collective-permute-start.4
  133.7 51.9 %all-to-all-done.4 = bf16[16,1024,128]{2,1,0:T(8,128)(2,1)} async-done(((bf16[16,1024,128]{2,1,0:T(8,128)(2,1)}), bf16[16,1024,128]{2,1,0:T(8,128)(2,1)}, u32[]{:S(2)}, u32[]{:S(2)}) %all-to-all-start.4) | async-done | bytes 4194336 | tf_op jit(solution)/shard_map/all_to_all | solution.py:237
  185.7 21.2 %all-to-all-start.2 = ((bf16[32,32,128]{2,1,0:T(8,128)(2,1)}), bf16[32,32,128]{2,1,0:T(8,128)(2,1)S(1)}, u32[]{:S(2)}, u32[]{:S(2)}) async-start(bf16[32,32,128]{2,1,0:T(8,128)(2,1)} %bitcast.15), calls=%async_computation.2 | async-start | bytes 524288 | tf_op jit(solution)/shard_map/all_to_all | solution.py:269
  206.9 2.6 collective-permute-start.2
  209.5 2.7 collective-permute-start.3
  214.1 4.6 %collective-permute-start.5 = (bf16[2048,256]{1,0:T(8,128)(2,1)}, bf16[2048,256]{1,0:T(8,128)(2,1)}, u32[]{:S(2)}, u32[]{:S(2)}) collective-permute-start(bf16[2048,256]{1,0:T(8,128)(2,1)} %collective-permute-done.4.refs_7_), channel_id=1, source_target_pairs={{0,3},{1,0},{2,1},{3,2},{4,7},{5,4},{6,5},{7,6},{8,11},{9,8},{10,9... | collective-permute-start | bytes 3145736 | tf_op jit(solution)/shard_map/ppermute | solution.py:232
  218.7 10.4 %all-to-all-done.2 = bf16[32,32,128]{2,1,0:T(8,128)(2,1)S(1)} async-done(((bf16[32,32,128]{2,1,0:T(8,128)(2,1)}), bf16[32,32,128]{2,1,0:T(8,128)(2,1)S(1)}, u32[]{:S(2)}, u32[]{:S(2)}) %all-to-all-start.2) | async-done | bytes 262176 | tf_op jit(solution)/shard_map/all_to_all | solution.py:269
  230.3 4.5 %all-to-all-start.3 = ((bf16[16,256,128]{2,1,0:T(8,128)(2,1)}), bf16[16,256,128]{2,1,0:T(8,128)(2,1)S(1)}, u32[]{:S(2)}, u32[]{:S(2)}) async-start(bf16[16,256,128]{2,1,0:T(8,128)(2,1)} %bitcast.17), calls=%async_computation.3 | async-start | bytes 2097152 | tf_op jit(solution)/shard_map/all_to_all | solution.py:276
  234.8 5.0 %copy_bitcast_fusion.refs_8_ = bf16[1024,2048]{1,0:T(8,128)(2,1)} fusion(bf16[16,1024,128]{2,1,0:T(8,128)(2,1)} %all-to-all-done.4), kind=kLoop, calls=%fused_computation | loop fusion | bytes 8388608 | tf_op jit(solution)/shard_map/reshape | solution.py:240
  239.8 23.8 %collective-permute-done.1.refs_2_ = bf16[2048,256]{1,0:T(8,128)(2,1)} collective-permute-done((bf16[2048,256]{1,0:T(8,128)(2,1)}, bf16[2048,256]{1,0:T(8,128)(2,1)}, u32[]{:S(2)}, u32[]{:S(2)}) %collective-permute-start.1) | collective-permute-done | bytes 1048608 | tf_op jit(solution)/shard_map/ppermute | solution.py:232
  263.6 7.6 %all-to-all-done.3.rows_ref = bf16[16,256,128]{2,1,0:T(8,128)(2,1)S(1)} async-done(((bf16[16,256,128]{2,1,0:T(8,128)(2,1)}), bf16[16,256,128]{2,1,0:T(8,128)(2,1)S(1)}, u32[]{:S(2)}, u32[]{:S(2)}) %all-to-all-start.3) | async-done | bytes 1048608 | tf_op jit(solution)/shard_map/all_to_all | solution.py:276
  271.2 8.5 %expert.1 = bf16[16,256,128]{2,1,0:T(8,128)(2,1)S(1)} custom-call(s32[1]{0:T(128)} %bitcast.14.x_ref, bf16[16,256,128]{2,1,0:T(8,128)(2,1)S(1)} %all-to-all-done.3.rows_ref, f32[1,2048]{1,0:T(1,128)S(1)} %bitcast.70, bf16[2048,256]{1,0:T(8,128)(2,1)S(1)} %bitcast.65, bf16[2048,256]{1,0:T(8,128)(2,1)} %collective-permute-done.refs_1_, ...), custom_call_target="tpu_custom_call" | custom-call | tf_op jit(solution)/shard_map/expert/pallas_call | solution.py:177
  279.6 20.3 %all_to_all.41 = bf16[16,256,128]{2,1,0:T(8,128)(2,1)S(1)} all-to-all(bf16[16,256,128]{2,1,0:T(8,128)(2,1)S(1)} %expert.1), channel_id=1, replica_groups=mesh['sp'=32,'y'=4,'x'=4] {'y','x'}, dimensions={0} | all-to-all | bytes 2097152 | tf_op jit(solution)/shard_map/all_to_all | solution.py:278
  300.8 13.4 %all-to-all-start.6 = ((bf16[32,32,128]{2,1,0:T(8,128)(2,1)}), bf16[32,32,128]{2,1,0:T(8,128)(2,1)S(1)}, u32[]{:S(2)}, u32[]{:S(2)}) async-start(bf16[32,32,128]{2,1,0:T(8,128)(2,1)} %bitcast.25), calls=%async_computation.6 | async-start | bytes 524288 | tf_op jit(solution)/shard_map/all_to_all | solution.py:282
  314.2 22.2 %all-to-all-done.6 = bf16[32,32,128]{2,1,0:T(8,128)(2,1)S(1)} async-done(((bf16[32,32,128]{2,1,0:T(8,128)(2,1)}), bf16[32,32,128]{2,1,0:T(8,128)(2,1)S(1)}, u32[]{:S(2)}, u32[]{:S(2)}) %all-to-all-start.6) | async-done | bytes 262176 | tf_op jit(solution)/shard_map/all_to_all | solution.py:282
  337.6 18.7 %all_to_all.42 = bf16[16,256,128]{2,1,0:T(8,128)(2,1)S(1)} all-to-all(bf16[16,256,128]{2,1,0:T(8,128)(2,1)S(1)} %broadcast_in_dim.62), channel_id=1, replica_groups=mesh['sp'=32,'y'=4,'x'=4] {'y','x'}, dimensions={0} | all-to-all | bytes 2097152 | tf_op jit(solution)/shard_map/all_to_all | solution.py:193
  (47 shorter events, 14.6 us)
Async XLA Ops:
  6.5 82.1 %all-gather.2.cloned.1.call-start = ((), (), s32[]{:S(2)}) async-start(), calls=%async_computation.8 | async-start | bytes 4325376 | tf_op jit(solution)/shard_map/all_gather | solution.py:225
  10.4 107.3 %copy-start.7 = (bf16[1,4096,128]{2,1,0:T(8,128)(2,1)S(1)}, bf16[1,4096,128]{2,1,0:T(8,128)(2,1)}, u32[]{:S(2)}) copy-start(bf16[1,4096,128]{2,1,0:T(8,128)(2,1)} %param.23) | copy-start | bytes 3145732
  10.4 84.3 %all-to-all-start.1 = ((bf16[16,128,128]{2,1,0:T(8,128)(2,1)}), bf16[16,128,128]{2,1,0:T(8,128)(2,1)S(1)}, u32[]{:S(2)}, u32[]{:S(2)}) async-start(bf16[16,128,128]{2,1,0:T(8,128)(2,1)} %bitcast.7), calls=%async_computation.1 | async-start | bytes 1048576 | tf_op jit(solution)/shard_map/all_to_all | solution.py:241
  88.7 2.2 copy-start
  90.8 0.8 copy-start.4
  91.7 0.7 copy-start.6
  120.6 11.2 %copy-start.9 = (s32[256,2]{0,1:T(2,128)S(1)}, s32[256,2]{0,1:T(2,128)}, u32[]{:S(2)}) copy-start(s32[256,2]{0,1:T(2,128)} %param.24) | copy-start | bytes 6148
  120.6 11.7 %copy-start.1 = (bf16[256,2048]{1,0:T(8,128)(2,1)S(1)}, bf16[256,2048]{1,0:T(8,128)(2,1)}, u32[]{:S(2)}) copy-start(bf16[256,2048]{1,0:T(8,128)(2,1)} %residual_ref.1) | copy-start | bytes 3145732
  120.6 65.1 %all-to-all-start.4 = ((bf16[16,1024,128]{2,1,0:T(8,128)(2,1)}), bf16[16,1024,128]{2,1,0:T(8,128)(2,1)}, u32[]{:S(2)}, u32[]{:S(2)}) async-start(bf16[16,1024,128]{2,1,0:T(8,128)(2,1)} %bitcast.72), calls=%async_computation.4 | async-start | bytes 8388608 | tf_op jit(solution)/shard_map/all_to_all | solution.py:237
  125.3 86.9 %collective-permute-start = (bf16[2048,256]{1,0:T(8,128)(2,1)}, bf16[2048,256]{1,0:T(8,128)(2,1)}, u32[]{:S(2)}, u32[]{:S(2)}) collective-permute-start(bf16[2048,256]{1,0:T(8,128)(2,1)} %bitcast.63), channel_id=1, source_target_pairs={{0,1},{1,2},{2,3},{3,0},{4,5},{5,6},{6,7},{7,4},{8,9},{9,10},{10,1... | collective-permute-start | bytes 3145736 | tf_op jit(solution)/shard_map/ppermute | solution.py:230
  128.4 85.8 %collective-permute-start.4 = (bf16[2048,256]{1,0:T(8,128)(2,1)}, bf16[2048,256]{1,0:T(8,128)(2,1)}, u32[]{:S(2)}, u32[]{:S(2)}) collective-permute-start(bf16[2048,256]{1,0:T(8,128)(2,1)} %bitcast.66), channel_id=1, source_target_pairs={{0,3},{1,0},{2,1},{3,2},{4,7},{5,4},{6,5},{7,6},{8,11},{9,8},{10,9... | collective-permute-start | bytes 3145736 | tf_op jit(solution)/shard_map/ppermute | solution.py:231
  185.7 43.5 %all-to-all-start.2 = ((bf16[32,32,128]{2,1,0:T(8,128)(2,1)}), bf16[32,32,128]{2,1,0:T(8,128)(2,1)S(1)}, u32[]{:S(2)}, u32[]{:S(2)}) async-start(bf16[32,32,128]{2,1,0:T(8,128)(2,1)} %bitcast.15), calls=%async_computation.2 | async-start | bytes 524288 | tf_op jit(solution)/shard_map/all_to_all | solution.py:269
  206.9 32.9 %collective-permute-start.2 = (bf16[2048,256]{1,0:T(8,128)(2,1)}, bf16[2048,256]{1,0:T(8,128)(2,1)}, u32[]{:S(2)}, u32[]{:S(2)}) collective-permute-start(bf16[2048,256]{1,0:T(8,128)(2,1)} %bitcast.64), channel_id=1, source_target_pairs={{0,3},{1,0},{2,1},{3,2},{4,7},{5,4},{6,5},{7,6},{8,11},{9,8},{10,9... | collective-permute-start | bytes 3145736 | tf_op jit(solution)/shard_map/ppermute | solution.py:231
  209.5 30.3 %collective-permute-start.3 = (bf16[2048,256]{1,0:T(8,128)(2,1)}, bf16[2048,256]{1,0:T(8,128)(2,1)}, u32[]{:S(2)}, u32[]{:S(2)}) collective-permute-start(bf16[2048,256]{1,0:T(8,128)(2,1)} %bitcast.67), channel_id=1, source_target_pairs={{0,1},{1,2},{2,3},{3,0},{4,5},{5,6},{6,7},{7,4},{8,9},{9,10},{10,1... | collective-permute-start | bytes 3145736 | tf_op jit(solution)/shard_map/ppermute | solution.py:230
  212.2 51.4 %collective-permute-start.1 = (bf16[2048,256]{1,0:T(8,128)(2,1)}, bf16[2048,256]{1,0:T(8,128)(2,1)}, u32[]{:S(2)}, u32[]{:S(2)}) collective-permute-start(bf16[2048,256]{1,0:T(8,128)(2,1)} %collective-permute-done.refs_1_), channel_id=1, source_target_pairs={{0,1},{1,2},{2,3},{3,0},{4,5},{5,6},{6,7},{7,4},{8,9},{9,10},{10,1... | collective-permute-start | bytes 3145736 | tf_op jit(solution)/shard_map/ppermute | solution.py:232
  214.1 49.4 %collective-permute-start.5 = (bf16[2048,256]{1,0:T(8,128)(2,1)}, bf16[2048,256]{1,0:T(8,128)(2,1)}, u32[]{:S(2)}, u32[]{:S(2)}) collective-permute-start(bf16[2048,256]{1,0:T(8,128)(2,1)} %collective-permute-done.4.refs_7_), channel_id=1, source_target_pairs={{0,3},{1,0},{2,1},{3,2},{4,7},{5,4},{6,5},{7,6},{8,11},{9,8},{10,9... | collective-permute-start | bytes 3145736 | tf_op jit(solution)/shard_map/ppermute | solution.py:232
  230.3 40.8 %all-to-all-start.3 = ((bf16[16,256,128]{2,1,0:T(8,128)(2,1)}), bf16[16,256,128]{2,1,0:T(8,128)(2,1)S(1)}, u32[]{:S(2)}, u32[]{:S(2)}) async-start(bf16[16,256,128]{2,1,0:T(8,128)(2,1)} %bitcast.17), calls=%async_computation.3 | async-start | bytes 2097152 | tf_op jit(solution)/shard_map/all_to_all | solution.py:276
  234.8 36.4 %copy-start.2 = (bf16[1,2048,256]{2,1,0:T(8,128)(2,1)S(1)}, bf16[1,2048,256]{2,1,0:T(8,128)(2,1)}, u32[]{:S(2)}) copy-start(bf16[1,2048,256]{2,1,0:T(8,128)(2,1)} %param.21) | copy-start | bytes 3145732
  234.8 36.4 %copy-start.3 = (bf16[1,2048,256]{2,1,0:T(8,128)(2,1)S(1)}, bf16[1,2048,256]{2,1,0:T(8,128)(2,1)}, u32[]{:S(2)}) copy-start(bf16[1,2048,256]{2,1,0:T(8,128)(2,1)} %param.22) | copy-start | bytes 3145732
  234.8 36.3 %copy-start.5 = (f32[2048]{0:T(1024)S(1)}, f32[2048]{0:T(1024)}, u32[]{:S(2)}) copy-start(f32[2048]{0:T(1024)} %param.20) | copy-start | bytes 24580
  271.1 43.1 %copy-start.8 = (f32[256,2]{0,1:T(2,128)S(1)}, f32[256,2]{0,1:T(2,128)}, u32[]{:S(2)}) copy-start(f32[256,2]{0,1:T(2,128)} %param.25) | copy-start | bytes 6148
  300.8 35.7 %all-to-all-start.6 = ((bf16[32,32,128]{2,1,0:T(8,128)(2,1)}), bf16[32,32,128]{2,1,0:T(8,128)(2,1)S(1)}, u32[]{:S(2)}, u32[]{:S(2)}) async-start(bf16[32,32,128]{2,1,0:T(8,128)(2,1)} %bitcast.25), calls=%async_computation.6 | async-start | bytes 524288 | tf_op jit(solution)/shard_map/all_to_all | solution.py:282
Sparse Core Ops, SparseCore 0:
  9.5 79.1 all-gather.1

commit v3 on v1

v3 whole, which is shorter than its diff:
```python
import jax
import jax.numpy as jnp
from jax import lax
from jax.experimental import pallas as pl
from jax.experimental.pallas import tpu as pltpu
from jax.sharding import PartitionSpec as P

norm_eps = 1e-06
KEY_BLOCK = 2048
ROW_BLOCK = 128
SHIFT = 4096.0
GROUPS = 4


def attention_body(where_ref, lam_ref, q_ref, kv_ref, gain_ref, weight_ref, out_ref, stacked, highest, accum):
    tok, width = q_ref.shape
    first_query = where_ref[0] * tok
    last = (first_query + tok - 1) // KEY_BLOCK
    scaled = q_ref[...] * jnp.asarray((width // 2) ** -0.5, jnp.bfloat16)
    low = lax.broadcasted_iota(jnp.int32, scaled.shape, 1) < width // 2
    zero = jnp.zeros_like(scaled)
    stacked[:tok] = jnp.where(low, scaled, zero)
    stacked[tok:] = jnp.where(low, zero, scaled)
    highest[...] = jnp.full(highest.shape, -1e30, jnp.float32)
    accum[...] = jnp.zeros(accum.shape, jnp.float32)

    def update(step, masked):
        block = kv_ref[pl.ds(pl.multiple_of(step * KEY_BLOCK, KEY_BLOCK), KEY_BLOCK), :]
        keys, values = block[:, :width], block[:, width:]
        wide = jnp.concatenate([values, jnp.ones_like(values)], axis=1)
        for at in range(0, 2 * tok, ROW_BLOCK):
            rows = slice(at, at + ROW_BLOCK)
            scores = lax.dot_general(
                stacked[rows], keys, (((1,), (1,)), ((), ())), preferred_element_type=jnp.float32
            )
            if masked:
                row = lax.broadcasted_iota(jnp.int32, scores.shape, 0) + at % tok
                col = lax.broadcasted_iota(jnp.int32, scores.shape, 1)
                scores = jnp.where(
                    col - row <= first_query - step * KEY_BLOCK, scores, -1e30
                )
            before = highest[rows]
            now = jnp.maximum(before, jnp.max(scores, axis=1, keepdims=True))
            weights = jnp.exp(scores - now[:, :1])
            shrink = jnp.exp(before - now)[:, :1]
            blended = jnp.dot(weights.astype(jnp.bfloat16), wide, preferred_element_type=jnp.float32)
            accum[rows] = accum[rows] * shrink + blended
            highest[rows] = now

    def whole(step, carry):
        update(step, False)
        return carry

    lax.fori_loop(0, last, whole, 0)
    update(last, True)
    both = accum[:, :width] / accum[:, width:]
    combined = both[:tok] - lam_ref[0] * both[tok:]
    square = jnp.mean(combined * combined, axis=1, keepdims=True)
    attended = (combined * lax.rsqrt(square + norm_eps) * gain_ref[...]).astype(jnp.bfloat16)
    part = jnp.dot(attended, weight_ref[...], preferred_element_type=jnp.float32)
    share = out_ref.shape[2]
    for p in range(out_ref.shape[0]):
        out_ref[p] = part[:, p * share : (p + 1) * share].astype(jnp.bfloat16)


def attention(where, lam, q, kv, gain, weight, peers):
    tok, width = q.shape
    share = weight.shape[1] // peers
    vmem = pl.BlockSpec(memory_space=pltpu.VMEM)
    smem = pl.BlockSpec(memory_space=pltpu.SMEM)
    return pl.pallas_call(
        attention_body,
        in_specs=[smem, smem, vmem, vmem, vmem, vmem],
        out_specs=vmem,
        out_shape=jax.ShapeDtypeStruct((peers, tok, share), jnp.bfloat16),
        scratch_shapes=[
            pltpu.VMEM((2 * tok, width), jnp.bfloat16),
            pltpu.VMEM((2 * tok, 128), jnp.float32),
            pltpu.VMEM((2 * tok, 2 * width), jnp.float32),
        ],
        compiler_params=pltpu.CompilerParams(vmem_limit_bytes=24 * 2**20),
        name="attention",
    )(where, lam, q, kv, gain, weight)


def project_body(column_ref, parts_ref, residual_ref, send_ref, stream_ref, out_ref):
    total = residual_ref[...].astype(jnp.float32)
    for p in range(parts_ref.shape[0]):
        total += parts_ref[p].astype(jnp.float32)
    stream_ref[...] = total
    picked = jnp.dot(send_ref[...], total.astype(jnp.bfloat16), preferred_element_type=jnp.float32)
    out_ref[...] = picked.astype(jnp.bfloat16)


def project(column, parts, residual, send):
    peers, tok, share = parts.shape
    slots = send.shape[0]

    def whole(rank):
        return lambda i, column_ref: (0,) * rank

    grid = pltpu.PrefetchScalarGridSpec(
        num_scalar_prefetch=1,
        grid=(1,),
        in_specs=[
            pl.BlockSpec((peers, tok, share), whole(3)),
            pl.BlockSpec((tok, share), lambda i, column_ref: (0, column_ref[0])),
            pl.BlockSpec((slots, tok), whole(2)),
        ],
        out_specs=[pl.BlockSpec((tok, share), whole(2)), pl.BlockSpec((slots, share), whole(2))],
    )
    return pl.pallas_call(
        project_body,
        grid_spec=grid,
        out_shape=[
            jax.ShapeDtypeStruct((tok, share), jnp.float32),
            jax.ShapeDtypeStruct((slots, share), jnp.bfloat16),
        ],
        compiler_params=pltpu.CompilerParams(vmem_limit_bytes=16 * 2**20),
        name="project",
    )(column, parts, residual, send)


def hidden_body(rows_ref, gain_ref, gate_ref, up_ref, out_ref):
    rows = rows_ref[...].astype(jnp.float32)
    square = jnp.mean(rows * rows, axis=1, keepdims=True)
    normed = (rows * lax.rsqrt(square + norm_eps) * gain_ref[...]).astype(jnp.bfloat16)
    gate = jnp.dot(normed, gate_ref[...], preferred_element_type=jnp.float32)
    up = jnp.dot(normed, up_ref[...], preferred_element_type=jnp.float32)
    out_ref[...] = (gate / (1.0 + jnp.exp(-gate)) * up).astype(jnp.bfloat16)


def hidden_units(rows, gain, gate, up):
    count, model = rows.shape
    hidden = gate.shape[1]
    tile = 256
    return pl.pallas_call(
        hidden_body,
        grid=(count // tile,),
        in_specs=[
            pl.BlockSpec((tile, model), lambda i: (i, 0)),
            pl.BlockSpec((1, model), lambda i: (0, 0)),
            pl.BlockSpec((model, hidden), lambda i: (0, 0)),
            pl.BlockSpec((model, hidden), lambda i: (0, 0)),
        ],
        out_specs=pl.BlockSpec((tile, hidden), lambda i: (i, 0)),
        out_shape=jax.ShapeDtypeStruct((count, hidden), jnp.bfloat16),
        compiler_params=pltpu.CompilerParams(vmem_limit_bytes=24 * 2**20),
        name="hidden",
    )(rows, gain, gate, up)


def gathered(array, axes, axis, scale):
    sent = (array.astype(jnp.float32) * scale).astype(jnp.float16)
    whole = lax.all_gather(sent, axes, axis=axis, tiled=True)
    return (whole.astype(jnp.float32) * (1.0 / scale)).astype(jnp.bfloat16)


def from_everyone(array, axes):
    peers = lax.axis_size(axes)
    return lax.all_to_all(
        jnp.broadcast_to(array[None], (peers, *array.shape)), axes, 0, 0, tiled=True
    )


def shards(
    residual,
    queries,
    key_vectors,
    value_rows,
    head_lambda,
    head_gain,
    out_weight,
    ffn_gain,
    expert_gate,
    expert_up,
    expert_down,
    routing,
    route_weight,
):
    tok, _, width = queries.shape
    experts = lax.axis_size("sp")
    peers = lax.axis_size("tp")
    model = residual.shape[1]
    share = model // peers
    where = lax.axis_index("sp").astype(jnp.int32)[None]
    column = lax.axis_index("tp").astype(jnp.int32)[None]
    kv = jnp.concatenate([key_vectors[:, 0], value_rows[:, 0]], axis=1)
    kv_all = gathered(kv, "sp", 0, SHIFT)

    capacity = tok // (experts // GROUPS)
    order = jnp.arange(tok, dtype=jnp.int32)
    ids = jnp.arange(experts, dtype=jnp.int32)
    named = routing[:, :, None] == ids
    member = jnp.any(named, axis=1)
    strict = (order[None, :] < order[:, None]).astype(jnp.bfloat16)
    earlier = jnp.dot(
        strict, member.astype(jnp.bfloat16), preferred_element_type=jnp.float32
    ).astype(jnp.int32)
    slot = jnp.arange(capacity, dtype=jnp.int32)
    send = (member.T[:, None, :] & (earlier.T[:, None, :] == slot[None, :, None])).reshape(
        experts * capacity, tok
    )
    send = send.astype(jnp.bfloat16)
    take = [
        (named[:, k, :, None] & (earlier[:, :, None] == slot))
        .reshape(tok, experts * capacity)
        .astype(jnp.bfloat16)
        for k in range(routing.shape[1])
    ]

    partial = attention(
        where, head_lambda, queries[:, 0], kv_all, head_gain[None], out_weight, peers
    )
    parts = lax.all_to_all(partial, "tp", 0, 0, tiled=True)
    own_stream, outgoing = project(column, parts, residual, send)
    landed = lax.all_to_all(
        outgoing.reshape(experts, capacity, share), "sp", 0, 0, tiled=True
    )
    rows = gathered(landed.reshape(experts * capacity, share), "tp", 1, 64.0)
    units = hidden_units(rows, ffn_gain[None], expert_gate[0], expert_up[0])
    all_units = gathered(units, "tp", 1, 0.25)
    expert_out = jnp.dot(
        all_units, expert_down[0], preferred_element_type=jnp.float32
    ).astype(jnp.bfloat16)
    back = lax.all_to_all(
        expert_out.reshape(experts, capacity, share), "sp", 0, 0, tiled=True
    ).reshape(experts * capacity, share)
    moe = sum(
        route_weight[:, k : k + 1] * jnp.dot(take[k], back, preferred_element_type=jnp.float32)
        for k in range(routing.shape[1])
    )
    own_out = (own_stream + moe).astype(jnp.bfloat16)
    whole = from_everyone(own_out, "tp")
    return whole.swapaxes(0, 1).reshape(tok, model)


def solution(mesh):
    in_specs = (
        P("sp", None),
        P("sp", "tp", None),
        P("sp", "tp", None),
        P("sp", "tp", None),
        P("tp"),
        P(),
        P("tp", None),
        P(),
        P("sp", None, "tp"),
        P("sp", None, "tp"),
        P("sp", None, "tp"),
        P("sp", None),
        P("sp", None),
    )
    return jax.shard_map(
        shards, mesh=mesh, in_specs=in_specs, out_specs=P("sp", None), check_vma=False
    )
```

time: 452 us -> 295 us (0.65)
  waiting for transfers between devices: 331 us -> 37.8 us
  blocking collectives: 60.3 us -> 216 us
  between operations: 13.9 us -> 0.96 us
    all_gather x4 -> x0, waiting for transfers between devices: 206 us -> none  [the longest x1 79.9 us: shards(): kv_all = lax.all_gather(kv, 'sp', axis=1, tiled=True)]
    all_gather x0 -> x3, blocking collectives: none -> 162 us  [gathered(): whole = lax.all_gather(sent, axes, axis=axis, tiled=True)]
    unnamed x6 -> x0, waiting for transfers between devices: 93.1 us -> none
    all_to_all x1, waiting for transfers between devices: 9.56 us -> 16.2 us  [shards(): parts = lax.all_to_all(partial, 'tp', 0, 0, tiled=True)]
    unnamed x26 -> x20, local copies, waits for them, and re-layouts: 7.03 us -> 1.26 us
    pallas_call x2 -> x3, Pallas kernels: 10.9 us -> 8.17 us  [the longest x1 3.93 us: hidden_units(): pl.pallas_call(hidden_body, grid=(count // tile,), in_specs=[pl.BlockSpec...]
  transfers between devices with their start and end apart: 7 -> 2, of which waited for: 7 -> 2; matrix products, arithmetic and copies ran while one was open for 1% -> 0% of each run, Pallas kernels for 0% -> 0%
where the time goes in v3:
time: 295 us; the launch traced here: 294 us
  blocking collectives  216 us (73%)
  waiting for transfers between devices  37.8 us (13%)
  starting transfers between devices  19 us (6%)
  Pallas kernels  8.17 us (3%)
  matrix products  4.16 us (1%)
  other arithmetic  4.13 us (1%)
  local copies, waits for them, and re-layouts  3.49 us (1%)
    all_gather x3, blocking collectives, gathered(): whole = lax.all_gather(sent, axes, axis=axis, tiled=True)  162 us
    all_to_all x1, blocking collectives, shards(): lax.all_to_all(outgoing.reshape(experts, capacity, share), 'sp', 0, 0, ti...  35.2 us
    all_to_all x1, waiting for transfers between devices, shards(): lax.all_to_all(expert_out.reshape(experts, capacity, share), 'sp', 0, 0,...  21.6 us
    all_to_all x1, blocking collectives, from_everyone(): lax.all_to_all(jnp.broadcast_to(array[None], (peers, *array.shape)), axes...  19.6 us
    all_to_all x1, waiting for transfers between devices, shards(): parts = lax.all_to_all(partial, 'tp', 0, 0, tiled=True)  16.2 us
    all_to_all x1, starting transfers between devices, shards(): lax.all_to_all(expert_out.reshape(experts, capacity, share), 'sp', 0, 0,...  12.3 us
    all_to_all x1, starting transfers between devices, shards(): parts = lax.all_to_all(partial, 'tp', 0, 0, tiled=True)  6.76 us
  transfers between devices with their start and end apart: 2, of which 2 were waited for; matrix products, arithmetic and copies ran while one was open for 0% of the time, Pallas kernels for 0%

profile of v3, /device:TPU:1, one launch (start us, length us, event | category | flops | bytes accessed | tf_op | source)
XLA Modules:
  0.0 294.2 jit_solution(6118074242835484597)
XLA Ops:
  0.8 0.9 multiply_convert_fusion.8
  1.7 51.5 %all-gather.3 = f16[8192,256]{1,0:T(8,128)(2,1)S(1)} all-gather(f16[256,256]{1,0:T(8,128)(2,1)S(1)} %multiply_convert_fusion.8), channel_id=1, replica_groups=mesh['sp'=32,'tp'=16] {'sp'}, dimensions={0}, use_global_device_ids=true | all-gather | bytes 4325376 | tf_op jit(solution)/shard_map/all_gather | solution.py:155
  53.2 1.2 multiply_convert_fusion.3.kv_ref
  54.4 3.8 %attention.1 = bf16[16,256,128]{2,1,0:T(8,128)(2,1)} custom-call(s32[1]{0:T(128)} %bitcast.1.where_ref, f32[1]{0:T(128)S(6)} %copy.16.lam_ref, bf16[256,128]{1,0:T(8,128)(2,1)S(1)} %bitcast.54, bf16[8192,256]{1,0:T(8,128)(2,1)S(1)} %multiply_convert_fusion.3.kv_ref, f32[1,128]{1,0:T(1,128)S(1)} %bitcast.56, bf16[128,2048]{1,0:T(8,128)(2,1)S(1)} %copy-done.4), custom_call_target="tpu_custom_call" | custom-call | tf_op jit(solution)/shard_map/attention/pallas_call | solution.py:71
  58.3 6.8 %all-to-all-start = ((bf16[16,256,128]{2,1,0:T(8,128)(2,1)}), bf16[16,256,128]{2,1,0:T(8,128)(2,1)S(1)}, u32[]{:S(2)}, u32[]{:S(2)}) async-start(bf16[16,256,128]{2,1,0:T(8,128)(2,1)} %attention.1), calls=%async_computation | async-start | bytes 2097152 | tf_op jit(solution)/shard_map/all_to_all | solution.py:215
  65.1 0.2 convolution_convert_fusion
  65.3 0.3 fusion.14.send_ref
  65.6 16.2 %all-to-all-done.parts_ref = bf16[16,256,128]{2,1,0:T(8,128)(2,1)S(1)} async-done(((bf16[16,256,128]{2,1,0:T(8,128)(2,1)}), bf16[16,256,128]{2,1,0:T(8,128)(2,1)S(1)}, u32[]{:S(2)}, u32[]{:S(2)}) %all-to-all-start) | async-done | bytes 1048608 | tf_op jit(solution)/shard_map/all_to_all | solution.py:215
  81.7 1.2 copy-done.1
  83.0 0.4 project.1
  83.4 35.2 %all_to_all.20 = bf16[32,32,128]{2,1,0:T(8,128)(2,1)S(1)} all-to-all(bf16[32,32,128]{2,1,0:T(8,128)(2,1)S(1)} %bitcast.53), channel_id=1, replica_groups=mesh['sp'=32,'tp'=16] {'sp'}, dimensions={0} | all-to-all | bytes 524288 | tf_op jit(solution)/shard_map/all_to_all | solution.py:217
  118.7 31.7 %all-gather.4 = f16[1024,2048]{1,0:T(8,128)(2,1)S(1)} all-gather(f16[1024,128]{1,0:T(8,128)(2,1)S(1)} %bitcast.58), channel_id=1, replica_groups=mesh['sp'=32,'tp'=16] {'tp'}, dimensions={1}, use_global_device_ids=true | all-gather | bytes 4456448 | tf_op jit(solution)/shard_map/all_gather | solution.py:155
  150.4 1.6 multiply_convert_fusion.2.rows_ref
  152.0 3.9 %hidden.1 = bf16[1024,256]{1,0:T(8,128)(2,1)S(1)} custom-call(bf16[1024,2048]{1,0:T(8,128)(2,1)S(1)} %multiply_convert_fusion.2.rows_ref, f32[1,2048]{1,0:T(1,128)S(1)} %bitcast.55, bf16[2048,256]{1,0:T(8,128)(2,1)S(1)} %bitcast.51, bf16[2048,256]{1,0:T(8,128)(2,1)S(1)} %bitcast.52), custom_call_target="tpu_custom_call" | custom-call | tf_op jit(solution)/shard_map/hidden/pallas_call | solution.py:137
  156.1 78.4 %all-gather.5 = f16[1024,4096]{1,0:T(8,128)(2,1)S(1)} all-gather(f16[1024,256]{1,0:T(8,128)(2,1)S(1)} %multiply_convert_fusion.6), channel_id=1, replica_groups=mesh['sp'=32,'tp'=16] {'tp'}, dimensions={1}, use_global_device_ids=true | all-gather | bytes 8912896 | tf_op jit(solution)/shard_map/all_gather | solution.py:155
  234.5 3.0 %fusion.2 = bf16[1024,128]{1,0:T(8,128)(2,1)} fusion(f16[1024,4096]{1,0:T(8,128)(2,1)S(1)} %all-gather.5, bf16[1,4096,128]{2,1,0:T(8,128)(2,1)S(1)} %copy-done), kind=kOutput, calls=%fused_computation.5 | convolution fusion | flops 1086455808 | bytes 9699328 | tf_op jit(solution)/shard_map/dot_general | solution.py:223
  237.5 12.3 %all-to-all-start.2 = ((bf16[32,32,128]{2,1,0:T(8,128)(2,1)}), bf16[32,32,128]{2,1,0:T(8,128)(2,1)S(1)}, u32[]{:S(2)}, u32[]{:S(2)}) async-start(bf16[32,32,128]{2,1,0:T(8,128)(2,1)} %bitcast.18), calls=%async_computation.2 | async-start | bytes 524288 | tf_op jit(solution)/shard_map/all_to_all | solution.py:226
  249.8 21.6 %all-to-all-done.2 = bf16[32,32,128]{2,1,0:T(8,128)(2,1)S(1)} async-done(((bf16[32,32,128]{2,1,0:T(8,128)(2,1)}), bf16[32,32,128]{2,1,0:T(8,128)(2,1)S(1)}, u32[]{:S(2)}, u32[]{:S(2)}) %all-to-all-start.2) | async-done | bytes 262176 | tf_op jit(solution)/shard_map/all_to_all | solution.py:226
  271.5 0.5 fusion.6
  271.9 0.5 fusion.7
  272.4 0.2 broadcast_in_dim.14
  272.6 19.6 %all_to_all.21 = bf16[16,256,128]{2,1,0:T(8,128)(2,1)S(1)} all-to-all(bf16[16,256,128]{2,1,0:T(8,128)(2,1)S(1)} %broadcast_in_dim.14), channel_id=1, replica_groups=mesh['sp'=32,'tp'=16] {'tp'}, dimensions={0} | all-to-all | bytes 2097152 | tf_op jit(solution)/shard_map/all_to_all | solution.py:161
  292.3 0.5 copy.14
  292.8 1.4 copy.15
  (26 shorter events, 0.3 us)
Async XLA Ops:
  0.0 234.5 %copy-start = (bf16[1,4096,128]{2,1,0:T(8,128)(2,1)S(1)}, bf16[1,4096,128]{2,1,0:T(8,128)(2,1)}, u32[]{:S(2)}) copy-start(bf16[1,4096,128]{2,1,0:T(8,128)(2,1)} %param.23) | copy-start | bytes 3145732
  0.0 54.4 %copy-start.5 = (bf16[256,1,128]{2,0,1:T(8,128)(2,1)S(1)}, bf16[256,1,128]{2,0,1:T(8,128)(2,1)}, u32[]{:S(2)}) copy-start(bf16[256,1,128]{2,0,1:T(8,128)(2,1)} %param.14) | copy-start | bytes 196612
  0.0 54.4 %copy-start.7 = (f32[128]{0:T(128)S(1)}, f32[128]{0:T(128)}, u32[]{:S(2)}) copy-start(f32[128]{0:T(128)} %param.18) | copy-start | bytes 1540
  0.0 54.4 %copy-start.4 = (bf16[128,2048]{1,0:T(8,128)(2,1)S(1)}, bf16[128,2048]{1,0:T(8,128)(2,1)}, u32[]{:S(2)}) copy-start(bf16[128,2048]{1,0:T(8,128)(2,1)} %weight_ref.1) | copy-start | bytes 1572868
  53.2 11.9 %copy-start.9 = (s32[256,2]{0,1:T(2,128)S(1)}, s32[256,2]{0,1:T(2,128)}, u32[]{:S(2)}) copy-start(s32[256,2]{0,1:T(2,128)} %param.24) | copy-start | bytes 6148
  58.3 23.5 %all-to-all-start = ((bf16[16,256,128]{2,1,0:T(8,128)(2,1)}), bf16[16,256,128]{2,1,0:T(8,128)(2,1)S(1)}, u32[]{:S(2)}, u32[]{:S(2)}) async-start(bf16[16,256,128]{2,1,0:T(8,128)(2,1)} %attention.1), calls=%async_computation | async-start | bytes 2097152 | tf_op jit(solution)/shard_map/all_to_all | solution.py:215
  65.3 86.7 %copy-start.6 = (f32[2048]{0:T(1024)S(1)}, f32[2048]{0:T(1024)}, u32[]{:S(2)}) copy-start(f32[2048]{0:T(1024)} %param.20) | copy-start | bytes 24580
  81.7 1.2 copy-start.1
  83.0 69.0 %copy-start.2 = (bf16[1,2048,256]{2,1,0:T(8,128)(2,1)S(1)}, bf16[1,2048,256]{2,1,0:T(8,128)(2,1)}, u32[]{:S(2)}) copy-start(bf16[1,2048,256]{2,1,0:T(8,128)(2,1)} %param.21) | copy-start | bytes 3145732
  83.0 69.0 %copy-start.3 = (bf16[1,2048,256]{2,1,0:T(8,128)(2,1)S(1)}, bf16[1,2048,256]{2,1,0:T(8,128)(2,1)}, u32[]{:S(2)}) copy-start(bf16[1,2048,256]{2,1,0:T(8,128)(2,1)} %param.22) | copy-start | bytes 3145732
  234.5 15.3 %copy-start.8 = (f32[256,2]{0,1:T(2,128)S(1)}, f32[256,2]{0,1:T(2,128)}, u32[]{:S(2)}) copy-start(f32[256,2]{0,1:T(2,128)} %param.25) | copy-start | bytes 6148
  237.5 33.9 %all-to-all-start.2 = ((bf16[32,32,128]{2,1,0:T(8,128)(2,1)}), bf16[32,32,128]{2,1,0:T(8,128)(2,1)S(1)}, u32[]{:S(2)}, u32[]{:S(2)}) async-start(bf16[32,32,128]{2,1,0:T(8,128)(2,1)} %bitcast.18), calls=%async_computation.2 | async-start | bytes 524288 | tf_op jit(solution)/shard_map/all_to_all | solution.py:226

commit v4 on v3

--- a/solution.py
+++ b/solution.py
@@ -83,7 +83,7 @@
     )(where, lam, q, kv, gain, weight)
 
 
-def project_body(column_ref, parts_ref, residual_ref, send_ref, stream_ref, out_ref):
+def project_body(parts_ref, residual_ref, send_ref, stream_ref, out_ref):
     total = residual_ref[...].astype(jnp.float32)
     for p in range(parts_ref.shape[0]):
         total += parts_ref[p].astype(jnp.float32)
@@ -92,62 +92,97 @@
     out_ref[...] = picked.astype(jnp.bfloat16)
 
 
-def project(column, parts, residual, send):
-    peers, tok, share = parts.shape
+def project(parts, residual, send):
+    _, tok, share = parts.shape
     slots = send.shape[0]
-
-    def whole(rank):
-        return lambda i, column_ref: (0,) * rank
-
-    grid = pltpu.PrefetchScalarGridSpec(
-        num_scalar_prefetch=1,
-        grid=(1,),
-        in_specs=[
-            pl.BlockSpec((peers, tok, share), whole(3)),
-            pl.BlockSpec((tok, share), lambda i, column_ref: (0, column_ref[0])),
-            pl.BlockSpec((slots, tok), whole(2)),
-        ],
-        out_specs=[pl.BlockSpec((tok, share), whole(2)), pl.BlockSpec((slots, share), whole(2))],
-    )
+    vmem = pl.BlockSpec(memory_space=pltpu.VMEM)
     return pl.pallas_call(
         project_body,
-        grid_spec=grid,
+        in_specs=[vmem] * 3,
+        out_specs=[vmem] * 2,
         out_shape=[
             jax.ShapeDtypeStruct((tok, share), jnp.float32),
             jax.ShapeDtypeStruct((slots, share), jnp.bfloat16),
         ],
         compiler_params=pltpu.CompilerParams(vmem_limit_bytes=16 * 2**20),
         name="project",
-    )(column, parts, residual, send)
-
-
-def hidden_body(rows_ref, gain_ref, gate_ref, up_ref, out_ref):
-    rows = rows_ref[...].astype(jnp.float32)
-    square = jnp.mean(rows * rows, axis=1, keepdims=True)
-    normed = (rows * lax.rsqrt(square + norm_eps) * gain_ref[...]).astype(jnp.bfloat16)
-    gate = jnp.dot(normed, gate_ref[...], preferred_element_type=jnp.float32)
-    up = jnp.dot(normed, up_ref[...], preferred_element_type=jnp.float32)
-    out_ref[...] = (gate / (1.0 + jnp.exp(-gate)) * up).astype(jnp.bfloat16)
-
-
-def hidden_units(rows, gain, gate, up):
-    count, model = rows.shape
-    hidden = gate.shape[1]
-    tile = 256
+    )(parts, residual, send)
+
+
+def hidden_body(x_ref, rows_ref, gain_ref, gate_ref, up_ref, left_ref, right_ref, gate_2_ref, up_2_ref, out_ref, normed_ref):
+    peers, count, share = rows_ref.shape
+    pieces = out_ref.shape[0]
+    total = jnp.zeros((count, 1), jnp.float32)
+    for p in range(peers):
+        part = rows_ref[p].astype(jnp.float32)
+        total += jnp.sum(part * part, axis=1, keepdims=True)
+    scale = lax.rsqrt(total / (peers * share) + norm_eps)
+    for p in range(peers):
+        cols = slice(p * share, (p + 1) * share)
+        normed_ref[:, cols] = (rows_ref[p].astype(jnp.float32) * scale * gain_ref[:, cols]).astype(
+            jnp.bfloat16
+        )
+    own = (gate_ref, up_ref)
+    right = (right_ref.at[0], right_ref.at[1])
+    left = (left_ref.at[0], left_ref.at[1])
+    for ahead, (gates, ups) in enumerate((own, right, (gate_2_ref, up_2_ref), left)):
+        normed = normed_ref[...]
+        gate = jnp.dot(normed, gates[...], preferred_element_type=jnp.float32)
+        up = jnp.dot(normed, ups[...], preferred_element_type=jnp.float32)
+        act = gate / (1.0 + jnp.exp(-gate)) * up
+        out_ref[lax.rem(x_ref[0] + ahead, pieces)] = act.astype(jnp.bfloat16)
+
+
+def hidden_units(x, rows, gain, *weights):
+    peers, count, share = rows.shape
+    hidden = weights[0].shape[1]
+    vmem = pl.BlockSpec(memory_space=pltpu.VMEM)
     return pl.pallas_call(
         hidden_body,
-        grid=(count // tile,),
-        in_specs=[
-            pl.BlockSpec((tile, model), lambda i: (i, 0)),
-            pl.BlockSpec((1, model), lambda i: (0, 0)),
-            pl.BlockSpec((model, hidden), lambda i: (0, 0)),
-            pl.BlockSpec((model, hidden), lambda i: (0, 0)),
-        ],
-        out_specs=pl.BlockSpec((tile, hidden), lambda i: (i, 0)),
-        out_shape=jax.ShapeDtypeStruct((count, hidden), jnp.bfloat16),
+        in_specs=[pl.BlockSpec(memory_space=pltpu.SMEM)] + [vmem] * (2 + len(weights)),
+        out_specs=vmem,
+        out_shape=jax.ShapeDtypeStruct((4, count, hidden), jnp.bfloat16),
+        scratch_shapes=[pltpu.VMEM((count, peers * share), jnp.bfloat16)],
         compiler_params=pltpu.CompilerParams(vmem_limit_bytes=24 * 2**20),
         name="hidden",
-    )(rows, gain, gate, up)
+    )(x, rows, gain, *weights)
+
+
+def down_body(x_ref, units_ref, own_ref, right_ref, low_ref, high_ref, left_ref, out_ref):
+    blocks, count, hidden = units_ref.shape
+    pieces = out_ref.shape[0]
+    share = own_ref.shape[1]
+    half = blocks // 2
+    first = jnp.zeros((count, 2 * share), jnp.float32)
+    second = jnp.zeros((count, 2 * share), jnp.float32)
+    for p in range(blocks):
+        rows = slice(p * hidden, (p + 1) * hidden)
+        part = slice(p % half * hidden, (p % half + 1) * hidden)
+        units = units_ref[p]
+        far = (low_ref if p < half else high_ref)[part]
+        near = jnp.concatenate([own_ref[rows], right_ref[rows]], axis=1)
+        rest = jnp.concatenate([far, left_ref[rows]], axis=1)
+        first += jnp.dot(units, near, preferred_element_type=jnp.float32)
+        second += jnp.dot(units, rest, preferred_element_type=jnp.float32)
+    at = [lax.rem(x_ref[0] + ahead, pieces) for ahead in range(pieces)]
+    out_ref[at[0]] = first[:, :share].astype(jnp.bfloat16)
+    out_ref[at[1]] = first[:, share:].astype(jnp.bfloat16)
+    out_ref[at[2]] = second[:, :share].astype(jnp.bfloat16)
+    out_ref[at[3]] = second[:, share:].astype(jnp.bfloat16)
+
+
+def down_product(x, units, *downs):
+    _, count, _ = units.shape
+    share = downs[0].shape[1]
+    vmem = pl.BlockSpec(memory_space=pltpu.VMEM)
+    return pl.pallas_call(
+        down_body,
+        in_specs=[pl.BlockSpec(memory_space=pltpu.SMEM)] + [vmem] * (1 + len(downs)),
+        out_specs=vmem,
+        out_shape=jax.ShapeDtypeStruct((4, count, share), jnp.bfloat16),
+        compiler_params=pltpu.CompilerParams(vmem_limit_bytes=24 * 2**20),
+        name="down",
+    )(x, units, *downs)
 
 
 def gathered(array, axes, axis, scale):
@@ -178,15 +213,35 @@
     routing,
     route_weight,
 ):
-    tok, _, width = queries.shape
+    tok, _, _ = queries.shape
     experts = lax.axis_size("sp")
-    peers = lax.axis_size("tp")
+    across = lax.axis_size("x")
+    along = lax.axis_size("y")
+    tp = ("y", "x")
+    peers = across * along
     model = residual.shape[1]
     share = model // peers
     where = lax.axis_index("sp").astype(jnp.int32)[None]
-    column = lax.axis_index("tp").astype(jnp.int32)[None]
+    x_at = lax.axis_index("x").astype(jnp.int32)[None]
+    column = (lax.axis_index("y") * across + lax.axis_index("x")) * share
+
+    ahead = [(i, (i + 1) % across) for i in range(across)]
+    behind = [(i, (i - 1) % across) for i in range(across)]
+    gate, up, down = expert_gate[0], expert_up[0], expert_down[0]
+    both = jnp.stack([gate, up])
+    left = lax.ppermute(both, "x", ahead)
+    right = lax.ppermute(both, "x", behind)
+    gate_2 = lax.ppermute(left[0], "x", ahead)
+    up_2 = lax.ppermute(right[1], "x", behind)
+    half = down.shape[0] // 2
+    down_left = lax.ppermute(down, "x", ahead)
+    down_right = lax.ppermute(down, "x", behind)
+    down_low = lax.ppermute(down_left[:half], "x", ahead)
+    down_high = lax.ppermute(down_right[half:], "x", behind)
+
     kv = jnp.concatenate([key_vectors[:, 0], value_rows[:, 0]], axis=1)
     kv_all = gathered(kv, "sp", 0, SHIFT)
+    own_residual = lax.dynamic_slice_in_dim(residual, column, share, 1)
 
     capacity = tok // (experts // GROUPS)
     order = jnp.arange(tok, dtype=jnp.int32)
@@ -212,17 +267,22 @@
     partial = attention(
         where, head_lambda, queries[:, 0], kv_all, head_gain[None], out_weight, peers
     )
-    parts = lax.all_to_all(partial, "tp", 0, 0, tiled=True)
-    own_stream, outgoing = project(column, parts, residual, send)
+    parts = lax.all_to_all(partial, tp, 0, 0, tiled=True)
+    own_stream, outgoing = project(parts, own_residual, send)
     landed = lax.all_to_all(
         outgoing.reshape(experts, capacity, share), "sp", 0, 0, tiled=True
     )
-    rows = gathered(landed.reshape(experts * capacity, share), "tp", 1, 64.0)
-    units = hidden_units(rows, ffn_gain[None], expert_gate[0], expert_up[0])
-    all_units = gathered(units, "tp", 1, 0.25)
-    expert_out = jnp.dot(
-        all_units, expert_down[0], preferred_element_type=jnp.float32
-    ).astype(jnp.bfloat16)
+    count = experts * capacity // across
+    quarters = jnp.broadcast_to(
+        landed.reshape(1, across, count, share), (along, across, count, share)
+    )
+    rows = lax.all_to_all(quarters.reshape(peers, count, share), tp, 0, 0, tiled=True)
+    units = hidden_units(
+        x_at, rows, ffn_gain[None], gate, up, left, right, gate_2, up_2
+    )
+    all_units = gathered(units, "y", 0, 0.25)
+    made = down_product(x_at, all_units, down, down_right, down_low, down_high, down_left)
+    expert_out = lax.all_to_all(made, "x", 0, 0, tiled=True)
     back = lax.all_to_all(
         expert_out.reshape(experts, capacity, share), "sp", 0, 0, tiled=True
     ).reshape(experts * capacity, share)
@@ -231,26 +291,31 @@
         for k in range(routing.shape[1])
     )
     own_out = (own_stream + moe).astype(jnp.bfloat16)
-    whole = from_everyone(own_out, "tp")
+    whole = from_everyone(own_out, tp)
     return whole.swapaxes(0, 1).reshape(tok, model)
 
 
 def solution(mesh):
+    sizes = mesh.devices.shape
+    split = jax.sharding.Mesh(
+        mesh.devices.reshape(sizes[0], sizes[1] // 4, 4), ("sp", "y", "x")
+    )
+    tp = ("y", "x")
     in_specs = (
         P("sp", None),
-        P("sp", "tp", None),
-        P("sp", "tp", None),
-        P("sp", "tp", None),
-        P("tp"),
+        P("sp", tp, None),
+        P("sp", tp, None),
+        P("sp", tp, None),
+        P(tp),
         P(),
-        P("tp", None),
+        P(tp, None),
         P(),
-        P("sp", None, "tp"),
-        P("sp", None, "tp"),
-        P("sp", None, "tp"),
+        P("sp", None, tp),
+        P("sp", None, tp),
+        P("sp", None, tp),
         P("sp", None),
         P("sp", None),
     )
     return jax.shard_map(
-        shards, mesh=mesh, in_specs=in_specs, out_specs=P("sp", None), check_vma=False
-    )
+        shards, mesh=split, in_specs=in_specs, out_specs=P("sp", None), check_vma=False
+    )

time: 295 us -> 260 us (0.88)
  blocking collectives: 216 us -> 97.8 us
  starting transfers between devices: 19 us -> 67.9 us
  local copies, waits for them, and re-layouts: 3.49 us -> 22.5 us
  waiting for transfers between devices: 37.8 us -> 49.7 us
  Pallas kernels: 8.17 us -> 13.5 us
  matrix products: 4.16 us -> 1.12 us
    all_gather x3 -> x2, blocking collectives: 162 us -> 69 us  [gathered(): whole = lax.all_gather(sent, axes, axis=axis, tiled=True)]
    ppermute x0 -> x8, starting transfers between devices: none -> 26.4 us  [the longest x1 4.48 us: shards(): up_2 = lax.ppermute(right[1], 'x', behind)]
    all_to_all x1, blocking collectives: 35.2 us -> 9.8 us  [shards(): expert_out = lax.all_to_all(made, 'x', 0, 0, tiled=True)]
    all_to_all x1 -> x3, starting transfers between devices: 6.76 us -> 23.8 us  [the longest x1 13.1 us: shards(): lax.all_to_all(outgoing.reshape(experts, capacity, share), 'sp', 0, 0, ti...]
    all_to_all x1 -> x3, waiting for transfers between devices: 16.2 us -> 27.5 us  [the longest x1 12.3 us: shards(): lax.all_to_all(outgoing.reshape(experts, capacity, share), 'sp', 0, 0, ti...]
    unnamed x20 -> x37, local copies, waits for them, and re-layouts: 1.26 us -> 10.7 us
    pallas_call x2 -> x3, Pallas kernels: 4.36 us -> 10.8 us  [the longest x1 5.4 us: hidden_units(): pl.pallas_call(hidden_body, in_specs=[pl.BlockSpec(memory_space=pltpu.SME...]
    all_to_all x1, starting transfers between devices: 12.3 us -> 17.7 us  [shards(): lax.all_to_all(expert_out.reshape(experts, capacity, share), 'sp', 0, 0,...]
  transfers between devices with their start and end apart: 2 -> 12, of which waited for: 2 -> 4; matrix products, arithmetic and copies ran while one was open for 0% -> 5% of each run, Pallas kernels for 0% -> 4%
where the time goes in v4:
time: 260 us; the launch traced here: 259 us
  blocking collectives  97.8 us (38%)
  starting transfers between devices  67.9 us (26%)
  waiting for transfers between devices  49.7 us (19%)
  local copies, waits for them, and re-layouts  22.5 us (9%)
  Pallas kernels  13.5 us (5%)
  other arithmetic  4.93 us (2%)
    all_gather x2, blocking collectives, gathered(): whole = lax.all_gather(sent, axes, axis=axis, tiled=True)  69 us
    all_to_all x1, waiting for transfers between devices, shards(): lax.all_to_all(expert_out.reshape(experts, capacity, share), 'sp', 0, 0,...  22.2 us
    all_to_all x1, blocking collectives, from_everyone(): lax.all_to_all(jnp.broadcast_to(array[None], (peers, *array.shape)), axes...  19 us
    all_to_all x1, starting transfers between devices, shards(): lax.all_to_all(expert_out.reshape(experts, capacity, share), 'sp', 0, 0,...  17.7 us
    all_to_all x1, starting transfers between devices, shards(): lax.all_to_all(outgoing.reshape(experts, capacity, share), 'sp', 0, 0, ti...  13.1 us
    all_to_all x1, waiting for transfers between devices, shards(): lax.all_to_all(outgoing.reshape(experts, capacity, share), 'sp', 0, 0, ti...  12.3 us
    unnamed x37, local copies, waits for them, and re-layouts  10.7 us
    all_to_all x1, blocking collectives, shards(): expert_out = lax.all_to_all(made, 'x', 0, 0, tiled=True)  9.8 us
  transfers between devices with their start and end apart: 12, of which 4 were waited for; matrix products, arithmetic and copies ran while one was open for 5% of the time, Pallas kernels for 4%

profile of v4, /device:TPU:1, one launch (start us, length us, event | category | flops | bytes accessed | tf_op | source)
XLA Modules:
  0.0 258.5 jit_solution(13590933448451741536)
XLA Ops:
  0.0 2.4 constant_dynamic-update-slice_fusion.1
  3.6 3.9 %collective-permute-start = (bf16[2,2048,256]{2,1,0:T(8,128)(2,1)}, bf16[2,2048,256]{2,1,0:T(8,128)(2,1)S(1)}, u32[]{:S(2)}, u32[]{:S(2)}) collective-permute-start(bf16[2,2048,256]{2,1,0:T(8,128)(2,1)} %constant_dynamic-update-slice_fusion), channel_id=1, source_target_pairs={{0,1},{1,2},{2,3},{3,0},{4,5},{5,6},{6,7},{7,4},{8,9},{9,10},{10,1... | collective-permute-start | bytes 6291464 | tf_op jit(solution)/shard_map/ppermute | solution.py:232
  7.5 3.2 %collective-permute-start.1 = (bf16[2,2048,256]{2,1,0:T(8,128)(2,1)}, bf16[2,2048,256]{2,1,0:T(8,128)(2,1)}, u32[]{:S(2)}, u32[]{:S(2)}) collective-permute-start(bf16[2,2048,256]{2,1,0:T(8,128)(2,1)} %constant_dynamic-update-slice_fusion), channel_id=1, source_target_pairs={{0,3},{1,0},{2,1},{3,2},{4,7},{5,4},{6,5},{7,6},{8,11},{9,8},{10,9... | collective-permute-start | bytes 6291464 | tf_op jit(solution)/shard_map/ppermute | solution.py:233
  10.8 50.7 %all-gather.2 = f16[8192,256]{1,0:T(8,128)(2,1)S(1)} all-gather(f16[256,256]{1,0:T(8,128)(2,1)S(1)} %multiply_convert_fusion.3), channel_id=1, replica_groups=mesh['sp'=32,'y'=4,'x'=4] {'sp'}, dimensions={0}, use_global_device_ids=true | all-gather | bytes 4325376 | tf_op jit(solution)/shard_map/all_gather | solution.py:190
  61.5 3.2 %multiply_convert_fusion.kv_ref = bf16[8192,256]{1,0:T(8,128)(2,1)} fusion(f16[8192,256]{1,0:T(8,128)(2,1)S(1)} %all-gather.2), kind=kLoop, calls=%fused_computation | loop fusion | flops 6291456 | bytes 8388608 | tf_op jit(solution)/shard_map/convert_element_type | solution.py:191
  68.6 2.6 %attention.1 = bf16[16,256,128]{2,1,0:T(8,128)(2,1)S(1)} custom-call(s32[1]{0:T(128)} %bitcast.where_ref, f32[1]{0:T(128)S(6)} %copy.17.lam_ref, bf16[256,128]{1,0:T(8,128)(2,1)S(1)} %bitcast.59, bf16[8192,256]{1,0:T(8,128)(2,1)S(1)} %copy-done.1, f32[1,128]{1,0:T(1,128)S(1)} %bitcast.61, bf16[128,2048]{1,0:T(8,128)(2,1)S(1)} %copy-done.8), custom_call_target="tpu_custom_call" | custom-call | tf_op jit(solution)/shard_map/attention/pallas_call | solution.py:71
  72.2 6.2 %all-to-all-start = ((bf16[16,256,128]{2,1,0:T(8,128)(2,1)}), bf16[16,256,128]{2,1,0:T(8,128)(2,1)}, u32[]{:S(2)}, u32[]{:S(2)}) async-start(bf16[16,256,128]{2,1,0:T(8,128)(2,1)} %copy-done.5), calls=%async_computation | async-start | bytes 2097152 | tf_op jit(solution)/shard_map/all_to_all | solution.py:270
  78.3 4.4 %collective-permute-start.4 = (bf16[4096,128]{1,0:T(8,128)(2,1)}, bf16[4096,128]{1,0:T(8,128)(2,1)}, u32[]{:S(2)}, u32[]{:S(2)}) collective-permute-start(bf16[4096,128]{1,0:T(8,128)(2,1)} %bitcast.56), channel_id=1, source_target_pairs={{0,3},{1,0},{2,1},{3,2},{4,7},{5,4},{6,5},{7,6},{8,11},{9,8},{10,9... | collective-permute-start | bytes 3145736 | tf_op jit(solution)/shard_map/ppermute | solution.py:238
  86.1 9.1 %all-to-all-done.parts_ref = bf16[16,256,128]{2,1,0:T(8,128)(2,1)} async-done(((bf16[16,256,128]{2,1,0:T(8,128)(2,1)}), bf16[16,256,128]{2,1,0:T(8,128)(2,1)}, u32[]{:S(2)}, u32[]{:S(2)}) %all-to-all-start) | async-done | bytes 1048608 | tf_op jit(solution)/shard_map/all_to_all | solution.py:270
  98.5 13.1 %all-to-all-start.1 = ((bf16[32,32,128]{2,1,0:T(8,128)(2,1)}), bf16[32,32,128]{2,1,0:T(8,128)(2,1)S(1)}, u32[]{:S(2)}, u32[]{:S(2)}) async-start(bf16[32,32,128]{2,1,0:T(8,128)(2,1)} %bitcast.12), calls=%async_computation.1 | async-start | bytes 524288 | tf_op jit(solution)/shard_map/all_to_all | solution.py:272
  114.8 2.4 slice_bitcast_fusion
  117.2 4.5 %collective-permute-start.3 = (bf16[2048,256]{1,0:T(8,128)(2,1)}, bf16[2048,256]{1,0:T(8,128)(2,1)}, u32[]{:S(2)}, u32[]{:S(2)}) collective-permute-start(bf16[2048,256]{1,0:T(8,128)(2,1)} %slice_bitcast_fusion), channel_id=1, source_target_pairs={{0,3},{1,0},{2,1},{3,2},{4,7},{5,4},{6,5},{7,6},{8,11},{9,8},{10,9... | collective-permute-start | bytes 3145736 | tf_op jit(solution)/shard_map/ppermute | solution.py:235
  121.7 12.3 %all-to-all-done.1 = bf16[32,32,128]{2,1,0:T(8,128)(2,1)S(1)} async-done(((bf16[32,32,128]{2,1,0:T(8,128)(2,1)}), bf16[32,32,128]{2,1,0:T(8,128)(2,1)S(1)}, u32[]{:S(2)}, u32[]{:S(2)}) %all-to-all-start.1) | async-done | bytes 262176 | tf_op jit(solution)/shard_map/all_to_all | solution.py:272
  135.1 4.5 %all-to-all-start.2 = ((bf16[16,256,128]{2,1,0:T(8,128)(2,1)}), bf16[16,256,128]{2,1,0:T(8,128)(2,1)}, u32[]{:S(2)}, u32[]{:S(2)}) async-start(bf16[16,256,128]{2,1,0:T(8,128)(2,1)} %bitcast.62), calls=%async_computation.2 | async-start | bytes 2097152 | tf_op jit(solution)/shard_map/all_to_all | solution.py:279
  141.5 3.1 %collective-permute-start.6 = (bf16[2048,128]{1,0:T(8,128)(2,1)}, bf16[2048,128]{1,0:T(8,128)(2,1)}, u32[]{:S(2)}, u32[]{:S(2)}) collective-permute-start(bf16[2048,128]{1,0:T(8,128)(2,1)} %slice.35), channel_id=1, source_target_pairs={{0,1},{1,2},{2,3},{3,0},{4,5},{5,6},{6,7},{7,4},{8,9},{9,10},{10,1... | collective-permute-start | bytes 1572872 | tf_op jit(solution)/shard_map/ppermute | solution.py:239
  146.4 3.4 %collective-permute-start.7 = (bf16[2048,128]{1,0:T(8,128)(2,1)}, bf16[2048,128]{1,0:T(8,128)(2,1)}, u32[]{:S(2)}, u32[]{:S(2)}) collective-permute-start(bf16[2048,128]{1,0:T(8,128)(2,1)} %slice.36), channel_id=1, source_target_pairs={{0,3},{1,0},{2,1},{3,2},{4,7},{5,4},{6,5},{7,6},{8,11},{9,8},{10,9... | collective-permute-start | bytes 1572872 | tf_op jit(solution)/shard_map/ppermute | solution.py:240
  149.8 6.1 %all-to-all-done.2.rows_ref = bf16[16,256,128]{2,1,0:T(8,128)(2,1)} async-done(((bf16[16,256,128]{2,1,0:T(8,128)(2,1)}), bf16[16,256,128]{2,1,0:T(8,128)(2,1)}, u32[]{:S(2)}, u32[]{:S(2)}) %all-to-all-start.2) | async-done | bytes 1048608 | tf_op jit(solution)/shard_map/all_to_all | solution.py:279
  158.4 5.4 %hidden.1 = bf16[4,256,256]{2,1,0:T(8,128)(2,1)S(1)} custom-call(s32[1]{0:T(128)} %bitcast.11.x_ref, bf16[16,256,128]{2,1,0:T(8,128)(2,1)} %all-to-all-done.2.rows_ref, f32[1,2048]{1,0:T(1,128)S(1)} %bitcast.60, bf16[2048,256]{1,0:T(8,128)(2,1)S(1)} %bitcast.54, bf16[2048,256]{1,0:T(8,128)(2,1)S(1)} %bitcast.55, ...), custom_call_target="tpu_custom_call" | custom-call | tf_op jit(solution)/shard_map/hidden/pallas_call | solution.py:140
  163.9 18.3 %all-gather.3 = f16[16,256,256]{2,1,0:T(8,128)(2,1)S(1)} all-gather(f16[4,256,256]{2,1,0:T(8,128)(2,1)S(1)} %multiply_convert_fusion.2), channel_id=1, replica_groups=mesh['sp'=32,'y'=4,'x'=4] {'y'}, dimensions={0}, use_global_device_ids=true | all-gather | bytes 2621440 | tf_op jit(solution)/shard_map/all_gather | solution.py:190
  183.5 3.1 %down.1 = bf16[4,256,128]{2,1,0:T(8,128)(2,1)S(1)} custom-call(s32[1]{0:T(128)} %bitcast.11.x_ref, bf16[16,256,256]{2,1,0:T(8,128)(2,1)S(1)} %multiply_convert_fusion.1.units_ref, bf16[4096,128]{1,0:T(8,128)(2,1)S(1)} %bitcast.58, bf16[4096,128]{1,0:T(8,128)(2,1)} %collective-permute-done.4.right_ref, bf16[2048,128]{1,0:T(8,128)(2,1)} %collective-permute-done.6.low_ref, ...), custom_call_target="tpu_custom_call" | custom-call | tf_op jit(solution)/shard_map/down/pallas_call | solution.py:178
  186.6 9.8 %all_to_all.30 = bf16[4,256,128]{2,1,0:T(8,128)(2,1)} all-to-all(bf16[4,256,128]{2,1,0:T(8,128)(2,1)S(1)} %down.1), channel_id=1, replica_groups=mesh['sp'=32,'y'=4,'x'=4] {'x'}, dimensions={0} | all-to-all | bytes 524288 | tf_op jit(solution)/shard_map/all_to_all | solution.py:285
  196.4 17.7 %all-to-all-start.4 = ((bf16[32,32,128]{2,1,0:T(8,128)(2,1)}), bf16[32,32,128]{2,1,0:T(8,128)(2,1)S(1)}, u32[]{:S(2)}, u32[]{:S(2)}) async-start(bf16[32,32,128]{2,1,0:T(8,128)(2,1)} %bitcast.21), calls=%async_computation.4 | async-start | bytes 524288 | tf_op jit(solution)/shard_map/all_to_all | solution.py:286
  214.1 22.2 %all-to-all-done.4 = bf16[32,32,128]{2,1,0:T(8,128)(2,1)S(1)} async-done(((bf16[32,32,128]{2,1,0:T(8,128)(2,1)}), bf16[32,32,128]{2,1,0:T(8,128)(2,1)S(1)}, u32[]{:S(2)}, u32[]{:S(2)}) %all-to-all-start.4) | async-done | bytes 262176 | tf_op jit(solution)/shard_map/all_to_all | solution.py:286
  237.5 19.0 %all_to_all.31 = bf16[16,256,128]{2,1,0:T(8,128)(2,1)S(1)} all-to-all(bf16[16,256,128]{2,1,0:T(8,128)(2,1)S(1)} %broadcast_in_dim.20), channel_id=1, replica_groups=mesh['sp'=32,'y'=4,'x'=4] {'y','x'}, dimensions={0} | all-to-all | bytes 2097152 | tf_op jit(solution)/shard_map/all_to_all | solution.py:196
  (68 shorter events, 26.9 us)
Async XLA Ops:
  0.0 86.0 %copy-start = (bf16[256,2048]{1,0:T(8,128)(2,1)S(1)}, bf16[256,2048]{1,0:T(8,128)(2,1)}, u32[]{:S(2)}) copy-start(bf16[256,2048]{1,0:T(8,128)(2,1)} %param.13) | copy-start | bytes 3145732
  0.0 2.4 copy-start.3
  0.0 10.7 %copy-start.12 = (bf16[256,1,128]{2,0,1:T(8,128)(2,1)S(1)}, bf16[256,1,128]{2,0,1:T(8,128)(2,1)}, u32[]{:S(2)}) copy-start(bf16[256,1,128]{2,0,1:T(8,128)(2,1)} %param.16) | copy-start | bytes 196612
  0.0 10.7 %copy-start.13 = (bf16[256,1,128]{2,0,1:T(8,128)(2,1)S(1)}, bf16[256,1,128]{2,0,1:T(8,128)(2,1)}, u32[]{:S(2)}) copy-start(bf16[256,1,128]{2,0,1:T(8,128)(2,1)} %param.15) | copy-start | bytes 196612
  3.6 108.1 %collective-permute-start = (bf16[2,2048,256]{2,1,0:T(8,128)(2,1)}, bf16[2,2048,256]{2,1,0:T(8,128)(2,1)S(1)}, u32[]{:S(2)}, u32[]{:S(2)}) collective-permute-start(bf16[2,2048,256]{2,1,0:T(8,128)(2,1)} %constant_dynamic-update-slice_fusion), channel_id=1, source_target_pairs={{0,1},{1,2},{2,3},{3,0},{4,5},{5,6},{6,7},{7,4},{8,9},{9,10},{10,1... | collective-permute-start | bytes 6291464 | tf_op jit(solution)/shard_map/ppermute | solution.py:232
  7.5 107.3 %collective-permute-start.1 = (bf16[2,2048,256]{2,1,0:T(8,128)(2,1)}, bf16[2,2048,256]{2,1,0:T(8,128)(2,1)}, u32[]{:S(2)}, u32[]{:S(2)}) collective-permute-start(bf16[2,2048,256]{2,1,0:T(8,128)(2,1)} %constant_dynamic-update-slice_fusion), channel_id=1, source_target_pairs={{0,3},{1,0},{2,1},{3,2},{4,7},{5,4},{6,5},{7,6},{8,11},{9,8},{10,9... | collective-permute-start | bytes 6291464 | tf_op jit(solution)/shard_map/ppermute | solution.py:233
  61.5 3.8 %copy-start.9 = (bf16[256,1,128]{2,0,1:T(8,128)(2,1)S(1)}, bf16[256,1,128]{2,0,1:T(8,128)(2,1)}, u32[]{:S(2)}) copy-start(bf16[256,1,128]{2,0,1:T(8,128)(2,1)} %param.14) | copy-start | bytes 196612
  61.5 3.8 %copy-start.11 = (f32[128]{0:T(128)S(1)}, f32[128]{0:T(128)}, u32[]{:S(2)}) copy-start(f32[128]{0:T(128)} %param.18) | copy-start | bytes 1540
  65.3 2.2 copy-start.1
  72.2 12.6 %copy-start.17 = (s32[256,2]{0,1:T(2,128)S(1)}, s32[256,2]{0,1:T(2,128)}, u32[]{:S(2)}) copy-start(s32[256,2]{0,1:T(2,128)} %param.24) | copy-start | bytes 6148
  72.2 23.0 %all-to-all-start = ((bf16[16,256,128]{2,1,0:T(8,128)(2,1)}), bf16[16,256,128]{2,1,0:T(8,128)(2,1)}, u32[]{:S(2)}, u32[]{:S(2)}) async-start(bf16[16,256,128]{2,1,0:T(8,128)(2,1)} %copy-done.5), calls=%async_computation | async-start | bytes 2097152 | tf_op jit(solution)/shard_map/all_to_all | solution.py:270
  78.3 66.2 %collective-permute-start.4 = (bf16[4096,128]{1,0:T(8,128)(2,1)}, bf16[4096,128]{1,0:T(8,128)(2,1)}, u32[]{:S(2)}, u32[]{:S(2)}) collective-permute-start(bf16[4096,128]{1,0:T(8,128)(2,1)} %bitcast.56), channel_id=1, source_target_pairs={{0,3},{1,0},{2,1},{3,2},{4,7},{5,4},{6,5},{7,6},{8,11},{9,8},{10,9... | collective-permute-start | bytes 3145736 | tf_op jit(solution)/shard_map/ppermute | solution.py:238
  82.8 56.8 %collective-permute-start.5 = (bf16[4096,128]{1,0:T(8,128)(2,1)}, bf16[4096,128]{1,0:T(8,128)(2,1)}, u32[]{:S(2)}, u32[]{:S(2)}) collective-permute-start(bf16[4096,128]{1,0:T(8,128)(2,1)} %bitcast.57), channel_id=1, source_target_pairs={{0,1},{1,2},{2,3},{3,0},{4,5},{5,6},{6,7},{7,4},{8,9},{9,10},{10,1... | collective-permute-start | bytes 3145736 | tf_op jit(solution)/shard_map/ppermute | solution.py:237
  98.5 35.4 %all-to-all-start.1 = ((bf16[32,32,128]{2,1,0:T(8,128)(2,1)}), bf16[32,32,128]{2,1,0:T(8,128)(2,1)S(1)}, u32[]{:S(2)}, u32[]{:S(2)}) async-start(bf16[32,32,128]{2,1,0:T(8,128)(2,1)} %bitcast.12), calls=%async_computation.1 | async-start | bytes 524288 | tf_op jit(solution)/shard_map/all_to_all | solution.py:272
  112.8 43.2 %collective-permute-start.2 = (bf16[2048,256]{1,0:T(8,128)(2,1)}, bf16[2048,256]{1,0:T(8,128)(2,1)}, u32[]{:S(2)}, u32[]{:S(2)}) collective-permute-start(bf16[2048,256]{1,0:T(8,128)(2,1)} %slice_bitcast_fusion.1), channel_id=1, source_target_pairs={{0,1},{1,2},{2,3},{3,0},{4,5},{5,6},{6,7},{7,4},{8,9},{9,10},{10,1... | collective-permute-start | bytes 3145736 | tf_op jit(solution)/shard_map/ppermute | solution.py:234
  117.2 38.8 %collective-permute-start.3 = (bf16[2048,256]{1,0:T(8,128)(2,1)}, bf16[2048,256]{1,0:T(8,128)(2,1)}, u32[]{:S(2)}, u32[]{:S(2)}) collective-permute-start(bf16[2048,256]{1,0:T(8,128)(2,1)} %slice_bitcast_fusion), channel_id=1, source_target_pairs={{0,3},{1,0},{2,1},{3,2},{4,7},{5,4},{6,5},{7,6},{8,11},{9,8},{10,9... | collective-permute-start | bytes 3145736 | tf_op jit(solution)/shard_map/ppermute | solution.py:235
  135.1 20.8 %copy-start.10 = (f32[2048]{0:T(1024)S(1)}, f32[2048]{0:T(1024)}, u32[]{:S(2)}) copy-start(f32[2048]{0:T(1024)} %param.20) | copy-start | bytes 24580
  135.1 20.8 %all-to-all-start.2 = ((bf16[16,256,128]{2,1,0:T(8,128)(2,1)}), bf16[16,256,128]{2,1,0:T(8,128)(2,1)}, u32[]{:S(2)}, u32[]{:S(2)}) async-start(bf16[16,256,128]{2,1,0:T(8,128)(2,1)} %bitcast.62), calls=%async_computation.2 | async-start | bytes 2097152 | tf_op jit(solution)/shard_map/all_to_all | solution.py:279
  141.5 41.4 %collective-permute-start.6 = (bf16[2048,128]{1,0:T(8,128)(2,1)}, bf16[2048,128]{1,0:T(8,128)(2,1)}, u32[]{:S(2)}, u32[]{:S(2)}) collective-permute-start(bf16[2048,128]{1,0:T(8,128)(2,1)} %slice.35), channel_id=1, source_target_pairs={{0,1},{1,2},{2,3},{3,0},{4,5},{5,6},{6,7},{7,4},{8,9},{9,10},{10,1... | collective-permute-start | bytes 1572872 | tf_op jit(solution)/shard_map/ppermute | solution.py:239
  146.4 36.4 %collective-permute-start.7 = (bf16[2048,128]{1,0:T(8,128)(2,1)}, bf16[2048,128]{1,0:T(8,128)(2,1)}, u32[]{:S(2)}, u32[]{:S(2)}) collective-permute-start(bf16[2048,128]{1,0:T(8,128)(2,1)} %slice.36), channel_id=1, source_target_pairs={{0,3},{1,0},{2,1},{3,2},{4,7},{5,4},{6,5},{7,6},{8,11},{9,8},{10,9... | collective-permute-start | bytes 1572872 | tf_op jit(solution)/shard_map/ppermute | solution.py:240
  156.0 1.2 copy-start.2
  182.8 31.3 %copy-start.16 = (f32[256,2]{0,1:T(2,128)S(1)}, f32[256,2]{0,1:T(2,128)}, u32[]{:S(2)}) copy-start(f32[256,2]{0,1:T(2,128)} %param.25) | copy-start | bytes 6148
  182.8 53.5 %copy-start.15 = (s32[256,32]{0,1:T(8,128)S(1)}, s32[256,32]{0,1:T(8,128)}, u32[]{:S(2)}) copy-start(s32[256,32]{0,1:T(8,128)} %copy-done.14) | copy-start | bytes 98308
  196.4 40.0 %all-to-all-start.4 = ((bf16[32,32,128]{2,1,0:T(8,128)(2,1)}), bf16[32,32,128]{2,1,0:T(8,128)(2,1)S(1)}, u32[]{:S(2)}, u32[]{:S(2)}) async-start(bf16[32,32,128]{2,1,0:T(8,128)(2,1)} %bitcast.21), calls=%async_computation.4 | async-start | bytes 524288 | tf_op jit(solution)/shard_map/all_to_all | solution.py:286
  (6 other events, 6.6 us)

commit v5 on v4

--- a/solution.py
+++ b/solution.py
@@ -12,7 +12,7 @@
 GROUPS = 4
 
 
-def attention_body(where_ref, lam_ref, q_ref, kv_ref, gain_ref, weight_ref, out_ref, stacked, highest, accum):
+def attention_body(where_ref, lam_ref, q_ref, kv_ref, gain_ref, weight_ref, out_ref, stacked, highest, accum, parts, sems):
     tok, width = q_ref.shape
     first_query = where_ref[0] * tok
     last = (first_query + tok - 1) // KEY_BLOCK
@@ -57,10 +57,20 @@
     combined = both[:tok] - lam_ref[0] * both[tok:]
     square = jnp.mean(combined * combined, axis=1, keepdims=True)
     attended = (combined * lax.rsqrt(square + norm_eps) * gain_ref[...]).astype(jnp.bfloat16)
-    part = jnp.dot(attended, weight_ref[...], preferred_element_type=jnp.float32)
     share = out_ref.shape[2]
-    for p in range(out_ref.shape[0]):
-        out_ref[p] = part[:, p * share : (p + 1) * share].astype(jnp.bfloat16)
+    copies = []
+    for p in range(0, out_ref.shape[0], 2):
+        cols = weight_ref[:, p * share : (p + 2) * share]
+        part = jnp.dot(attended, cols, preferred_element_type=jnp.float32).astype(jnp.bfloat16)
+        parts[p] = part[:, :share]
+        parts[p + 1] = part[:, share:]
+        copy = pltpu.make_async_copy(
+            parts.at[pl.ds(p, 2)], out_ref.at[pl.ds(p, 2)], sems.at[p // 2]
+        )
+        copy.start()
+        copies.append(copy)
+    for copy in copies:
+        copy.wait()
 
 
 def attention(where, lam, q, kv, gain, weight, peers):
@@ -71,30 +81,67 @@
     return pl.pallas_call(
         attention_body,
         in_specs=[smem, smem, vmem, vmem, vmem, vmem],
-        out_specs=vmem,
+        out_specs=pl.BlockSpec(memory_space=pl.ANY),
         out_shape=jax.ShapeDtypeStruct((peers, tok, share), jnp.bfloat16),
         scratch_shapes=[
             pltpu.VMEM((2 * tok, width), jnp.bfloat16),
             pltpu.VMEM((2 * tok, 128), jnp.float32),
             pltpu.VMEM((2 * tok, 2 * width), jnp.float32),
+            pltpu.VMEM((peers, tok, share), jnp.bfloat16),
+            pltpu.SemaphoreType.DMA((peers // 2,)),
         ],
         compiler_params=pltpu.CompilerParams(vmem_limit_bytes=24 * 2**20),
         name="attention",
     )(where, lam, q, kv, gain, weight)
 
 
-def project_body(parts_ref, residual_ref, send_ref, stream_ref, out_ref):
+def pack_body(gate_ref, up_ref, out_ref, sems):
+    width = out_ref.shape[2]
+    copies = []
+    for k, source in enumerate((gate_ref, gate_ref, up_ref, up_ref)):
+        cols = source.at[:, pl.ds(k % 2 * width, width)]
+        copies.append(pltpu.make_async_copy(cols, out_ref.at[k], sems.at[k]))
+    for copy in copies:
+        copy.start()
+    for copy in copies:
+        copy.wait()
+
+
+def pack(gate, up):
+    model, hidden = gate.shape
+    anywhere = pl.BlockSpec(memory_space=pl.ANY)
+    return pl.pallas_call(
+        pack_body,
+        in_specs=[anywhere] * 2,
+        out_specs=anywhere,
+        out_shape=jax.ShapeDtypeStruct((4, model, hidden // 2), gate.dtype),
+        scratch_shapes=[pltpu.SemaphoreType.DMA((4,))],
+        name="pack",
+    )(gate, up)
+
+
+def project_body(parts_ref, residual_ref, place_ref, stream_ref, out_ref):
     total = residual_ref[...].astype(jnp.float32)
     for p in range(parts_ref.shape[0]):
         total += parts_ref[p].astype(jnp.float32)
     stream_ref[...] = total
-    picked = jnp.dot(send_ref[...], total.astype(jnp.bfloat16), preferred_element_type=jnp.float32)
-    out_ref[...] = picked.astype(jnp.bfloat16)
-
-
-def project(parts, residual, send):
+    rows = total.astype(jnp.bfloat16)
+    experts, tok = place_ref.shape
+    capacity = out_ref.shape[0] // experts
+    slot = lax.broadcasted_iota(jnp.int32, (capacity, tok), 0)
+    for first in range(0, experts, 8):
+        send = [
+            jnp.where(place_ref[e : e + 1, :] == slot, 1.0, 0.0).astype(jnp.bfloat16)
+            for e in range(first, first + 8)
+        ]
+        picked = jnp.dot(jnp.concatenate(send, axis=0), rows, preferred_element_type=jnp.float32)
+        out_ref[first * capacity : (first + 8) * capacity] = picked.astype(jnp.bfloat16)
+
+
+def project(parts, residual, place):
     _, tok, share = parts.shape
-    slots = send.shape[0]
+    experts = place.shape[0]
+    slots = tok // (experts // GROUPS) * experts
     vmem = pl.BlockSpec(memory_space=pltpu.VMEM)
     return pl.pallas_call(
         project_body,
@@ -106,12 +153,35 @@
         ],
         compiler_params=pltpu.CompilerParams(vmem_limit_bytes=16 * 2**20),
         name="project",
-    )(parts, residual, send)
-
-
-def hidden_body(x_ref, rows_ref, gain_ref, gate_ref, up_ref, left_ref, right_ref, gate_2_ref, up_2_ref, out_ref, normed_ref):
+    )(parts, residual, place)
+
+
+def hidden_body(x_ref, rows_ref, gain_ref, gate_ref, up_ref, left_ref, right_ref, gate_2_ref, up_2_ref, out_ref, normed_ref, weights, sems):
     peers, count, share = rows_ref.shape
     pieces = out_ref.shape[0]
+    width = weights.shape[3]
+    low, high = pl.ds(0, width), pl.ds(width, width)
+    near, far = pl.ds(0, 2), pl.ds(2, 2)
+    groups = [
+        [(right_ref, weights.at[1])],
+        [(gate_2_ref, weights.at[2, near]), (up_2_ref, weights.at[2, far])],
+        [(left_ref, weights.at[3])],
+        [
+            (gate_ref.at[:, low], weights.at[0, 0]),
+            (gate_ref.at[:, high], weights.at[0, 1]),
+            (up_ref.at[:, low], weights.at[0, 2]),
+            (up_ref.at[:, high], weights.at[0, 3]),
+        ],
+    ]
+    copies, at = [], 0
+    for group in groups:
+        started = []
+        for source, target in group:
+            copy = pltpu.make_async_copy(source, target, sems.at[at])
+            copy.start()
+            started.append(copy)
+            at += 1
+        copies.append(started)
     total = jnp.zeros((count, 1), jnp.float32)
     for p in range(peers):
         part = rows_ref[p].astype(jnp.float32)
@@ -122,46 +192,62 @@
         normed_ref[:, cols] = (rows_ref[p].astype(jnp.float32) * scale * gain_ref[:, cols]).astype(
             jnp.bfloat16
         )
-    own = (gate_ref, up_ref)
-    right = (right_ref.at[0], right_ref.at[1])
-    left = (left_ref.at[0], left_ref.at[1])
-    for ahead, (gates, ups) in enumerate((own, right, (gate_2_ref, up_2_ref), left)):
+    for ahead, started in zip((1, 2, 3, 0), copies):
+        for copy in started:
+            copy.wait()
         normed = normed_ref[...]
-        gate = jnp.dot(normed, gates[...], preferred_element_type=jnp.float32)
-        up = jnp.dot(normed, ups[...], preferred_element_type=jnp.float32)
+        gates = jnp.concatenate([weights[ahead, 0], weights[ahead, 1]], axis=1)
+        ups = jnp.concatenate([weights[ahead, 2], weights[ahead, 3]], axis=1)
+        gate = jnp.dot(normed, gates, preferred_element_type=jnp.float32)
+        up = jnp.dot(normed, ups, preferred_element_type=jnp.float32)
         act = gate / (1.0 + jnp.exp(-gate)) * up
         out_ref[lax.rem(x_ref[0] + ahead, pieces)] = act.astype(jnp.bfloat16)
 
 
 def hidden_units(x, rows, gain, *weights):
     peers, count, share = rows.shape
-    hidden = weights[0].shape[1]
+    model, hidden = weights[0].shape
     vmem = pl.BlockSpec(memory_space=pltpu.VMEM)
+    anywhere = pl.BlockSpec(memory_space=pl.ANY)
     return pl.pallas_call(
         hidden_body,
-        in_specs=[pl.BlockSpec(memory_space=pltpu.SMEM)] + [vmem] * (2 + len(weights)),
+        in_specs=[pl.BlockSpec(memory_space=pltpu.SMEM), vmem, vmem] + [anywhere] * len(weights),
         out_specs=vmem,
         out_shape=jax.ShapeDtypeStruct((4, count, hidden), jnp.bfloat16),
-        scratch_shapes=[pltpu.VMEM((count, peers * share), jnp.bfloat16)],
+        scratch_shapes=[
+            pltpu.VMEM((count, peers * share), jnp.bfloat16),
+            pltpu.VMEM((4, 4, model, hidden // 2), jnp.bfloat16),
+            pltpu.SemaphoreType.DMA((8,)),
+        ],
         compiler_params=pltpu.CompilerParams(vmem_limit_bytes=24 * 2**20),
         name="hidden",
     )(x, rows, gain, *weights)
 
 
-def down_body(x_ref, units_ref, own_ref, right_ref, low_ref, high_ref, left_ref, out_ref):
+def down_body(x_ref, units_ref, own_ref, right_ref, far_ref, left_ref, out_ref, downs, sems):
     blocks, count, hidden = units_ref.shape
     pieces = out_ref.shape[0]
     share = own_ref.shape[1]
-    half = blocks // 2
+    parts = sems.shape[0]
+    step = own_ref.shape[0] // parts
+    copies = []
+    for c in range(parts):
+        rows = pl.ds(c * step, step)
+        for k, source in enumerate((own_ref, right_ref, far_ref, left_ref)):
+            copy = pltpu.make_async_copy(source.at[rows], downs.at[k, rows], sems.at[c, k])
+            copy.start()
+            copies.append(copy)
     first = jnp.zeros((count, 2 * share), jnp.float32)
     second = jnp.zeros((count, 2 * share), jnp.float32)
     for p in range(blocks):
+        if p % (blocks // parts) == 0:
+            c = p // (blocks // parts)
+            for copy in copies[c * pieces : (c + 1) * pieces]:
+                copy.wait()
         rows = slice(p * hidden, (p + 1) * hidden)
-        part = slice(p % half * hidden, (p % half + 1) * hidden)
         units = units_ref[p]
-        far = (low_ref if p < half else high_ref)[part]
-        near = jnp.concatenate([own_ref[rows], right_ref[rows]], axis=1)
-        rest = jnp.concatenate([far, left_ref[rows]], axis=1)
+        near = jnp.concatenate([downs[0, rows], downs[1, rows]], axis=1)
+        rest = jnp.concatenate([downs[2, rows], downs[3, rows]], axis=1)
         first += jnp.dot(units, near, preferred_element_type=jnp.float32)
         second += jnp.dot(units, rest, preferred_element_type=jnp.float32)
     at = [lax.rem(x_ref[0] + ahead, pieces) for ahead in range(pieces)]
@@ -173,16 +259,48 @@
 
 def down_product(x, units, *downs):
     _, count, _ = units.shape
-    share = downs[0].shape[1]
+    total, share = downs[0].shape
     vmem = pl.BlockSpec(memory_space=pltpu.VMEM)
+    anywhere = pl.BlockSpec(memory_space=pl.ANY)
     return pl.pallas_call(
         down_body,
-        in_specs=[pl.BlockSpec(memory_space=pltpu.SMEM)] + [vmem] * (1 + len(downs)),
+        in_specs=[pl.BlockSpec(memory_space=pltpu.SMEM), vmem] + [anywhere] * len(downs),
         out_specs=vmem,
         out_shape=jax.ShapeDtypeStruct((4, count, share), jnp.bfloat16),
+        scratch_shapes=[
+            pltpu.VMEM((4, total, share), jnp.bfloat16),
+            pltpu.SemaphoreType.DMA((4, 4)),
+        ],
         compiler_params=pltpu.CompilerParams(vmem_limit_bytes=24 * 2**20),
         name="down",
     )(x, units, *downs)
+
+
+def assemble_body(whole_ref, out_ref, sems):
+    peers, _, share = whole_ref.shape
+    copies = [
+        pltpu.make_async_copy(
+            whole_ref.at[p], out_ref.at[:, pl.ds(p * share, share)], sems.at[p]
+        )
+        for p in range(peers)
+    ]
+    for copy in copies:
+        copy.start()
+    for copy in copies:
+        copy.wait()
+
+
+def assemble(whole):
+    peers, tok, share = whole.shape
+    anywhere = pl.BlockSpec(memory_space=pl.ANY)
+    return pl.pallas_call(
+        assemble_body,
+        in_specs=[anywhere],
+        out_specs=anywhere,
+        out_shape=jax.ShapeDtypeStruct((tok, peers * share), whole.dtype),
+        scratch_shapes=[pltpu.SemaphoreType.DMA((peers,))],
+        name="assemble",
+    )(whole)
 
 
 def gathered(array, axes, axis, scale):
@@ -228,16 +346,14 @@
     ahead = [(i, (i + 1) % across) for i in range(across)]
     behind = [(i, (i - 1) % across) for i in range(across)]
     gate, up, down = expert_gate[0], expert_up[0], expert_down[0]
-    both = jnp.stack([gate, up])
+    both = pack(gate, up)
     left = lax.ppermute(both, "x", ahead)
     right = lax.ppermute(both, "x", behind)
-    gate_2 = lax.ppermute(left[0], "x", ahead)
-    up_2 = lax.ppermute(right[1], "x", behind)
-    half = down.shape[0] // 2
+    gate_2 = lax.ppermute(left[:2], "x", ahead)
+    up_2 = lax.ppermute(right[2:], "x", behind)
     down_left = lax.ppermute(down, "x", ahead)
     down_right = lax.ppermute(down, "x", behind)
-    down_low = lax.ppermute(down_left[:half], "x", ahead)
-    down_high = lax.ppermute(down_right[half:], "x", behind)
+    down_2 = lax.ppermute(down_left, "x", ahead)
 
     kv = jnp.concatenate([key_vectors[:, 0], value_rows[:, 0]], axis=1)
     kv_all = gathered(kv, "sp", 0, SHIFT)
@@ -253,10 +369,7 @@
         strict, member.astype(jnp.bfloat16), preferred_element_type=jnp.float32
     ).astype(jnp.int32)
     slot = jnp.arange(capacity, dtype=jnp.int32)
-    send = (member.T[:, None, :] & (earlier.T[:, None, :] == slot[None, :, None])).reshape(
-        experts * capacity, tok
-    )
-    send = send.astype(jnp.bfloat16)
+    place = jnp.where(member, earlier, -1).T
     take = [
         (named[:, k, :, None] & (earlier[:, :, None] == slot))
         .reshape(tok, experts * capacity)
@@ -268,7 +381,7 @@
         where, head_lambda, queries[:, 0], kv_all, head_gain[None], out_weight, peers
     )
     parts = lax.all_to_all(partial, tp, 0, 0, tiled=True)
-    own_stream, outgoing = project(parts, own_residual, send)
+    own_stream, outgoing = project(parts, own_residual, place)
     landed = lax.all_to_all(
         outgoing.reshape(experts, capacity, share), "sp", 0, 0, tiled=True
     )
@@ -281,7 +394,7 @@
         x_at, rows, ffn_gain[None], gate, up, left, right, gate_2, up_2
     )
     all_units = gathered(units, "y", 0, 0.25)
-    made = down_product(x_at, all_units, down, down_right, down_low, down_high, down_left)
+    made = down_product(x_at, all_units, down, down_right, down_2, down_left)
     expert_out = lax.all_to_all(made, "x", 0, 0, tiled=True)
     back = lax.all_to_all(
         expert_out.reshape(experts, capacity, share), "sp", 0, 0, tiled=True
@@ -292,7 +405,7 @@
     )
     own_out = (own_stream + moe).astype(jnp.bfloat16)
     whole = from_everyone(own_out, tp)
-    return whole.swapaxes(0, 1).reshape(tok, model)
+    return assemble(whole)
 
 
 def solution(mesh):

time: 260 us -> 368 us (1.42)
  Pallas kernels: 13.5 us -> 114 us
  waiting for transfers between devices: 49.7 us -> 75.3 us
  local copies, waits for them, and re-layouts: 22.5 us -> 12.1 us
  starting transfers between devices: 67.9 us -> 60.4 us
    pallas_call x0 -> x2, Pallas kernels: none -> 97.7 us  [the longest x1 64.7 us: pack(): pl.pallas_call(pack_body, in_specs=[anywhere] * 2, out_specs=anywhere, ou...]
    all_to_all x1, waiting for transfers between devices: 6.1 us -> 27.4 us  [shards(): lax.all_to_all(quarters.reshape(peers, count, share), tp, 0, 0, tiled=True)]
    all_to_all x1, waiting for transfers between devices: 9.08 us -> 15.3 us  [shards(): parts = lax.all_to_all(partial, tp, 0, 0, tiled=True)]
    ppermute x4 -> x3, starting transfers between devices: 12.9 us -> 8.57 us  [the longest x1 4.56 us: shards(): up_2 = lax.ppermute(right[2:], 'x', behind)]
    unnamed x37 -> x34, local copies, waits for them, and re-layouts: 10.7 us -> 7.31 us
  transfers between devices with their start and end apart: 12 -> 11, of which waited for: 4 -> 4; matrix products, arithmetic and copies ran while one was open for 5% -> 3% of each run, Pallas kernels for 4% -> 4%
where the time goes in v5:
time: 368 us; the launch traced here: 367 us
  Pallas kernels  114 us (31%)
  blocking collectives  98.7 us (27%)
  waiting for transfers between devices  75.3 us (20%)
  starting transfers between devices  60.4 us (16%)
  local copies, waits for them, and re-layouts  12.1 us (3%)
  other arithmetic  4.49 us (1%)
    all_gather x2, blocking collectives, gathered(): whole = lax.all_gather(sent, axes, axis=axis, tiled=True)  70 us
    pallas_call x1, Pallas kernels, pack(): pl.pallas_call(pack_body, in_specs=[anywhere] * 2, out_specs=anywhere, ou...  64.7 us
    pallas_call x1, Pallas kernels, assemble(): pl.pallas_call(assemble_body, in_specs=[anywhere], out_specs=anywhere, ou...  33 us
    all_to_all x1, waiting for transfers between devices, shards(): lax.all_to_all(quarters.reshape(peers, count, share), tp, 0, 0, tiled=True)  27.4 us
    all_to_all x1, waiting for transfers between devices, shards(): lax.all_to_all(expert_out.reshape(experts, capacity, share), 'sp', 0, 0,...  22.2 us
    all_to_all x1, blocking collectives, from_everyone(): lax.all_to_all(jnp.broadcast_to(array[None], (peers, *array.shape)), axes...  20.1 us
    all_to_all x1, starting transfers between devices, shards(): lax.all_to_all(expert_out.reshape(experts, capacity, share), 'sp', 0, 0,...  15.4 us
    all_to_all x1, waiting for transfers between devices, shards(): parts = lax.all_to_all(partial, tp, 0, 0, tiled=True)  15.3 us
  transfers between devices with their start and end apart: 11, of which 4 were waited for; matrix products, arithmetic and copies ran while one was open for 3% of the time, Pallas kernels for 4%

profile of v5, /device:TPU:1, one launch (start us, length us, event | category | flops | bytes accessed | tf_op | source)
XLA Modules:
  0.0 367.0 jit_solution(14961455867616904798)
XLA Ops:
  0.0 64.7 %pack.1 = bf16[4,2048,128]{2,1,0:T(8,128)(2,1)} custom-call(bf16[2048,256]{1,0:T(8,128)(2,1)} %bitcast.39, bf16[2048,256]{1,0:T(8,128)(2,1)} %bitcast.41), custom_call_target="tpu_custom_call" | custom-call | tf_op jit(solution)/shard_map/pack/pallas_call | solution.py:113
  64.7 3.9 %collective-permute-start = (bf16[4,2048,128]{2,1,0:T(8,128)(2,1)}, bf16[4,2048,128]{2,1,0:T(8,128)(2,1)S(1)}, u32[]{:S(2)}, u32[]{:S(2)}) collective-permute-start(bf16[4,2048,128]{2,1,0:T(8,128)(2,1)} %pack.1), channel_id=1, source_target_pairs={{0,1},{1,2},{2,3},{3,0},{4,5},{5,6},{6,7},{7,4},{8,9},{9,10},{10,1... | collective-permute-start | bytes 6291464 | tf_op jit(solution)/shard_map/ppermute | solution.py:350
  68.6 3.2 collective-permute-start.1
  71.9 50.7 %all-gather.2 = f16[8192,256]{1,0:T(8,128)(2,1)S(1)} all-gather(f16[256,256]{1,0:T(8,128)(2,1)S(1)} %multiply_convert_fusion.3), channel_id=1, replica_groups=mesh['sp'=32,'y'=4,'x'=4] {'sp'}, dimensions={0}, use_global_device_ids=true | all-gather | bytes 4325376 | tf_op jit(solution)/shard_map/all_gather | solution.py:308
  122.6 3.2 multiply_convert_fusion.kv_ref
  129.7 5.1 %attention.1 = bf16[16,256,128]{2,1,0:T(8,128)(2,1)S(1)} custom-call(s32[1]{0:T(128)} %bitcast.where_ref, f32[1]{0:T(128)S(6)} %copy.14.lam_ref, bf16[256,128]{1,0:T(8,128)(2,1)S(1)} %bitcast.46, bf16[8192,256]{1,0:T(8,128)(2,1)S(1)} %copy-done.1, f32[1,128]{1,0:T(1,128)S(1)} %bitcast.48, bf16[128,2048]{1,0:T(8,128)(2,1)S(1)} %copy-done.6), custom_call_target="tpu_custom_call" | custom-call | tf_op jit(solution)/shard_map/attention/pallas_call | solution.py:81
  135.7 6.0 %all-to-all-start = ((bf16[16,256,128]{2,1,0:T(8,128)(2,1)}), bf16[16,256,128]{2,1,0:T(8,128)(2,1)}, u32[]{:S(2)}, u32[]{:S(2)}) async-start(bf16[16,256,128]{2,1,0:T(8,128)(2,1)} %copy-done.2), calls=%async_computation | async-start | bytes 2097152 | tf_op jit(solution)/shard_map/all_to_all | solution.py:383
  143.3 15.3 %all-to-all-done.parts_ref = bf16[16,256,128]{2,1,0:T(8,128)(2,1)} async-done(((bf16[16,256,128]{2,1,0:T(8,128)(2,1)}), bf16[16,256,128]{2,1,0:T(8,128)(2,1)}, u32[]{:S(2)}, u32[]{:S(2)}) %all-to-all-start) | async-done | bytes 1048608 | tf_op jit(solution)/shard_map/all_to_all | solution.py:383
  158.5 2.3 project.1
  160.9 12.8 %all-to-all-start.1 = ((bf16[32,32,128]{2,1,0:T(8,128)(2,1)}), bf16[32,32,128]{2,1,0:T(8,128)(2,1)S(1)}, u32[]{:S(2)}, u32[]{:S(2)}) async-start(bf16[32,32,128]{2,1,0:T(8,128)(2,1)} %bitcast.9), calls=%async_computation.1 | async-start | bytes 524288 | tf_op jit(solution)/shard_map/all_to_all | solution.py:385
  178.6 2.3 slice.26
  180.9 4.6 %collective-permute-start.3 = (bf16[2,2048,128]{2,1,0:T(8,128)(2,1)}, bf16[2,2048,128]{2,1,0:T(8,128)(2,1)}, u32[]{:S(2)}, u32[]{:S(2)}) collective-permute-start(bf16[2,2048,128]{2,1,0:T(8,128)(2,1)} %slice.26), channel_id=1, source_target_pairs={{0,3},{1,0},{2,1},{3,2},{4,7},{5,4},{6,5},{7,6},{8,11},{9,8},{10,9... | collective-permute-start | bytes 3145736 | tf_op jit(solution)/shard_map/ppermute | solution.py:353
  185.5 10.4 %all-to-all-done.1 = bf16[32,32,128]{2,1,0:T(8,128)(2,1)S(1)} async-done(((bf16[32,32,128]{2,1,0:T(8,128)(2,1)}), bf16[32,32,128]{2,1,0:T(8,128)(2,1)S(1)}, u32[]{:S(2)}, u32[]{:S(2)}) %all-to-all-start.1) | async-done | bytes 262176 | tf_op jit(solution)/shard_map/all_to_all | solution.py:385
  197.1 4.3 %all-to-all-start.2 = ((bf16[16,256,128]{2,1,0:T(8,128)(2,1)}), bf16[16,256,128]{2,1,0:T(8,128)(2,1)}, u32[]{:S(2)}, u32[]{:S(2)}) async-start(bf16[16,256,128]{2,1,0:T(8,128)(2,1)} %bitcast.49), calls=%async_computation.2 | async-start | bytes 2097152 | tf_op jit(solution)/shard_map/all_to_all | solution.py:392
  201.4 4.3 %collective-permute-start.4 = (bf16[4096,128]{1,0:T(8,128)(2,1)}, bf16[4096,128]{1,0:T(8,128)(2,1)}, u32[]{:S(2)}, u32[]{:S(2)}) collective-permute-start(bf16[4096,128]{1,0:T(8,128)(2,1)} %bitcast.44), channel_id=1, source_target_pairs={{0,3},{1,0},{2,1},{3,2},{4,7},{5,4},{6,5},{7,6},{8,11},{9,8},{10,9... | collective-permute-start | bytes 3145736 | tf_op jit(solution)/shard_map/ppermute | solution.py:355
  207.9 27.4 %all-to-all-done.2.rows_ref = bf16[16,256,128]{2,1,0:T(8,128)(2,1)} async-done(((bf16[16,256,128]{2,1,0:T(8,128)(2,1)}), bf16[16,256,128]{2,1,0:T(8,128)(2,1)}, u32[]{:S(2)}, u32[]{:S(2)}) %all-to-all-start.2) | async-done | bytes 1048608 | tf_op jit(solution)/shard_map/all_to_all | solution.py:392
  237.7 5.8 %hidden.1 = bf16[4,256,256]{2,1,0:T(8,128)(2,1)S(1)} custom-call(s32[1]{0:T(128)} %bitcast.8.x_ref, bf16[16,256,128]{2,1,0:T(8,128)(2,1)} %all-to-all-done.2.rows_ref, f32[1,2048]{1,0:T(1,128)S(1)} %bitcast.47, bf16[2048,256]{1,0:T(8,128)(2,1)S(1)} %bitcast.40, bf16[2048,256]{1,0:T(8,128)(2,1)S(1)} %bitcast.42, ...), custom_call_target="tpu_custom_call" | custom-call | tf_op jit(solution)/shard_map/hidden/pallas_call | solution.py:212
  243.7 19.3 %all-gather.3 = f16[16,256,256]{2,1,0:T(8,128)(2,1)S(1)} all-gather(f16[4,256,256]{2,1,0:T(8,128)(2,1)S(1)} %multiply_convert_fusion.2), channel_id=1, replica_groups=mesh['sp'=32,'y'=4,'x'=4] {'y'}, dimensions={0}, use_global_device_ids=true | all-gather | bytes 2621440 | tf_op jit(solution)/shard_map/all_gather | solution.py:308
  263.6 2.7 down.1
  266.3 8.6 %all_to_all.30 = bf16[4,256,128]{2,1,0:T(8,128)(2,1)} all-to-all(bf16[4,256,128]{2,1,0:T(8,128)(2,1)S(1)} %down.1), channel_id=1, replica_groups=mesh['sp'=32,'y'=4,'x'=4] {'x'}, dimensions={0} | all-to-all | bytes 524288 | tf_op jit(solution)/shard_map/all_to_all | solution.py:398
  274.9 15.4 %all-to-all-start.4 = ((bf16[32,32,128]{2,1,0:T(8,128)(2,1)}), bf16[32,32,128]{2,1,0:T(8,128)(2,1)S(1)}, u32[]{:S(2)}, u32[]{:S(2)}) async-start(bf16[32,32,128]{2,1,0:T(8,128)(2,1)} %bitcast.16), calls=%async_computation.4 | async-start | bytes 524288 | tf_op jit(solution)/shard_map/all_to_all | solution.py:399
  290.4 22.2 %all-to-all-done.4 = bf16[32,32,128]{2,1,0:T(8,128)(2,1)S(1)} async-done(((bf16[32,32,128]{2,1,0:T(8,128)(2,1)}), bf16[32,32,128]{2,1,0:T(8,128)(2,1)S(1)}, u32[]{:S(2)}, u32[]{:S(2)}) %all-to-all-start.4) | async-done | bytes 262176 | tf_op jit(solution)/shard_map/all_to_all | solution.py:399
  313.8 20.1 %all_to_all.31.whole_ref = bf16[16,256,128]{2,1,0:T(8,128)(2,1)} all-to-all(bf16[16,256,128]{2,1,0:T(8,128)(2,1)S(1)} %broadcast_in_dim.44), channel_id=1, replica_groups=mesh['sp'=32,'y'=4,'x'=4] {'y','x'}, dimensions={0} | all-to-all | bytes 2097152 | tf_op jit(solution)/shard_map/all_to_all | solution.py:314
  333.9 33.0 %assemble.1 = bf16[256,2048]{1,0:T(8,128)(2,1)} custom-call(bf16[16,256,128]{2,1,0:T(8,128)(2,1)} %all_to_all.31.whole_ref), custom_call_target="tpu_custom_call" | custom-call | tf_op jit(solution)/shard_map/assemble/pallas_call | solution.py:296
  (58 shorter events, 18.2 us)
Async XLA Ops:
  0.0 141.8 %copy-start = (bf16[256,2048]{1,0:T(8,128)(2,1)S(1)}, bf16[256,2048]{1,0:T(8,128)(2,1)}, u32[]{:S(2)}) copy-start(bf16[256,2048]{1,0:T(8,128)(2,1)} %param.13) | copy-start | bytes 3145732
  0.0 71.8 %copy-start.11 = (bf16[256,1,128]{2,0,1:T(8,128)(2,1)S(1)}, bf16[256,1,128]{2,0,1:T(8,128)(2,1)}, u32[]{:S(2)}) copy-start(bf16[256,1,128]{2,0,1:T(8,128)(2,1)} %param.16) | copy-start | bytes 196612
  0.0 71.8 %copy-start.12 = (bf16[256,1,128]{2,0,1:T(8,128)(2,1)S(1)}, bf16[256,1,128]{2,0,1:T(8,128)(2,1)}, u32[]{:S(2)}) copy-start(bf16[256,1,128]{2,0,1:T(8,128)(2,1)} %param.15) | copy-start | bytes 196612
  64.7 110.9 %collective-permute-start = (bf16[4,2048,128]{2,1,0:T(8,128)(2,1)}, bf16[4,2048,128]{2,1,0:T(8,128)(2,1)S(1)}, u32[]{:S(2)}, u32[]{:S(2)}) collective-permute-start(bf16[4,2048,128]{2,1,0:T(8,128)(2,1)} %pack.1), channel_id=1, source_target_pairs={{0,1},{1,2},{2,3},{3,0},{4,5},{5,6},{6,7},{7,4},{8,9},{9,10},{10,1... | collective-permute-start | bytes 6291464 | tf_op jit(solution)/shard_map/ppermute | solution.py:350
  68.6 110.0 %collective-permute-start.1 = (bf16[4,2048,128]{2,1,0:T(8,128)(2,1)}, bf16[4,2048,128]{2,1,0:T(8,128)(2,1)}, u32[]{:S(2)}, u32[]{:S(2)}) collective-permute-start(bf16[4,2048,128]{2,1,0:T(8,128)(2,1)} %pack.1), channel_id=1, source_target_pairs={{0,3},{1,0},{2,1},{3,2},{4,7},{5,4},{6,5},{7,6},{8,11},{9,8},{10,9... | collective-permute-start | bytes 6291464 | tf_op jit(solution)/shard_map/ppermute | solution.py:351
  122.6 3.8 %copy-start.7 = (bf16[256,1,128]{2,0,1:T(8,128)(2,1)S(1)}, bf16[256,1,128]{2,0,1:T(8,128)(2,1)}, u32[]{:S(2)}) copy-start(bf16[256,1,128]{2,0,1:T(8,128)(2,1)} %param.14) | copy-start | bytes 196612
  122.6 3.8 %copy-start.9 = (f32[128]{0:T(128)S(1)}, f32[128]{0:T(128)}, u32[]{:S(2)}) copy-start(f32[128]{0:T(128)} %param.18) | copy-start | bytes 1540
  125.8 16.1 %copy-start.16 = (s32[256,2]{0,1:T(2,128)S(1)}, s32[256,2]{0,1:T(2,128)}, u32[]{:S(2)}) copy-start(s32[256,2]{0,1:T(2,128)} %param.24) | copy-start | bytes 6148
  126.5 2.2 copy-start.1
  135.7 22.8 %all-to-all-start = ((bf16[16,256,128]{2,1,0:T(8,128)(2,1)}), bf16[16,256,128]{2,1,0:T(8,128)(2,1)}, u32[]{:S(2)}, u32[]{:S(2)}) async-start(bf16[16,256,128]{2,1,0:T(8,128)(2,1)} %copy-done.2), calls=%async_computation | async-start | bytes 2097152 | tf_op jit(solution)/shard_map/all_to_all | solution.py:383
  160.9 74.4 %copy-start.8 = (f32[2048]{0:T(1024)S(1)}, f32[2048]{0:T(1024)}, u32[]{:S(2)}) copy-start(f32[2048]{0:T(1024)} %param.20) | copy-start | bytes 24580
  160.9 35.0 %all-to-all-start.1 = ((bf16[32,32,128]{2,1,0:T(8,128)(2,1)}), bf16[32,32,128]{2,1,0:T(8,128)(2,1)S(1)}, u32[]{:S(2)}, u32[]{:S(2)}) async-start(bf16[32,32,128]{2,1,0:T(8,128)(2,1)} %bitcast.9), calls=%async_computation.1 | async-start | bytes 524288 | tf_op jit(solution)/shard_map/all_to_all | solution.py:385
  173.6 32.1 %collective-permute-start.5 = (bf16[4096,128]{1,0:T(8,128)(2,1)}, bf16[4096,128]{1,0:T(8,128)(2,1)}, u32[]{:S(2)}, u32[]{:S(2)}) collective-permute-start(bf16[4096,128]{1,0:T(8,128)(2,1)} %bitcast.43), channel_id=1, source_target_pairs={{0,1},{1,2},{2,3},{3,0},{4,5},{5,6},{6,7},{7,4},{8,9},{9,10},{10,1... | collective-permute-start | bytes 3145736 | tf_op jit(solution)/shard_map/ppermute | solution.py:354
  176.7 58.6 %collective-permute-start.2 = (bf16[2,2048,128]{2,1,0:T(8,128)(2,1)}, bf16[2,2048,128]{2,1,0:T(8,128)(2,1)}, u32[]{:S(2)}, u32[]{:S(2)}) collective-permute-start(bf16[2,2048,128]{2,1,0:T(8,128)(2,1)} %slice.25), channel_id=1, source_target_pairs={{0,1},{1,2},{2,3},{3,0},{4,5},{5,6},{6,7},{7,4},{8,9},{9,10},{10,1... | collective-permute-start | bytes 3145736 | tf_op jit(solution)/shard_map/ppermute | solution.py:352
  180.9 54.3 %collective-permute-start.3 = (bf16[2,2048,128]{2,1,0:T(8,128)(2,1)}, bf16[2,2048,128]{2,1,0:T(8,128)(2,1)}, u32[]{:S(2)}, u32[]{:S(2)}) collective-permute-start(bf16[2,2048,128]{2,1,0:T(8,128)(2,1)} %slice.26), channel_id=1, source_target_pairs={{0,3},{1,0},{2,1},{3,2},{4,7},{5,4},{6,5},{7,6},{8,11},{9,8},{10,9... | collective-permute-start | bytes 3145736 | tf_op jit(solution)/shard_map/ppermute | solution.py:353
  197.1 38.2 %all-to-all-start.2 = ((bf16[16,256,128]{2,1,0:T(8,128)(2,1)}), bf16[16,256,128]{2,1,0:T(8,128)(2,1)}, u32[]{:S(2)}, u32[]{:S(2)}) async-start(bf16[16,256,128]{2,1,0:T(8,128)(2,1)} %bitcast.49), calls=%async_computation.2 | async-start | bytes 2097152 | tf_op jit(solution)/shard_map/all_to_all | solution.py:392
  201.4 62.2 %collective-permute-start.4 = (bf16[4096,128]{1,0:T(8,128)(2,1)}, bf16[4096,128]{1,0:T(8,128)(2,1)}, u32[]{:S(2)}, u32[]{:S(2)}) collective-permute-start(bf16[4096,128]{1,0:T(8,128)(2,1)} %bitcast.44), channel_id=1, source_target_pairs={{0,3},{1,0},{2,1},{3,2},{4,7},{5,4},{6,5},{7,6},{8,11},{9,8},{10,9... | collective-permute-start | bytes 3145736 | tf_op jit(solution)/shard_map/ppermute | solution.py:355
  205.8 57.8 %collective-permute-start.6 = (bf16[4096,128]{1,0:T(8,128)(2,1)}, bf16[4096,128]{1,0:T(8,128)(2,1)}, u32[]{:S(2)}, u32[]{:S(2)}) collective-permute-start(bf16[4096,128]{1,0:T(8,128)(2,1)} %collective-permute-done.5.left_ref), channel_id=1, source_target_pairs={{0,1},{1,2},{2,3},{3,0},{4,5},{5,6},{6,7},{7,4},{8,9},{9,10},{10,1... | collective-permute-start | bytes 3145736 | tf_op jit(solution)/shard_map/ppermute | solution.py:356
  235.3 1.2 copy-start.3
  243.5 20.1 %copy-start.5 = (bf16[1,4096,128]{2,1,0:T(8,128)(2,1)S(1)}, bf16[1,4096,128]{2,1,0:T(8,128)(2,1)}, u32[]{:S(2)}) copy-start(bf16[1,4096,128]{2,1,0:T(8,128)(2,1)} %param.23) | copy-start | bytes 3145732
  263.5 26.8 %copy-start.15 = (f32[256,2]{0,1:T(2,128)S(1)}, f32[256,2]{0,1:T(2,128)}, u32[]{:S(2)}) copy-start(f32[256,2]{0,1:T(2,128)} %param.25) | copy-start | bytes 6148
  263.6 26.8 %copy-start.10 = (pred[256,2,32]{0,2,1:T(8,128)(4,1)S(1)}, pred[256,2,32]{0,2,1:T(8,128)(4,1)}, u32[]{:S(2)}) copy-start(pred[256,2,32]{0,2,1:T(8,128)(4,1)} %get-tuple-element.13) | copy-start | bytes 49156
  263.6 49.0 %copy-start.14 = (s32[256,32]{0,1:T(8,128)S(1)}, s32[256,32]{0,1:T(8,128)}, u32[]{:S(2)}) copy-start(s32[256,32]{0,1:T(8,128)} %copy-done.13) | copy-start | bytes 98308
  274.9 37.7 %all-to-all-start.4 = ((bf16[32,32,128]{2,1,0:T(8,128)(2,1)}), bf16[32,32,128]{2,1,0:T(8,128)(2,1)S(1)}, u32[]{:S(2)}, u32[]{:S(2)}) async-start(bf16[32,32,128]{2,1,0:T(8,128)(2,1)} %bitcast.16), calls=%async_computation.4 | async-start | bytes 524288 | tf_op jit(solution)/shard_map/all_to_all | solution.py:399
  (4 other events, 3.9 us)

commit v6 on v5

--- a/solution.py
+++ b/solution.py
@@ -81,7 +81,7 @@
     return pl.pallas_call(
         attention_body,
         in_specs=[smem, smem, vmem, vmem, vmem, vmem],
-        out_specs=pl.BlockSpec(memory_space=pl.ANY),
+        out_specs=pl.BlockSpec(memory_space=pltpu.HBM),
         out_shape=jax.ShapeDtypeStruct((peers, tok, share), jnp.bfloat16),
         scratch_shapes=[
             pltpu.VMEM((2 * tok, width), jnp.bfloat16),
@@ -95,29 +95,35 @@
     )(where, lam, q, kv, gain, weight)
 
 
-def pack_body(gate_ref, up_ref, out_ref, sems):
+def pack_body(gate_ref, up_ref, down_ref, out_ref):
     width = out_ref.shape[2]
-    copies = []
-    for k, source in enumerate((gate_ref, gate_ref, up_ref, up_ref)):
-        cols = source.at[:, pl.ds(k % 2 * width, width)]
-        copies.append(pltpu.make_async_copy(cols, out_ref.at[k], sems.at[k]))
-    for copy in copies:
-        copy.start()
-    for copy in copies:
-        copy.wait()
-
-
-def pack(gate, up):
+    out_ref[0] = gate_ref[:, :width]
+    out_ref[1] = gate_ref[:, width:]
+    out_ref[2] = up_ref[:, :width]
+    out_ref[3] = up_ref[:, width:]
+    out_ref[4] = down_ref[0]
+    out_ref[5] = down_ref[1]
+
+
+def pack(gate, up, down):
     model, hidden = gate.shape
-    anywhere = pl.BlockSpec(memory_space=pl.ANY)
+    width = hidden // 2
+    tile = model // 4
     return pl.pallas_call(
         pack_body,
-        in_specs=[anywhere] * 2,
-        out_specs=anywhere,
-        out_shape=jax.ShapeDtypeStruct((4, model, hidden // 2), gate.dtype),
-        scratch_shapes=[pltpu.SemaphoreType.DMA((4,))],
+        grid=(4,),
+        in_specs=[
+            pl.BlockSpec((tile, hidden), lambda i: (i, 0)),
+            pl.BlockSpec((tile, hidden), lambda i: (i, 0)),
+            pl.BlockSpec((2, tile, width), lambda i: (0, i, 0)),
+        ],
+        out_specs=pl.BlockSpec((6, tile, width), lambda i: (0, i, 0)),
+        out_shape=jax.ShapeDtypeStruct((6, model, width), gate.dtype),
+        compiler_params=pltpu.CompilerParams(
+            dimension_semantics=("arbitrary",), vmem_limit_bytes=16 * 2**20
+        ),
         name="pack",
-    )(gate, up)
+    )(gate, up, down.reshape(2, model, width))
 
 
 def project_body(parts_ref, residual_ref, place_ref, stream_ref, out_ref):
@@ -156,22 +162,15 @@
     )(parts, residual, place)
 
 
-def hidden_body(x_ref, rows_ref, gain_ref, gate_ref, up_ref, left_ref, right_ref, gate_2_ref, up_2_ref, out_ref, normed_ref, weights, sems):
+def hidden_body(x_ref, rows_ref, gain_ref, own_ref, left_ref, right_ref, gate_2_ref, up_2_ref, out_ref, normed_ref, weights, sems):
     peers, count, share = rows_ref.shape
     pieces = out_ref.shape[0]
-    width = weights.shape[3]
-    low, high = pl.ds(0, width), pl.ds(width, width)
-    near, far = pl.ds(0, 2), pl.ds(2, 2)
+    near, far, both = pl.ds(0, 2), pl.ds(2, 2), pl.ds(0, 4)
     groups = [
-        [(right_ref, weights.at[1])],
+        [(own_ref.at[both], weights.at[0])],
+        [(right_ref.at[both], weights.at[1])],
+        [(left_ref.at[both], weights.at[3])],
         [(gate_2_ref, weights.at[2, near]), (up_2_ref, weights.at[2, far])],
-        [(left_ref, weights.at[3])],
-        [
-            (gate_ref.at[:, low], weights.at[0, 0]),
-            (gate_ref.at[:, high], weights.at[0, 1]),
-            (up_ref.at[:, low], weights.at[0, 2]),
-            (up_ref.at[:, high], weights.at[0, 3]),
-        ],
     ]
     copies, at = [], 0
     for group in groups:
@@ -192,7 +191,7 @@
         normed_ref[:, cols] = (rows_ref[p].astype(jnp.float32) * scale * gain_ref[:, cols]).astype(
             jnp.bfloat16
         )
-    for ahead, started in zip((1, 2, 3, 0), copies):
+    for ahead, started in zip((0, 1, 3, 2), copies):
         for copy in started:
             copy.wait()
         normed = normed_ref[...]
@@ -206,18 +205,18 @@
 
 def hidden_units(x, rows, gain, *weights):
     peers, count, share = rows.shape
-    model, hidden = weights[0].shape
+    _, model, half = weights[0].shape
     vmem = pl.BlockSpec(memory_space=pltpu.VMEM)
-    anywhere = pl.BlockSpec(memory_space=pl.ANY)
+    anywhere = pl.BlockSpec(memory_space=pltpu.HBM)
     return pl.pallas_call(
         hidden_body,
         in_specs=[pl.BlockSpec(memory_space=pltpu.SMEM), vmem, vmem] + [anywhere] * len(weights),
         out_specs=vmem,
-        out_shape=jax.ShapeDtypeStruct((4, count, hidden), jnp.bfloat16),
+        out_shape=jax.ShapeDtypeStruct((4, count, 2 * half), jnp.bfloat16),
         scratch_shapes=[
             pltpu.VMEM((count, peers * share), jnp.bfloat16),
-            pltpu.VMEM((4, 4, model, hidden // 2), jnp.bfloat16),
-            pltpu.SemaphoreType.DMA((8,)),
+            pltpu.VMEM((4, 4, model, half), jnp.bfloat16),
+            pltpu.SemaphoreType.DMA((5,)),
         ],
         compiler_params=pltpu.CompilerParams(vmem_limit_bytes=24 * 2**20),
         name="hidden",
@@ -226,15 +225,24 @@
 
 def down_body(x_ref, units_ref, own_ref, right_ref, far_ref, left_ref, out_ref, downs, sems):
     blocks, count, hidden = units_ref.shape
-    pieces = out_ref.shape[0]
-    share = own_ref.shape[1]
+    chips, pieces, rows_each, _ = out_ref.shape
     parts = sems.shape[0]
-    step = own_ref.shape[0] // parts
+    half, share = own_ref.shape[1:]
+    step = 2 * half // parts
     copies = []
     for c in range(parts):
-        rows = pl.ds(c * step, step)
-        for k, source in enumerate((own_ref, right_ref, far_ref, left_ref)):
-            copy = pltpu.make_async_copy(source.at[rows], downs.at[k, rows], sems.at[c, k])
+        at = c * step
+        rows = pl.ds(at, step)
+        inner = pl.ds(at % half, step)
+        page = at // half
+        sources = (
+            own_ref.at[4 + page, inner],
+            right_ref.at[4 + page, inner],
+            far_ref.at[page, inner],
+            left_ref.at[4 + page, inner],
+        )
+        for k, source in enumerate(sources):
+            copy = pltpu.make_async_copy(source, downs.at[k, rows], sems.at[c, k])
             copy.start()
             copies.append(copy)
     first = jnp.zeros((count, 2 * share), jnp.float32)
@@ -250,25 +258,24 @@
         rest = jnp.concatenate([downs[2, rows], downs[3, rows]], axis=1)
         first += jnp.dot(units, near, preferred_element_type=jnp.float32)
         second += jnp.dot(units, rest, preferred_element_type=jnp.float32)
-    at = [lax.rem(x_ref[0] + ahead, pieces) for ahead in range(pieces)]
-    out_ref[at[0]] = first[:, :share].astype(jnp.bfloat16)
-    out_ref[at[1]] = first[:, share:].astype(jnp.bfloat16)
-    out_ref[at[2]] = second[:, :share].astype(jnp.bfloat16)
-    out_ref[at[3]] = second[:, share:].astype(jnp.bfloat16)
-
-
-def down_product(x, units, *downs):
+    made = (first[:, :share], first[:, share:], second[:, :share], second[:, share:])
+    for ahead, value in enumerate(made):
+        at = lax.rem(x_ref[0] + ahead, pieces)
+        out_ref[:, at] = value.reshape(chips, rows_each, share).astype(jnp.bfloat16)
+
+
+def down_product(x, units, chips, *downs):
     _, count, _ = units.shape
-    total, share = downs[0].shape
+    _, half, share = downs[0].shape
     vmem = pl.BlockSpec(memory_space=pltpu.VMEM)
-    anywhere = pl.BlockSpec(memory_space=pl.ANY)
+    anywhere = pl.BlockSpec(memory_space=pltpu.HBM)
     return pl.pallas_call(
         down_body,
         in_specs=[pl.BlockSpec(memory_space=pltpu.SMEM), vmem] + [anywhere] * len(downs),
         out_specs=vmem,
-        out_shape=jax.ShapeDtypeStruct((4, count, share), jnp.bfloat16),
+        out_shape=jax.ShapeDtypeStruct((chips, 4, count // chips, share), jnp.bfloat16),
         scratch_shapes=[
-            pltpu.VMEM((4, total, share), jnp.bfloat16),
+            pltpu.VMEM((4, 2 * half, share), jnp.bfloat16),
             pltpu.SemaphoreType.DMA((4, 4)),
         ],
         compiler_params=pltpu.CompilerParams(vmem_limit_bytes=24 * 2**20),
@@ -276,29 +283,24 @@
     )(x, units, *downs)
 
 
-def assemble_body(whole_ref, out_ref, sems):
+def assemble_body(whole_ref, out_ref):
     peers, _, share = whole_ref.shape
-    copies = [
-        pltpu.make_async_copy(
-            whole_ref.at[p], out_ref.at[:, pl.ds(p * share, share)], sems.at[p]
-        )
-        for p in range(peers)
-    ]
-    for copy in copies:
-        copy.start()
-    for copy in copies:
-        copy.wait()
+    for p in range(peers):
+        out_ref[:, p * share : (p + 1) * share] = whole_ref[p]
 
 
 def assemble(whole):
     peers, tok, share = whole.shape
-    anywhere = pl.BlockSpec(memory_space=pl.ANY)
+    tile = tok // 4
     return pl.pallas_call(
         assemble_body,
-        in_specs=[anywhere],
-        out_specs=anywhere,
+        grid=(4,),
+        in_specs=[pl.BlockSpec((peers, tile, share), lambda i: (0, i, 0))],
+        out_specs=pl.BlockSpec((tile, peers * share), lambda i: (i, 0)),
         out_shape=jax.ShapeDtypeStruct((tok, peers * share), whole.dtype),
-        scratch_shapes=[pltpu.SemaphoreType.DMA((peers,))],
+        compiler_params=pltpu.CompilerParams(
+            dimension_semantics=("arbitrary",), vmem_limit_bytes=16 * 2**20
+        ),
         name="assemble",
     )(whole)
 
@@ -346,14 +348,12 @@
     ahead = [(i, (i + 1) % across) for i in range(across)]
     behind = [(i, (i - 1) % across) for i in range(across)]
     gate, up, down = expert_gate[0], expert_up[0], expert_down[0]
-    both = pack(gate, up)
-    left = lax.ppermute(both, "x", ahead)
-    right = lax.ppermute(both, "x", behind)
+    packed = pack(gate, up, down)
+    left = lax.ppermute(packed, "x", ahead)
+    right = lax.ppermute(packed, "x", behind)
     gate_2 = lax.ppermute(left[:2], "x", ahead)
-    up_2 = lax.ppermute(right[2:], "x", behind)
-    down_left = lax.ppermute(down, "x", ahead)
-    down_right = lax.ppermute(down, "x", behind)
-    down_2 = lax.ppermute(down_left, "x", ahead)
+    up_2 = lax.ppermute(right[2:4], "x", behind)
+    down_2 = lax.ppermute(left[4:], "x", ahead)
 
     kv = jnp.concatenate([key_vectors[:, 0], value_rows[:, 0]], axis=1)
     kv_all = gathered(kv, "sp", 0, SHIFT)
@@ -382,23 +382,20 @@
     )
     parts = lax.all_to_all(partial, tp, 0, 0, tiled=True)
     own_stream, outgoing = project(parts, own_residual, place)
-    landed = lax.all_to_all(
-        outgoing.reshape(experts, capacity, share), "sp", 0, 0, tiled=True
-    )
-    count = experts * capacity // across
-    quarters = jnp.broadcast_to(
-        landed.reshape(1, across, count, share), (along, across, count, share)
-    )
-    rows = lax.all_to_all(quarters.reshape(peers, count, share), tp, 0, 0, tiled=True)
+    targets = experts * across
+    each = capacity // across
+    landed = lax.all_to_all(outgoing.reshape(targets, each, share), ("sp", "x"), 0, 0, tiled=True)
+    landed = landed.reshape(experts, across, each, share).swapaxes(0, 1)
+    rows = gathered(landed.reshape(across, experts * each, share), "y", 0, 64.0)
     units = hidden_units(
-        x_at, rows, ffn_gain[None], gate, up, left, right, gate_2, up_2
+        x_at, rows, ffn_gain[None], packed, left, right, gate_2, up_2
     )
     all_units = gathered(units, "y", 0, 0.25)
-    made = down_product(x_at, all_units, down, down_right, down_2, down_left)
-    expert_out = lax.all_to_all(made, "x", 0, 0, tiled=True)
+    made = down_product(x_at, all_units, experts, packed, right, down_2, left)
     back = lax.all_to_all(
-        expert_out.reshape(experts, capacity, share), "sp", 0, 0, tiled=True
-    ).reshape(experts * capacity, share)
+        made.reshape(targets, each, share), ("sp", "x"), 0, 0, tiled=True
+    )
+    back = back.reshape(experts * capacity, share)
     moe = sum(
         route_weight[:, k : k + 1] * jnp.dot(take[k], back, preferred_element_type=jnp.float32)
         for k in range(routing.shape[1])

time: 368 us -> 244 us (0.66)
  Pallas kernels: 114 us -> 16.7 us
  waiting for transfers between devices: 75.3 us -> 51.3 us
  blocking collectives: 98.7 us -> 105 us
  starting transfers between devices: 60.4 us -> 55.7 us
    pallas_call x2, Pallas kernels: 97.7 us -> 4.03 us  [the longest x1 2.37 us: pack(): pl.pallas_call(pack_body, grid=(4,), in_specs=[pl.BlockSpec((tile, hidden...]
    all_to_all x3 -> x2, waiting for transfers between devices: 60 us -> 34.4 us  [the longest x1 23 us: shards(): lax.all_to_all(made.reshape(targets, each, share), ('sp', 'x'), 0, 0, til...]
    all_gather x2 -> x3, blocking collectives: 70 us -> 83.9 us  [gathered(): whole = lax.all_gather(sent, axes, axis=axis, tiled=True)]
    all_to_all x1 -> x0, blocking collectives: 8.59 us -> none  [shards(): expert_out = lax.all_to_all(made, 'x', 0, 0, tiled=True)]
    ppermute x6 -> x4, starting transfers between devices: 20 us -> 12.8 us  [the longest x1 3.93 us: shards(): left = lax.ppermute(packed, 'x', ahead)]
    all_to_all x3 -> x2, starting transfers between devices: 32.5 us -> 33.2 us  [the longest x1 20.8 us: shards(): lax.all_to_all(outgoing.reshape(targets, each, share), ('sp', 'x'), 0, 0,...]
  transfers between devices with their start and end apart: 11 -> 8, of which waited for: 4 -> 3; matrix products, arithmetic and copies ran while one was open for 3% -> 4% of each run, Pallas kernels for 4% -> 4%
where the time goes in v6:
time: 244 us
  blocking collectives  105 us (43%)
  starting transfers between devices  55.7 us (23%)
  waiting for transfers between devices  51.3 us (21%)
  Pallas kernels  16.7 us (7%)
  local copies, waits for them, and re-layouts  10.1 us (4%)
  other arithmetic  3 us (1%)
    all_gather x3, blocking collectives, gathered(): whole = lax.all_gather(sent, axes, axis=axis, tiled=True)  83.9 us
    all_to_all x1, waiting for transfers between devices, shards(): lax.all_to_all(made.reshape(targets, each, share), ('sp', 'x'), 0, 0, til...  23 us
    all_to_all x1, blocking collectives, from_everyone(): lax.all_to_all(jnp.broadcast_to(array[None], (peers, *array.shape)), axes...  20.9 us
    all_to_all x1, starting transfers between devices, shards(): lax.all_to_all(outgoing.reshape(targets, each, share), ('sp', 'x'), 0, 0,...  20.8 us
    all_to_all x1, waiting for transfers between devices, shards(): parts = lax.all_to_all(partial, tp, 0, 0, tiled=True)  16.8 us
    all_to_all x1, starting transfers between devices, shards(): lax.all_to_all(made.reshape(targets, each, share), ('sp', 'x'), 0, 0, til...  12.4 us
    all_to_all x1, waiting for transfers between devices, shards(): lax.all_to_all(outgoing.reshape(targets, each, share), ('sp', 'x'), 0, 0,...  11.5 us
    all_to_all x1, starting transfers between devices, shards(): parts = lax.all_to_all(partial, tp, 0, 0, tiled=True)  6.37 us
  transfers between devices with their start and end apart: 8, of which 3 were waited for; matrix products, arithmetic and copies ran while one was open for 4% of the time, Pallas kernels for 4%

profile of v6, /device:TPU:1, one launch (start us, length us, event | category | flops | bytes accessed | tf_op | source)
XLA Modules:
  0.0 243.6 jit_solution(17983355084370609015)
XLA Ops:
  0.0 1.3 copy-done.1
  1.3 1.2 copy-done.2
  3.8 2.4 pack.1.own_ref
  6.1 3.9 %collective-permute-start = (bf16[6,2048,128]{2,1,0:T(8,128)(2,1)}, bf16[6,2048,128]{2,1,0:T(8,128)(2,1)}, u32[]{:S(2)}, u32[]{:S(2)}) collective-permute-start(bf16[6,2048,128]{2,1,0:T(8,128)(2,1)} %pack.1.own_ref), channel_id=1, source_target_pairs={{0,1},{1,2},{2,3},{3,0},{4,5},{5,6},{6,7},{7,4},{8,9},{9,10},{10,1... | collective-permute-start | bytes 9437192 | tf_op jit(solution)/shard_map/ppermute | solution.py:352
  10.1 3.2 %collective-permute-start.1 = (bf16[6,2048,128]{2,1,0:T(8,128)(2,1)}, bf16[6,2048,128]{2,1,0:T(8,128)(2,1)}, u32[]{:S(2)}, u32[]{:S(2)}) collective-permute-start(bf16[6,2048,128]{2,1,0:T(8,128)(2,1)} %pack.1.own_ref), channel_id=1, source_target_pairs={{0,3},{1,0},{2,1},{3,2},{4,7},{5,4},{6,5},{7,6},{8,11},{9,8},{10,9... | collective-permute-start | bytes 9437192 | tf_op jit(solution)/shard_map/ppermute | solution.py:353
  13.3 50.3 %all-gather.3 = f16[8192,256]{1,0:T(8,128)(2,1)S(1)} all-gather(f16[256,256]{1,0:T(8,128)(2,1)S(1)} %multiply_convert_fusion.5), channel_id=1, replica_groups=mesh['sp'=32,'y'=4,'x'=4] {'sp'}, dimensions={0}, use_global_device_ids=true | all-gather | bytes 4325376 | tf_op jit(solution)/shard_map/all_gather | solution.py:310
  65.4 3.6 %attention.1 = bf16[16,256,128]{2,1,0:T(8,128)(2,1)} custom-call(s32[1]{0:T(128)} %bitcast.where_ref, f32[1]{0:T(128)S(6)} %copy.24.lam_ref, bf16[256,128]{1,0:T(8,128)(2,1)S(1)} %bitcast.39, bf16[8192,256]{1,0:T(8,128)(2,1)S(1)} %multiply_convert_fusion.kv_ref, f32[1,128]{1,0:T(1,128)S(1)} %bitcast.41, bf16[128,2048]{1,0:T(8,128)(2,1)S(1)} %copy-done.4), custom_call_target="tpu_custom_call" | custom-call | tf_op jit(solution)/shard_map/attention/pallas_call | solution.py:81
  69.0 6.4 %all-to-all-start = ((bf16[16,256,128]{2,1,0:T(8,128)(2,1)}), bf16[16,256,128]{2,1,0:T(8,128)(2,1)S(1)}, u32[]{:S(2)}, u32[]{:S(2)}) async-start(bf16[16,256,128]{2,1,0:T(8,128)(2,1)} %attention.1), calls=%async_computation | async-start | bytes 2097152 | tf_op jit(solution)/shard_map/all_to_all | solution.py:383
  76.9 16.8 %all-to-all-done.parts_ref = bf16[16,256,128]{2,1,0:T(8,128)(2,1)S(1)} async-done(((bf16[16,256,128]{2,1,0:T(8,128)(2,1)}), bf16[16,256,128]{2,1,0:T(8,128)(2,1)S(1)}, u32[]{:S(2)}, u32[]{:S(2)}) %all-to-all-start) | async-done | bytes 1048608 | tf_op jit(solution)/shard_map/all_to_all | solution.py:383
  94.8 20.8 %all-to-all-start.1 = ((bf16[128,8,128]{2,1,0:T(8,128)(2,1)}), bf16[128,8,128]{2,1,0:T(8,128)(2,1)S(1)}, u32[]{:S(2)}, u32[]{:S(2)}) async-start(bf16[128,8,128]{2,1,0:T(8,128)(2,1)} %bitcast.10), calls=%async_computation.1 | async-start | bytes 524288 | tf_op jit(solution)/shard_map/all_to_all | solution.py:387
  115.6 3.0 %fusion.8 = (bf16[2,2048,128]{2,1,0:T(8,128)(2,1)}, bf16[2,2048,128]{2,1,0:T(8,128)(2,1)}) fusion(bf16[6,2048,128]{2,1,0:T(8,128)(2,1)} %collective-permute-done.left_ref), kind=kLoop, calls=%fused_computation.25 | loop fusion | bytes 4194304 | tf_op jit(solution)/shard_map/slice | solution.py:356
  118.6 3.4 %collective-permute-start.2 = (bf16[2,2048,128]{2,1,0:T(8,128)(2,1)}, bf16[2,2048,128]{2,1,0:T(8,128)(2,1)S(1)}, u32[]{:S(2)}, u32[]{:S(2)}) collective-permute-start(bf16[2,2048,128]{2,1,0:T(8,128)(2,1)} %get-tuple-element.10), channel_id=1, source_target_pairs={{0,1},{1,2},{2,3},{3,0},{4,5},{5,6},{6,7},{7,4},{8,9},{9,10},{10,1... | collective-permute-start | bytes 3145736 | tf_op jit(solution)/shard_map/ppermute | solution.py:354
  122.0 2.3 slice.30
  124.3 3.2 %collective-permute-start.3 = (bf16[2,2048,128]{2,1,0:T(8,128)(2,1)}, bf16[2,2048,128]{2,1,0:T(8,128)(2,1)S(1)}, u32[]{:S(2)}, u32[]{:S(2)}) collective-permute-start(bf16[2,2048,128]{2,1,0:T(8,128)(2,1)} %slice.30), channel_id=1, source_target_pairs={{0,3},{1,0},{2,1},{3,2},{4,7},{5,4},{6,5},{7,6},{8,11},{9,8},{10,9... | collective-permute-start | bytes 3145736 | tf_op jit(solution)/shard_map/ppermute | solution.py:355
  127.5 11.5 %all-to-all-done.1 = bf16[128,8,128]{2,1,0:T(8,128)(2,1)S(1)} async-done(((bf16[128,8,128]{2,1,0:T(8,128)(2,1)}), bf16[128,8,128]{2,1,0:T(8,128)(2,1)S(1)}, u32[]{:S(2)}, u32[]{:S(2)}) %all-to-all-start.1) | async-done | bytes 262176 | tf_op jit(solution)/shard_map/all_to_all | solution.py:387
  139.1 13.1 %all-gather.4 = f16[16,256,128]{2,1,0:T(8,128)(2,1)S(1)} all-gather(f16[4,256,128]{2,1,0:T(8,128)(2,1)S(1)} %bitcast.43), channel_id=1, replica_groups=mesh['sp'=32,'y'=4,'x'=4] {'y'}, dimensions={0}, use_global_device_ids=true | all-gather | bytes 1310720 | tf_op jit(solution)/shard_map/all_gather | solution.py:310
  152.5 2.4 %collective-permute-start.4 = (bf16[2,2048,128]{2,1,0:T(8,128)(2,1)S(1)}, bf16[2,2048,128]{2,1,0:T(8,128)(2,1)S(1)}, u32[]{:S(2)}, u32[]{:S(2)}) collective-permute-start(bf16[2,2048,128]{2,1,0:T(8,128)(2,1)S(1)} %copy-done.8), channel_id=1, source_target_pairs={{0,1},{1,2},{2,3},{3,0},{4,5},{5,6},{6,7},{7,4},{8,9},{9,10},{10,1... | collective-permute-start | bytes 3145736 | tf_op jit(solution)/shard_map/ppermute | solution.py:356
  155.0 4.6 %hidden.1 = bf16[4,256,256]{2,1,0:T(8,128)(2,1)S(1)} custom-call(s32[1]{0:T(128)} %bitcast.9.x_ref, bf16[16,256,128]{2,1,0:T(8,128)(2,1)S(1)} %multiply_convert_fusion.2.rows_ref, f32[1,2048]{1,0:T(1,128)S(1)} %bitcast.40, bf16[6,2048,128]{2,1,0:T(8,128)(2,1)} %pack.1.own_ref, bf16[6,2048,128]{2,1,0:T(8,128)(2,1)} %collective-permute-done.left_ref, ...), custom_call_target="tpu_custom_call" | custom-call | tf_op jit(solution)/shard_map/hidden/pallas_call | solution.py:211
  159.7 20.4 %all-gather.5 = f16[16,256,256]{2,1,0:T(8,128)(2,1)S(1)} all-gather(f16[4,256,256]{2,1,0:T(8,128)(2,1)S(1)} %multiply_convert_fusion.3), channel_id=1, replica_groups=mesh['sp'=32,'y'=4,'x'=4] {'y'}, dimensions={0}, use_global_device_ids=true | all-gather | bytes 2621440 | tf_op jit(solution)/shard_map/all_gather | solution.py:310
  180.7 3.4 %down.1 = bf16[32,4,8,128]{3,2,1,0:T(8,128)(2,1)} custom-call(s32[1]{0:T(128)} %bitcast.9.x_ref, bf16[16,256,256]{2,1,0:T(8,128)(2,1)S(1)} %multiply_convert_fusion.1.units_ref, bf16[6,2048,128]{2,1,0:T(8,128)(2,1)} %pack.1.own_ref, bf16[6,2048,128]{2,1,0:T(8,128)(2,1)} %collective-permute-done.1.right_ref, ...), custom_call_target="tpu_custom_call" | custom-call | tf_op jit(solution)/shard_map/down/pallas_call | solution.py:272
  184.1 12.4 %all-to-all-start.2 = ((bf16[128,8,128]{2,1,0:T(8,128)(2,1)}), bf16[128,8,128]{2,1,0:T(8,128)(2,1)S(1)}, u32[]{:S(2)}, u32[]{:S(2)}) async-start(bf16[128,8,128]{2,1,0:T(8,128)(2,1)} %bitcast.18), calls=%async_computation.2 | async-start | bytes 524288 | tf_op jit(solution)/shard_map/all_to_all | solution.py:395
  196.9 23.0 %all-to-all-done.2 = bf16[128,8,128]{2,1,0:T(8,128)(2,1)S(1)} async-done(((bf16[128,8,128]{2,1,0:T(8,128)(2,1)}), bf16[128,8,128]{2,1,0:T(8,128)(2,1)S(1)}, u32[]{:S(2)}, u32[]{:S(2)}) %all-to-all-start.2) | async-done | bytes 262176 | tf_op jit(solution)/shard_map/all_to_all | solution.py:395
  221.1 20.9 %all_to_all.20.whole_ref = bf16[16,256,128]{2,1,0:T(8,128)(2,1)S(1)} all-to-all(bf16[16,256,128]{2,1,0:T(8,128)(2,1)S(1)} %broadcast_in_dim.35), channel_id=1, replica_groups=mesh['sp'=32,'y'=4,'x'=4] {'y','x'}, dimensions={0} | all-to-all | bytes 2097152 | tf_op jit(solution)/shard_map/all_to_all | solution.py:316
  241.9 1.7 assemble.1
  (53 shorter events, 7.5 us)
Async XLA Ops:
  0.0 75.4 %copy-start = (bf16[256,2048]{1,0:T(8,128)(2,1)S(1)}, bf16[256,2048]{1,0:T(8,128)(2,1)}, u32[]{:S(2)}) copy-start(bf16[256,2048]{1,0:T(8,128)(2,1)} %param.13) | copy-start | bytes 3145732
  0.0 1.3 copy-start.1
  1.3 1.2 copy-start.2
  2.5 1.2 copy-start.3
  3.8 9.5 %copy-start.12 = (bf16[256,1,128]{2,0,1:T(8,128)(2,1)S(1)}, bf16[256,1,128]{2,0,1:T(8,128)(2,1)}, u32[]{:S(2)}) copy-start(bf16[256,1,128]{2,0,1:T(8,128)(2,1)} %param.16) | copy-start | bytes 196612
  3.8 9.5 %copy-start.13 = (bf16[256,1,128]{2,0,1:T(8,128)(2,1)S(1)}, bf16[256,1,128]{2,0,1:T(8,128)(2,1)}, u32[]{:S(2)}) copy-start(bf16[256,1,128]{2,0,1:T(8,128)(2,1)} %param.15) | copy-start | bytes 196612
  6.1 109.4 %collective-permute-start = (bf16[6,2048,128]{2,1,0:T(8,128)(2,1)}, bf16[6,2048,128]{2,1,0:T(8,128)(2,1)}, u32[]{:S(2)}, u32[]{:S(2)}) collective-permute-start(bf16[6,2048,128]{2,1,0:T(8,128)(2,1)} %pack.1.own_ref), channel_id=1, source_target_pairs={{0,1},{1,2},{2,3},{3,0},{4,5},{5,6},{6,7},{7,4},{8,9},{9,10},{10,1... | collective-permute-start | bytes 9437192 | tf_op jit(solution)/shard_map/ppermute | solution.py:352
  10.1 111.9 %collective-permute-start.1 = (bf16[6,2048,128]{2,1,0:T(8,128)(2,1)}, bf16[6,2048,128]{2,1,0:T(8,128)(2,1)}, u32[]{:S(2)}, u32[]{:S(2)}) collective-permute-start(bf16[6,2048,128]{2,1,0:T(8,128)(2,1)} %pack.1.own_ref), channel_id=1, source_target_pairs={{0,3},{1,0},{2,1},{3,2},{4,7},{5,4},{6,5},{7,6},{8,11},{9,8},{10,9... | collective-permute-start | bytes 9437192 | tf_op jit(solution)/shard_map/ppermute | solution.py:353
  64.3 1.0 copy-start.4
  64.3 1.0 copy-start.5
  64.3 1.0 copy-start.7
  65.4 10.1 %copy-start.15 = (s32[256,2]{0,1:T(2,128)S(1)}, s32[256,2]{0,1:T(2,128)}, u32[]{:S(2)}) copy-start(s32[256,2]{0,1:T(2,128)} %param.24) | copy-start | bytes 6148
  69.0 24.7 %all-to-all-start = ((bf16[16,256,128]{2,1,0:T(8,128)(2,1)}), bf16[16,256,128]{2,1,0:T(8,128)(2,1)S(1)}, u32[]{:S(2)}, u32[]{:S(2)}) async-start(bf16[16,256,128]{2,1,0:T(8,128)(2,1)} %attention.1), calls=%async_computation | async-start | bytes 2097152 | tf_op jit(solution)/shard_map/all_to_all | solution.py:383
  76.2 0.6 copy-start.9
  94.8 44.2 %all-to-all-start.1 = ((bf16[128,8,128]{2,1,0:T(8,128)(2,1)}), bf16[128,8,128]{2,1,0:T(8,128)(2,1)S(1)}, u32[]{:S(2)}, u32[]{:S(2)}) async-start(bf16[128,8,128]{2,1,0:T(8,128)(2,1)} %bitcast.10), calls=%async_computation.1 | async-start | bytes 524288 | tf_op jit(solution)/shard_map/all_to_all | solution.py:387
  118.6 36.4 %copy-start.6 = (f32[2048]{0:T(1024)S(1)}, f32[2048]{0:T(1024)}, u32[]{:S(2)}) copy-start(f32[2048]{0:T(1024)} %param.20) | copy-start | bytes 24580
  118.6 36.4 %collective-permute-start.2 = (bf16[2,2048,128]{2,1,0:T(8,128)(2,1)}, bf16[2,2048,128]{2,1,0:T(8,128)(2,1)S(1)}, u32[]{:S(2)}, u32[]{:S(2)}) collective-permute-start(bf16[2,2048,128]{2,1,0:T(8,128)(2,1)} %get-tuple-element.10), channel_id=1, source_target_pairs={{0,1},{1,2},{2,3},{3,0},{4,5},{5,6},{6,7},{7,4},{8,9},{9,10},{10,1... | collective-permute-start | bytes 3145736 | tf_op jit(solution)/shard_map/ppermute | solution.py:354
  124.3 30.7 %collective-permute-start.3 = (bf16[2,2048,128]{2,1,0:T(8,128)(2,1)}, bf16[2,2048,128]{2,1,0:T(8,128)(2,1)S(1)}, u32[]{:S(2)}, u32[]{:S(2)}) collective-permute-start(bf16[2,2048,128]{2,1,0:T(8,128)(2,1)} %slice.30), channel_id=1, source_target_pairs={{0,3},{1,0},{2,1},{3,2},{4,7},{5,4},{6,5},{7,6},{8,11},{9,8},{10,9... | collective-permute-start | bytes 3145736 | tf_op jit(solution)/shard_map/ppermute | solution.py:355
  138.9 13.6 %copy-start.8 = (bf16[2,2048,128]{2,1,0:T(8,128)(2,1)S(1)}, bf16[2,2048,128]{2,1,0:T(8,128)(2,1)}, u32[]{:S(2)}) copy-start(bf16[2,2048,128]{2,1,0:T(8,128)(2,1)} %get-tuple-element.9) | copy-start | bytes 3145732
  152.5 28.1 %collective-permute-start.4 = (bf16[2,2048,128]{2,1,0:T(8,128)(2,1)S(1)}, bf16[2,2048,128]{2,1,0:T(8,128)(2,1)S(1)}, u32[]{:S(2)}, u32[]{:S(2)}) collective-permute-start(bf16[2,2048,128]{2,1,0:T(8,128)(2,1)S(1)} %copy-done.8), channel_id=1, source_target_pairs={{0,1},{1,2},{2,3},{3,0},{4,5},{5,6},{6,7},{7,4},{8,9},{9,10},{10,1... | collective-permute-start | bytes 3145736 | tf_op jit(solution)/shard_map/ppermute | solution.py:356
  180.6 15.9 %copy-start.14 = (f32[256,2]{0,1:T(2,128)S(1)}, f32[256,2]{0,1:T(2,128)}, u32[]{:S(2)}) copy-start(f32[256,2]{0,1:T(2,128)} %param.25) | copy-start | bytes 6148
  180.6 15.9 %copy-start.11 = (pred[256,2,32]{0,2,1:T(8,128)(4,1)S(1)}, pred[256,2,32]{0,2,1:T(8,128)(4,1)}, u32[]{:S(2)}) copy-start(pred[256,2,32]{0,2,1:T(8,128)(4,1)} %get-tuple-element.17) | copy-start | bytes 49156
  180.6 15.9 %copy-start.10 = (s32[256,32]{0,1:T(8,128)S(1)}, s32[256,32]{0,1:T(8,128)}, u32[]{:S(2)}) copy-start(s32[256,32]{0,1:T(8,128)} %copy-done.9) | copy-start | bytes 98308
  184.1 35.8 %all-to-all-start.2 = ((bf16[128,8,128]{2,1,0:T(8,128)(2,1)}), bf16[128,8,128]{2,1,0:T(8,128)(2,1)S(1)}, u32[]{:S(2)}, u32[]{:S(2)}) async-start(bf16[128,8,128]{2,1,0:T(8,128)(2,1)} %bitcast.18), calls=%async_computation.2 | async-start | bytes 524288 | tf_op jit(solution)/shard_map/all_to_all | solution.py:395

commit v7 on v6

--- a/solution.py
+++ b/solution.py
@@ -95,38 +95,43 @@
     )(where, lam, q, kv, gain, weight)
 
 
-def pack_body(gate_ref, up_ref, down_ref, out_ref):
-    width = out_ref.shape[2]
-    out_ref[0] = gate_ref[:, :width]
-    out_ref[1] = gate_ref[:, width:]
-    out_ref[2] = up_ref[:, :width]
-    out_ref[3] = up_ref[:, width:]
-    out_ref[4] = down_ref[0]
-    out_ref[5] = down_ref[1]
+def pack_body(gate_ref, up_ref, down_ref, out_ref, sems):
+    rows, width = out_ref.shape[1:]
+    low, high = pl.ds(0, width), pl.ds(width, width)
+    sources = (
+        gate_ref.at[:, low],
+        gate_ref.at[:, high],
+        down_ref.at[pl.ds(0, rows)],
+        down_ref.at[pl.ds(rows, rows)],
+        up_ref.at[:, low],
+        up_ref.at[:, high],
+    )
+    copies = [
+        pltpu.make_async_copy(source, out_ref.at[k], sems.at[k])
+        for k, source in enumerate(sources)
+    ]
+    for copy in copies:
+        copy.start()
+    for copy in copies:
+        copy.wait()
 
 
 def pack(gate, up, down):
     model, hidden = gate.shape
-    width = hidden // 2
-    tile = model // 4
     return pl.pallas_call(
         pack_body,
-        grid=(4,),
-        in_specs=[
-            pl.BlockSpec((tile, hidden), lambda i: (i, 0)),
-            pl.BlockSpec((tile, hidden), lambda i: (i, 0)),
-            pl.BlockSpec((2, tile, width), lambda i: (0, i, 0)),
-        ],
-        out_specs=pl.BlockSpec((6, tile, width), lambda i: (0, i, 0)),
-        out_shape=jax.ShapeDtypeStruct((6, model, width), gate.dtype),
-        compiler_params=pltpu.CompilerParams(
-            dimension_semantics=("arbitrary",), vmem_limit_bytes=16 * 2**20
-        ),
+        in_specs=[pl.BlockSpec(memory_space=pltpu.HBM)] * 3,
+        out_specs=pl.BlockSpec(memory_space=pltpu.HBM),
+        out_shape=jax.ShapeDtypeStruct((6, model, hidden // 2), gate.dtype),
+        scratch_shapes=[pltpu.SemaphoreType.DMA((6,))],
+        compiler_params=pltpu.CompilerParams(vmem_limit_bytes=16 * 2**20),
         name="pack",
-    )(gate, up, down.reshape(2, model, width))
-
-
-def project_body(parts_ref, residual_ref, place_ref, stream_ref, out_ref):
+    )(gate, up, down)
+
+
+def project_body(parts_ref, residual_ref, place_ref, slots_ref, factors_ref, stream_ref, out_ref, slots_out, factors_out):
+    slots_out[...] = slots_ref[...]
+    factors_out[...] = factors_ref[...]
     total = residual_ref[...].astype(jnp.float32)
     for p in range(parts_ref.shape[0]):
         total += parts_ref[p].astype(jnp.float32)
@@ -144,34 +149,65 @@
         out_ref[first * capacity : (first + 8) * capacity] = picked.astype(jnp.bfloat16)
 
 
-def project(parts, residual, place):
+def project(parts, residual, place, slots, factors):
     _, tok, share = parts.shape
     experts = place.shape[0]
-    slots = tok // (experts // GROUPS) * experts
+    rows = tok // (experts // GROUPS) * experts
     vmem = pl.BlockSpec(memory_space=pltpu.VMEM)
     return pl.pallas_call(
         project_body,
-        in_specs=[vmem] * 3,
-        out_specs=[vmem] * 2,
+        in_specs=[vmem] * 5,
+        out_specs=[vmem] * 4,
         out_shape=[
             jax.ShapeDtypeStruct((tok, share), jnp.float32),
-            jax.ShapeDtypeStruct((slots, share), jnp.bfloat16),
+            jax.ShapeDtypeStruct((rows, share), jnp.bfloat16),
+            jax.ShapeDtypeStruct(slots.shape, slots.dtype),
+            jax.ShapeDtypeStruct(factors.shape, factors.dtype),
         ],
         compiler_params=pltpu.CompilerParams(vmem_limit_bytes=16 * 2**20),
         name="project",
-    )(parts, residual, place)
-
-
-def hidden_body(x_ref, rows_ref, gain_ref, own_ref, left_ref, right_ref, gate_2_ref, up_2_ref, out_ref, normed_ref, weights, sems):
+    )(parts, residual, place, slots, factors)
+
+
+def combine_body(back_ref, stream_ref, slots_ref, factors_ref, out_ref):
+    tok = stream_ref.shape[0]
+    rows = back_ref.shape[0]
+    slot = lax.broadcasted_iota(jnp.int32, (tok, rows), 1)
+    total = stream_ref[...]
+    for k in range(slots_ref.shape[1]):
+        take = jnp.where(slots_ref[:, k : k + 1] == slot, 1.0, 0.0).astype(jnp.bfloat16)
+        found = jnp.dot(take, back_ref[...], preferred_element_type=jnp.float32)
+        total += factors_ref[:, k : k + 1] * found
+    done = total.astype(jnp.bfloat16)
+    for p in range(out_ref.shape[0]):
+        out_ref[p] = done
+
+
+def combine(back, stream, slots, factors, peers):
+    tok, share = stream.shape
+    vmem = pl.BlockSpec(memory_space=pltpu.VMEM)
+    return pl.pallas_call(
+        combine_body,
+        in_specs=[vmem] * 4,
+        out_specs=vmem,
+        out_shape=jax.ShapeDtypeStruct((peers, tok, share), jnp.bfloat16),
+        compiler_params=pltpu.CompilerParams(vmem_limit_bytes=16 * 2**20),
+        name="combine",
+    )(back, stream, slots, factors)
+
+
+def hidden_body(x_ref, rows_ref, gain_ref, own_ref, left_ref, right_ref, far_ref, far_up_ref, out_ref, normed_ref, weights, sems):
     peers, count, share = rows_ref.shape
     pieces = out_ref.shape[0]
-    near, far, both = pl.ds(0, 2), pl.ds(2, 2), pl.ds(0, 4)
+    gate, up = pl.ds(0, 2), pl.ds(4, 2)
+    first, second = pl.ds(0, 2), pl.ds(2, 2)
     groups = [
-        [(own_ref.at[both], weights.at[0])],
-        [(right_ref.at[both], weights.at[1])],
-        [(left_ref.at[both], weights.at[3])],
-        [(gate_2_ref, weights.at[2, near]), (up_2_ref, weights.at[2, far])],
+        [(source.at[gate], weights.at[k, first]), (source.at[up], weights.at[k, second])]
+        for k, source in ((0, own_ref), (1, right_ref), (3, left_ref))
     ]
+    groups.append(
+        [(far_ref.at[gate], weights.at[2, first]), (far_up_ref, weights.at[2, second])]
+    )
     copies, at = [], 0
     for group in groups:
         started = []
@@ -216,7 +252,7 @@
         scratch_shapes=[
             pltpu.VMEM((count, peers * share), jnp.bfloat16),
             pltpu.VMEM((4, 4, model, half), jnp.bfloat16),
-            pltpu.SemaphoreType.DMA((5,)),
+            pltpu.SemaphoreType.DMA((8,)),
         ],
         compiler_params=pltpu.CompilerParams(vmem_limit_bytes=24 * 2**20),
         name="hidden",
@@ -236,10 +272,10 @@
         inner = pl.ds(at % half, step)
         page = at // half
         sources = (
-            own_ref.at[4 + page, inner],
-            right_ref.at[4 + page, inner],
-            far_ref.at[page, inner],
-            left_ref.at[4 + page, inner],
+            own_ref.at[2 + page, inner],
+            right_ref.at[2 + page, inner],
+            far_ref.at[2 + page, inner],
+            left_ref.at[2 + page, inner],
         )
         for k, source in enumerate(sources):
             copy = pltpu.make_async_copy(source, downs.at[k, rows], sems.at[c, k])
@@ -309,13 +345,6 @@
     sent = (array.astype(jnp.float32) * scale).astype(jnp.float16)
     whole = lax.all_gather(sent, axes, axis=axis, tiled=True)
     return (whole.astype(jnp.float32) * (1.0 / scale)).astype(jnp.bfloat16)
-
-
-def from_everyone(array, axes):
-    peers = lax.axis_size(axes)
-    return lax.all_to_all(
-        jnp.broadcast_to(array[None], (peers, *array.shape)), axes, 0, 0, tiled=True
-    )
 
 
 def shards(
@@ -351,9 +380,8 @@
     packed = pack(gate, up, down)
     left = lax.ppermute(packed, "x", ahead)
     right = lax.ppermute(packed, "x", behind)
-    gate_2 = lax.ppermute(left[:2], "x", ahead)
-    up_2 = lax.ppermute(right[2:4], "x", behind)
-    down_2 = lax.ppermute(left[4:], "x", ahead)
+    far = lax.ppermute(left[:4], "x", ahead)
+    far_up = lax.ppermute(right[4:], "x", behind)
 
     kv = jnp.concatenate([key_vectors[:, 0], value_rows[:, 0]], axis=1)
     kv_all = gathered(kv, "sp", 0, SHIFT)
@@ -368,40 +396,33 @@
     earlier = jnp.dot(
         strict, member.astype(jnp.bfloat16), preferred_element_type=jnp.float32
     ).astype(jnp.int32)
-    slot = jnp.arange(capacity, dtype=jnp.int32)
     place = jnp.where(member, earlier, -1).T
-    take = [
-        (named[:, k, :, None] & (earlier[:, :, None] == slot))
-        .reshape(tok, experts * capacity)
-        .astype(jnp.bfloat16)
-        for k in range(routing.shape[1])
-    ]
+    picked = jnp.sum(jnp.where(named, earlier[:, None, :], 0), axis=2)
+    slots = routing * capacity + picked
 
     partial = attention(
         where, head_lambda, queries[:, 0], kv_all, head_gain[None], out_weight, peers
     )
     parts = lax.all_to_all(partial, tp, 0, 0, tiled=True)
-    own_stream, outgoing = project(parts, own_residual, place)
+    own_stream, outgoing, slots, factors = project(
+        parts, own_residual, place, slots, route_weight
+    )
     targets = experts * across
     each = capacity // across
     landed = lax.all_to_all(outgoing.reshape(targets, each, share), ("sp", "x"), 0, 0, tiled=True)
     landed = landed.reshape(experts, across, each, share).swapaxes(0, 1)
     rows = gathered(landed.reshape(across, experts * each, share), "y", 0, 64.0)
     units = hidden_units(
-        x_at, rows, ffn_gain[None], packed, left, right, gate_2, up_2
+        x_at, rows, ffn_gain[None], packed, left, right, far, far_up
     )
     all_units = gathered(units, "y", 0, 0.25)
-    made = down_product(x_at, all_units, experts, packed, right, down_2, left)
+    made = down_product(x_at, all_units, experts, packed, right, far, left)
     back = lax.all_to_all(
         made.reshape(targets, each, share), ("sp", "x"), 0, 0, tiled=True
     )
     back = back.reshape(experts * capacity, share)
-    moe = sum(
-        route_weight[:, k : k + 1] * jnp.dot(take[k], back, preferred_element_type=jnp.float32)
-        for k in range(routing.shape[1])
-    )
-    own_out = (own_stream + moe).astype(jnp.bfloat16)
-    whole = from_everyone(own_out, tp)
+    spread = combine(back, own_stream, slots, factors, peers)
+    whole = lax.all_to_all(spread, tp, 0, 0, tiled=True)
     return assemble(whole)
 
 

time: 244 us -> 248 us (1.016)
  blocking collectives: 105 us -> 148 us
  waiting for transfers between devices: 51.3 us -> 26.4 us
  starting transfers between devices: 55.7 us -> 39.6 us
    all_to_all x1 -> x2, blocking collectives: 20.9 us -> 64.1 us  [the longest x1 43.6 us: shards(): lax.all_to_all(made.reshape(targets, each, share), ('sp', 'x'), 0, 0, til...]
    all_to_all x1 -> x0, waiting for transfers between devices: 23 us -> none  [shards(): lax.all_to_all(made.reshape(targets, each, share), ('sp', 'x'), 0, 0, til...]
    all_to_all x1 -> x0, starting transfers between devices: 12.4 us -> none  [shards(): lax.all_to_all(made.reshape(targets, each, share), ('sp', 'x'), 0, 0, til...]
    all_to_all x1, waiting for transfers between devices: 16.8 us -> 9.68 us  [shards(): parts = lax.all_to_all(partial, tp, 0, 0, tiled=True)]
    all_to_all x1, waiting for transfers between devices: 11.5 us -> 16.7 us  [shards(): lax.all_to_all(outgoing.reshape(targets, each, share), ('sp', 'x'), 0, 0,...]
    unnamed x32 -> x39, local copies, waits for them, and re-layouts: 4.48 us -> 6.6 us
    ppermute x3 -> x2, starting transfers between devices: 9.04 us -> 7.67 us  [the longest x1 4.46 us: shards(): far_up = lax.ppermute(right[4:], 'x', behind)]
    slice x3 -> x2, local copies, waits for them, and re-layouts: 5.3 us -> 5.32 us  [the longest x1 3.05 us: shards(): far = lax.ppermute(left[:4], 'x', ahead)]
  transfers between devices with their start and end apart: 8 -> 6, of which waited for: 3 -> 2; matrix products, arithmetic and copies ran while one was open for 4% -> 4% of each run, Pallas kernels for 4% -> 2%
where the time goes in v7:
time: 248 us
  blocking collectives  148 us (60%)
  starting transfers between devices  39.6 us (16%)
  waiting for transfers between devices  26.4 us (11%)
  Pallas kernels  16.5 us (7%)
  local copies, waits for them, and re-layouts  12.1 us (5%)
  other arithmetic  4.35 us (2%)
    all_gather x3, blocking collectives, gathered(): whole = lax.all_gather(sent, axes, axis=axis, tiled=True)  83.6 us
    all_to_all x1, blocking collectives, shards(): lax.all_to_all(made.reshape(targets, each, share), ('sp', 'x'), 0, 0, til...  43.6 us
    all_to_all x1, blocking collectives, shards(): whole = lax.all_to_all(spread, tp, 0, 0, tiled=True)  20.5 us
    all_to_all x1, starting transfers between devices, shards(): lax.all_to_all(outgoing.reshape(targets, each, share), ('sp', 'x'), 0, 0,...  19 us
    all_to_all x1, waiting for transfers between devices, shards(): lax.all_to_all(outgoing.reshape(targets, each, share), ('sp', 'x'), 0, 0,...  16.7 us
    all_to_all x1, waiting for transfers between devices, shards(): parts = lax.all_to_all(partial, tp, 0, 0, tiled=True)  9.68 us
    unnamed x39, local copies, waits for them, and re-layouts  6.6 us
    all_to_all x1, starting transfers between devices, shards(): parts = lax.all_to_all(partial, tp, 0, 0, tiled=True)  5.82 us
  transfers between devices with their start and end apart: 6, of which 2 were waited for; matrix products, arithmetic and copies ran while one was open for 4% of the time, Pallas kernels for 2%

profile of v7, /device:TPU:1, one launch (start us, length us, event | category | flops | bytes accessed | tf_op | source)
XLA Modules:
  0.0 247.8 jit_solution(8089219876501230684)
XLA Ops:
  0.0 1.3 copy-done.1
  1.3 1.2 copy-done.2
  3.8 1.7 pack.1.own_ref
  5.5 3.9 %collective-permute-start = (bf16[6,2048,128]{2,1,0:T(8,128)(2,1)}, bf16[6,2048,128]{2,1,0:T(8,128)(2,1)}, u32[]{:S(2)}, u32[]{:S(2)}) collective-permute-start(bf16[6,2048,128]{2,1,0:T(8,128)(2,1)} %pack.1.own_ref), channel_id=1, source_target_pairs={{0,1},{1,2},{2,3},{3,0},{4,5},{5,6},{6,7},{7,4},{8,9},{9,10},{10,1... | collective-permute-start | bytes 9437192 | tf_op jit(solution)/shard_map/ppermute | solution.py:381
  9.5 3.2 %collective-permute-start.1 = (bf16[6,2048,128]{2,1,0:T(8,128)(2,1)}, bf16[6,2048,128]{2,1,0:T(8,128)(2,1)}, u32[]{:S(2)}, u32[]{:S(2)}) collective-permute-start(bf16[6,2048,128]{2,1,0:T(8,128)(2,1)} %pack.1.own_ref), channel_id=1, source_target_pairs={{0,3},{1,0},{2,1},{3,2},{4,7},{5,4},{6,5},{7,6},{8,11},{9,8},{10,9... | collective-permute-start | bytes 9437192 | tf_op jit(solution)/shard_map/ppermute | solution.py:382
  12.7 52.2 %all-gather.3 = f16[8192,256]{1,0:T(8,128)(2,1)} all-gather(f16[256,256]{1,0:T(8,128)(2,1)S(1)} %multiply_convert_fusion.5), channel_id=1, replica_groups=mesh['sp'=32,'y'=4,'x'=4] {'sp'}, dimensions={0}, use_global_device_ids=true | all-gather | bytes 4325376 | tf_op jit(solution)/shard_map/all_gather | solution.py:346
  65.6 3.2 %multiply_convert_fusion.kv_ref = bf16[8192,256]{1,0:T(8,128)(2,1)S(1)} fusion(f16[8192,256]{1,0:T(8,128)(2,1)} %all-gather.3), kind=kLoop, calls=%fused_computation | loop fusion | flops 6291456 | bytes 8388608 | tf_op jit(solution)/shard_map/convert_element_type | solution.py:347
  68.9 3.6 %attention.1 = bf16[16,256,128]{2,1,0:T(8,128)(2,1)} custom-call(s32[1]{0:T(128)} %bitcast.1.where_ref, f32[1]{0:T(128)S(6)} %copy.46.lam_ref, bf16[256,128]{1,0:T(8,128)(2,1)S(1)} %bitcast.28, bf16[8192,256]{1,0:T(8,128)(2,1)S(1)} %multiply_convert_fusion.kv_ref, f32[1,128]{1,0:T(1,128)S(1)} %bitcast.30, bf16[128,2048]{1,0:T(8,128)(2,1)S(1)} %copy-done.4), custom_call_target="tpu_custom_call" | custom-call | tf_op jit(solution)/shard_map/attention/pallas_call | solution.py:81
  72.5 5.8 %all-to-all-start = ((bf16[16,256,128]{2,1,0:T(8,128)(2,1)}), bf16[16,256,128]{2,1,0:T(8,128)(2,1)}, u32[]{:S(2)}, u32[]{:S(2)}) async-start(bf16[16,256,128]{2,1,0:T(8,128)(2,1)} %attention.1), calls=%async_computation | async-start | bytes 2097152 | tf_op jit(solution)/shard_map/all_to_all | solution.py:406
  78.6 3.1 %slice.8 = bf16[4,2048,128]{2,1,0:T(8,128)(2,1)} slice(bf16[6,2048,128]{2,1,0:T(8,128)(2,1)} %collective-permute-done.left_ref), slice={[0:4], [0:2048], [0:128]} | slice | bytes 4194304 | tf_op jit(solution)/shard_map/slice | solution.py:383
  81.7 3.2 %collective-permute-start.2 = (bf16[4,2048,128]{2,1,0:T(8,128)(2,1)}, bf16[4,2048,128]{2,1,0:T(8,128)(2,1)S(1)}, u32[]{:S(2)}, u32[]{:S(2)}) collective-permute-start(bf16[4,2048,128]{2,1,0:T(8,128)(2,1)} %slice.8), channel_id=1, source_target_pairs={{0,1},{1,2},{2,3},{3,0},{4,5},{5,6},{6,7},{7,4},{8,9},{9,10},{10,1... | collective-permute-start | bytes 6291464 | tf_op jit(solution)/shard_map/ppermute | solution.py:383
  85.3 9.7 %all-to-all-done.parts_ref = bf16[16,256,128]{2,1,0:T(8,128)(2,1)} async-done(((bf16[16,256,128]{2,1,0:T(8,128)(2,1)}), bf16[16,256,128]{2,1,0:T(8,128)(2,1)}, u32[]{:S(2)}, u32[]{:S(2)}) %all-to-all-start) | async-done | bytes 1048608 | tf_op jit(solution)/shard_map/all_to_all | solution.py:406
  94.9 1.7 project.1
  99.2 19.0 %all-to-all-start.1 = ((bf16[128,8,128]{2,1,0:T(8,128)(2,1)}), bf16[128,8,128]{2,1,0:T(8,128)(2,1)S(1)}, u32[]{:S(2)}, u32[]{:S(2)}) async-start(bf16[128,8,128]{2,1,0:T(8,128)(2,1)} %bitcast.27), calls=%async_computation.1 | async-start | bytes 524288 | tf_op jit(solution)/shard_map/all_to_all | solution.py:412
  118.3 2.3 slice.9
  120.5 4.5 %collective-permute-start.3 = (bf16[2,2048,128]{2,1,0:T(8,128)(2,1)}, bf16[2,2048,128]{2,1,0:T(8,128)(2,1)}, u32[]{:S(2)}, u32[]{:S(2)}) collective-permute-start(bf16[2,2048,128]{2,1,0:T(8,128)(2,1)} %slice.9), channel_id=1, source_target_pairs={{0,3},{1,0},{2,1},{3,2},{4,7},{5,4},{6,5},{7,6},{8,11},{9,8},{10,9... | collective-permute-start | bytes 3145736 | tf_op jit(solution)/shard_map/ppermute | solution.py:384
  125.0 16.7 %all-to-all-done.1 = bf16[128,8,128]{2,1,0:T(8,128)(2,1)S(1)} async-done(((bf16[128,8,128]{2,1,0:T(8,128)(2,1)}), bf16[128,8,128]{2,1,0:T(8,128)(2,1)S(1)}, u32[]{:S(2)}, u32[]{:S(2)}) %all-to-all-start.1) | async-done | bytes 262176 | tf_op jit(solution)/shard_map/all_to_all | solution.py:412
  141.8 13.3 %all-gather.4 = f16[16,256,128]{2,1,0:T(8,128)(2,1)S(1)} all-gather(f16[4,256,128]{2,1,0:T(8,128)(2,1)S(1)} %bitcast.31), channel_id=1, replica_groups=mesh['sp'=32,'y'=4,'x'=4] {'y'}, dimensions={0}, use_global_device_ids=true | all-gather | bytes 1310720 | tf_op jit(solution)/shard_map/all_gather | solution.py:346
  155.4 4.5 %hidden.1 = bf16[4,256,256]{2,1,0:T(8,128)(2,1)S(1)} custom-call(s32[1]{0:T(128)} %bitcast.x_ref, bf16[16,256,128]{2,1,0:T(8,128)(2,1)S(1)} %multiply_convert_fusion.2.rows_ref, f32[1,2048]{1,0:T(1,128)S(1)} %bitcast.29, bf16[6,2048,128]{2,1,0:T(8,128)(2,1)} %pack.1.own_ref, bf16[6,2048,128]{2,1,0:T(8,128)(2,1)} %collective-permute-done.left_ref, ...), custom_call_target="tpu_custom_call" | custom-call | tf_op jit(solution)/shard_map/hidden/pallas_call | solution.py:247
  160.1 18.1 %all-gather.5 = f16[16,256,256]{2,1,0:T(8,128)(2,1)S(1)} all-gather(f16[4,256,256]{2,1,0:T(8,128)(2,1)S(1)} %multiply_convert_fusion.3), channel_id=1, replica_groups=mesh['sp'=32,'y'=4,'x'=4] {'y'}, dimensions={0}, use_global_device_ids=true | all-gather | bytes 2621440 | tf_op jit(solution)/shard_map/all_gather | solution.py:346
  178.8 2.7 %down.1 = bf16[32,4,8,128]{3,2,1,0:T(8,128)(2,1)S(1)} custom-call(s32[1]{0:T(128)} %bitcast.x_ref, bf16[16,256,256]{2,1,0:T(8,128)(2,1)S(1)} %multiply_convert_fusion.1.units_ref, bf16[6,2048,128]{2,1,0:T(8,128)(2,1)} %pack.1.own_ref, bf16[6,2048,128]{2,1,0:T(8,128)(2,1)} %collective-permute-done.1.right_ref, ...), custom_call_target="tpu_custom_call" | custom-call | tf_op jit(solution)/shard_map/down/pallas_call | solution.py:308
  181.5 43.6 %all_to_all.20 = bf16[128,8,128]{2,1,0:T(8,128)(2,1)S(1)} all-to-all(bf16[128,8,128]{2,1,0:T(8,128)(2,1)S(1)} %bitcast.22), channel_id=1, replica_groups=mesh['sp'=32,'y'=4,'x'=4] {'sp','x'}, dimensions={0} | all-to-all | bytes 524288 | tf_op jit(solution)/shard_map/all_to_all | solution.py:420
  225.7 20.5 %all_to_all.21.whole_ref = bf16[16,256,128]{2,1,0:T(8,128)(2,1)S(1)} all-to-all(bf16[16,256,128]{2,1,0:T(8,128)(2,1)S(1)} %combine.1), channel_id=1, replica_groups=mesh['sp'=32,'y'=4,'x'=4] {'y','x'}, dimensions={0} | all-to-all | bytes 2097152 | tf_op jit(solution)/shard_map/all_to_all | solution.py:425
  246.2 1.7 assemble.1
  (55 shorter events, 6.1 us)
Async XLA Ops:
  0.0 85.2 %copy-start = (bf16[256,2048]{1,0:T(8,128)(2,1)S(1)}, bf16[256,2048]{1,0:T(8,128)(2,1)}, u32[]{:S(2)}) copy-start(bf16[256,2048]{1,0:T(8,128)(2,1)} %param.13) | copy-start | bytes 3145732
  0.0 1.3 copy-start.1
  1.3 1.2 copy-start.2
  2.5 1.2 copy-start.3
  3.8 8.9 %copy-start.15 = (bf16[256,1,128]{2,0,1:T(8,128)(2,1)S(1)}, bf16[256,1,128]{2,0,1:T(8,128)(2,1)}, u32[]{:S(2)}) copy-start(bf16[256,1,128]{2,0,1:T(8,128)(2,1)} %param.16) | copy-start | bytes 196612
  3.8 8.9 %copy-start.16 = (bf16[256,1,128]{2,0,1:T(8,128)(2,1)S(1)}, bf16[256,1,128]{2,0,1:T(8,128)(2,1)}, u32[]{:S(2)}) copy-start(bf16[256,1,128]{2,0,1:T(8,128)(2,1)} %param.15) | copy-start | bytes 196612
  5.5 73.1 %collective-permute-start = (bf16[6,2048,128]{2,1,0:T(8,128)(2,1)}, bf16[6,2048,128]{2,1,0:T(8,128)(2,1)}, u32[]{:S(2)}, u32[]{:S(2)}) collective-permute-start(bf16[6,2048,128]{2,1,0:T(8,128)(2,1)} %pack.1.own_ref), channel_id=1, source_target_pairs={{0,1},{1,2},{2,3},{3,0},{4,5},{5,6},{6,7},{7,4},{8,9},{9,10},{10,1... | collective-permute-start | bytes 9437192 | tf_op jit(solution)/shard_map/ppermute | solution.py:381
  9.5 108.8 %collective-permute-start.1 = (bf16[6,2048,128]{2,1,0:T(8,128)(2,1)}, bf16[6,2048,128]{2,1,0:T(8,128)(2,1)}, u32[]{:S(2)}, u32[]{:S(2)}) collective-permute-start(bf16[6,2048,128]{2,1,0:T(8,128)(2,1)} %pack.1.own_ref), channel_id=1, source_target_pairs={{0,3},{1,0},{2,1},{3,2},{4,7},{5,4},{6,5},{7,6},{8,11},{9,8},{10,9... | collective-permute-start | bytes 9437192 | tf_op jit(solution)/shard_map/ppermute | solution.py:382
  65.6 3.3 %copy-start.4 = (bf16[128,2048]{1,0:T(8,128)(2,1)S(1)}, bf16[128,2048]{1,0:T(8,128)(2,1)}, u32[]{:S(2)}) copy-start(bf16[128,2048]{1,0:T(8,128)(2,1)} %weight_ref.1) | copy-start | bytes 1572868
  65.6 3.3 %copy-start.12 = (bf16[256,1,128]{2,0,1:T(8,128)(2,1)S(1)}, bf16[256,1,128]{2,0,1:T(8,128)(2,1)}, u32[]{:S(2)}) copy-start(bf16[256,1,128]{2,0,1:T(8,128)(2,1)} %param.14) | copy-start | bytes 196612
  65.6 3.3 %copy-start.14 = (f32[128]{0:T(128)S(1)}, f32[128]{0:T(128)}, u32[]{:S(2)}) copy-start(f32[128]{0:T(128)} %param.18) | copy-start | bytes 1540
  68.9 9.5 %copy-start.17 = (s32[256,2]{0,1:T(2,128)S(1)}, s32[256,2]{0,1:T(2,128)}, u32[]{:S(2)}) copy-start(s32[256,2]{0,1:T(2,128)} %param.24) | copy-start | bytes 6148
  72.5 12.5 %copy-start.18 = (f32[256,2]{0,1:T(2,128)S(1)}, f32[256,2]{0,1:T(2,128)}, u32[]{:S(2)}) copy-start(f32[256,2]{0,1:T(2,128)} %param.25) | copy-start | bytes 6148
  72.5 22.4 %all-to-all-start = ((bf16[16,256,128]{2,1,0:T(8,128)(2,1)}), bf16[16,256,128]{2,1,0:T(8,128)(2,1)}, u32[]{:S(2)}, u32[]{:S(2)}) async-start(bf16[16,256,128]{2,1,0:T(8,128)(2,1)} %attention.1), calls=%async_computation | async-start | bytes 2097152 | tf_op jit(solution)/shard_map/all_to_all | solution.py:406
  81.7 73.7 %collective-permute-start.2 = (bf16[4,2048,128]{2,1,0:T(8,128)(2,1)}, bf16[4,2048,128]{2,1,0:T(8,128)(2,1)S(1)}, u32[]{:S(2)}, u32[]{:S(2)}) collective-permute-start(bf16[4,2048,128]{2,1,0:T(8,128)(2,1)} %slice.8), channel_id=1, source_target_pairs={{0,1},{1,2},{2,3},{3,0},{4,5},{5,6},{6,7},{7,4},{8,9},{9,10},{10,1... | collective-permute-start | bytes 6291464 | tf_op jit(solution)/shard_map/ppermute | solution.py:383
  96.6 0.7 copy-start.5
  97.3 0.6 copy-start.6
  98.6 0.7 copy-start.10
  99.2 42.4 %all-to-all-start.1 = ((bf16[128,8,128]{2,1,0:T(8,128)(2,1)}), bf16[128,8,128]{2,1,0:T(8,128)(2,1)S(1)}, u32[]{:S(2)}, u32[]{:S(2)}) async-start(bf16[128,8,128]{2,1,0:T(8,128)(2,1)} %bitcast.27), calls=%async_computation.1 | async-start | bytes 524288 | tf_op jit(solution)/shard_map/all_to_all | solution.py:412
  118.2 37.1 %copy-start.13 = (f32[2048]{0:T(1024)S(1)}, f32[2048]{0:T(1024)}, u32[]{:S(2)}) copy-start(f32[2048]{0:T(1024)} %param.20) | copy-start | bytes 24580
  120.5 34.8 %collective-permute-start.3 = (bf16[2,2048,128]{2,1,0:T(8,128)(2,1)}, bf16[2,2048,128]{2,1,0:T(8,128)(2,1)}, u32[]{:S(2)}, u32[]{:S(2)}) collective-permute-start(bf16[2,2048,128]{2,1,0:T(8,128)(2,1)} %slice.9), channel_id=1, source_target_pairs={{0,3},{1,0},{2,1},{3,2},{4,7},{5,4},{6,5},{7,6},{8,11},{9,8},{10,9... | collective-permute-start | bytes 3145736 | tf_op jit(solution)/shard_map/ppermute | solution.py:384
  178.7 46.4 %copy-start.7 = (f32[256,128]{1,0:T(8,128)S(1)}, f32[256,128]{1,0:T(8,128)}, u32[]{:S(2)}) copy-start(f32[256,128]{1,0:T(8,128)} %copy-done.6) | copy-start | bytes 393220
  178.8 46.4 %copy-start.9 = (s32[256,2]{1,0:T(8,128)S(1)}, s32[256,2]{1,0:T(8,128)}, u32[]{:S(2)}) copy-start(s32[256,2]{1,0:T(8,128)} %copy-done.8) | copy-start | bytes 6148
  178.8 46.4 %copy-start.11 = (f32[256,2]{1,0:T(8,128)S(1)}, f32[256,2]{1,0:T(8,128)}, u32[]{:S(2)}) copy-start(f32[256,2]{1,0:T(8,128)} %copy-done.10) | copy-start | bytes 6148
  (1 other events, 0.6 us)

commit v8 on v7

--- a/solution.py
+++ b/solution.py
@@ -90,7 +90,7 @@
             pltpu.VMEM((peers, tok, share), jnp.bfloat16),
             pltpu.SemaphoreType.DMA((peers // 2,)),
         ],
-        compiler_params=pltpu.CompilerParams(vmem_limit_bytes=24 * 2**20),
+        compiler_params=pltpu.CompilerParams(vmem_limit_bytes=14 * 2**20),
         name="attention",
     )(where, lam, q, kv, gain, weight)
 
@@ -118,15 +118,34 @@
 
 def pack(gate, up, down):
     model, hidden = gate.shape
+    vmem = pl.BlockSpec(memory_space=pltpu.VMEM)
     return pl.pallas_call(
         pack_body,
-        in_specs=[pl.BlockSpec(memory_space=pltpu.HBM)] * 3,
+        in_specs=[vmem] * 3,
         out_specs=pl.BlockSpec(memory_space=pltpu.HBM),
         out_shape=jax.ShapeDtypeStruct((6, model, hidden // 2), gate.dtype),
         scratch_shapes=[pltpu.SemaphoreType.DMA((6,))],
-        compiler_params=pltpu.CompilerParams(vmem_limit_bytes=16 * 2**20),
+        compiler_params=pltpu.CompilerParams(vmem_limit_bytes=8 * 2**20),
         name="pack",
     )(gate, up, down)
+
+
+def arrange_body(landed_ref, out_ref):
+    for k in range(out_ref.shape[0]):
+        out_ref[k] = landed_ref[:, k]
+
+
+def arrange(landed):
+    experts, across, each, share = landed.shape
+    vmem = pl.BlockSpec(memory_space=pltpu.VMEM)
+    return pl.pallas_call(
+        arrange_body,
+        in_specs=[vmem],
+        out_specs=vmem,
+        out_shape=jax.ShapeDtypeStruct((across, experts, each, share), landed.dtype),
+        compiler_params=pltpu.CompilerParams(vmem_limit_bytes=2 * 2**20),
+        name="arrange",
+    )(landed)
 
 
 def project_body(parts_ref, residual_ref, place_ref, slots_ref, factors_ref, stream_ref, out_ref, slots_out, factors_out):
@@ -196,18 +215,15 @@
     )(back, stream, slots, factors)
 
 
-def hidden_body(x_ref, rows_ref, gain_ref, own_ref, left_ref, right_ref, far_ref, far_up_ref, out_ref, normed_ref, weights, sems):
+def hidden_body(turn_ref, rows_ref, gain_ref, own_ref, one_ref, two_ref, three_ref, out_ref, normed_ref, weights, sems):
     peers, count, share = rows_ref.shape
     pieces = out_ref.shape[0]
     gate, up = pl.ds(0, 2), pl.ds(4, 2)
     first, second = pl.ds(0, 2), pl.ds(2, 2)
     groups = [
         [(source.at[gate], weights.at[k, first]), (source.at[up], weights.at[k, second])]
-        for k, source in ((0, own_ref), (1, right_ref), (3, left_ref))
+        for k, source in enumerate((own_ref, one_ref, two_ref, three_ref))
     ]
-    groups.append(
-        [(far_ref.at[gate], weights.at[2, first]), (far_up_ref, weights.at[2, second])]
-    )
     copies, at = [], 0
     for group in groups:
         started = []
@@ -227,19 +243,19 @@
         normed_ref[:, cols] = (rows_ref[p].astype(jnp.float32) * scale * gain_ref[:, cols]).astype(
             jnp.bfloat16
         )
-    for ahead, started in zip((0, 1, 3, 2), copies):
+    for k, started in enumerate(copies):
         for copy in started:
             copy.wait()
         normed = normed_ref[...]
-        gates = jnp.concatenate([weights[ahead, 0], weights[ahead, 1]], axis=1)
-        ups = jnp.concatenate([weights[ahead, 2], weights[ahead, 3]], axis=1)
+        gates = jnp.concatenate([weights[k, 0], weights[k, 1]], axis=1)
+        ups = jnp.concatenate([weights[k, 2], weights[k, 3]], axis=1)
         gate = jnp.dot(normed, gates, preferred_element_type=jnp.float32)
         up = jnp.dot(normed, ups, preferred_element_type=jnp.float32)
         act = gate / (1.0 + jnp.exp(-gate)) * up
-        out_ref[lax.rem(x_ref[0] + ahead, pieces)] = act.astype(jnp.bfloat16)
-
-
-def hidden_units(x, rows, gain, *weights):
+        out_ref[lax.rem(turn_ref[0] + k * turn_ref[1], pieces)] = act.astype(jnp.bfloat16)
+
+
+def hidden_units(turn, rows, gain, *weights):
     peers, count, share = rows.shape
     _, model, half = weights[0].shape
     vmem = pl.BlockSpec(memory_space=pltpu.VMEM)
@@ -256,10 +272,10 @@
         ],
         compiler_params=pltpu.CompilerParams(vmem_limit_bytes=24 * 2**20),
         name="hidden",
-    )(x, rows, gain, *weights)
-
-
-def down_body(x_ref, units_ref, own_ref, right_ref, far_ref, left_ref, out_ref, downs, sems):
+    )(turn, rows, gain, *weights)
+
+
+def down_body(turn_ref, units_ref, own_ref, one_ref, two_ref, three_ref, out_ref, downs, sems):
     blocks, count, hidden = units_ref.shape
     chips, pieces, rows_each, _ = out_ref.shape
     parts = sems.shape[0]
@@ -271,12 +287,9 @@
         rows = pl.ds(at, step)
         inner = pl.ds(at % half, step)
         page = at // half
-        sources = (
-            own_ref.at[2 + page, inner],
-            right_ref.at[2 + page, inner],
-            far_ref.at[2 + page, inner],
-            left_ref.at[2 + page, inner],
-        )
+        sources = [
+            source.at[2 + page, inner] for source in (own_ref, one_ref, two_ref, three_ref)
+        ]
         for k, source in enumerate(sources):
             copy = pltpu.make_async_copy(source, downs.at[k, rows], sems.at[c, k])
             copy.start()
@@ -295,12 +308,12 @@
         first += jnp.dot(units, near, preferred_element_type=jnp.float32)
         second += jnp.dot(units, rest, preferred_element_type=jnp.float32)
     made = (first[:, :share], first[:, share:], second[:, :share], second[:, share:])
-    for ahead, value in enumerate(made):
-        at = lax.rem(x_ref[0] + ahead, pieces)
+    for k, value in enumerate(made):
+        at = lax.rem(turn_ref[0] + k * turn_ref[1], pieces)
         out_ref[:, at] = value.reshape(chips, rows_each, share).astype(jnp.bfloat16)
 
 
-def down_product(x, units, chips, *downs):
+def down_product(turn, units, chips, *downs):
     _, count, _ = units.shape
     _, half, share = downs[0].shape
     vmem = pl.BlockSpec(memory_space=pltpu.VMEM)
@@ -316,7 +329,7 @@
         ],
         compiler_params=pltpu.CompilerParams(vmem_limit_bytes=24 * 2**20),
         name="down",
-    )(x, units, *downs)
+    )(turn, units, *downs)
 
 
 def assemble_body(whole_ref, out_ref):
@@ -363,28 +376,28 @@
     route_weight,
 ):
     tok, _, _ = queries.shape
-    experts = lax.axis_size("sp")
+    sp = ("z", "c")
+    experts = lax.axis_size(sp)
     across = lax.axis_size("x")
     along = lax.axis_size("y")
     tp = ("y", "x")
     peers = across * along
     model = residual.shape[1]
     share = model // peers
-    where = lax.axis_index("sp").astype(jnp.int32)[None]
-    x_at = lax.axis_index("x").astype(jnp.int32)[None]
+    where = lax.axis_index(sp).astype(jnp.int32)[None]
+    core = lax.axis_index("c")
+    turn = jnp.stack([lax.axis_index("x"), 3 - 2 * core]).astype(jnp.int32)
     column = (lax.axis_index("y") * across + lax.axis_index("x")) * share
 
-    ahead = [(i, (i + 1) % across) for i in range(across)]
-    behind = [(i, (i - 1) % across) for i in range(across)]
-    gate, up, down = expert_gate[0], expert_up[0], expert_down[0]
-    packed = pack(gate, up, down)
-    left = lax.ppermute(packed, "x", ahead)
-    right = lax.ppermute(packed, "x", behind)
-    far = lax.ppermute(left[:4], "x", ahead)
-    far_up = lax.ppermute(right[4:], "x", behind)
+    round_x = [(i, (i + 1) % across) for i in range(across)]
+    round_x += [(across + i, across + (i - 1) % across) for i in range(across)]
+    packed = pack(expert_gate[0], expert_up[0], expert_down[0])
+    one = lax.ppermute(packed, ("c", "x"), round_x)
+    two = lax.ppermute(one, ("c", "x"), round_x)
+    three = lax.ppermute(two, ("c", "x"), round_x)
 
     kv = jnp.concatenate([key_vectors[:, 0], value_rows[:, 0]], axis=1)
-    kv_all = gathered(kv, "sp", 0, SHIFT)
+    kv_all = gathered(kv, sp, 0, SHIFT)
     own_residual = lax.dynamic_slice_in_dim(residual, column, share, 1)
 
     capacity = tok // (experts // GROUPS)
@@ -409,16 +422,18 @@
     )
     targets = experts * across
     each = capacity // across
-    landed = lax.all_to_all(outgoing.reshape(targets, each, share), ("sp", "x"), 0, 0, tiled=True)
-    landed = landed.reshape(experts, across, each, share).swapaxes(0, 1)
+    landed = lax.all_to_all(
+        outgoing.reshape(targets, each, share), ("z", "c", "x"), 0, 0, tiled=True
+    )
+    landed = arrange(landed.reshape(experts, across, each, share))
     rows = gathered(landed.reshape(across, experts * each, share), "y", 0, 64.0)
     units = hidden_units(
-        x_at, rows, ffn_gain[None], packed, left, right, far, far_up
+        turn, rows, ffn_gain[None], packed, one, two, three
     )
     all_units = gathered(units, "y", 0, 0.25)
-    made = down_product(x_at, all_units, experts, packed, right, far, left)
+    made = down_product(turn, all_units, experts, packed, one, two, three)
     back = lax.all_to_all(
-        made.reshape(targets, each, share), ("sp", "x"), 0, 0, tiled=True
+        made.reshape(targets, each, share), ("z", "c", "x"), 0, 0, tiled=True
     )
     back = back.reshape(experts * capacity, share)
     spread = combine(back, own_stream, slots, factors, peers)
@@ -429,24 +444,24 @@
 def solution(mesh):
     sizes = mesh.devices.shape
     split = jax.sharding.Mesh(
-        mesh.devices.reshape(sizes[0], sizes[1] // 4, 4), ("sp", "y", "x")
-    )
-    tp = ("y", "x")
+        mesh.devices.reshape(sizes[0] // 2, 2, sizes[1] // 4, 4), ("z", "c", "y", "x")
+    )
+    sp, tp = ("z", "c"), ("y", "x")
     in_specs = (
-        P("sp", None),
-        P("sp", tp, None),
-        P("sp", tp, None),
-        P("sp", tp, None),
+        P(sp, None),
+        P(sp, tp, None),
+        P(sp, tp, None),
+        P(sp, tp, None),
         P(tp),
         P(),
         P(tp, None),
         P(),
-        P("sp", None, tp),
-        P("sp", None, tp),
-        P("sp", None, tp),
-        P("sp", None),
-        P("sp", None),
+        P(sp, None, tp),
+        P(sp, None, tp),
+        P(sp, None, tp),
+        P(sp, None),
+        P(sp, None),
     )
     return jax.shard_map(
-        shards, mesh=split, in_specs=in_specs, out_specs=P("sp", None), check_vma=False
-    )
+        shards, mesh=split, in_specs=in_specs, out_specs=P(sp, None), check_vma=False
+    )

time: 248 us -> 287 us (1.16)
  waiting for transfers between devices: 26.4 us -> 88.4 us
  blocking collectives: 148 us -> 135 us
  starting transfers between devices: 39.6 us -> 30.7 us
    ppermute x4 -> x3, waiting for transfers between devices: 0.01 us -> 32.5 us  [the longest x1 32.5 us: shards(): one = lax.ppermute(packed, ('c', 'x'), round_x)]
    all_to_all x1, waiting for transfers between devices: 9.68 us -> 32.5 us  [shards(): parts = lax.all_to_all(partial, tp, 0, 0, tiled=True)]
    all_to_all x1, blocking collectives: 43.6 us -> 29.9 us  [shards(): lax.all_to_all(made.reshape(targets, each, share), ('z', 'c', 'x'), 0, 0,...]
    all_to_all x1, starting transfers between devices: 19 us -> 12.1 us  [shards(): lax.all_to_all(outgoing.reshape(targets, each, share), ('z', 'c', 'x'), 0...]
    all_to_all x1, waiting for transfers between devices: 16.7 us -> 23.3 us  [shards(): lax.all_to_all(outgoing.reshape(targets, each, share), ('z', 'c', 'x'), 0...]
    slice x2 -> x0, local copies, waits for them, and re-layouts: 5.32 us -> none  [the longest x1 3.05 us: shards(): far = lax.ppermute(left[:4], 'x', ahead)]
    unnamed x39 -> x35, local copies, waits for them, and re-layouts: 6.6 us -> 11.3 us
    ppermute x4 -> x3, starting transfers between devices: 14.8 us -> 14.3 us  [the longest x1 5.2 us: shards(): one = lax.ppermute(packed, ('c', 'x'), round_x)]
  transfers between devices with their start and end apart: 6 -> 5, of which waited for: 2 -> 3; matrix products, arithmetic and copies ran while one was open for 4% -> 1% of each run, Pallas kernels for 2% -> 2%
where the time goes in v8:
time: 287 us; the launch traced here: 286 us
  blocking collectives  135 us (47%)
  waiting for transfers between devices  88.4 us (31%)
  starting transfers between devices  30.7 us (11%)
  Pallas kernels  15.3 us (5%)
  local copies, waits for them, and re-layouts  11.5 us (4%)
  other arithmetic  4.36 us (2%)
    all_gather x3, blocking collectives, gathered(): whole = lax.all_gather(sent, axes, axis=axis, tiled=True)  83.9 us
    all_to_all x1, waiting for transfers between devices, shards(): parts = lax.all_to_all(partial, tp, 0, 0, tiled=True)  32.5 us
    ppermute x1, waiting for transfers between devices, shards(): one = lax.ppermute(packed, ('c', 'x'), round_x)  32.5 us
    all_to_all x1, blocking collectives, shards(): lax.all_to_all(made.reshape(targets, each, share), ('z', 'c', 'x'), 0, 0,...  29.9 us
    all_to_all x1, waiting for transfers between devices, shards(): lax.all_to_all(outgoing.reshape(targets, each, share), ('z', 'c', 'x'), 0...  23.3 us
    all_to_all x1, blocking collectives, shards(): whole = lax.all_to_all(spread, tp, 0, 0, tiled=True)  21.1 us
    all_to_all x1, starting transfers between devices, shards(): lax.all_to_all(outgoing.reshape(targets, each, share), ('z', 'c', 'x'), 0...  12.1 us
    unnamed x35, local copies, waits for them, and re-layouts  11.3 us
  transfers between devices with their start and end apart: 5, of which 3 were waited for; matrix products, arithmetic and copies ran while one was open for 1% of the time, Pallas kernels for 2%

profile of v8, /device:TPU:1, one launch (start us, length us, event | category | flops | bytes accessed | tf_op | source)
XLA Modules:
  0.0 286.2 jit_solution(4680046405228724527)
XLA Ops:
  0.0 1.3 copy-done.6
  1.3 1.2 copy-done.7
  4.3 5.2 %collective-permute-start = (bf16[6,2048,128]{2,1,0:T(8,128)(2,1)S(1)}, bf16[6,2048,128]{2,1,0:T(8,128)(2,1)S(1)}, u32[]{:S(2)}, u32[]{:S(2)}) collective-permute-start(bf16[6,2048,128]{2,1,0:T(8,128)(2,1)S(1)} %pack.1.own_ref), channel_id=1, source_target_pairs={{0,1},{1,2},{2,3},{3,0},{16,19},{17,16},{18,17},{19,18},{4,5},{5,6... | collective-permute-start | bytes 9437192 | tf_op jit(solution)/shard_map/ppermute | solution.py:395
  9.5 1.7 copy-done.1
  11.2 32.5 %collective-permute-done.one_ref = bf16[6,2048,128]{2,1,0:T(8,128)(2,1)S(1)} collective-permute-done((bf16[6,2048,128]{2,1,0:T(8,128)(2,1)S(1)}, bf16[6,2048,128]{2,1,0:T(8,128)(2,1)S(1)}, u32[]{:S(2)}, u32[]{:S(2)}) %collective-permute-start) | collective-permute-done | bytes 3145760 | tf_op jit(solution)/shard_map/ppermute | solution.py:395
  43.7 5.0 %collective-permute-start.1 = (bf16[6,2048,128]{2,1,0:T(8,128)(2,1)S(1)}, bf16[6,2048,128]{2,1,0:T(8,128)(2,1)}, u32[]{:S(2)}, u32[]{:S(2)}) collective-permute-start(bf16[6,2048,128]{2,1,0:T(8,128)(2,1)S(1)} %collective-permute-done.one_ref), channel_id=1, source_target_pairs={{0,1},{1,2},{2,3},{3,0},{16,19},{17,16},{18,17},{19,18},{4,5},{5,6... | collective-permute-start | bytes 9437192 | tf_op jit(solution)/shard_map/ppermute | solution.py:396
  48.7 1.6 copy-done.4
  50.4 50.0 %all-gather.3 = f16[8192,256]{1,0:T(8,128)(2,1)S(1)} all-gather(f16[256,256]{1,0:T(8,128)(2,1)S(1)} %multiply_convert_fusion.5), channel_id=1, replica_groups=mesh['z'=16,'c'=2,'y'=4,'x'=4] {'z','c'}, dimensions={0}, use_global_device_ids=true | all-gather | bytes 4325376 | tf_op jit(solution)/shard_map/all_gather | solution.py:359
  100.4 4.0 %collective-permute-start.2 = (bf16[6,2048,128]{2,1,0:T(8,128)(2,1)}, bf16[6,2048,128]{2,1,0:T(8,128)(2,1)}, u32[]{:S(2)}, u32[]{:S(2)}) collective-permute-start(bf16[6,2048,128]{2,1,0:T(8,128)(2,1)} %collective-permute-done.1.two_ref), channel_id=1, source_target_pairs={{0,1},{1,2},{2,3},{3,0},{16,19},{17,16},{18,17},{19,18},{4,5},{5,6... | collective-permute-start | bytes 9437192 | tf_op jit(solution)/shard_map/ppermute | solution.py:397
  104.4 3.2 %multiply_convert_fusion.kv_ref = bf16[8192,256]{1,0:T(8,128)(2,1)} fusion(f16[8192,256]{1,0:T(8,128)(2,1)S(1)} %all-gather.3), kind=kLoop, calls=%fused_computation | loop fusion | flops 6291456 | bytes 8388608 | tf_op jit(solution)/shard_map/convert_element_type | solution.py:360
  108.3 2.2 copy-done.3
  110.5 3.5 %attention.1 = bf16[16,256,128]{2,1,0:T(8,128)(2,1)} custom-call(s32[1]{0:T(128)} %bitcast.2.where_ref, f32[1]{0:T(128)S(6)} %copy.30.lam_ref, bf16[256,128]{1,0:T(8,128)(2,1)S(1)} %bitcast.26, bf16[8192,256]{1,0:T(8,128)(2,1)S(1)} %copy-done.3, f32[1,128]{1,0:T(1,128)S(1)} %bitcast.28, bf16[128,2048]{1,0:T(8,128)(2,1)S(1)} %copy-done.9), custom_call_target="tpu_custom_call" | custom-call | tf_op jit(solution)/shard_map/attention/pallas_call | solution.py:81
  114.0 4.3 %all-to-all-start = ((bf16[16,256,128]{2,1,0:T(8,128)(2,1)}), bf16[16,256,128]{2,1,0:T(8,128)(2,1)S(1)}, u32[]{:S(2)}, u32[]{:S(2)}) async-start(bf16[16,256,128]{2,1,0:T(8,128)(2,1)} %attention.1), calls=%async_computation | async-start | bytes 2097152 | tf_op jit(solution)/shard_map/all_to_all | solution.py:419
  119.0 32.5 %all-to-all-done.parts_ref = bf16[16,256,128]{2,1,0:T(8,128)(2,1)S(1)} async-done(((bf16[16,256,128]{2,1,0:T(8,128)(2,1)}), bf16[16,256,128]{2,1,0:T(8,128)(2,1)S(1)}, u32[]{:S(2)}, u32[]{:S(2)}) %all-to-all-start) | async-done | bytes 1048608 | tf_op jit(solution)/shard_map/all_to_all | solution.py:419
  152.7 12.1 %all-to-all-start.1 = ((bf16[128,8,128]{2,1,0:T(8,128)(2,1)}), bf16[128,8,128]{2,1,0:T(8,128)(2,1)S(1)}, u32[]{:S(2)}, u32[]{:S(2)}) async-start(bf16[128,8,128]{2,1,0:T(8,128)(2,1)} %bitcast.8), calls=%async_computation.1 | async-start | bytes 524288 | tf_op jit(solution)/shard_map/all_to_all | solution.py:425
  164.9 23.3 %all-to-all-done.1 = bf16[128,8,128]{2,1,0:T(8,128)(2,1)S(1)} async-done(((bf16[128,8,128]{2,1,0:T(8,128)(2,1)}), bf16[128,8,128]{2,1,0:T(8,128)(2,1)S(1)}, u32[]{:S(2)}, u32[]{:S(2)}) %all-to-all-start.1) | async-done | bytes 262176 | tf_op jit(solution)/shard_map/all_to_all | solution.py:425
  188.4 13.2 %all-gather.4 = f16[16,256,128]{2,1,0:T(8,128)(2,1)S(1)} all-gather(f16[4,256,128]{2,1,0:T(8,128)(2,1)S(1)} %fusion), channel_id=1, replica_groups=mesh['z'=16,'c'=2,'y'=4,'x'=4] {'y'}, dimensions={0}, use_global_device_ids=true | all-gather | bytes 1310720 | tf_op jit(solution)/shard_map/all_gather | solution.py:359
  201.9 1.9 copy-done.5
  203.8 4.7 %hidden.1 = bf16[4,256,256]{2,1,0:T(8,128)(2,1)S(1)} custom-call(s32[2]{0:T(128)S(1)} %pad_add_fusion.turn_ref, bf16[16,256,128]{2,1,0:T(8,128)(2,1)S(1)} %multiply_convert_fusion.2.rows_ref, f32[1,2048]{1,0:T(1,128)S(1)} %bitcast.27, bf16[6,2048,128]{2,1,0:T(8,128)(2,1)S(1)} %copy-done.2, bf16[6,2048,128]{2,1,0:T(8,128)(2,1)S(1)} %copy-done.5, ...), custom_call_target="tpu_custom_call" | custom-call | tf_op jit(solution)/shard_map/hidden/pallas_call | solution.py:263
  208.7 20.6 %all-gather.5 = f16[16,256,256]{2,1,0:T(8,128)(2,1)S(1)} all-gather(f16[4,256,256]{2,1,0:T(8,128)(2,1)S(1)} %multiply_convert_fusion.3), channel_id=1, replica_groups=mesh['z'=16,'c'=2,'y'=4,'x'=4] {'y'}, dimensions={0}, use_global_device_ids=true | all-gather | bytes 2621440 | tf_op jit(solution)/shard_map/all_gather | solution.py:359
  229.9 3.2 %down.1 = bf16[32,4,8,128]{3,2,1,0:T(8,128)(2,1)S(1)} custom-call(s32[2]{0:T(128)S(1)} %pad_add_fusion.turn_ref, bf16[16,256,256]{2,1,0:T(8,128)(2,1)S(1)} %multiply_convert_fusion.1.units_ref, bf16[6,2048,128]{2,1,0:T(8,128)(2,1)S(1)} %copy-done.2, bf16[6,2048,128]{2,1,0:T(8,128)(2,1)S(1)} %copy-done.5, ...), custom_call_target="tpu_custom_call" | custom-call | tf_op jit(solution)/shard_map/down/pallas_call | solution.py:321
  233.0 29.9 %all_to_all.20 = bf16[128,8,128]{2,1,0:T(8,128)(2,1)S(1)} all-to-all(bf16[128,8,128]{2,1,0:T(8,128)(2,1)S(1)} %bitcast.20), channel_id=1, replica_groups=mesh['z'=16,'c'=2,'y'=4,'x'=4] {'z','c','x'}, dimensions={0} | all-to-all | bytes 524288 | tf_op jit(solution)/shard_map/all_to_all | solution.py:435
  263.4 21.1 %all_to_all.21.whole_ref = bf16[16,256,128]{2,1,0:T(8,128)(2,1)S(1)} all-to-all(bf16[16,256,128]{2,1,0:T(8,128)(2,1)S(1)} %combine.1), channel_id=1, replica_groups=mesh['z'=16,'c'=2,'y'=4,'x'=4] {'y','x'}, dimensions={0} | all-to-all | bytes 2097152 | tf_op jit(solution)/shard_map/all_to_all | solution.py:440
  284.5 1.7 assemble.1
  (48 shorter events, 5.1 us)
Async XLA Ops:
  0.0 118.9 %copy-start = (bf16[256,2048]{1,0:T(8,128)(2,1)S(1)}, bf16[256,2048]{1,0:T(8,128)(2,1)}, u32[]{:S(2)}) copy-start(bf16[256,2048]{1,0:T(8,128)(2,1)} %param.13) | copy-start | bytes 3145732
  0.0 1.3 copy-start.6
  1.3 1.2 copy-start.7
  2.5 1.2 copy-start.8
  3.8 46.5 %copy-start.13 = (bf16[256,1,128]{2,0,1:T(8,128)(2,1)S(1)}, bf16[256,1,128]{2,0,1:T(8,128)(2,1)}, u32[]{:S(2)}) copy-start(bf16[256,1,128]{2,0,1:T(8,128)(2,1)} %param.16) | copy-start | bytes 196612
  3.8 46.5 %copy-start.14 = (bf16[256,1,128]{2,0,1:T(8,128)(2,1)S(1)}, bf16[256,1,128]{2,0,1:T(8,128)(2,1)}, u32[]{:S(2)}) copy-start(bf16[256,1,128]{2,0,1:T(8,128)(2,1)} %param.15) | copy-start | bytes 196612
  4.3 39.4 %collective-permute-start = (bf16[6,2048,128]{2,1,0:T(8,128)(2,1)S(1)}, bf16[6,2048,128]{2,1,0:T(8,128)(2,1)S(1)}, u32[]{:S(2)}, u32[]{:S(2)}) collective-permute-start(bf16[6,2048,128]{2,1,0:T(8,128)(2,1)S(1)} %pack.1.own_ref), channel_id=1, source_target_pairs={{0,1},{1,2},{2,3},{3,0},{16,19},{17,16},{18,17},{19,18},{4,5},{5,6... | collective-permute-start | bytes 9437192 | tf_op jit(solution)/shard_map/ppermute | solution.py:395
  9.5 1.7 copy-start.1
  43.7 56.7 %collective-permute-start.1 = (bf16[6,2048,128]{2,1,0:T(8,128)(2,1)S(1)}, bf16[6,2048,128]{2,1,0:T(8,128)(2,1)}, u32[]{:S(2)}, u32[]{:S(2)}) collective-permute-start(bf16[6,2048,128]{2,1,0:T(8,128)(2,1)S(1)} %collective-permute-done.one_ref), channel_id=1, source_target_pairs={{0,1},{1,2},{2,3},{3,0},{16,19},{17,16},{18,17},{19,18},{4,5},{5,6... | collective-permute-start | bytes 9437192 | tf_op jit(solution)/shard_map/ppermute | solution.py:396
  48.7 1.6 copy-start.4
  100.4 7.9 %copy-start.9 = (bf16[128,2048]{1,0:T(8,128)(2,1)S(1)}, bf16[128,2048]{1,0:T(8,128)(2,1)}, u32[]{:S(2)}) copy-start(bf16[128,2048]{1,0:T(8,128)(2,1)} %weight_ref.1) | copy-start | bytes 1572868
  100.4 7.9 %copy-start.10 = (bf16[256,1,128]{2,0,1:T(8,128)(2,1)S(1)}, bf16[256,1,128]{2,0,1:T(8,128)(2,1)}, u32[]{:S(2)}) copy-start(bf16[256,1,128]{2,0,1:T(8,128)(2,1)} %param.14) | copy-start | bytes 196612
  100.4 7.9 %copy-start.12 = (f32[128]{0:T(128)S(1)}, f32[128]{0:T(128)}, u32[]{:S(2)}) copy-start(f32[128]{0:T(128)} %param.18) | copy-start | bytes 1540
  100.4 101.5 %collective-permute-start.2 = (bf16[6,2048,128]{2,1,0:T(8,128)(2,1)}, bf16[6,2048,128]{2,1,0:T(8,128)(2,1)}, u32[]{:S(2)}, u32[]{:S(2)}) collective-permute-start(bf16[6,2048,128]{2,1,0:T(8,128)(2,1)} %collective-permute-done.1.two_ref), channel_id=1, source_target_pairs={{0,1},{1,2},{2,3},{3,0},{16,19},{17,16},{18,17},{19,18},{4,5},{5,6... | collective-permute-start | bytes 9437192 | tf_op jit(solution)/shard_map/ppermute | solution.py:397
  108.3 2.2 copy-start.3
  110.5 7.9 %copy-start.15 = (s32[256,2]{0,1:T(2,128)S(1)}, s32[256,2]{0,1:T(2,128)}, u32[]{:S(2)}) copy-start(s32[256,2]{0,1:T(2,128)} %param.24) | copy-start | bytes 6148
  110.5 8.3 %copy-start.16 = (f32[256,2]{0,1:T(2,128)S(1)}, f32[256,2]{0,1:T(2,128)}, u32[]{:S(2)}) copy-start(f32[256,2]{0,1:T(2,128)} %param.25) | copy-start | bytes 6148
  114.0 37.5 %all-to-all-start = ((bf16[16,256,128]{2,1,0:T(8,128)(2,1)}), bf16[16,256,128]{2,1,0:T(8,128)(2,1)S(1)}, u32[]{:S(2)}, u32[]{:S(2)}) async-start(bf16[16,256,128]{2,1,0:T(8,128)(2,1)} %attention.1), calls=%async_computation | async-start | bytes 2097152 | tf_op jit(solution)/shard_map/all_to_all | solution.py:419
  119.0 82.9 %copy-start.11 = (f32[2048]{0:T(1024)S(1)}, f32[2048]{0:T(1024)}, u32[]{:S(2)}) copy-start(f32[2048]{0:T(1024)} %param.20) | copy-start | bytes 24580
  152.7 35.6 %all-to-all-start.1 = ((bf16[128,8,128]{2,1,0:T(8,128)(2,1)}), bf16[128,8,128]{2,1,0:T(8,128)(2,1)S(1)}, u32[]{:S(2)}, u32[]{:S(2)}) async-start(bf16[128,8,128]{2,1,0:T(8,128)(2,1)} %bitcast.8), calls=%async_computation.1 | async-start | bytes 524288 | tf_op jit(solution)/shard_map/all_to_all | solution.py:425
  188.2 13.7 %copy-start.2 = (bf16[6,2048,128]{2,1,0:T(8,128)(2,1)S(1)}, bf16[6,2048,128]{2,1,0:T(8,128)(2,1)}, u32[]{:S(2)}) copy-start(bf16[6,2048,128]{2,1,0:T(8,128)(2,1)} %copy-done.1) | copy-start | bytes 9437188
  201.9 1.9 copy-start.5

commit v9 on v8

--- a/solution.py
+++ b/solution.py
@@ -215,14 +215,24 @@
     )(back, stream, slots, factors)
 
 
-def hidden_body(turn_ref, rows_ref, gain_ref, own_ref, one_ref, two_ref, three_ref, out_ref, normed_ref, weights, sems):
+def hidden_body(turn_ref, rows_ref, gain_ref, own_ref, own_up_ref, one_ref, two_ref, three_ref, out_ref, normed_ref, weights, sems):
     peers, count, share = rows_ref.shape
     pieces = out_ref.shape[0]
     gate, up = pl.ds(0, 2), pl.ds(4, 2)
     first, second = pl.ds(0, 2), pl.ds(2, 2)
+    width = weights.shape[3]
+    low, high = pl.ds(0, width), pl.ds(width, width)
     groups = [
+        [
+            (own_ref.at[:, low], weights.at[0, 0]),
+            (own_ref.at[:, high], weights.at[0, 1]),
+            (own_up_ref.at[:, low], weights.at[0, 2]),
+            (own_up_ref.at[:, high], weights.at[0, 3]),
+        ]
+    ]
+    groups += [
         [(source.at[gate], weights.at[k, first]), (source.at[up], weights.at[k, second])]
-        for k, source in enumerate((own_ref, one_ref, two_ref, three_ref))
+        for k, source in ((1, one_ref), (2, two_ref), (3, three_ref))
     ]
     copies, at = [], 0
     for group in groups:
@@ -257,7 +267,7 @@
 
 def hidden_units(turn, rows, gain, *weights):
     peers, count, share = rows.shape
-    _, model, half = weights[0].shape
+    _, model, half = weights[-1].shape
     vmem = pl.BlockSpec(memory_space=pltpu.VMEM)
     anywhere = pl.BlockSpec(memory_space=pltpu.HBM)
     return pl.pallas_call(
@@ -268,7 +278,7 @@
         scratch_shapes=[
             pltpu.VMEM((count, peers * share), jnp.bfloat16),
             pltpu.VMEM((4, 4, model, half), jnp.bfloat16),
-            pltpu.SemaphoreType.DMA((8,)),
+            pltpu.SemaphoreType.DMA((10,)),
         ],
         compiler_params=pltpu.CompilerParams(vmem_limit_bytes=24 * 2**20),
         name="hidden",
@@ -279,7 +289,7 @@
     blocks, count, hidden = units_ref.shape
     chips, pieces, rows_each, _ = out_ref.shape
     parts = sems.shape[0]
-    half, share = own_ref.shape[1:]
+    half, share = one_ref.shape[1:]
     step = 2 * half // parts
     copies = []
     for c in range(parts):
@@ -287,8 +297,8 @@
         rows = pl.ds(at, step)
         inner = pl.ds(at % half, step)
         page = at // half
-        sources = [
-            source.at[2 + page, inner] for source in (own_ref, one_ref, two_ref, three_ref)
+        sources = [own_ref.at[rows]] + [
+            source.at[2 + page, inner] for source in (one_ref, two_ref, three_ref)
         ]
         for k, source in enumerate(sources):
             copy = pltpu.make_async_copy(source, downs.at[k, rows], sems.at[c, k])
@@ -315,7 +325,7 @@
 
 def down_product(turn, units, chips, *downs):
     _, count, _ = units.shape
-    _, half, share = downs[0].shape
+    _, half, share = downs[-1].shape
     vmem = pl.BlockSpec(memory_space=pltpu.VMEM)
     anywhere = pl.BlockSpec(memory_space=pltpu.HBM)
     return pl.pallas_call(
@@ -428,10 +438,10 @@
     landed = arrange(landed.reshape(experts, across, each, share))
     rows = gathered(landed.reshape(across, experts * each, share), "y", 0, 64.0)
     units = hidden_units(
-        turn, rows, ffn_gain[None], packed, one, two, three
+        turn, rows, ffn_gain[None], expert_gate[0], expert_up[0], one, two, three
     )
     all_units = gathered(units, "y", 0, 0.25)
-    made = down_product(turn, all_units, experts, packed, one, two, three)
+    made = down_product(turn, all_units, experts, expert_down[0], one, two, three)
     back = lax.all_to_all(
         made.reshape(targets, each, share), ("z", "c", "x"), 0, 0, tiled=True
     )

time: 287 us -> 289 us (level)
    unnamed x35 -> x51, local copies, waits for them, and re-layouts: 11.3 us -> 10.5 us
where the time goes in v9:
time: 289 us; the launch traced here: 288 us
  blocking collectives  135 us (47%)
  waiting for transfers between devices  90.2 us (31%)
  starting transfers between devices  30.8 us (11%)
  Pallas kernels  15.9 us (6%)
  local copies, waits for them, and re-layouts  10.7 us (4%)
  other arithmetic  4.36 us (2%)
    all_gather x3, blocking collectives, gathered(): whole = lax.all_gather(sent, axes, axis=axis, tiled=True)  84 us
    ppermute x1, waiting for transfers between devices, shards(): one = lax.ppermute(packed, ('c', 'x'), round_x)  34.2 us
    all_to_all x1, waiting for transfers between devices, shards(): parts = lax.all_to_all(partial, tp, 0, 0, tiled=True)  32.7 us
    all_to_all x1, blocking collectives, shards(): lax.all_to_all(made.reshape(targets, each, share), ('z', 'c', 'x'), 0, 0,...  29.9 us
    all_to_all x1, waiting for transfers between devices, shards(): lax.all_to_all(outgoing.reshape(targets, each, share), ('z', 'c', 'x'), 0...  23.3 us
    all_to_all x1, blocking collectives, shards(): whole = lax.all_to_all(spread, tp, 0, 0, tiled=True)  21.1 us
    all_to_all x1, starting transfers between devices, shards(): lax.all_to_all(outgoing.reshape(targets, each, share), ('z', 'c', 'x'), 0...  12.1 us
    unnamed x51, local copies, waits for them, and re-layouts  10.5 us
  transfers between devices with their start and end apart: 5, of which 3 were waited for; matrix products, arithmetic and copies ran while one was open for 1% of the time, Pallas kernels for 2%

profile of v9, /device:TPU:1, one launch (start us, length us, event | category | flops | bytes accessed | tf_op | source)
XLA Modules:
  0.0 288.1 jit_solution(2795174040011339720)
XLA Ops:
  0.0 1.3 copy-done.4
  1.3 1.2 copy-done.6
  2.5 1.2 copy-done.8
  4.3 5.2 %collective-permute-start = (bf16[6,2048,128]{2,1,0:T(8,128)(2,1)S(1)}, bf16[6,2048,128]{2,1,0:T(8,128)(2,1)S(1)}, u32[]{:S(2)}, u32[]{:S(2)}) collective-permute-start(bf16[6,2048,128]{2,1,0:T(8,128)(2,1)S(1)} %pack.1), channel_id=1, source_target_pairs={{0,1},{1,2},{2,3},{3,0},{16,19},{17,16},{18,17},{19,18},{4,5},{5,6... | collective-permute-start | bytes 9437192 | tf_op jit(solution)/shard_map/ppermute | solution.py:405
  9.5 34.2 %collective-permute-done.one_ref = bf16[6,2048,128]{2,1,0:T(8,128)(2,1)S(1)} collective-permute-done((bf16[6,2048,128]{2,1,0:T(8,128)(2,1)S(1)}, bf16[6,2048,128]{2,1,0:T(8,128)(2,1)S(1)}, u32[]{:S(2)}, u32[]{:S(2)}) %collective-permute-start) | collective-permute-done | bytes 3145760 | tf_op jit(solution)/shard_map/ppermute | solution.py:405
  43.7 5.0 %collective-permute-start.1 = (bf16[6,2048,128]{2,1,0:T(8,128)(2,1)S(1)}, bf16[6,2048,128]{2,1,0:T(8,128)(2,1)}, u32[]{:S(2)}, u32[]{:S(2)}) collective-permute-start(bf16[6,2048,128]{2,1,0:T(8,128)(2,1)S(1)} %collective-permute-done.one_ref), channel_id=1, source_target_pairs={{0,1},{1,2},{2,3},{3,0},{16,19},{17,16},{18,17},{19,18},{4,5},{5,6... | collective-permute-start | bytes 9437192 | tf_op jit(solution)/shard_map/ppermute | solution.py:406
  48.7 1.8 copy-done.2
  50.5 50.0 %all-gather.3 = f16[8192,256]{1,0:T(8,128)(2,1)S(1)} all-gather(f16[256,256]{1,0:T(8,128)(2,1)S(1)} %multiply_convert_fusion.5), channel_id=1, replica_groups=mesh['z'=16,'c'=2,'y'=4,'x'=4] {'z','c'}, dimensions={0}, use_global_device_ids=true | all-gather | bytes 4325376 | tf_op jit(solution)/shard_map/all_gather | solution.py:369
  100.6 4.0 %collective-permute-start.2 = (bf16[6,2048,128]{2,1,0:T(8,128)(2,1)}, bf16[6,2048,128]{2,1,0:T(8,128)(2,1)}, u32[]{:S(2)}, u32[]{:S(2)}) collective-permute-start(bf16[6,2048,128]{2,1,0:T(8,128)(2,1)} %collective-permute-done.1.two_ref), channel_id=1, source_target_pairs={{0,1},{1,2},{2,3},{3,0},{16,19},{17,16},{18,17},{19,18},{4,5},{5,6... | collective-permute-start | bytes 9437192 | tf_op jit(solution)/shard_map/ppermute | solution.py:407
  104.6 3.1 %multiply_convert_fusion.kv_ref = bf16[8192,256]{1,0:T(8,128)(2,1)} fusion(f16[8192,256]{1,0:T(8,128)(2,1)S(1)} %all-gather.3), kind=kLoop, calls=%fused_computation | loop fusion | flops 6291456 | bytes 8388608 | tf_op jit(solution)/shard_map/convert_element_type | solution.py:370
  108.4 2.2 copy-done.1
  110.6 3.4 %attention.1 = bf16[16,256,128]{2,1,0:T(8,128)(2,1)} custom-call(s32[1]{0:T(128)} %bitcast.2.where_ref, f32[1]{0:T(128)S(6)} %copy.30.lam_ref, bf16[256,128]{1,0:T(8,128)(2,1)S(1)} %bitcast.30, bf16[8192,256]{1,0:T(8,128)(2,1)S(1)} %copy-done.1, f32[1,128]{1,0:T(1,128)S(1)} %bitcast.32, bf16[128,2048]{1,0:T(8,128)(2,1)S(1)} %copy-done.10), custom_call_target="tpu_custom_call" | custom-call | tf_op jit(solution)/shard_map/attention/pallas_call | solution.py:81
  114.0 4.4 %all-to-all-start = ((bf16[16,256,128]{2,1,0:T(8,128)(2,1)}), bf16[16,256,128]{2,1,0:T(8,128)(2,1)}, u32[]{:S(2)}, u32[]{:S(2)}) async-start(bf16[16,256,128]{2,1,0:T(8,128)(2,1)} %attention.1), calls=%async_computation | async-start | bytes 2097152 | tf_op jit(solution)/shard_map/all_to_all | solution.py:429
  119.1 32.7 %all-to-all-done.parts_ref = bf16[16,256,128]{2,1,0:T(8,128)(2,1)} async-done(((bf16[16,256,128]{2,1,0:T(8,128)(2,1)}), bf16[16,256,128]{2,1,0:T(8,128)(2,1)}, u32[]{:S(2)}, u32[]{:S(2)}) %all-to-all-start) | async-done | bytes 1048608 | tf_op jit(solution)/shard_map/all_to_all | solution.py:429
  151.8 1.7 project.1
  156.1 12.1 %all-to-all-start.1 = ((bf16[128,8,128]{2,1,0:T(8,128)(2,1)}), bf16[128,8,128]{2,1,0:T(8,128)(2,1)S(1)}, u32[]{:S(2)}, u32[]{:S(2)}) async-start(bf16[128,8,128]{2,1,0:T(8,128)(2,1)} %bitcast.29), calls=%async_computation.1 | async-start | bytes 524288 | tf_op jit(solution)/shard_map/all_to_all | solution.py:435
  168.3 23.3 %all-to-all-done.1 = bf16[128,8,128]{2,1,0:T(8,128)(2,1)S(1)} async-done(((bf16[128,8,128]{2,1,0:T(8,128)(2,1)}), bf16[128,8,128]{2,1,0:T(8,128)(2,1)S(1)}, u32[]{:S(2)}, u32[]{:S(2)}) %all-to-all-start.1) | async-done | bytes 262176 | tf_op jit(solution)/shard_map/all_to_all | solution.py:435
  191.8 13.2 %all-gather.4 = f16[16,256,128]{2,1,0:T(8,128)(2,1)S(1)} all-gather(f16[4,256,128]{2,1,0:T(8,128)(2,1)S(1)} %fusion), channel_id=1, replica_groups=mesh['z'=16,'c'=2,'y'=4,'x'=4] {'y'}, dimensions={0}, use_global_device_ids=true | all-gather | bytes 1310720 | tf_op jit(solution)/shard_map/all_gather | solution.py:369
  205.3 5.0 %hidden.1 = bf16[4,256,256]{2,1,0:T(8,128)(2,1)S(1)} custom-call(s32[2]{0:T(128)S(1)} %pad_add_fusion.turn_ref, bf16[16,256,128]{2,1,0:T(8,128)(2,1)S(1)} %multiply_convert_fusion.2.rows_ref, f32[1,2048]{1,0:T(1,128)S(1)} %bitcast.31, bf16[2048,256]{1,0:T(8,128)(2,1)S(1)} %bitcast.21, bf16[2048,256]{1,0:T(8,128)(2,1)S(1)} %bitcast.23, ...), custom_call_target="tpu_custom_call" | custom-call | tf_op jit(solution)/shard_map/hidden/pallas_call | solution.py:273
  210.5 20.8 %all-gather.5 = f16[16,256,256]{2,1,0:T(8,128)(2,1)S(1)} all-gather(f16[4,256,256]{2,1,0:T(8,128)(2,1)S(1)} %multiply_convert_fusion.3), channel_id=1, replica_groups=mesh['z'=16,'c'=2,'y'=4,'x'=4] {'y'}, dimensions={0}, use_global_device_ids=true | all-gather | bytes 2621440 | tf_op jit(solution)/shard_map/all_gather | solution.py:369
  231.8 3.2 %down.1 = bf16[32,4,8,128]{3,2,1,0:T(8,128)(2,1)S(1)} custom-call(s32[2]{0:T(128)S(1)} %pad_add_fusion.turn_ref, bf16[16,256,256]{2,1,0:T(8,128)(2,1)S(1)} %multiply_convert_fusion.1.units_ref, bf16[4096,128]{1,0:T(8,128)(2,1)S(1)} %bitcast.25, bf16[6,2048,128]{2,1,0:T(8,128)(2,1)S(1)} %copy-done.3, bf16[6,2048,128]{2,1,0:T(8,128)(2,1)} %collective-permute-done.1.two_ref, ...), custom_call_target="tpu_custom_call" | custom-call | tf_op jit(solution)/shard_map/down/pallas_call | solution.py:331
  235.0 29.9 %all_to_all.20 = bf16[128,8,128]{2,1,0:T(8,128)(2,1)S(1)} all-to-all(bf16[128,8,128]{2,1,0:T(8,128)(2,1)S(1)} %bitcast.26), channel_id=1, replica_groups=mesh['z'=16,'c'=2,'y'=4,'x'=4] {'z','c','x'}, dimensions={0} | all-to-all | bytes 524288 | tf_op jit(solution)/shard_map/all_to_all | solution.py:445
  265.4 21.1 %all_to_all.21.whole_ref = bf16[16,256,128]{2,1,0:T(8,128)(2,1)S(1)} all-to-all(bf16[16,256,128]{2,1,0:T(8,128)(2,1)S(1)} %combine.1), channel_id=1, replica_groups=mesh['z'=16,'c'=2,'y'=4,'x'=4] {'y','x'}, dimensions={0} | all-to-all | bytes 2097152 | tf_op jit(solution)/shard_map/all_to_all | solution.py:450
  286.5 1.7 assemble.1
  (64 shorter events, 5.4 us)
Async XLA Ops:
  0.0 119.0 %copy-start = (bf16[256,2048]{1,0:T(8,128)(2,1)S(1)}, bf16[256,2048]{1,0:T(8,128)(2,1)}, u32[]{:S(2)}) copy-start(bf16[256,2048]{1,0:T(8,128)(2,1)} %param.13) | copy-start | bytes 3145732
  0.0 1.3 copy-start.4
  3.8 46.7 %copy-start.21 = (bf16[256,1,128]{2,0,1:T(8,128)(2,1)S(1)}, bf16[256,1,128]{2,0,1:T(8,128)(2,1)}, u32[]{:S(2)}) copy-start(bf16[256,1,128]{2,0,1:T(8,128)(2,1)} %param.16) | copy-start | bytes 196612
  3.8 46.7 %copy-start.22 = (bf16[256,1,128]{2,0,1:T(8,128)(2,1)S(1)}, bf16[256,1,128]{2,0,1:T(8,128)(2,1)}, u32[]{:S(2)}) copy-start(bf16[256,1,128]{2,0,1:T(8,128)(2,1)} %param.15) | copy-start | bytes 196612
  4.3 39.4 %collective-permute-start = (bf16[6,2048,128]{2,1,0:T(8,128)(2,1)S(1)}, bf16[6,2048,128]{2,1,0:T(8,128)(2,1)S(1)}, u32[]{:S(2)}, u32[]{:S(2)}) collective-permute-start(bf16[6,2048,128]{2,1,0:T(8,128)(2,1)S(1)} %pack.1), channel_id=1, source_target_pairs={{0,1},{1,2},{2,3},{3,0},{16,19},{17,16},{18,17},{19,18},{4,5},{5,6... | collective-permute-start | bytes 9437192 | tf_op jit(solution)/shard_map/ppermute | solution.py:405
  43.7 56.9 %collective-permute-start.1 = (bf16[6,2048,128]{2,1,0:T(8,128)(2,1)S(1)}, bf16[6,2048,128]{2,1,0:T(8,128)(2,1)}, u32[]{:S(2)}, u32[]{:S(2)}) collective-permute-start(bf16[6,2048,128]{2,1,0:T(8,128)(2,1)S(1)} %collective-permute-done.one_ref), channel_id=1, source_target_pairs={{0,1},{1,2},{2,3},{3,0},{16,19},{17,16},{18,17},{19,18},{4,5},{5,6... | collective-permute-start | bytes 9437192 | tf_op jit(solution)/shard_map/ppermute | solution.py:406
  48.7 1.8 copy-start.2
  100.5 7.9 %copy-start.10 = (bf16[128,2048]{1,0:T(8,128)(2,1)S(1)}, bf16[128,2048]{1,0:T(8,128)(2,1)}, u32[]{:S(2)}) copy-start(bf16[128,2048]{1,0:T(8,128)(2,1)} %weight_ref.1) | copy-start | bytes 1572868
  100.5 7.9 %copy-start.18 = (bf16[256,1,128]{2,0,1:T(8,128)(2,1)S(1)}, bf16[256,1,128]{2,0,1:T(8,128)(2,1)}, u32[]{:S(2)}) copy-start(bf16[256,1,128]{2,0,1:T(8,128)(2,1)} %param.14) | copy-start | bytes 196612
  100.5 7.9 %copy-start.20 = (f32[128]{0:T(128)S(1)}, f32[128]{0:T(128)}, u32[]{:S(2)}) copy-start(f32[128]{0:T(128)} %param.18) | copy-start | bytes 1540
  100.6 104.7 %collective-permute-start.2 = (bf16[6,2048,128]{2,1,0:T(8,128)(2,1)}, bf16[6,2048,128]{2,1,0:T(8,128)(2,1)}, u32[]{:S(2)}, u32[]{:S(2)}) collective-permute-start(bf16[6,2048,128]{2,1,0:T(8,128)(2,1)} %collective-permute-done.1.two_ref), channel_id=1, source_target_pairs={{0,1},{1,2},{2,3},{3,0},{16,19},{17,16},{18,17},{19,18},{4,5},{5,6... | collective-permute-start | bytes 9437192 | tf_op jit(solution)/shard_map/ppermute | solution.py:407
  108.4 2.2 copy-start.1
  110.6 7.8 %copy-start.23 = (s32[256,2]{0,1:T(2,128)S(1)}, s32[256,2]{0,1:T(2,128)}, u32[]{:S(2)}) copy-start(s32[256,2]{0,1:T(2,128)} %param.24) | copy-start | bytes 6148
  110.6 8.2 %copy-start.24 = (f32[256,2]{0,1:T(2,128)S(1)}, f32[256,2]{0,1:T(2,128)}, u32[]{:S(2)}) copy-start(f32[256,2]{0,1:T(2,128)} %param.25) | copy-start | bytes 6148
  114.0 37.8 %all-to-all-start = ((bf16[16,256,128]{2,1,0:T(8,128)(2,1)}), bf16[16,256,128]{2,1,0:T(8,128)(2,1)}, u32[]{:S(2)}, u32[]{:S(2)}) async-start(bf16[16,256,128]{2,1,0:T(8,128)(2,1)} %attention.1), calls=%async_computation | async-start | bytes 2097152 | tf_op jit(solution)/shard_map/all_to_all | solution.py:429
  119.1 86.2 %copy-start.5 = (bf16[1,2048,256]{2,1,0:T(8,128)(2,1)S(1)}, bf16[1,2048,256]{2,1,0:T(8,128)(2,1)}, u32[]{:S(2)}) copy-start(bf16[1,2048,256]{2,1,0:T(8,128)(2,1)} %param.21) | copy-start | bytes 3145732
  119.1 86.2 %copy-start.7 = (bf16[1,2048,256]{2,1,0:T(8,128)(2,1)S(1)}, bf16[1,2048,256]{2,1,0:T(8,128)(2,1)}, u32[]{:S(2)}) copy-start(bf16[1,2048,256]{2,1,0:T(8,128)(2,1)} %param.22) | copy-start | bytes 3145732
  119.1 86.2 %copy-start.19 = (f32[2048]{0:T(1024)S(1)}, f32[2048]{0:T(1024)}, u32[]{:S(2)}) copy-start(f32[2048]{0:T(1024)} %param.20) | copy-start | bytes 24580
  156.1 35.6 %all-to-all-start.1 = ((bf16[128,8,128]{2,1,0:T(8,128)(2,1)}), bf16[128,8,128]{2,1,0:T(8,128)(2,1)S(1)}, u32[]{:S(2)}, u32[]{:S(2)}) async-start(bf16[128,8,128]{2,1,0:T(8,128)(2,1)} %bitcast.29), calls=%async_computation.1 | async-start | bytes 524288 | tf_op jit(solution)/shard_map/all_to_all | solution.py:435
  191.7 13.7 %copy-start.3 = (bf16[6,2048,128]{2,1,0:T(8,128)(2,1)S(1)}, bf16[6,2048,128]{2,1,0:T(8,128)(2,1)}, u32[]{:S(2)}) copy-start(bf16[6,2048,128]{2,1,0:T(8,128)(2,1)} %copy-done.2) | copy-start | bytes 9437188
  210.5 21.3 %copy-start.9 = (bf16[1,4096,128]{2,1,0:T(8,128)(2,1)S(1)}, bf16[1,4096,128]{2,1,0:T(8,128)(2,1)}, u32[]{:S(2)}) copy-start(bf16[1,4096,128]{2,1,0:T(8,128)(2,1)} %param.23) | copy-start | bytes 3145732
  231.8 33.1 %copy-start.13 = (f32[256,128]{1,0:T(8,128)S(1)}, f32[256,128]{1,0:T(8,128)}, u32[]{:S(2)}) copy-start(f32[256,128]{1,0:T(8,128)} %copy-done.12) | copy-start | bytes 393220
  231.8 33.1 %copy-start.15 = (s32[256,2]{1,0:T(8,128)S(1)}, s32[256,2]{1,0:T(8,128)}, u32[]{:S(2)}) copy-start(s32[256,2]{1,0:T(8,128)} %copy-done.14) | copy-start | bytes 6148
  231.8 33.1 %copy-start.17 = (f32[256,2]{1,0:T(8,128)S(1)}, f32[256,2]{1,0:T(8,128)}, u32[]{:S(2)}) copy-start(f32[256,2]{1,0:T(8,128)} %copy-done.16) | copy-start | bytes 6148
  (6 other events, 5.1 us)

commit v10 on v7

--- a/solution.py
+++ b/solution.py
@@ -90,7 +90,7 @@
             pltpu.VMEM((peers, tok, share), jnp.bfloat16),
             pltpu.SemaphoreType.DMA((peers // 2,)),
         ],
-        compiler_params=pltpu.CompilerParams(vmem_limit_bytes=24 * 2**20),
+        compiler_params=pltpu.CompilerParams(vmem_limit_bytes=14 * 2**20),
         name="attention",
     )(where, lam, q, kv, gain, weight)
 
@@ -124,9 +124,27 @@
         out_specs=pl.BlockSpec(memory_space=pltpu.HBM),
         out_shape=jax.ShapeDtypeStruct((6, model, hidden // 2), gate.dtype),
         scratch_shapes=[pltpu.SemaphoreType.DMA((6,))],
-        compiler_params=pltpu.CompilerParams(vmem_limit_bytes=16 * 2**20),
+        compiler_params=pltpu.CompilerParams(vmem_limit_bytes=4 * 2**20),
         name="pack",
     )(gate, up, down)
+
+
+def arrange_body(landed_ref, out_ref):
+    for k in range(out_ref.shape[0]):
+        out_ref[k] = landed_ref[:, k]
+
+
+def arrange(landed):
+    experts, across, each, share = landed.shape
+    vmem = pl.BlockSpec(memory_space=pltpu.VMEM)
+    return pl.pallas_call(
+        arrange_body,
+        in_specs=[vmem],
+        out_specs=vmem,
+        out_shape=jax.ShapeDtypeStruct((across, experts, each, share), landed.dtype),
+        compiler_params=pltpu.CompilerParams(vmem_limit_bytes=2 * 2**20),
+        name="arrange",
+    )(landed)
 
 
 def project_body(parts_ref, residual_ref, place_ref, slots_ref, factors_ref, stream_ref, out_ref, slots_out, factors_out):
@@ -164,7 +182,7 @@
             jax.ShapeDtypeStruct(slots.shape, slots.dtype),
             jax.ShapeDtypeStruct(factors.shape, factors.dtype),
         ],
-        compiler_params=pltpu.CompilerParams(vmem_limit_bytes=16 * 2**20),
+        compiler_params=pltpu.CompilerParams(vmem_limit_bytes=6 * 2**20),
         name="project",
     )(parts, residual, place, slots, factors)
 
@@ -191,7 +209,7 @@
         in_specs=[vmem] * 4,
         out_specs=vmem,
         out_shape=jax.ShapeDtypeStruct((peers, tok, share), jnp.bfloat16),
-        compiler_params=pltpu.CompilerParams(vmem_limit_bytes=16 * 2**20),
+        compiler_params=pltpu.CompilerParams(vmem_limit_bytes=8 * 2**20),
         name="combine",
     )(back, stream, slots, factors)
 
@@ -206,7 +224,7 @@
         for k, source in ((0, own_ref), (1, right_ref), (3, left_ref))
     ]
     groups.append(
-        [(far_ref.at[gate], weights.at[2, first]), (far_up_ref, weights.at[2, second])]
+        [(far_ref, weights.at[2, first]), (far_up_ref, weights.at[2, second])]
     )
     copies, at = [], 0
     for group in groups:
@@ -254,7 +272,7 @@
             pltpu.VMEM((4, 4, model, half), jnp.bfloat16),
             pltpu.SemaphoreType.DMA((8,)),
         ],
-        compiler_params=pltpu.CompilerParams(vmem_limit_bytes=24 * 2**20),
+        compiler_params=pltpu.CompilerParams(vmem_limit_bytes=18 * 2**20),
         name="hidden",
     )(x, rows, gain, *weights)
 
@@ -274,7 +292,7 @@
         sources = (
             own_ref.at[2 + page, inner],
             right_ref.at[2 + page, inner],
-            far_ref.at[2 + page, inner],
+            far_ref.at[page, inner],
             left_ref.at[2 + page, inner],
         )
         for k, source in enumerate(sources):
@@ -314,7 +332,7 @@
             pltpu.VMEM((4, 2 * half, share), jnp.bfloat16),
             pltpu.SemaphoreType.DMA((4, 4)),
         ],
-        compiler_params=pltpu.CompilerParams(vmem_limit_bytes=24 * 2**20),
+        compiler_params=pltpu.CompilerParams(vmem_limit_bytes=10 * 2**20),
         name="down",
     )(x, units, *downs)
 
@@ -335,7 +353,7 @@
         out_specs=pl.BlockSpec((tile, peers * share), lambda i: (i, 0)),
         out_shape=jax.ShapeDtypeStruct((tok, peers * share), whole.dtype),
         compiler_params=pltpu.CompilerParams(
-            dimension_semantics=("arbitrary",), vmem_limit_bytes=16 * 2**20
+            dimension_semantics=("arbitrary",), vmem_limit_bytes=6 * 2**20
         ),
         name="assemble",
     )(whole)
@@ -380,8 +398,9 @@
     packed = pack(gate, up, down)
     left = lax.ppermute(packed, "x", ahead)
     right = lax.ppermute(packed, "x", behind)
-    far = lax.ppermute(left[:4], "x", ahead)
-    far_up = lax.ppermute(right[4:], "x", behind)
+    gate_2 = lax.ppermute(left[:2], "x", ahead)
+    up_2 = lax.ppermute(right[4:], "x", behind)
+    down_2 = lax.ppermute(left[2:4], "x", ahead)
 
     kv = jnp.concatenate([key_vectors[:, 0], value_rows[:, 0]], axis=1)
     kv_all = gathered(kv, "sp", 0, SHIFT)
@@ -410,13 +429,13 @@
     targets = experts * across
     each = capacity // across
     landed = lax.all_to_all(outgoing.reshape(targets, each, share), ("sp", "x"), 0, 0, tiled=True)
-    landed = landed.reshape(experts, across, each, share).swapaxes(0, 1)
+    landed = arrange(landed.reshape(experts, across, each, share))
     rows = gathered(landed.reshape(across, experts * each, share), "y", 0, 64.0)
     units = hidden_units(
-        x_at, rows, ffn_gain[None], packed, left, right, far, far_up
+        x_at, rows, ffn_gain[None], packed, left, right, gate_2, up_2
     )
     all_units = gathered(units, "y", 0, 0.25)
-    made = down_product(x_at, all_units, experts, packed, right, far, left)
+    made = down_product(x_at, all_units, experts, packed, right, down_2, left)
     back = lax.all_to_all(
         made.reshape(targets, each, share), ("sp", "x"), 0, 0, tiled=True
     )

time: 248 us -> 243 us (0.980)
  blocking collectives: 148 us -> 140 us
  starting transfers between devices: 39.6 us -> 43.3 us
  waiting for transfers between devices: 26.4 us -> 29.3 us
    all_to_all x1, blocking collectives: 43.6 us -> 35.6 us  [shards(): lax.all_to_all(made.reshape(targets, each, share), ('sp', 'x'), 0, 0, til...]
    all_to_all x1, waiting for transfers between devices: 9.68 us -> 17.7 us  [shards(): parts = lax.all_to_all(partial, tp, 0, 0, tiled=True)]
    all_to_all x1, waiting for transfers between devices: 16.7 us -> 11.6 us  [shards(): lax.all_to_all(outgoing.reshape(targets, each, share), ('sp', 'x'), 0, 0,...]
    unnamed x39 -> x35, local copies, waits for them, and re-layouts: 6.6 us -> 4.63 us
    ppermute x2 -> x3, starting transfers between devices: 7.67 us -> 9.08 us  [the longest x1 3.38 us: shards(): gate_2 = lax.ppermute(left[:2], 'x', ahead)]
  transfers between devices with their start and end apart: 6 -> 7, of which waited for: 2 -> 2; matrix products, arithmetic and copies ran while one was open for 4% -> 3% of each run, Pallas kernels for 2% -> 4%
where the time goes in v10:
time: 243 us; the launch traced here: 242 us
  blocking collectives  140 us (58%)
  starting transfers between devices  43.3 us (18%)
  waiting for transfers between devices  29.3 us (12%)
  Pallas kernels  16 us (7%)
  local copies, waits for them, and re-layouts  10.1 us (4%)
    all_gather x3, blocking collectives, gathered(): whole = lax.all_gather(sent, axes, axis=axis, tiled=True)  83.7 us
    all_to_all x1, blocking collectives, shards(): lax.all_to_all(made.reshape(targets, each, share), ('sp', 'x'), 0, 0, til...  35.6 us
    all_to_all x1, blocking collectives, shards(): whole = lax.all_to_all(spread, tp, 0, 0, tiled=True)  20.9 us
    all_to_all x1, starting transfers between devices, shards(): lax.all_to_all(outgoing.reshape(targets, each, share), ('sp', 'x'), 0, 0,...  20.7 us
    all_to_all x1, waiting for transfers between devices, shards(): parts = lax.all_to_all(partial, tp, 0, 0, tiled=True)  17.7 us
    all_to_all x1, waiting for transfers between devices, shards(): lax.all_to_all(outgoing.reshape(targets, each, share), ('sp', 'x'), 0, 0,...  11.6 us
    all_to_all x1, starting transfers between devices, shards(): parts = lax.all_to_all(partial, tp, 0, 0, tiled=True)  6.38 us
  transfers between devices with their start and end apart: 7, of which 2 were waited for; matrix products, arithmetic and copies ran while one was open for 3% of the time, Pallas kernels for 4%

profile of v10, /device:TPU:1, one launch (start us, length us, event | category | flops | bytes accessed | tf_op | source)
XLA Modules:
  0.0 242.1 jit_solution(6752397088911570660)
XLA Ops:
  0.0 1.3 copy-done.1
  1.3 1.2 copy-done.2
  2.5 1.2 copy-done.3
  3.8 1.7 pack.1.own_ref
  5.5 3.9 %collective-permute-start = (bf16[6,2048,128]{2,1,0:T(8,128)(2,1)}, bf16[6,2048,128]{2,1,0:T(8,128)(2,1)}, u32[]{:S(2)}, u32[]{:S(2)}) collective-permute-start(bf16[6,2048,128]{2,1,0:T(8,128)(2,1)} %pack.1.own_ref), channel_id=1, source_target_pairs={{0,1},{1,2},{2,3},{3,0},{4,5},{5,6},{6,7},{7,4},{8,9},{9,10},{10,1... | collective-permute-start | bytes 9437192 | tf_op jit(solution)/shard_map/ppermute | solution.py:399
  9.4 3.2 %collective-permute-start.1 = (bf16[6,2048,128]{2,1,0:T(8,128)(2,1)}, bf16[6,2048,128]{2,1,0:T(8,128)(2,1)}, u32[]{:S(2)}, u32[]{:S(2)}) collective-permute-start(bf16[6,2048,128]{2,1,0:T(8,128)(2,1)} %pack.1.own_ref), channel_id=1, source_target_pairs={{0,3},{1,0},{2,1},{3,2},{4,7},{5,4},{6,5},{7,6},{8,11},{9,8},{10,9... | collective-permute-start | bytes 9437192 | tf_op jit(solution)/shard_map/ppermute | solution.py:400
  12.7 50.3 %all-gather.3 = f16[8192,256]{1,0:T(8,128)(2,1)S(1)} all-gather(f16[256,256]{1,0:T(8,128)(2,1)S(1)} %multiply_convert_fusion.5), channel_id=1, replica_groups=mesh['sp'=32,'y'=4,'x'=4] {'sp'}, dimensions={0}, use_global_device_ids=true | all-gather | bytes 4325376 | tf_op jit(solution)/shard_map/all_gather | solution.py:364
  64.7 3.6 %attention.1 = bf16[16,256,128]{2,1,0:T(8,128)(2,1)} custom-call(s32[1]{0:T(128)} %bitcast.1.where_ref, f32[1]{0:T(128)S(6)} %copy.30.lam_ref, bf16[256,128]{1,0:T(8,128)(2,1)S(1)} %bitcast.25, bf16[8192,256]{1,0:T(8,128)(2,1)S(1)} %multiply_convert_fusion.kv_ref, f32[1,128]{1,0:T(1,128)S(1)} %bitcast.27, bf16[128,2048]{1,0:T(8,128)(2,1)S(1)} %copy-done.4), custom_call_target="tpu_custom_call" | custom-call | tf_op jit(solution)/shard_map/attention/pallas_call | solution.py:81
  68.3 6.4 %all-to-all-start = ((bf16[16,256,128]{2,1,0:T(8,128)(2,1)}), bf16[16,256,128]{2,1,0:T(8,128)(2,1)S(1)}, u32[]{:S(2)}, u32[]{:S(2)}) async-start(bf16[16,256,128]{2,1,0:T(8,128)(2,1)} %attention.1), calls=%async_computation | async-start | bytes 2097152 | tf_op jit(solution)/shard_map/all_to_all | solution.py:425
  75.4 17.7 %all-to-all-done.parts_ref = bf16[16,256,128]{2,1,0:T(8,128)(2,1)S(1)} async-done(((bf16[16,256,128]{2,1,0:T(8,128)(2,1)}), bf16[16,256,128]{2,1,0:T(8,128)(2,1)S(1)}, u32[]{:S(2)}, u32[]{:S(2)}) %all-to-all-start) | async-done | bytes 1048608 | tf_op jit(solution)/shard_map/all_to_all | solution.py:425
  94.8 20.7 %all-to-all-start.1 = ((bf16[128,8,128]{2,1,0:T(8,128)(2,1)}), bf16[128,8,128]{2,1,0:T(8,128)(2,1)S(1)}, u32[]{:S(2)}, u32[]{:S(2)}) async-start(bf16[128,8,128]{2,1,0:T(8,128)(2,1)} %bitcast.7), calls=%async_computation.1 | async-start | bytes 524288 | tf_op jit(solution)/shard_map/all_to_all | solution.py:431
  115.6 3.0 %fusion.2 = (bf16[2,2048,128]{2,1,0:T(8,128)(2,1)}, bf16[2,2048,128]{2,1,0:T(8,128)(2,1)}) fusion(bf16[6,2048,128]{2,1,0:T(8,128)(2,1)} %collective-permute-done.left_ref), kind=kLoop, calls=%fused_computation.15 | loop fusion | bytes 4194304 | tf_op jit(solution)/shard_map/slice | solution.py:403
  118.6 3.4 %collective-permute-start.2 = (bf16[2,2048,128]{2,1,0:T(8,128)(2,1)}, bf16[2,2048,128]{2,1,0:T(8,128)(2,1)S(1)}, u32[]{:S(2)}, u32[]{:S(2)}) collective-permute-start(bf16[2,2048,128]{2,1,0:T(8,128)(2,1)} %get-tuple-element.14), channel_id=1, source_target_pairs={{0,1},{1,2},{2,3},{3,0},{4,5},{5,6},{6,7},{7,4},{8,9},{9,10},{10,1... | collective-permute-start | bytes 3145736 | tf_op jit(solution)/shard_map/ppermute | solution.py:401
  122.0 2.3 slice.13
  124.3 3.2 %collective-permute-start.3 = (bf16[2,2048,128]{2,1,0:T(8,128)(2,1)}, bf16[2,2048,128]{2,1,0:T(8,128)(2,1)S(1)}, u32[]{:S(2)}, u32[]{:S(2)}) collective-permute-start(bf16[2,2048,128]{2,1,0:T(8,128)(2,1)} %slice.13), channel_id=1, source_target_pairs={{0,3},{1,0},{2,1},{3,2},{4,7},{5,4},{6,5},{7,6},{8,11},{9,8},{10,9... | collective-permute-start | bytes 3145736 | tf_op jit(solution)/shard_map/ppermute | solution.py:402
  127.5 11.6 %all-to-all-done.1 = bf16[128,8,128]{2,1,0:T(8,128)(2,1)S(1)} async-done(((bf16[128,8,128]{2,1,0:T(8,128)(2,1)}), bf16[128,8,128]{2,1,0:T(8,128)(2,1)S(1)}, u32[]{:S(2)}, u32[]{:S(2)}) %all-to-all-start.1) | async-done | bytes 262176 | tf_op jit(solution)/shard_map/all_to_all | solution.py:431
  139.2 13.0 %all-gather.4 = f16[16,256,128]{2,1,0:T(8,128)(2,1)S(1)} all-gather(f16[4,256,128]{2,1,0:T(8,128)(2,1)S(1)} %fusion), channel_id=1, replica_groups=mesh['sp'=32,'y'=4,'x'=4] {'y'}, dimensions={0}, use_global_device_ids=true | all-gather | bytes 1310720 | tf_op jit(solution)/shard_map/all_gather | solution.py:364
  152.6 2.5 %collective-permute-start.4 = (bf16[2,2048,128]{2,1,0:T(8,128)(2,1)S(1)}, bf16[2,2048,128]{2,1,0:T(8,128)(2,1)S(1)}, u32[]{:S(2)}, u32[]{:S(2)}) collective-permute-start(bf16[2,2048,128]{2,1,0:T(8,128)(2,1)S(1)} %copy-done.12), channel_id=1, source_target_pairs={{0,1},{1,2},{2,3},{3,0},{4,5},{5,6},{6,7},{7,4},{8,9},{9,10},{10,1... | collective-permute-start | bytes 3145736 | tf_op jit(solution)/shard_map/ppermute | solution.py:403
  155.1 4.5 %hidden.1 = bf16[4,256,256]{2,1,0:T(8,128)(2,1)S(1)} custom-call(s32[1]{0:T(128)} %bitcast.x_ref, bf16[16,256,128]{2,1,0:T(8,128)(2,1)S(1)} %multiply_convert_fusion.2.rows_ref, f32[1,2048]{1,0:T(1,128)S(1)} %bitcast.26, bf16[6,2048,128]{2,1,0:T(8,128)(2,1)} %pack.1.own_ref, bf16[6,2048,128]{2,1,0:T(8,128)(2,1)} %collective-permute-done.left_ref, ...), custom_call_target="tpu_custom_call" | custom-call | tf_op jit(solution)/shard_map/hidden/pallas_call | solution.py:265
  159.8 20.4 %all-gather.5 = f16[16,256,256]{2,1,0:T(8,128)(2,1)S(1)} all-gather(f16[4,256,256]{2,1,0:T(8,128)(2,1)S(1)} %multiply_convert_fusion.3), channel_id=1, replica_groups=mesh['sp'=32,'y'=4,'x'=4] {'y'}, dimensions={0}, use_global_device_ids=true | all-gather | bytes 2621440 | tf_op jit(solution)/shard_map/all_gather | solution.py:364
  180.7 2.8 %down.1 = bf16[32,4,8,128]{3,2,1,0:T(8,128)(2,1)S(1)} custom-call(s32[1]{0:T(128)} %bitcast.x_ref, bf16[16,256,256]{2,1,0:T(8,128)(2,1)S(1)} %multiply_convert_fusion.1.units_ref, bf16[6,2048,128]{2,1,0:T(8,128)(2,1)} %pack.1.own_ref, bf16[6,2048,128]{2,1,0:T(8,128)(2,1)} %collective-permute-done.1.right_ref, ...), custom_call_target="tpu_custom_call" | custom-call | tf_op jit(solution)/shard_map/down/pallas_call | solution.py:326
  183.5 35.6 %all_to_all.20 = bf16[128,8,128]{2,1,0:T(8,128)(2,1)S(1)} all-to-all(bf16[128,8,128]{2,1,0:T(8,128)(2,1)S(1)} %bitcast.19), channel_id=1, replica_groups=mesh['sp'=32,'y'=4,'x'=4] {'sp','x'}, dimensions={0} | all-to-all | bytes 524288 | tf_op jit(solution)/shard_map/all_to_all | solution.py:439
  219.6 20.9 %all_to_all.21.whole_ref = bf16[16,256,128]{2,1,0:T(8,128)(2,1)S(1)} all-to-all(bf16[16,256,128]{2,1,0:T(8,128)(2,1)S(1)} %combine.1), channel_id=1, replica_groups=mesh['sp'=32,'y'=4,'x'=4] {'y','x'}, dimensions={0} | all-to-all | bytes 2097152 | tf_op jit(solution)/shard_map/all_to_all | solution.py:444
  240.4 1.7 assemble.1
  (53 shorter events, 5.0 us)
Async XLA Ops:
  0.0 75.3 %copy-start = (bf16[256,2048]{1,0:T(8,128)(2,1)S(1)}, bf16[256,2048]{1,0:T(8,128)(2,1)}, u32[]{:S(2)}) copy-start(bf16[256,2048]{1,0:T(8,128)(2,1)} %param.13) | copy-start | bytes 3145732
  0.0 1.3 copy-start.1
  1.3 1.2 copy-start.2
  2.5 1.2 copy-start.3
  3.8 8.9 %copy-start.13 = (bf16[256,1,128]{2,0,1:T(8,128)(2,1)S(1)}, bf16[256,1,128]{2,0,1:T(8,128)(2,1)}, u32[]{:S(2)}) copy-start(bf16[256,1,128]{2,0,1:T(8,128)(2,1)} %param.16) | copy-start | bytes 196612
  3.8 8.9 %copy-start.14 = (bf16[256,1,128]{2,0,1:T(8,128)(2,1)S(1)}, bf16[256,1,128]{2,0,1:T(8,128)(2,1)}, u32[]{:S(2)}) copy-start(bf16[256,1,128]{2,0,1:T(8,128)(2,1)} %param.15) | copy-start | bytes 196612
  5.5 110.1 %collective-permute-start = (bf16[6,2048,128]{2,1,0:T(8,128)(2,1)}, bf16[6,2048,128]{2,1,0:T(8,128)(2,1)}, u32[]{:S(2)}, u32[]{:S(2)}) collective-permute-start(bf16[6,2048,128]{2,1,0:T(8,128)(2,1)} %pack.1.own_ref), channel_id=1, source_target_pairs={{0,1},{1,2},{2,3},{3,0},{4,5},{5,6},{6,7},{7,4},{8,9},{9,10},{10,1... | collective-permute-start | bytes 9437192 | tf_op jit(solution)/shard_map/ppermute | solution.py:399
  9.4 112.5 %collective-permute-start.1 = (bf16[6,2048,128]{2,1,0:T(8,128)(2,1)}, bf16[6,2048,128]{2,1,0:T(8,128)(2,1)}, u32[]{:S(2)}, u32[]{:S(2)}) collective-permute-start(bf16[6,2048,128]{2,1,0:T(8,128)(2,1)} %pack.1.own_ref), channel_id=1, source_target_pairs={{0,3},{1,0},{2,1},{3,2},{4,7},{5,4},{6,5},{7,6},{8,11},{9,8},{10,9... | collective-permute-start | bytes 9437192 | tf_op jit(solution)/shard_map/ppermute | solution.py:400
  63.7 1.0 copy-start.4
  63.7 1.0 copy-start.9
  63.7 1.0 copy-start.11
  64.7 10.0 %copy-start.15 = (s32[256,2]{0,1:T(2,128)S(1)}, s32[256,2]{0,1:T(2,128)}, u32[]{:S(2)}) copy-start(s32[256,2]{0,1:T(2,128)} %param.24) | copy-start | bytes 6148
  64.7 10.4 %copy-start.16 = (f32[256,2]{0,1:T(2,128)S(1)}, f32[256,2]{0,1:T(2,128)}, u32[]{:S(2)}) copy-start(f32[256,2]{0,1:T(2,128)} %param.25) | copy-start | bytes 6148
  68.3 24.7 %all-to-all-start = ((bf16[16,256,128]{2,1,0:T(8,128)(2,1)}), bf16[16,256,128]{2,1,0:T(8,128)(2,1)S(1)}, u32[]{:S(2)}, u32[]{:S(2)}) async-start(bf16[16,256,128]{2,1,0:T(8,128)(2,1)} %attention.1), calls=%async_computation | async-start | bytes 2097152 | tf_op jit(solution)/shard_map/all_to_all | solution.py:425
  94.1 0.6 copy-start.5
  94.8 27.2 %copy-start.7 = (f32[256,2]{1,0:T(8,128)}, f32[256,2]{1,0:T(8,128)S(1)}, u32[]{:S(2)}) copy-start(f32[256,2]{1,0:T(8,128)S(1)} %get-tuple-element.12.factors_ref) | copy-start | bytes 6148
  94.8 44.3 %all-to-all-start.1 = ((bf16[128,8,128]{2,1,0:T(8,128)(2,1)}), bf16[128,8,128]{2,1,0:T(8,128)(2,1)S(1)}, u32[]{:S(2)}, u32[]{:S(2)}) async-start(bf16[128,8,128]{2,1,0:T(8,128)(2,1)} %bitcast.7), calls=%async_computation.1 | async-start | bytes 524288 | tf_op jit(solution)/shard_map/all_to_all | solution.py:431
  118.6 36.5 %copy-start.10 = (f32[2048]{0:T(1024)S(1)}, f32[2048]{0:T(1024)}, u32[]{:S(2)}) copy-start(f32[2048]{0:T(1024)} %param.20) | copy-start | bytes 24580
  118.6 36.5 %collective-permute-start.2 = (bf16[2,2048,128]{2,1,0:T(8,128)(2,1)}, bf16[2,2048,128]{2,1,0:T(8,128)(2,1)S(1)}, u32[]{:S(2)}, u32[]{:S(2)}) collective-permute-start(bf16[2,2048,128]{2,1,0:T(8,128)(2,1)} %get-tuple-element.14), channel_id=1, source_target_pairs={{0,1},{1,2},{2,3},{3,0},{4,5},{5,6},{6,7},{7,4},{8,9},{9,10},{10,1... | collective-permute-start | bytes 3145736 | tf_op jit(solution)/shard_map/ppermute | solution.py:401
  124.3 30.8 %collective-permute-start.3 = (bf16[2,2048,128]{2,1,0:T(8,128)(2,1)}, bf16[2,2048,128]{2,1,0:T(8,128)(2,1)S(1)}, u32[]{:S(2)}, u32[]{:S(2)}) collective-permute-start(bf16[2,2048,128]{2,1,0:T(8,128)(2,1)} %slice.13), channel_id=1, source_target_pairs={{0,3},{1,0},{2,1},{3,2},{4,7},{5,4},{6,5},{7,6},{8,11},{9,8},{10,9... | collective-permute-start | bytes 3145736 | tf_op jit(solution)/shard_map/ppermute | solution.py:402
  139.1 13.4 %copy-start.12 = (bf16[2,2048,128]{2,1,0:T(8,128)(2,1)S(1)}, bf16[2,2048,128]{2,1,0:T(8,128)(2,1)}, u32[]{:S(2)}) copy-start(bf16[2,2048,128]{2,1,0:T(8,128)(2,1)} %get-tuple-element.13) | copy-start | bytes 3145732
  152.6 28.1 %collective-permute-start.4 = (bf16[2,2048,128]{2,1,0:T(8,128)(2,1)S(1)}, bf16[2,2048,128]{2,1,0:T(8,128)(2,1)S(1)}, u32[]{:S(2)}, u32[]{:S(2)}) collective-permute-start(bf16[2,2048,128]{2,1,0:T(8,128)(2,1)S(1)} %copy-done.12), channel_id=1, source_target_pairs={{0,1},{1,2},{2,3},{3,0},{4,5},{5,6},{6,7},{7,4},{8,9},{9,10},{10,1... | collective-permute-start | bytes 3145736 | tf_op jit(solution)/shard_map/ppermute | solution.py:403
  180.6 38.4 %copy-start.6 = (s32[256,2]{1,0:T(8,128)S(1)}, s32[256,2]{1,0:T(8,128)}, u32[]{:S(2)}) copy-start(s32[256,2]{1,0:T(8,128)} %copy-done.5) | copy-start | bytes 6148
  180.7 38.4 %copy-start.8 = (f32[256,2]{1,0:T(8,128)S(1)}, f32[256,2]{1,0:T(8,128)}, u32[]{:S(2)}) copy-start(f32[256,2]{1,0:T(8,128)} %copy-done.7) | copy-start | bytes 6148

commit v11 on v10

--- a/solution.py
+++ b/solution.py
@@ -214,27 +214,27 @@
     )(back, stream, slots, factors)
 
 
-def hidden_body(x_ref, rows_ref, gain_ref, own_ref, left_ref, right_ref, far_ref, far_up_ref, out_ref, normed_ref, weights, sems):
+def swiglu(normed, pages):
+    gates = jnp.concatenate([pages[0], pages[1]], axis=1)
+    ups = jnp.concatenate([pages[2], pages[3]], axis=1)
+    gate = jnp.dot(normed, gates, preferred_element_type=jnp.float32)
+    up = jnp.dot(normed, ups, preferred_element_type=jnp.float32)
+    return (gate / (1.0 + jnp.exp(-gate)) * up).astype(jnp.bfloat16)
+
+
+def near_body(rows_ref, gain_ref, own_ref, right_ref, left_ref, out_ref, normed_ref, weights, sems):
     peers, count, share = rows_ref.shape
-    pieces = out_ref.shape[0]
     gate, up = pl.ds(0, 2), pl.ds(4, 2)
     first, second = pl.ds(0, 2), pl.ds(2, 2)
-    groups = [
-        [(source.at[gate], weights.at[k, first]), (source.at[up], weights.at[k, second])]
-        for k, source in ((0, own_ref), (1, right_ref), (3, left_ref))
-    ]
-    groups.append(
-        [(far_ref, weights.at[2, first]), (far_up_ref, weights.at[2, second])]
-    )
-    copies, at = [], 0
-    for group in groups:
-        started = []
-        for source, target in group:
-            copy = pltpu.make_async_copy(source, target, sems.at[at])
+    copies = []
+    for k, source in enumerate((own_ref, right_ref, left_ref)):
+        pair = (
+            pltpu.make_async_copy(source.at[gate], weights.at[k, first], sems.at[k, 0]),
+            pltpu.make_async_copy(source.at[up], weights.at[k, second], sems.at[k, 1]),
+        )
+        for copy in pair:
             copy.start()
-            started.append(copy)
-            at += 1
-        copies.append(started)
+        copies.append(pair)
     total = jnp.zeros((count, 1), jnp.float32)
     for p in range(peers):
         part = rows_ref[p].astype(jnp.float32)
@@ -245,36 +245,63 @@
         normed_ref[:, cols] = (rows_ref[p].astype(jnp.float32) * scale * gain_ref[:, cols]).astype(
             jnp.bfloat16
         )
-    for ahead, started in zip((0, 1, 3, 2), copies):
-        for copy in started:
+    for k, pair in enumerate(copies):
+        for copy in pair:
             copy.wait()
-        normed = normed_ref[...]
-        gates = jnp.concatenate([weights[ahead, 0], weights[ahead, 1]], axis=1)
-        ups = jnp.concatenate([weights[ahead, 2], weights[ahead, 3]], axis=1)
-        gate = jnp.dot(normed, gates, preferred_element_type=jnp.float32)
-        up = jnp.dot(normed, ups, preferred_element_type=jnp.float32)
-        act = gate / (1.0 + jnp.exp(-gate)) * up
-        out_ref[lax.rem(x_ref[0] + ahead, pieces)] = act.astype(jnp.bfloat16)
-
-
-def hidden_units(x, rows, gain, *weights):
+        out_ref[k] = swiglu(normed_ref[...], [weights[k, page] for page in range(4)])
+
+
+def near_units(rows, gain, *sources):
     peers, count, share = rows.shape
-    _, model, half = weights[0].shape
+    _, model, half = sources[0].shape
     vmem = pl.BlockSpec(memory_space=pltpu.VMEM)
     anywhere = pl.BlockSpec(memory_space=pltpu.HBM)
     return pl.pallas_call(
-        hidden_body,
-        in_specs=[pl.BlockSpec(memory_space=pltpu.SMEM), vmem, vmem] + [anywhere] * len(weights),
+        near_body,
+        in_specs=[vmem, vmem] + [anywhere] * len(sources),
+        out_specs=[vmem, vmem],
+        out_shape=[
+            jax.ShapeDtypeStruct((len(sources), count, 2 * half), jnp.bfloat16),
+            jax.ShapeDtypeStruct((count, peers * share), jnp.bfloat16),
+        ],
+        scratch_shapes=[
+            pltpu.VMEM((len(sources), 4, model, half), jnp.bfloat16),
+            pltpu.SemaphoreType.DMA((len(sources), 2)),
+        ],
+        compiler_params=pltpu.CompilerParams(vmem_limit_bytes=16 * 2**20),
+        name="near",
+    )(rows, gain, *sources)
+
+
+def far_body(normed_ref, gate_ref, up_ref, out_ref, weights, sems):
+    copies = (
+        pltpu.make_async_copy(gate_ref, weights.at[pl.ds(0, 2)], sems.at[0]),
+        pltpu.make_async_copy(up_ref, weights.at[pl.ds(2, 2)], sems.at[1]),
+    )
+    for copy in copies:
+        copy.start()
+    for copy in copies:
+        copy.wait()
+    out_ref[0] = swiglu(normed_ref[...], [weights[page] for page in range(4)])
+
+
+def far_units(normed, gate, up):
+    count = normed.shape[0]
+    _, model, half = gate.shape
+    vmem = pl.BlockSpec(memory_space=pltpu.VMEM)
+    anywhere = pl.BlockSpec(memory_space=pltpu.HBM)
+    return pl.pallas_call(
+        far_body,
+        in_specs=[vmem, anywhere, anywhere],
         out_specs=vmem,
-        out_shape=jax.ShapeDtypeStruct((4, count, 2 * half), jnp.bfloat16),
+        out_shape=jax.ShapeDtypeStruct((1, count, 2 * half), jnp.bfloat16),
         scratch_shapes=[
-            pltpu.VMEM((count, peers * share), jnp.bfloat16),
-            pltpu.VMEM((4, 4, model, half), jnp.bfloat16),
-            pltpu.SemaphoreType.DMA((8,)),
+            pltpu.VMEM((4, model, half), jnp.bfloat16),
+            pltpu.SemaphoreType.DMA((2,)),
         ],
-        compiler_params=pltpu.CompilerParams(vmem_limit_bytes=18 * 2**20),
-        name="hidden",
-    )(x, rows, gain, *weights)
+        compiler_params=pltpu.CompilerParams(vmem_limit_bytes=8 * 2**20),
+        name="far",
+    )(normed, gate, up)
 
 
 def down_body(x_ref, units_ref, own_ref, right_ref, far_ref, left_ref, out_ref, downs, sems):
@@ -306,7 +333,9 @@
             c = p // (blocks // parts)
             for copy in copies[c * pieces : (c + 1) * pieces]:
                 copy.wait()
-        rows = slice(p * hidden, (p + 1) * hidden)
+        ahead = (0, 1, 3, 2)[p % pieces]
+        block = p // pieces * pieces + lax.rem(x_ref[0] + ahead, pieces)
+        rows = pl.ds(pl.multiple_of(block * hidden, hidden), hidden)
         units = units_ref[p]
         near = jnp.concatenate([downs[0, rows], downs[1, rows]], axis=1)
         rest = jnp.concatenate([downs[2, rows], downs[3, rows]], axis=1)
@@ -431,9 +460,9 @@
     landed = lax.all_to_all(outgoing.reshape(targets, each, share), ("sp", "x"), 0, 0, tiled=True)
     landed = arrange(landed.reshape(experts, across, each, share))
     rows = gathered(landed.reshape(across, experts * each, share), "y", 0, 64.0)
-    units = hidden_units(
-        x_at, rows, ffn_gain[None], packed, left, right, gate_2, up_2
-    )
+    near, normed = near_units(rows, ffn_gain[None], packed, right, left)
+    far = far_units(normed, gate_2, up_2)
+    units = jnp.concatenate([near, far], axis=0)
     all_units = gathered(units, "y", 0, 0.25)
     made = down_product(x_at, all_units, experts, packed, right, down_2, left)
     back = lax.all_to_all(

time: 243 us -> 239 us (0.984)
  blocking collectives: 140 us -> 136 us
    all_to_all x1, blocking collectives: 35.6 us -> 31.8 us  [shards(): lax.all_to_all(made.reshape(targets, each, share), ('sp', 'x'), 0, 0, til...]
where the time goes in v11:
time: 239 us
  blocking collectives  136 us (57%)
  starting transfers between devices  41.6 us (17%)
  waiting for transfers between devices  31.6 us (13%)
  Pallas kernels  16.2 us (7%)
  local copies, waits for them, and re-layouts  10.1 us (4%)
    all_gather x3, blocking collectives, gathered(): whole = lax.all_gather(sent, axes, axis=axis, tiled=True)  83.1 us
    all_to_all x1, blocking collectives, shards(): lax.all_to_all(made.reshape(targets, each, share), ('sp', 'x'), 0, 0, til...  31.8 us
    all_to_all x1, blocking collectives, shards(): whole = lax.all_to_all(spread, tp, 0, 0, tiled=True)  20.8 us
    all_to_all x1, waiting for transfers between devices, shards(): parts = lax.all_to_all(partial, tp, 0, 0, tiled=True)  20 us
    all_to_all x1, starting transfers between devices, shards(): lax.all_to_all(outgoing.reshape(targets, each, share), ('sp', 'x'), 0, 0,...  18.3 us
    all_to_all x1, waiting for transfers between devices, shards(): lax.all_to_all(outgoing.reshape(targets, each, share), ('sp', 'x'), 0, 0,...  11.6 us
    all_to_all x1, starting transfers between devices, shards(): parts = lax.all_to_all(partial, tp, 0, 0, tiled=True)  6.97 us
    ppermute x1, starting transfers between devices, shards(): right = lax.ppermute(packed, 'x', behind)  5.21 us
  transfers between devices with their start and end apart: 7, of which 2 were waited for; matrix products, arithmetic and copies ran while one was open for 3% of the time, Pallas kernels for 4%

profile of v11, /device:TPU:1, one launch (start us, length us, event | category | flops | bytes accessed | tf_op | source)
XLA Modules:
  0.0 238.5 jit_solution(17260082225896333543)
XLA Ops:
  0.0 1.3 copy-done.1
  1.3 1.2 copy-done.2
  2.5 1.2 copy-done.3
  3.8 1.7 pack.1.own_ref
  5.5 5.2 %collective-permute-start = (bf16[6,2048,128]{2,1,0:T(8,128)(2,1)}, bf16[6,2048,128]{2,1,0:T(8,128)(2,1)}, u32[]{:S(2)}, u32[]{:S(2)}) collective-permute-start(bf16[6,2048,128]{2,1,0:T(8,128)(2,1)} %pack.1.own_ref), channel_id=1, source_target_pairs={{0,3},{1,0},{2,1},{3,2},{4,7},{5,4},{6,5},{7,6},{8,11},{9,8},{10,9... | collective-permute-start | bytes 9437192 | tf_op jit(solution)/shard_map/ppermute | solution.py:429
  10.7 1.9 collective-permute-start.1
  12.7 49.9 %all-gather.3 = f16[8192,256]{1,0:T(8,128)(2,1)S(1)} all-gather(f16[256,256]{1,0:T(8,128)(2,1)S(1)} %multiply_convert_fusion.5), channel_id=1, replica_groups=mesh['sp'=32,'y'=4,'x'=4] {'sp'}, dimensions={0}, use_global_device_ids=true | all-gather | bytes 4325376 | tf_op jit(solution)/shard_map/all_gather | solution.py:393
  64.3 3.6 %attention.1 = bf16[16,256,128]{2,1,0:T(8,128)(2,1)} custom-call(s32[1]{0:T(128)} %bitcast.1.where_ref, f32[1]{0:T(128)S(6)} %copy.30.lam_ref, bf16[256,128]{1,0:T(8,128)(2,1)S(1)} %bitcast.25, bf16[8192,256]{1,0:T(8,128)(2,1)S(1)} %multiply_convert_fusion.kv_ref, f32[1,128]{1,0:T(1,128)S(1)} %bitcast.27, bf16[128,2048]{1,0:T(8,128)(2,1)S(1)} %copy-done.4), custom_call_target="tpu_custom_call" | custom-call | tf_op jit(solution)/shard_map/attention/pallas_call | solution.py:81
  67.9 7.0 %all-to-all-start = ((bf16[16,256,128]{2,1,0:T(8,128)(2,1)}), bf16[16,256,128]{2,1,0:T(8,128)(2,1)S(1)}, u32[]{:S(2)}, u32[]{:S(2)}) async-start(bf16[16,256,128]{2,1,0:T(8,128)(2,1)} %attention.1), calls=%async_computation | async-start | bytes 2097152 | tf_op jit(solution)/shard_map/all_to_all | solution.py:454
  75.5 20.0 %all-to-all-done.parts_ref = bf16[16,256,128]{2,1,0:T(8,128)(2,1)S(1)} async-done(((bf16[16,256,128]{2,1,0:T(8,128)(2,1)}), bf16[16,256,128]{2,1,0:T(8,128)(2,1)S(1)}, u32[]{:S(2)}, u32[]{:S(2)}) %all-to-all-start) | async-done | bytes 1048608 | tf_op jit(solution)/shard_map/all_to_all | solution.py:454
  97.3 18.3 %all-to-all-start.1 = ((bf16[128,8,128]{2,1,0:T(8,128)(2,1)}), bf16[128,8,128]{2,1,0:T(8,128)(2,1)S(1)}, u32[]{:S(2)}, u32[]{:S(2)}) async-start(bf16[128,8,128]{2,1,0:T(8,128)(2,1)} %bitcast.7), calls=%async_computation.1 | async-start | bytes 524288 | tf_op jit(solution)/shard_map/all_to_all | solution.py:460
  115.6 3.0 %fusion.2 = (bf16[2,2048,128]{2,1,0:T(8,128)(2,1)}, bf16[2,2048,128]{2,1,0:T(8,128)(2,1)}) fusion(bf16[6,2048,128]{2,1,0:T(8,128)(2,1)} %collective-permute-done.1.left_ref), kind=kLoop, calls=%fused_computation.15 | loop fusion | bytes 4194304 | tf_op jit(solution)/shard_map/slice | solution.py:432
  118.6 3.4 %collective-permute-start.2 = (bf16[2,2048,128]{2,1,0:T(8,128)(2,1)}, bf16[2,2048,128]{2,1,0:T(8,128)(2,1)S(1)}, u32[]{:S(2)}, u32[]{:S(2)}) collective-permute-start(bf16[2,2048,128]{2,1,0:T(8,128)(2,1)} %get-tuple-element.18), channel_id=1, source_target_pairs={{0,1},{1,2},{2,3},{3,0},{4,5},{5,6},{6,7},{7,4},{8,9},{9,10},{10,1... | collective-permute-start | bytes 3145736 | tf_op jit(solution)/shard_map/ppermute | solution.py:430
  122.1 2.3 slice.13
  124.3 3.2 %collective-permute-start.3 = (bf16[2,2048,128]{2,1,0:T(8,128)(2,1)}, bf16[2,2048,128]{2,1,0:T(8,128)(2,1)S(1)}, u32[]{:S(2)}, u32[]{:S(2)}) collective-permute-start(bf16[2,2048,128]{2,1,0:T(8,128)(2,1)} %slice.13), channel_id=1, source_target_pairs={{0,3},{1,0},{2,1},{3,2},{4,7},{5,4},{6,5},{7,6},{8,11},{9,8},{10,9... | collective-permute-start | bytes 3145736 | tf_op jit(solution)/shard_map/ppermute | solution.py:431
  127.6 11.6 %all-to-all-done.1 = bf16[128,8,128]{2,1,0:T(8,128)(2,1)S(1)} async-done(((bf16[128,8,128]{2,1,0:T(8,128)(2,1)}), bf16[128,8,128]{2,1,0:T(8,128)(2,1)S(1)}, u32[]{:S(2)}, u32[]{:S(2)}) %all-to-all-start.1) | async-done | bytes 262176 | tf_op jit(solution)/shard_map/all_to_all | solution.py:460
  139.3 12.9 %all-gather.4 = f16[16,256,128]{2,1,0:T(8,128)(2,1)S(1)} all-gather(f16[4,256,128]{2,1,0:T(8,128)(2,1)S(1)} %fusion), channel_id=1, replica_groups=mesh['sp'=32,'y'=4,'x'=4] {'y'}, dimensions={0}, use_global_device_ids=true | all-gather | bytes 1310720 | tf_op jit(solution)/shard_map/all_gather | solution.py:393
  152.5 2.6 %collective-permute-start.4 = (bf16[2,2048,128]{2,1,0:T(8,128)(2,1)S(1)}, bf16[2,2048,128]{2,1,0:T(8,128)(2,1)S(1)}, u32[]{:S(2)}, u32[]{:S(2)}) collective-permute-start(bf16[2,2048,128]{2,1,0:T(8,128)(2,1)S(1)} %copy-done.12), channel_id=1, source_target_pairs={{0,1},{1,2},{2,3},{3,0},{4,5},{5,6},{6,7},{7,4},{8,9},{9,10},{10,1... | collective-permute-start | bytes 3145736 | tf_op jit(solution)/shard_map/ppermute | solution.py:432
  155.1 3.8 %near.1 = (bf16[3,256,256]{2,1,0:T(8,128)(2,1)S(1)}, bf16[256,2048]{1,0:T(8,128)(2,1)S(1)}) custom-call(bf16[16,256,128]{2,1,0:T(8,128)(2,1)S(1)} %multiply_convert_fusion.2.rows_ref, f32[1,2048]{1,0:T(1,128)S(1)} %bitcast.26, bf16[6,2048,128]{2,1,0:T(8,128)(2,1)} %pack.1.own_ref, bf16[6,2048,128]{2,1,0:T(8,128)(2,1)} %collective-permute-done.right_ref, ...), custom_call_target="tpu_custom_call" | custom-call | tf_op jit(solution)/shard_map/near/pallas_call | solution.py:259
  160.0 20.3 %all-gather.5 = f16[16,256,256]{2,1,0:T(8,128)(2,1)S(1)} all-gather(f16[4,256,256]{2,1,0:T(8,128)(2,1)S(1)} %multiply_convert_fusion.3), channel_id=1, replica_groups=mesh['sp'=32,'y'=4,'x'=4] {'y'}, dimensions={0}, use_global_device_ids=true | all-gather | bytes 2621440 | tf_op jit(solution)/shard_map/all_gather | solution.py:393
  180.9 2.8 %down.1 = bf16[32,4,8,128]{3,2,1,0:T(8,128)(2,1)S(1)} custom-call(s32[1]{0:T(128)} %bitcast.x_ref, bf16[16,256,256]{2,1,0:T(8,128)(2,1)S(1)} %multiply_convert_fusion.1.units_ref, bf16[6,2048,128]{2,1,0:T(8,128)(2,1)} %pack.1.own_ref, bf16[6,2048,128]{2,1,0:T(8,128)(2,1)} %collective-permute-done.right_ref, ...), custom_call_target="tpu_custom_call" | custom-call | tf_op jit(solution)/shard_map/down/pallas_call | solution.py:355
  183.7 31.8 %all_to_all.20 = bf16[128,8,128]{2,1,0:T(8,128)(2,1)S(1)} all-to-all(bf16[128,8,128]{2,1,0:T(8,128)(2,1)S(1)} %bitcast.19), channel_id=1, replica_groups=mesh['sp'=32,'y'=4,'x'=4] {'sp','x'}, dimensions={0} | all-to-all | bytes 524288 | tf_op jit(solution)/shard_map/all_to_all | solution.py:468
  216.0 20.8 %all_to_all.21.whole_ref = bf16[16,256,128]{2,1,0:T(8,128)(2,1)S(1)} all-to-all(bf16[16,256,128]{2,1,0:T(8,128)(2,1)S(1)} %combine.1), channel_id=1, replica_groups=mesh['sp'=32,'y'=4,'x'=4] {'y','x'}, dimensions={0} | all-to-all | bytes 2097152 | tf_op jit(solution)/shard_map/all_to_all | solution.py:473
  236.9 1.7 assemble.1
  (54 shorter events, 5.9 us)
Async XLA Ops:
  0.0 75.4 %copy-start = (bf16[256,2048]{1,0:T(8,128)(2,1)S(1)}, bf16[256,2048]{1,0:T(8,128)(2,1)}, u32[]{:S(2)}) copy-start(bf16[256,2048]{1,0:T(8,128)(2,1)} %param.13) | copy-start | bytes 3145732
  0.0 1.3 copy-start.1
  1.3 1.2 copy-start.2
  2.5 1.2 copy-start.3
  3.8 8.9 %copy-start.13 = (bf16[256,1,128]{2,0,1:T(8,128)(2,1)S(1)}, bf16[256,1,128]{2,0,1:T(8,128)(2,1)}, u32[]{:S(2)}) copy-start(bf16[256,1,128]{2,0,1:T(8,128)(2,1)} %param.16) | copy-start | bytes 196612
  3.8 8.9 %copy-start.14 = (bf16[256,1,128]{2,0,1:T(8,128)(2,1)S(1)}, bf16[256,1,128]{2,0,1:T(8,128)(2,1)}, u32[]{:S(2)}) copy-start(bf16[256,1,128]{2,0,1:T(8,128)(2,1)} %param.15) | copy-start | bytes 196612
  5.5 116.6 %collective-permute-start = (bf16[6,2048,128]{2,1,0:T(8,128)(2,1)}, bf16[6,2048,128]{2,1,0:T(8,128)(2,1)}, u32[]{:S(2)}, u32[]{:S(2)}) collective-permute-start(bf16[6,2048,128]{2,1,0:T(8,128)(2,1)} %pack.1.own_ref), channel_id=1, source_target_pairs={{0,3},{1,0},{2,1},{3,2},{4,7},{5,4},{6,5},{7,6},{8,11},{9,8},{10,9... | collective-permute-start | bytes 9437192 | tf_op jit(solution)/shard_map/ppermute | solution.py:429
  10.7 104.9 %collective-permute-start.1 = (bf16[6,2048,128]{2,1,0:T(8,128)(2,1)}, bf16[6,2048,128]{2,1,0:T(8,128)(2,1)}, u32[]{:S(2)}, u32[]{:S(2)}) collective-permute-start(bf16[6,2048,128]{2,1,0:T(8,128)(2,1)} %pack.1.own_ref), channel_id=1, source_target_pairs={{0,1},{1,2},{2,3},{3,0},{4,5},{5,6},{6,7},{7,4},{8,9},{9,10},{10,1... | collective-permute-start | bytes 9437192 | tf_op jit(solution)/shard_map/ppermute | solution.py:428
  63.2 1.0 copy-start.4
  63.2 1.0 copy-start.9
  63.2 1.0 copy-start.11
  64.2 10.6 %copy-start.15 = (s32[256,2]{0,1:T(2,128)S(1)}, s32[256,2]{0,1:T(2,128)}, u32[]{:S(2)}) copy-start(s32[256,2]{0,1:T(2,128)} %param.24) | copy-start | bytes 6148
  64.2 11.0 %copy-start.16 = (f32[256,2]{0,1:T(2,128)S(1)}, f32[256,2]{0,1:T(2,128)}, u32[]{:S(2)}) copy-start(f32[256,2]{0,1:T(2,128)} %param.25) | copy-start | bytes 6148
  67.9 27.6 %all-to-all-start = ((bf16[16,256,128]{2,1,0:T(8,128)(2,1)}), bf16[16,256,128]{2,1,0:T(8,128)(2,1)S(1)}, u32[]{:S(2)}, u32[]{:S(2)}) async-start(bf16[16,256,128]{2,1,0:T(8,128)(2,1)} %attention.1), calls=%async_computation | async-start | bytes 2097152 | tf_op jit(solution)/shard_map/all_to_all | solution.py:454
  96.6 0.6 copy-start.5
  97.3 24.8 %copy-start.7 = (f32[256,2]{1,0:T(8,128)}, f32[256,2]{1,0:T(8,128)S(1)}, u32[]{:S(2)}) copy-start(f32[256,2]{1,0:T(8,128)S(1)} %get-tuple-element.16.factors_ref) | copy-start | bytes 6148
  97.3 41.9 %all-to-all-start.1 = ((bf16[128,8,128]{2,1,0:T(8,128)(2,1)}), bf16[128,8,128]{2,1,0:T(8,128)(2,1)S(1)}, u32[]{:S(2)}, u32[]{:S(2)}) async-start(bf16[128,8,128]{2,1,0:T(8,128)(2,1)} %bitcast.7), calls=%async_computation.1 | async-start | bytes 524288 | tf_op jit(solution)/shard_map/all_to_all | solution.py:460
  118.6 36.5 %copy-start.10 = (f32[2048]{0:T(1024)S(1)}, f32[2048]{0:T(1024)}, u32[]{:S(2)}) copy-start(f32[2048]{0:T(1024)} %param.20) | copy-start | bytes 24580
  118.6 40.3 %collective-permute-start.2 = (bf16[2,2048,128]{2,1,0:T(8,128)(2,1)}, bf16[2,2048,128]{2,1,0:T(8,128)(2,1)S(1)}, u32[]{:S(2)}, u32[]{:S(2)}) collective-permute-start(bf16[2,2048,128]{2,1,0:T(8,128)(2,1)} %get-tuple-element.18), channel_id=1, source_target_pairs={{0,1},{1,2},{2,3},{3,0},{4,5},{5,6},{6,7},{7,4},{8,9},{9,10},{10,1... | collective-permute-start | bytes 3145736 | tf_op jit(solution)/shard_map/ppermute | solution.py:430
  124.3 34.6 %collective-permute-start.3 = (bf16[2,2048,128]{2,1,0:T(8,128)(2,1)}, bf16[2,2048,128]{2,1,0:T(8,128)(2,1)S(1)}, u32[]{:S(2)}, u32[]{:S(2)}) collective-permute-start(bf16[2,2048,128]{2,1,0:T(8,128)(2,1)} %slice.13), channel_id=1, source_target_pairs={{0,3},{1,0},{2,1},{3,2},{4,7},{5,4},{6,5},{7,6},{8,11},{9,8},{10,9... | collective-permute-start | bytes 3145736 | tf_op jit(solution)/shard_map/ppermute | solution.py:431
  139.1 13.4 %copy-start.12 = (bf16[2,2048,128]{2,1,0:T(8,128)(2,1)S(1)}, bf16[2,2048,128]{2,1,0:T(8,128)(2,1)}, u32[]{:S(2)}) copy-start(bf16[2,2048,128]{2,1,0:T(8,128)(2,1)} %get-tuple-element.17) | copy-start | bytes 3145732
  152.5 28.4 %collective-permute-start.4 = (bf16[2,2048,128]{2,1,0:T(8,128)(2,1)S(1)}, bf16[2,2048,128]{2,1,0:T(8,128)(2,1)S(1)}, u32[]{:S(2)}, u32[]{:S(2)}) collective-permute-start(bf16[2,2048,128]{2,1,0:T(8,128)(2,1)S(1)} %copy-done.12), channel_id=1, source_target_pairs={{0,1},{1,2},{2,3},{3,0},{4,5},{5,6},{6,7},{7,4},{8,9},{9,10},{10,1... | collective-permute-start | bytes 3145736 | tf_op jit(solution)/shard_map/ppermute | solution.py:432
  180.9 34.6 %copy-start.6 = (s32[256,2]{1,0:T(8,128)S(1)}, s32[256,2]{1,0:T(8,128)}, u32[]{:S(2)}) copy-start(s32[256,2]{1,0:T(8,128)} %copy-done.5) | copy-start | bytes 6148
  180.9 34.6 %copy-start.8 = (f32[256,2]{1,0:T(8,128)S(1)}, f32[256,2]{1,0:T(8,128)}, u32[]{:S(2)}) copy-start(f32[256,2]{1,0:T(8,128)} %copy-done.7) | copy-start | bytes 6148

commit v12 on v11

--- a/solution.py
+++ b/solution.py
@@ -127,6 +127,32 @@
         compiler_params=pltpu.CompilerParams(vmem_limit_bytes=4 * 2**20),
         name="pack",
     )(gate, up, down)
+
+
+def cut_body(left_ref, right_ref, gate_ref, down_ref, up_ref, sems):
+    copies = (
+        pltpu.make_async_copy(left_ref.at[pl.ds(0, 2)], gate_ref, sems.at[0]),
+        pltpu.make_async_copy(right_ref.at[pl.ds(4, 2)], up_ref, sems.at[1]),
+        pltpu.make_async_copy(left_ref.at[pl.ds(2, 2)], down_ref, sems.at[2]),
+    )
+    for copy in copies:
+        copy.start()
+    for copy in copies:
+        copy.wait()
+
+
+def cut(left, right):
+    _, model, half = left.shape
+    anywhere = pl.BlockSpec(memory_space=pltpu.HBM)
+    return pl.pallas_call(
+        cut_body,
+        in_specs=[anywhere] * 2,
+        out_specs=[pl.BlockSpec(memory_space=pltpu.VMEM)] * 3,
+        out_shape=[jax.ShapeDtypeStruct((2, model, half), left.dtype)] * 3,
+        scratch_shapes=[pltpu.SemaphoreType.DMA((3,))],
+        compiler_params=pltpu.CompilerParams(vmem_limit_bytes=6 * 2**20),
+        name="cut",
+    )(left, right)
 
 
 def arrange_body(landed_ref, out_ref):
@@ -427,9 +453,10 @@
     packed = pack(gate, up, down)
     left = lax.ppermute(packed, "x", ahead)
     right = lax.ppermute(packed, "x", behind)
-    gate_2 = lax.ppermute(left[:2], "x", ahead)
-    up_2 = lax.ppermute(right[4:], "x", behind)
-    down_2 = lax.ppermute(left[2:4], "x", ahead)
+    gate_1, down_1, up_1 = cut(left, right)
+    gate_2 = lax.ppermute(gate_1, "x", ahead)
+    up_2 = lax.ppermute(up_1, "x", behind)
+    down_2 = lax.ppermute(down_1, "x", ahead)
 
     kv = jnp.concatenate([key_vectors[:, 0], value_rows[:, 0]], axis=1)
     kv_all = gathered(kv, "sp", 0, SHIFT)

time: 239 us -> 239 us (level)
  local copies, waits for them, and re-layouts: 10.1 us -> 5.75 us
  Pallas kernels: 16.2 us -> 19.4 us
    slice x2 -> x0, local copies, waits for them, and re-layouts: 5.3 us -> none  [the longest x1 3.02 us: shards(): down_2 = lax.ppermute(left[2:4], 'x', ahead)]
    pallas_call x0 -> x1, Pallas kernels: none -> 3.22 us  [cut(): pl.pallas_call(cut_body, in_specs=[anywhere] * 2, out_specs=[pl.BlockSpec...]
    unnamed x35 -> x37, local copies, waits for them, and re-layouts: 4.62 us -> 5.59 us
  transfers between devices with their start and end apart: 7 -> 7, of which waited for: 2 -> 2; matrix products, arithmetic and copies ran while one was open for 3% -> 1% of each run, Pallas kernels for 4% -> 5%
where the time goes in v12:
time: 239 us; the launch traced here: 238 us
  blocking collectives  136 us (57%)
  starting transfers between devices  41.3 us (17%)
  waiting for transfers between devices  32.7 us (14%)
  Pallas kernels  19.4 us (8%)
  local copies, waits for them, and re-layouts  5.75 us (2%)
    all_gather x3, blocking collectives, gathered(): whole = lax.all_gather(sent, axes, axis=axis, tiled=True)  83.4 us
    all_to_all x1, blocking collectives, shards(): lax.all_to_all(made.reshape(targets, each, share), ('sp', 'x'), 0, 0, til...  31.5 us
    all_to_all x1, blocking collectives, shards(): whole = lax.all_to_all(spread, tp, 0, 0, tiled=True)  20.9 us
    all_to_all x1, waiting for transfers between devices, shards(): parts = lax.all_to_all(partial, tp, 0, 0, tiled=True)  20 us
    all_to_all x1, starting transfers between devices, shards(): lax.all_to_all(outgoing.reshape(targets, each, share), ('sp', 'x'), 0, 0,...  18.3 us
    all_to_all x1, waiting for transfers between devices, shards(): lax.all_to_all(outgoing.reshape(targets, each, share), ('sp', 'x'), 0, 0,...  12.6 us
    all_to_all x1, starting transfers between devices, shards(): parts = lax.all_to_all(partial, tp, 0, 0, tiled=True)  6.96 us
    unnamed x37, local copies, waits for them, and re-layouts  5.59 us
  transfers between devices with their start and end apart: 7, of which 2 were waited for; matrix products, arithmetic and copies ran while one was open for 1% of the time, Pallas kernels for 5%

profile of v12, /device:TPU:1, one launch (start us, length us, event | category | flops | bytes accessed | tf_op | source)
XLA Modules:
  0.0 238.3 jit_solution(9739432543897690906)
XLA Ops:
  0.0 1.3 copy-done.1
  1.3 1.2 copy-done.2
  2.5 1.2 copy-done.3
  3.8 1.7 pack.1.own_ref
  5.5 5.2 %collective-permute-start = (bf16[6,2048,128]{2,1,0:T(8,128)(2,1)}, bf16[6,2048,128]{2,1,0:T(8,128)(2,1)}, u32[]{:S(2)}, u32[]{:S(2)}) collective-permute-start(bf16[6,2048,128]{2,1,0:T(8,128)(2,1)} %pack.1.own_ref), channel_id=1, source_target_pairs={{0,3},{1,0},{2,1},{3,2},{4,7},{5,4},{6,5},{7,6},{8,11},{9,8},{10,9... | collective-permute-start | bytes 9437192 | tf_op jit(solution)/shard_map/ppermute | solution.py:455
  10.7 1.9 collective-permute-start.1
  12.7 49.9 %all-gather.3 = f16[8192,256]{1,0:T(8,128)(2,1)S(1)} all-gather(f16[256,256]{1,0:T(8,128)(2,1)S(1)} %multiply_convert_fusion.5), channel_id=1, replica_groups=mesh['sp'=32,'y'=4,'x'=4] {'sp'}, dimensions={0}, use_global_device_ids=true | all-gather | bytes 4325376 | tf_op jit(solution)/shard_map/all_gather | solution.py:419
  64.3 3.6 %attention.1 = bf16[16,256,128]{2,1,0:T(8,128)(2,1)} custom-call(s32[1]{0:T(128)} %bitcast.1.where_ref, f32[1]{0:T(128)S(6)} %copy.30.lam_ref, bf16[256,128]{1,0:T(8,128)(2,1)S(1)} %bitcast.25, bf16[8192,256]{1,0:T(8,128)(2,1)S(1)} %multiply_convert_fusion.kv_ref, f32[1,128]{1,0:T(1,128)S(1)} %bitcast.27, bf16[128,2048]{1,0:T(8,128)(2,1)S(1)} %copy-done.4), custom_call_target="tpu_custom_call" | custom-call | tf_op jit(solution)/shard_map/attention/pallas_call | solution.py:81
  67.9 7.0 %all-to-all-start = ((bf16[16,256,128]{2,1,0:T(8,128)(2,1)}), bf16[16,256,128]{2,1,0:T(8,128)(2,1)S(1)}, u32[]{:S(2)}, u32[]{:S(2)}) async-start(bf16[16,256,128]{2,1,0:T(8,128)(2,1)} %attention.1), calls=%async_computation | async-start | bytes 2097152 | tf_op jit(solution)/shard_map/all_to_all | solution.py:481
  75.5 20.0 %all-to-all-done.parts_ref = bf16[16,256,128]{2,1,0:T(8,128)(2,1)S(1)} async-done(((bf16[16,256,128]{2,1,0:T(8,128)(2,1)}), bf16[16,256,128]{2,1,0:T(8,128)(2,1)S(1)}, u32[]{:S(2)}, u32[]{:S(2)}) %all-to-all-start) | async-done | bytes 1048608 | tf_op jit(solution)/shard_map/all_to_all | solution.py:481
  95.5 1.1 project.1
  97.3 18.3 %all-to-all-start.1 = ((bf16[128,8,128]{2,1,0:T(8,128)(2,1)}), bf16[128,8,128]{2,1,0:T(8,128)(2,1)S(1)}, u32[]{:S(2)}, u32[]{:S(2)}) async-start(bf16[128,8,128]{2,1,0:T(8,128)(2,1)} %bitcast.7), calls=%async_computation.1 | async-start | bytes 524288 | tf_op jit(solution)/shard_map/all_to_all | solution.py:487
  115.7 3.2 %cut.1 = (bf16[2,2048,128]{2,1,0:T(8,128)(2,1)}, bf16[2,2048,128]{2,1,0:T(8,128)(2,1)S(1)}, bf16[2,2048,128]{2,1,0:T(8,128)(2,1)}) custom-call(bf16[6,2048,128]{2,1,0:T(8,128)(2,1)} %collective-permute-done.1.left_ref, bf16[6,2048,128]{2,1,0:T(8,128)(2,1)} %collective-permute-done.right_ref), custom_call_target="tpu_custom_call" | custom-call | tf_op jit(solution)/shard_map/cut/pallas_call | solution.py:147
  119.9 3.2 %collective-permute-start.2 = (bf16[2,2048,128]{2,1,0:T(8,128)(2,1)}, bf16[2,2048,128]{2,1,0:T(8,128)(2,1)S(1)}, u32[]{:S(2)}, u32[]{:S(2)}) collective-permute-start(bf16[2,2048,128]{2,1,0:T(8,128)(2,1)} %get-tuple-element.17), channel_id=1, source_target_pairs={{0,1},{1,2},{2,3},{3,0},{4,5},{5,6},{6,7},{7,4},{8,9},{9,10},{10,1... | collective-permute-start | bytes 3145736 | tf_op jit(solution)/shard_map/ppermute | solution.py:457
  123.1 3.2 %collective-permute-start.3 = (bf16[2,2048,128]{2,1,0:T(8,128)(2,1)}, bf16[2,2048,128]{2,1,0:T(8,128)(2,1)S(1)}, u32[]{:S(2)}, u32[]{:S(2)}) collective-permute-start(bf16[2,2048,128]{2,1,0:T(8,128)(2,1)} %get-tuple-element.18), channel_id=1, source_target_pairs={{0,3},{1,0},{2,1},{3,2},{4,7},{5,4},{6,5},{7,6},{8,11},{9,8},{10,9... | collective-permute-start | bytes 3145736 | tf_op jit(solution)/shard_map/ppermute | solution.py:458
  126.4 12.6 %all-to-all-done.1 = bf16[128,8,128]{2,1,0:T(8,128)(2,1)S(1)} async-done(((bf16[128,8,128]{2,1,0:T(8,128)(2,1)}), bf16[128,8,128]{2,1,0:T(8,128)(2,1)S(1)}, u32[]{:S(2)}, u32[]{:S(2)}) %all-to-all-start.1) | async-done | bytes 262176 | tf_op jit(solution)/shard_map/all_to_all | solution.py:487
  139.1 13.2 %all-gather.4 = f16[16,256,128]{2,1,0:T(8,128)(2,1)S(1)} all-gather(f16[4,256,128]{2,1,0:T(8,128)(2,1)S(1)} %fusion), channel_id=1, replica_groups=mesh['sp'=32,'y'=4,'x'=4] {'y'}, dimensions={0}, use_global_device_ids=true | all-gather | bytes 1310720 | tf_op jit(solution)/shard_map/all_gather | solution.py:419
  152.6 2.4 collective-permute-start.4
  155.0 3.8 %near.1 = (bf16[3,256,256]{2,1,0:T(8,128)(2,1)S(1)}, bf16[256,2048]{1,0:T(8,128)(2,1)S(1)}) custom-call(bf16[16,256,128]{2,1,0:T(8,128)(2,1)S(1)} %multiply_convert_fusion.2.rows_ref, f32[1,2048]{1,0:T(1,128)S(1)} %bitcast.26, bf16[6,2048,128]{2,1,0:T(8,128)(2,1)} %pack.1.own_ref, bf16[6,2048,128]{2,1,0:T(8,128)(2,1)} %collective-permute-done.right_ref, ...), custom_call_target="tpu_custom_call" | custom-call | tf_op jit(solution)/shard_map/near/pallas_call | solution.py:285
  159.9 20.3 %all-gather.5 = f16[16,256,256]{2,1,0:T(8,128)(2,1)S(1)} all-gather(f16[4,256,256]{2,1,0:T(8,128)(2,1)S(1)} %multiply_convert_fusion.3), channel_id=1, replica_groups=mesh['sp'=32,'y'=4,'x'=4] {'y'}, dimensions={0}, use_global_device_ids=true | all-gather | bytes 2621440 | tf_op jit(solution)/shard_map/all_gather | solution.py:419
  180.8 2.8 %down.1 = bf16[32,4,8,128]{3,2,1,0:T(8,128)(2,1)S(1)} custom-call(s32[1]{0:T(128)} %bitcast.x_ref, bf16[16,256,256]{2,1,0:T(8,128)(2,1)S(1)} %multiply_convert_fusion.1.units_ref, bf16[6,2048,128]{2,1,0:T(8,128)(2,1)} %pack.1.own_ref, bf16[6,2048,128]{2,1,0:T(8,128)(2,1)} %collective-permute-done.right_ref, ...), custom_call_target="tpu_custom_call" | custom-call | tf_op jit(solution)/shard_map/down/pallas_call | solution.py:381
  183.6 31.5 %all_to_all.20 = bf16[128,8,128]{2,1,0:T(8,128)(2,1)S(1)} all-to-all(bf16[128,8,128]{2,1,0:T(8,128)(2,1)S(1)} %bitcast.19), channel_id=1, replica_groups=mesh['sp'=32,'y'=4,'x'=4] {'sp','x'}, dimensions={0} | all-to-all | bytes 524288 | tf_op jit(solution)/shard_map/all_to_all | solution.py:495
  215.7 20.9 %all_to_all.21.whole_ref = bf16[16,256,128]{2,1,0:T(8,128)(2,1)S(1)} all-to-all(bf16[16,256,128]{2,1,0:T(8,128)(2,1)S(1)} %combine.1), channel_id=1, replica_groups=mesh['sp'=32,'y'=4,'x'=4] {'y','x'}, dimensions={0} | all-to-all | bytes 2097152 | tf_op jit(solution)/shard_map/all_to_all | solution.py:500
  236.6 1.7 assemble.1
  (55 shorter events, 5.7 us)
Async XLA Ops:
  0.0 75.4 %copy-start = (bf16[256,2048]{1,0:T(8,128)(2,1)S(1)}, bf16[256,2048]{1,0:T(8,128)(2,1)}, u32[]{:S(2)}) copy-start(bf16[256,2048]{1,0:T(8,128)(2,1)} %param.13) | copy-start | bytes 3145732
  0.0 1.3 copy-start.1
  1.3 1.2 copy-start.2
  2.5 1.2 copy-start.3
  3.8 8.8 %copy-start.14 = (bf16[256,1,128]{2,0,1:T(8,128)(2,1)S(1)}, bf16[256,1,128]{2,0,1:T(8,128)(2,1)}, u32[]{:S(2)}) copy-start(bf16[256,1,128]{2,0,1:T(8,128)(2,1)} %param.16) | copy-start | bytes 196612
  3.8 8.9 %copy-start.15 = (bf16[256,1,128]{2,0,1:T(8,128)(2,1)S(1)}, bf16[256,1,128]{2,0,1:T(8,128)(2,1)}, u32[]{:S(2)}) copy-start(bf16[256,1,128]{2,0,1:T(8,128)(2,1)} %param.15) | copy-start | bytes 196612
  5.5 110.2 %collective-permute-start = (bf16[6,2048,128]{2,1,0:T(8,128)(2,1)}, bf16[6,2048,128]{2,1,0:T(8,128)(2,1)}, u32[]{:S(2)}, u32[]{:S(2)}) collective-permute-start(bf16[6,2048,128]{2,1,0:T(8,128)(2,1)} %pack.1.own_ref), channel_id=1, source_target_pairs={{0,3},{1,0},{2,1},{3,2},{4,7},{5,4},{6,5},{7,6},{8,11},{9,8},{10,9... | collective-permute-start | bytes 9437192 | tf_op jit(solution)/shard_map/ppermute | solution.py:455
  10.7 105.0 %collective-permute-start.1 = (bf16[6,2048,128]{2,1,0:T(8,128)(2,1)}, bf16[6,2048,128]{2,1,0:T(8,128)(2,1)}, u32[]{:S(2)}, u32[]{:S(2)}) collective-permute-start(bf16[6,2048,128]{2,1,0:T(8,128)(2,1)} %pack.1.own_ref), channel_id=1, source_target_pairs={{0,1},{1,2},{2,3},{3,0},{4,5},{5,6},{6,7},{7,4},{8,9},{9,10},{10,1... | collective-permute-start | bytes 9437192 | tf_op jit(solution)/shard_map/ppermute | solution.py:454
  63.2 1.0 copy-start.4
  63.2 1.0 copy-start.9
  63.2 1.0 copy-start.11
  64.2 10.7 %copy-start.16 = (s32[256,2]{0,1:T(2,128)S(1)}, s32[256,2]{0,1:T(2,128)}, u32[]{:S(2)}) copy-start(s32[256,2]{0,1:T(2,128)} %param.24) | copy-start | bytes 6148
  64.2 11.0 %copy-start.17 = (f32[256,2]{0,1:T(2,128)S(1)}, f32[256,2]{0,1:T(2,128)}, u32[]{:S(2)}) copy-start(f32[256,2]{0,1:T(2,128)} %param.25) | copy-start | bytes 6148
  67.9 27.6 %all-to-all-start = ((bf16[16,256,128]{2,1,0:T(8,128)(2,1)}), bf16[16,256,128]{2,1,0:T(8,128)(2,1)S(1)}, u32[]{:S(2)}, u32[]{:S(2)}) async-start(bf16[16,256,128]{2,1,0:T(8,128)(2,1)} %attention.1), calls=%async_computation | async-start | bytes 2097152 | tf_op jit(solution)/shard_map/all_to_all | solution.py:481
  97.3 25.8 %copy-start.7 = (f32[256,2]{1,0:T(8,128)}, f32[256,2]{1,0:T(8,128)S(1)}, u32[]{:S(2)}) copy-start(f32[256,2]{1,0:T(8,128)S(1)} %get-tuple-element.22.factors_ref) | copy-start | bytes 6148
  97.3 41.7 %all-to-all-start.1 = ((bf16[128,8,128]{2,1,0:T(8,128)(2,1)}), bf16[128,8,128]{2,1,0:T(8,128)(2,1)S(1)}, u32[]{:S(2)}, u32[]{:S(2)}) async-start(bf16[128,8,128]{2,1,0:T(8,128)(2,1)} %bitcast.7), calls=%async_computation.1 | async-start | bytes 524288 | tf_op jit(solution)/shard_map/all_to_all | solution.py:487
  115.6 39.4 %copy-start.10 = (f32[2048]{0:T(1024)S(1)}, f32[2048]{0:T(1024)}, u32[]{:S(2)}) copy-start(f32[2048]{0:T(1024)} %param.20) | copy-start | bytes 24580
  118.9 1.0 copy-start.12
  119.9 39.0 %collective-permute-start.2 = (bf16[2,2048,128]{2,1,0:T(8,128)(2,1)}, bf16[2,2048,128]{2,1,0:T(8,128)(2,1)S(1)}, u32[]{:S(2)}, u32[]{:S(2)}) collective-permute-start(bf16[2,2048,128]{2,1,0:T(8,128)(2,1)} %get-tuple-element.17), channel_id=1, source_target_pairs={{0,1},{1,2},{2,3},{3,0},{4,5},{5,6},{6,7},{7,4},{8,9},{9,10},{10,1... | collective-permute-start | bytes 3145736 | tf_op jit(solution)/shard_map/ppermute | solution.py:457
  123.1 35.7 %collective-permute-start.3 = (bf16[2,2048,128]{2,1,0:T(8,128)(2,1)}, bf16[2,2048,128]{2,1,0:T(8,128)(2,1)S(1)}, u32[]{:S(2)}, u32[]{:S(2)}) collective-permute-start(bf16[2,2048,128]{2,1,0:T(8,128)(2,1)} %get-tuple-element.18), channel_id=1, source_target_pairs={{0,3},{1,0},{2,1},{3,2},{4,7},{5,4},{6,5},{7,6},{8,11},{9,8},{10,9... | collective-permute-start | bytes 3145736 | tf_op jit(solution)/shard_map/ppermute | solution.py:458
  139.0 13.6 %copy-start.13 = (bf16[2,2048,128]{2,1,0:T(8,128)(2,1)S(1)}, bf16[2,2048,128]{2,1,0:T(8,128)(2,1)}, u32[]{:S(2)}) copy-start(bf16[2,2048,128]{2,1,0:T(8,128)(2,1)} %copy-done.12) | copy-start | bytes 3145732
  152.6 28.1 %collective-permute-start.4 = (bf16[2,2048,128]{2,1,0:T(8,128)(2,1)S(1)}, bf16[2,2048,128]{2,1,0:T(8,128)(2,1)S(1)}, u32[]{:S(2)}, u32[]{:S(2)}) collective-permute-start(bf16[2,2048,128]{2,1,0:T(8,128)(2,1)S(1)} %copy-done.13), channel_id=1, source_target_pairs={{0,1},{1,2},{2,3},{3,0},{4,5},{5,6},{6,7},{7,4},{8,9},{9,10},{10,1... | collective-permute-start | bytes 3145736 | tf_op jit(solution)/shard_map/ppermute | solution.py:459
  180.8 34.4 %copy-start.6 = (s32[256,2]{1,0:T(8,128)S(1)}, s32[256,2]{1,0:T(8,128)}, u32[]{:S(2)}) copy-start(s32[256,2]{1,0:T(8,128)} %copy-done.5) | copy-start | bytes 6148
  180.8 34.4 %copy-start.8 = (f32[256,2]{1,0:T(8,128)S(1)}, f32[256,2]{1,0:T(8,128)}, u32[]{:S(2)}) copy-start(f32[256,2]{1,0:T(8,128)} %copy-done.7) | copy-start | bytes 6148
  (1 other events, 0.6 us)

commit v13 on v12

--- a/solution.py
+++ b/solution.py
@@ -400,16 +400,13 @@
 
 def assemble(whole):
     peers, tok, share = whole.shape
-    tile = tok // 4
+    vmem = pl.BlockSpec(memory_space=pltpu.VMEM)
     return pl.pallas_call(
         assemble_body,
-        grid=(4,),
-        in_specs=[pl.BlockSpec((peers, tile, share), lambda i: (0, i, 0))],
-        out_specs=pl.BlockSpec((tile, peers * share), lambda i: (i, 0)),
+        in_specs=[vmem],
+        out_specs=vmem,
         out_shape=jax.ShapeDtypeStruct((tok, peers * share), whole.dtype),
-        compiler_params=pltpu.CompilerParams(
-            dimension_semantics=("arbitrary",), vmem_limit_bytes=6 * 2**20
-        ),
+        compiler_params=pltpu.CompilerParams(vmem_limit_bytes=6 * 2**20),
         name="assemble",
     )(whole)
 

time: 239 us -> 238 us (level)
  no operation moved by 1% of the time
where the time goes in v13:
time: 238 us
  blocking collectives  136 us (57%)
  starting transfers between devices  41.3 us (17%)
  waiting for transfers between devices  32.7 us (14%)
  Pallas kernels  19 us (8%)
  local copies, waits for them, and re-layouts  5.75 us (2%)
    all_gather x3, blocking collectives, gathered(): whole = lax.all_gather(sent, axes, axis=axis, tiled=True)  83.4 us
    all_to_all x1, blocking collectives, shards(): lax.all_to_all(made.reshape(targets, each, share), ('sp', 'x'), 0, 0, til...  31.5 us
    all_to_all x1, blocking collectives, shards(): whole = lax.all_to_all(spread, tp, 0, 0, tiled=True)  20.9 us
    all_to_all x1, waiting for transfers between devices, shards(): parts = lax.all_to_all(partial, tp, 0, 0, tiled=True)  20 us
    all_to_all x1, starting transfers between devices, shards(): lax.all_to_all(outgoing.reshape(targets, each, share), ('sp', 'x'), 0, 0,...  18.3 us
    all_to_all x1, waiting for transfers between devices, shards(): lax.all_to_all(outgoing.reshape(targets, each, share), ('sp', 'x'), 0, 0,...  12.6 us
    all_to_all x1, starting transfers between devices, shards(): parts = lax.all_to_all(partial, tp, 0, 0, tiled=True)  6.96 us
    unnamed x37, local copies, waits for them, and re-layouts  5.59 us
  transfers between devices with their start and end apart: 7, of which 2 were waited for; matrix products, arithmetic and copies ran while one was open for 1% of the time, Pallas kernels for 5%

profile of v13, /device:TPU:1, one launch (start us, length us, event | category | flops | bytes accessed | tf_op | source)
XLA Modules:
  0.0 237.9 jit_solution(17718098145354980382)
XLA Ops:
  0.0 1.3 copy-done.1
  1.3 1.2 copy-done.2
  2.5 1.2 copy-done.3
  3.8 1.7 pack.1.own_ref
  5.5 5.2 %collective-permute-start = (bf16[6,2048,128]{2,1,0:T(8,128)(2,1)}, bf16[6,2048,128]{2,1,0:T(8,128)(2,1)}, u32[]{:S(2)}, u32[]{:S(2)}) collective-permute-start(bf16[6,2048,128]{2,1,0:T(8,128)(2,1)} %pack.1.own_ref), channel_id=1, source_target_pairs={{0,3},{1,0},{2,1},{3,2},{4,7},{5,4},{6,5},{7,6},{8,11},{9,8},{10,9... | collective-permute-start | bytes 9437192 | tf_op jit(solution)/shard_map/ppermute | solution.py:452
  10.7 1.9 collective-permute-start.1
  12.7 49.9 %all-gather.3 = f16[8192,256]{1,0:T(8,128)(2,1)S(1)} all-gather(f16[256,256]{1,0:T(8,128)(2,1)S(1)} %multiply_convert_fusion.5), channel_id=1, replica_groups=mesh['sp'=32,'y'=4,'x'=4] {'sp'}, dimensions={0}, use_global_device_ids=true | all-gather | bytes 4325376 | tf_op jit(solution)/shard_map/all_gather | solution.py:416
  64.3 3.6 %attention.1 = bf16[16,256,128]{2,1,0:T(8,128)(2,1)} custom-call(s32[1]{0:T(128)} %bitcast.1.where_ref, f32[1]{0:T(128)S(6)} %copy.30.lam_ref, bf16[256,128]{1,0:T(8,128)(2,1)S(1)} %bitcast.25, bf16[8192,256]{1,0:T(8,128)(2,1)S(1)} %multiply_convert_fusion.kv_ref, f32[1,128]{1,0:T(1,128)S(1)} %bitcast.27, bf16[128,2048]{1,0:T(8,128)(2,1)S(1)} %copy-done.4), custom_call_target="tpu_custom_call" | custom-call | tf_op jit(solution)/shard_map/attention/pallas_call | solution.py:81
  67.9 7.0 %all-to-all-start = ((bf16[16,256,128]{2,1,0:T(8,128)(2,1)}), bf16[16,256,128]{2,1,0:T(8,128)(2,1)S(1)}, u32[]{:S(2)}, u32[]{:S(2)}) async-start(bf16[16,256,128]{2,1,0:T(8,128)(2,1)} %attention.1), calls=%async_computation | async-start | bytes 2097152 | tf_op jit(solution)/shard_map/all_to_all | solution.py:478
  75.5 20.0 %all-to-all-done.parts_ref = bf16[16,256,128]{2,1,0:T(8,128)(2,1)S(1)} async-done(((bf16[16,256,128]{2,1,0:T(8,128)(2,1)}), bf16[16,256,128]{2,1,0:T(8,128)(2,1)S(1)}, u32[]{:S(2)}, u32[]{:S(2)}) %all-to-all-start) | async-done | bytes 1048608 | tf_op jit(solution)/shard_map/all_to_all | solution.py:478
  95.5 1.1 project.1
  97.3 18.3 %all-to-all-start.1 = ((bf16[128,8,128]{2,1,0:T(8,128)(2,1)}), bf16[128,8,128]{2,1,0:T(8,128)(2,1)S(1)}, u32[]{:S(2)}, u32[]{:S(2)}) async-start(bf16[128,8,128]{2,1,0:T(8,128)(2,1)} %bitcast.7), calls=%async_computation.1 | async-start | bytes 524288 | tf_op jit(solution)/shard_map/all_to_all | solution.py:484
  115.7 3.2 %cut.1 = (bf16[2,2048,128]{2,1,0:T(8,128)(2,1)}, bf16[2,2048,128]{2,1,0:T(8,128)(2,1)S(1)}, bf16[2,2048,128]{2,1,0:T(8,128)(2,1)}) custom-call(bf16[6,2048,128]{2,1,0:T(8,128)(2,1)} %collective-permute-done.1.left_ref, bf16[6,2048,128]{2,1,0:T(8,128)(2,1)} %collective-permute-done.right_ref), custom_call_target="tpu_custom_call" | custom-call | tf_op jit(solution)/shard_map/cut/pallas_call | solution.py:147
  119.9 3.2 %collective-permute-start.2 = (bf16[2,2048,128]{2,1,0:T(8,128)(2,1)}, bf16[2,2048,128]{2,1,0:T(8,128)(2,1)S(1)}, u32[]{:S(2)}, u32[]{:S(2)}) collective-permute-start(bf16[2,2048,128]{2,1,0:T(8,128)(2,1)} %get-tuple-element.17), channel_id=1, source_target_pairs={{0,1},{1,2},{2,3},{3,0},{4,5},{5,6},{6,7},{7,4},{8,9},{9,10},{10,1... | collective-permute-start | bytes 3145736 | tf_op jit(solution)/shard_map/ppermute | solution.py:454
  123.1 3.2 %collective-permute-start.3 = (bf16[2,2048,128]{2,1,0:T(8,128)(2,1)}, bf16[2,2048,128]{2,1,0:T(8,128)(2,1)S(1)}, u32[]{:S(2)}, u32[]{:S(2)}) collective-permute-start(bf16[2,2048,128]{2,1,0:T(8,128)(2,1)} %get-tuple-element.18), channel_id=1, source_target_pairs={{0,3},{1,0},{2,1},{3,2},{4,7},{5,4},{6,5},{7,6},{8,11},{9,8},{10,9... | collective-permute-start | bytes 3145736 | tf_op jit(solution)/shard_map/ppermute | solution.py:455
  126.4 12.6 %all-to-all-done.1 = bf16[128,8,128]{2,1,0:T(8,128)(2,1)S(1)} async-done(((bf16[128,8,128]{2,1,0:T(8,128)(2,1)}), bf16[128,8,128]{2,1,0:T(8,128)(2,1)S(1)}, u32[]{:S(2)}, u32[]{:S(2)}) %all-to-all-start.1) | async-done | bytes 262176 | tf_op jit(solution)/shard_map/all_to_all | solution.py:484
  139.1 13.2 %all-gather.4 = f16[16,256,128]{2,1,0:T(8,128)(2,1)S(1)} all-gather(f16[4,256,128]{2,1,0:T(8,128)(2,1)S(1)} %fusion), channel_id=1, replica_groups=mesh['sp'=32,'y'=4,'x'=4] {'y'}, dimensions={0}, use_global_device_ids=true | all-gather | bytes 1310720 | tf_op jit(solution)/shard_map/all_gather | solution.py:416
  152.6 2.4 collective-permute-start.4
  155.0 3.8 %near.1 = (bf16[3,256,256]{2,1,0:T(8,128)(2,1)S(1)}, bf16[256,2048]{1,0:T(8,128)(2,1)S(1)}) custom-call(bf16[16,256,128]{2,1,0:T(8,128)(2,1)S(1)} %multiply_convert_fusion.2.rows_ref, f32[1,2048]{1,0:T(1,128)S(1)} %bitcast.26, bf16[6,2048,128]{2,1,0:T(8,128)(2,1)} %pack.1.own_ref, bf16[6,2048,128]{2,1,0:T(8,128)(2,1)} %collective-permute-done.right_ref, ...), custom_call_target="tpu_custom_call" | custom-call | tf_op jit(solution)/shard_map/near/pallas_call | solution.py:285
  159.9 20.3 %all-gather.5 = f16[16,256,256]{2,1,0:T(8,128)(2,1)S(1)} all-gather(f16[4,256,256]{2,1,0:T(8,128)(2,1)S(1)} %multiply_convert_fusion.3), channel_id=1, replica_groups=mesh['sp'=32,'y'=4,'x'=4] {'y'}, dimensions={0}, use_global_device_ids=true | all-gather | bytes 2621440 | tf_op jit(solution)/shard_map/all_gather | solution.py:416
  180.8 2.8 %down.1 = bf16[32,4,8,128]{3,2,1,0:T(8,128)(2,1)S(1)} custom-call(s32[1]{0:T(128)} %bitcast.x_ref, bf16[16,256,256]{2,1,0:T(8,128)(2,1)S(1)} %multiply_convert_fusion.1.units_ref, bf16[6,2048,128]{2,1,0:T(8,128)(2,1)} %pack.1.own_ref, bf16[6,2048,128]{2,1,0:T(8,128)(2,1)} %collective-permute-done.right_ref, ...), custom_call_target="tpu_custom_call" | custom-call | tf_op jit(solution)/shard_map/down/pallas_call | solution.py:381
  183.6 31.5 %all_to_all.20 = bf16[128,8,128]{2,1,0:T(8,128)(2,1)S(1)} all-to-all(bf16[128,8,128]{2,1,0:T(8,128)(2,1)S(1)} %bitcast.19), channel_id=1, replica_groups=mesh['sp'=32,'y'=4,'x'=4] {'sp','x'}, dimensions={0} | all-to-all | bytes 524288 | tf_op jit(solution)/shard_map/all_to_all | solution.py:492
  215.7 20.9 %all_to_all.21.whole_ref = bf16[16,256,128]{2,1,0:T(8,128)(2,1)S(1)} all-to-all(bf16[16,256,128]{2,1,0:T(8,128)(2,1)S(1)} %combine.1), channel_id=1, replica_groups=mesh['sp'=32,'y'=4,'x'=4] {'y','x'}, dimensions={0} | all-to-all | bytes 2097152 | tf_op jit(solution)/shard_map/all_to_all | solution.py:497
  236.6 1.3 assemble.1
  (55 shorter events, 5.7 us)
Async XLA Ops:
  0.0 75.4 %copy-start = (bf16[256,2048]{1,0:T(8,128)(2,1)S(1)}, bf16[256,2048]{1,0:T(8,128)(2,1)}, u32[]{:S(2)}) copy-start(bf16[256,2048]{1,0:T(8,128)(2,1)} %param.13) | copy-start | bytes 3145732
  0.0 1.3 copy-start.1
  1.3 1.2 copy-start.2
  2.5 1.2 copy-start.3
  3.8 8.8 %copy-start.14 = (bf16[256,1,128]{2,0,1:T(8,128)(2,1)S(1)}, bf16[256,1,128]{2,0,1:T(8,128)(2,1)}, u32[]{:S(2)}) copy-start(bf16[256,1,128]{2,0,1:T(8,128)(2,1)} %param.16) | copy-start | bytes 196612
  3.8 8.9 %copy-start.15 = (bf16[256,1,128]{2,0,1:T(8,128)(2,1)S(1)}, bf16[256,1,128]{2,0,1:T(8,128)(2,1)}, u32[]{:S(2)}) copy-start(bf16[256,1,128]{2,0,1:T(8,128)(2,1)} %param.15) | copy-start | bytes 196612
  5.5 110.2 %collective-permute-start = (bf16[6,2048,128]{2,1,0:T(8,128)(2,1)}, bf16[6,2048,128]{2,1,0:T(8,128)(2,1)}, u32[]{:S(2)}, u32[]{:S(2)}) collective-permute-start(bf16[6,2048,128]{2,1,0:T(8,128)(2,1)} %pack.1.own_ref), channel_id=1, source_target_pairs={{0,3},{1,0},{2,1},{3,2},{4,7},{5,4},{6,5},{7,6},{8,11},{9,8},{10,9... | collective-permute-start | bytes 9437192 | tf_op jit(solution)/shard_map/ppermute | solution.py:452
  10.7 105.0 %collective-permute-start.1 = (bf16[6,2048,128]{2,1,0:T(8,128)(2,1)}, bf16[6,2048,128]{2,1,0:T(8,128)(2,1)}, u32[]{:S(2)}, u32[]{:S(2)}) collective-permute-start(bf16[6,2048,128]{2,1,0:T(8,128)(2,1)} %pack.1.own_ref), channel_id=1, source_target_pairs={{0,1},{1,2},{2,3},{3,0},{4,5},{5,6},{6,7},{7,4},{8,9},{9,10},{10,1... | collective-permute-start | bytes 9437192 | tf_op jit(solution)/shard_map/ppermute | solution.py:451
  63.2 1.0 copy-start.4
  63.2 1.0 copy-start.9
  63.2 1.0 copy-start.11
  64.2 10.7 %copy-start.16 = (s32[256,2]{0,1:T(2,128)S(1)}, s32[256,2]{0,1:T(2,128)}, u32[]{:S(2)}) copy-start(s32[256,2]{0,1:T(2,128)} %param.24) | copy-start | bytes 6148
  64.2 11.0 %copy-start.17 = (f32[256,2]{0,1:T(2,128)S(1)}, f32[256,2]{0,1:T(2,128)}, u32[]{:S(2)}) copy-start(f32[256,2]{0,1:T(2,128)} %param.25) | copy-start | bytes 6148
  67.9 27.6 %all-to-all-start = ((bf16[16,256,128]{2,1,0:T(8,128)(2,1)}), bf16[16,256,128]{2,1,0:T(8,128)(2,1)S(1)}, u32[]{:S(2)}, u32[]{:S(2)}) async-start(bf16[16,256,128]{2,1,0:T(8,128)(2,1)} %attention.1), calls=%async_computation | async-start | bytes 2097152 | tf_op jit(solution)/shard_map/all_to_all | solution.py:478
  97.3 25.8 %copy-start.7 = (f32[256,2]{1,0:T(8,128)}, f32[256,2]{1,0:T(8,128)S(1)}, u32[]{:S(2)}) copy-start(f32[256,2]{1,0:T(8,128)S(1)} %get-tuple-element.22.factors_ref) | copy-start | bytes 6148
  97.3 41.7 %all-to-all-start.1 = ((bf16[128,8,128]{2,1,0:T(8,128)(2,1)}), bf16[128,8,128]{2,1,0:T(8,128)(2,1)S(1)}, u32[]{:S(2)}, u32[]{:S(2)}) async-start(bf16[128,8,128]{2,1,0:T(8,128)(2,1)} %bitcast.7), calls=%async_computation.1 | async-start | bytes 524288 | tf_op jit(solution)/shard_map/all_to_all | solution.py:484
  115.6 39.4 %copy-start.10 = (f32[2048]{0:T(1024)S(1)}, f32[2048]{0:T(1024)}, u32[]{:S(2)}) copy-start(f32[2048]{0:T(1024)} %param.20) | copy-start | bytes 24580
  118.9 1.0 copy-start.12
  119.9 39.0 %collective-permute-start.2 = (bf16[2,2048,128]{2,1,0:T(8,128)(2,1)}, bf16[2,2048,128]{2,1,0:T(8,128)(2,1)S(1)}, u32[]{:S(2)}, u32[]{:S(2)}) collective-permute-start(bf16[2,2048,128]{2,1,0:T(8,128)(2,1)} %get-tuple-element.17), channel_id=1, source_target_pairs={{0,1},{1,2},{2,3},{3,0},{4,5},{5,6},{6,7},{7,4},{8,9},{9,10},{10,1... | collective-permute-start | bytes 3145736 | tf_op jit(solution)/shard_map/ppermute | solution.py:454
  123.1 35.7 %collective-permute-start.3 = (bf16[2,2048,128]{2,1,0:T(8,128)(2,1)}, bf16[2,2048,128]{2,1,0:T(8,128)(2,1)S(1)}, u32[]{:S(2)}, u32[]{:S(2)}) collective-permute-start(bf16[2,2048,128]{2,1,0:T(8,128)(2,1)} %get-tuple-element.18), channel_id=1, source_target_pairs={{0,3},{1,0},{2,1},{3,2},{4,7},{5,4},{6,5},{7,6},{8,11},{9,8},{10,9... | collective-permute-start | bytes 3145736 | tf_op jit(solution)/shard_map/ppermute | solution.py:455
  139.0 13.6 %copy-start.13 = (bf16[2,2048,128]{2,1,0:T(8,128)(2,1)S(1)}, bf16[2,2048,128]{2,1,0:T(8,128)(2,1)}, u32[]{:S(2)}) copy-start(bf16[2,2048,128]{2,1,0:T(8,128)(2,1)} %copy-done.12) | copy-start | bytes 3145732
  152.6 28.1 %collective-permute-start.4 = (bf16[2,2048,128]{2,1,0:T(8,128)(2,1)S(1)}, bf16[2,2048,128]{2,1,0:T(8,128)(2,1)S(1)}, u32[]{:S(2)}, u32[]{:S(2)}) collective-permute-start(bf16[2,2048,128]{2,1,0:T(8,128)(2,1)S(1)} %copy-done.13), channel_id=1, source_target_pairs={{0,1},{1,2},{2,3},{3,0},{4,5},{5,6},{6,7},{7,4},{8,9},{9,10},{10,1... | collective-permute-start | bytes 3145736 | tf_op jit(solution)/shard_map/ppermute | solution.py:456
  180.8 34.4 %copy-start.6 = (s32[256,2]{1,0:T(8,128)S(1)}, s32[256,2]{1,0:T(8,128)}, u32[]{:S(2)}) copy-start(s32[256,2]{1,0:T(8,128)} %copy-done.5) | copy-start | bytes 6148
  180.8 34.4 %copy-start.8 = (f32[256,2]{1,0:T(8,128)S(1)}, f32[256,2]{1,0:T(8,128)}, u32[]{:S(2)}) copy-start(f32[256,2]{1,0:T(8,128)} %copy-done.7) | copy-start | bytes 6148
  (1 other events, 0.6 us)
